TPU v7x, 128 devices: a whole 4x4x4 slice. The times are simulated.
128 devices in a mesh: sp: 16 (over z, y), dp: 8 (over x, core).
Axes of the slice: x: 4, y: 4, z: 4, core: 2. Of those that a mesh axis runs over, the one named last changes fastest.
Arguments:
- residual: bfloat16 [8, 2048, 2048], P('dp', 'sp'), may hold values from -6 to 6
- head_input: bfloat16 [8, 2048, 2048], P('dp', 'sp'), may hold values from -6 to 6
- gate_input: bfloat16 [8, 2048, 2048], P('dp', 'sp'), may hold values from -6 to 6
- b_input: bfloat16 [8, 2048, 1024], P('dp', 'sp'), may hold values from -6 to 6
- c_input: bfloat16 [8, 2048, 1024], P('dp', 'sp'), may hold values from -6 to 6
- step_input: bfloat16 [8, 2048, 32], P('dp', 'sp'), may hold values from -4.8 to 4.8
- conv_weight: bfloat16 [4, 2048], replicated, may hold values from -3 to 3
- conv_b_weight: bfloat16 [4, 1024], replicated, may hold values from -3 to 3
- conv_c_weight: bfloat16 [4, 1024], replicated, may hold values from -3 to 3
- step_bias: float32 [32], replicated, may hold values from -1 to 1
- decay_log: float32 [32], replicated, may hold values from -9.92 to -2.99
- skip: float32 [32], replicated, may hold values from 0.5 to 1.5
- norm_gain: float32 [2048], replicated, may hold values from 0.1 to 1.9
- out_weight: bfloat16 [2048, 2048], P('dp'), may hold values from -0.125 to 0.125
- ffn_gain: float32 [2048], replicated, may hold values from 0.1 to 1.9
- shared_gate: bfloat16 [2048, 512], replicated, may hold values from -0.125 to 0.125
- shared_up: bfloat16 [2048, 512], replicated, may hold values from -0.125 to 0.125
- shared_down: bfloat16 [512, 2048], replicated, may hold values from -0.25 to 0.25
- expert_gate: bfloat16 [128, 2048, 512], P(('sp', 'dp')), may hold values from -0.125 to 0.125
- expert_up: bfloat16 [128, 2048, 512], P(('sp', 'dp')), may hold values from -0.125 to 0.125
- expert_down: bfloat16 [128, 512, 2048], P(('sp', 'dp')), may hold values from -0.25 to 0.25
- routes: int32 [8, 2048, 2], P('dp', 'sp'), may hold values from 0 to 127, all different within a row; in each aligned block of 128 rows (0 to 127, 128 to 255, ..., all dimensions but the last counted through in order) at most 4 rows name the same one
- route_weights: float32 [8, 2048, 2], P('dp', 'sp'), may hold values from 0.25 to 1.25
Outputs:
- layer_out: bfloat16 [8, 2048, 2048], P('dp', 'sp')
Inputs may be any that keep to these rules, and one draw needn't show every extreme that they name: `routes`: each token names 2 different experts; among the rows of one device no expert is named more than 4 times, a bound that some block reaches.
All inputs are finite; a program needn't handle non-finite values.
Results may differ from a plain program's by a relative error of at most 0.015.
Values may be sent and summed in bfloat16 or wider, within the bound.
No kernel may reach another device: no remote copies, remote signals or barrier semaphores. Data moves between devices by JAX's collectives and lax.ppermute only.
A program may use at most 128 MiB of HBM per device.

v0:
```python
import jax
import jax.numpy as jnp
import numpy as np
from jax import lax
from jax.sharding import PartitionSpec as P

D = 2048
HEADS = 32
HEAD_DIM = 64
GROUPS = 8
STATE = 128
CONV_K = 4
BLOCK = 128
TOP_K = 2
INNER = 2048


EPS = 1e-06


def conv_silu(padded, weight, length):
    total = jnp.zeros((length, padded.shape[1]), jnp.float32)
    for tap in range(weight.shape[0]):
        total = total + padded[tap : tap + length].astype(jnp.float32) * weight[tap].astype(
            jnp.float32
        )
    return jax.nn.silu(total)


def block_scan(xs, step, rate, bmat, cmat, block, init):
    length, heads, width = xs.shape
    count = length // block
    logs = (step * rate[None, :]).reshape(count, block, heads)
    weighted = (xs * step[:, :, None]).reshape(count, block, heads, width)
    bb = bmat.reshape(count, block, heads, -1)
    cc = cmat.reshape(count, block, heads, -1)
    cum = jnp.cumsum(logs, axis=1)
    lower = jnp.tril(jnp.ones((block, block), dtype=bool))[None, :, :, None]
    diff = cum[:, :, None, :] - cum[:, None, :, :]
    decay = jnp.where(lower, jnp.exp(jnp.where(lower, diff, 0.0)), 0.0)
    scores = jnp.einsum("clhn,cshn->clsh", cc, bb) * decay
    inner = jnp.einsum("clsh,cshp->clhp", scores, weighted)
    to_end = jnp.exp(cum[:, -1:, :] - cum)
    states = jnp.einsum("cshn,cshp->chpn", bb * to_end[..., None], weighted)
    totals = jnp.exp(cum[:, -1, :])

    def advance(carry, item):
        fresh, factor = item
        return (carry * factor[:, None, None] + fresh, carry)

    last, before = lax.scan(advance, init, (states, totals))
    outer = jnp.einsum("clhn,chpn->clhp", cc * jnp.exp(cum)[..., None], before)
    return ((inner + outer).reshape(length, heads, width), last)


def serve_experts(arrived, gate_w, up_w, down_w):
    local = gate_w.shape[0]
    shaped = arrived.reshape(-1, local, arrived.shape[1], arrived.shape[2])
    gate = jnp.einsum("aenc,ecf->aenf", shaped, gate_w, preferred_element_type=jnp.float32)
    up = jnp.einsum("aenc,ecf->aenf", shaped, up_w, preferred_element_type=jnp.float32)
    hidden = (jax.nn.silu(gate) * up).astype(jnp.bfloat16)
    done = jnp.einsum("aenf,efc->aenc", hidden, down_w, preferred_element_type=jnp.float32).astype(
        jnp.bfloat16
    )
    return done.reshape(arrived.shape)


def body(
    residual,
    head_input,
    gate_input,
    b_input,
    c_input,
    step_input,
    conv_weight,
    conv_b_weight,
    conv_c_weight,
    step_bias,
    decay_log,
    skip,
    norm_gain,
    out_weight,
    ffn_gain,
    shared_gate,
    shared_up,
    shared_down,
    expert_gate,
    expert_up,
    expert_down,
    routes,
    route_weights,
):
    tokens = head_input.shape[1]
    x_rows = head_input[0]
    b_rows = b_input[0]
    c_rows = c_input[0]
    step_rows = step_input[0]
    per_group = HEADS // GROUPS
    ways = lax.axis_size("sp")
    place = lax.axis_index("sp")
    local = HEADS // ways
    width = local * HEAD_DIM
    targets = np.arange(ways) * local // per_group
    paired = jnp.concatenate(
        [b_rows.reshape(tokens, GROUPS, STATE), c_rows.reshape(tokens, GROUPS, STATE)], axis=2
    )
    outgoing = (
        x_rows.reshape(tokens, ways, width),
        paired[:, targets],
        step_rows.reshape(tokens, ways, local),
    )
    got_x, got_pair, got_step = (
        lax.all_to_all(outgoing[0], "sp", split_axis=1, concat_axis=0, tiled=True),
        lax.all_to_all(outgoing[1], "sp", split_axis=1, concat_axis=0, tiled=True),
        lax.all_to_all(outgoing[2], "sp", split_axis=1, concat_axis=0, tiled=True),
    )
    length = got_x.shape[0]
    group = place * local // per_group
    taps = jnp.concatenate(
        [
            lax.dynamic_slice_in_dim(conv_weight, place * width, width, 1),
            lax.dynamic_slice_in_dim(conv_b_weight, group * STATE, STATE, 1),
            lax.dynamic_slice_in_dim(conv_c_weight, group * STATE, STATE, 1),
        ],
        axis=1,
    )
    rows = jnp.concatenate(
        [got_x.reshape(length, width), got_pair.reshape(length, 2 * STATE)], axis=1
    )
    act = conv_silu(jnp.pad(rows, ((CONV_K - 1, 0), (0, 0))), taps, length)
    xs = act[:, :width].reshape(length, local, HEAD_DIM)
    bm = jnp.broadcast_to(act[:, width : width + STATE][:, None, :], (length, local, STATE))
    cm = jnp.broadcast_to(act[:, width + STATE :][:, None, :], (length, local, STATE))
    step = jax.nn.softplus(
        got_step.reshape(length, local).astype(jnp.float32)
        + lax.dynamic_slice_in_dim(step_bias, place * local, local, 0)[None, :]
    )
    rate = -jnp.exp(lax.dynamic_slice_in_dim(decay_log, place * local, local, 0))
    skip_local = lax.dynamic_slice_in_dim(skip, place * local, local, 0)
    y, _ = block_scan(
        xs, step, rate, bm, cm, BLOCK, jnp.zeros((local, HEAD_DIM, STATE), jnp.float32)
    )
    y = (y + skip_local[None, :, None] * xs).astype(jnp.bfloat16).reshape(ways, tokens, width)
    scanned = lax.all_to_all(y, "sp", split_axis=0, concat_axis=2, tiled=True).reshape(
        tokens, INNER
    )
    gated = (scanned.astype(jnp.float32) * jax.nn.silu(gate_input[0].astype(jnp.float32))).reshape(
        tokens, GROUPS, INNER // GROUPS
    )
    gated = gated * lax.rsqrt(jnp.mean(gated * gated, axis=2, keepdims=True) + EPS)
    normed = (gated.reshape(tokens, INNER) * norm_gain[None, :]).astype(jnp.bfloat16)
    projected = jnp.dot(
        normed,
        lax.all_gather(out_weight, "dp", axis=0, tiled=True),
        preferred_element_type=jnp.float32,
    )
    mixed = (residual[0].astype(jnp.float32) + projected).astype(jnp.bfloat16)
    mixed_f = mixed.astype(jnp.float32)
    expert_in = (
        mixed_f
        * lax.rsqrt(jnp.mean(mixed_f * mixed_f, axis=1, keepdims=True) + EPS)
        * ffn_gain[None, :]
    ).astype(jnp.bfloat16)
    shared_hidden = (
        jax.nn.silu(jnp.dot(expert_in, shared_gate, preferred_element_type=jnp.float32))
        * jnp.dot(expert_in, shared_up, preferred_element_type=jnp.float32)
    ).astype(jnp.bfloat16)
    shared = jnp.dot(shared_hidden, shared_down, preferred_element_type=jnp.float32)
    ways_sp = lax.axis_size("sp")
    ways_dp = lax.axis_size("dp")
    experts = ways_sp * ways_dp * expert_gate.shape[0]
    slots = 2 * tokens * TOP_K // experts
    chosen = routes[0].reshape(-1)
    pairs = chosen.shape[0]
    onehot = (chosen[:, None] == jnp.arange(experts, dtype=jnp.int32)[None, :]).astype(jnp.int32)
    position = jnp.sum((jnp.cumsum(onehot, axis=0) - onehot) * onehot, axis=1)
    target = chosen * slots + position
    owner = jnp.arange(pairs, dtype=jnp.int32) // TOP_K
    outgoing = jnp.zeros((experts * slots, D), jnp.bfloat16).at[target].set(expert_in[owner])
    outgoing = outgoing.reshape(experts, slots, D)
    done = serve_experts(
        lax.all_to_all(outgoing, ("sp", "dp"), split_axis=0, concat_axis=0, tiled=True),
        expert_gate,
        expert_up,
        expert_down,
    )
    returned = lax.all_to_all(done, ("sp", "dp"), split_axis=0, concat_axis=0, tiled=True)
    pair_out = returned.reshape(experts * slots, D)[target]
    routed = jnp.sum(
        pair_out.reshape(tokens, TOP_K, D).astype(jnp.float32) * route_weights[0][:, :, None],
        axis=1,
    )
    return (mixed_f + shared + routed).astype(jnp.bfloat16)[None]


def solution(mesh):
    return jax.shard_map(
        body,
        mesh=mesh,
        in_specs=(
            P("dp", "sp", None),
            P("dp", "sp", None),
            P("dp", "sp", None),
            P("dp", "sp", None),
            P("dp", "sp", None),
            P("dp", "sp", None),
            P(),
            P(),
            P(),
            P(),
            P(),
            P(),
            P(),
            P("dp", None),
            P(),
            P(),
            P(),
            P(),
            P(("sp", "dp"), None, None),
            P(("sp", "dp"), None, None),
            P(("sp", "dp"), None, None),
            P("dp", "sp", None),
            P("dp", "sp", None),
        ),
        out_specs=P("dp", "sp", None),
        check_vma=False,
    )
```

profile of v0, /device:TPU:1, one launch (start us, length us, event | category | flops | bytes accessed | tf_op | source)
XLA Modules:
  0.0 263.5 jit_solution(8860318031569980960)
XLA Ops:
  6.5 8.9 %all-to-all-start.2 = ((bf16[128,16,2]{0,2,1:T(2,128)(2,1)}), bf16[128,16,2]{0,2,1:T(2,128)(2,1)S(1)}, u32[]{:S(2)}, u32[]{:S(2)}) async-start(bf16[128,16,2]{0,2,1:T(2,128)(2,1)} %bitcast.206), calls=%async_computation.2 | async-start | bytes 16384 | tf_op jit(solution)/shard_map/all_to_all | solution.py:115
  21.8 5.6 %all-to-all-start = ((bf16[128,16,128]{0,2,1:T(8,128)(2,1)}), bf16[128,16,128]{0,2,1:T(8,128)(2,1)S(1)}, u32[]{:S(2)}, u32[]{:S(2)}) async-start(bf16[128,16,128]{0,2,1:T(8,128)(2,1)} %bitcast.1), calls=%async_computation | async-start | bytes 1048576 | tf_op jit(solution)/shard_map/all_to_all | solution.py:113
  32.9 4.7 %all-to-all-done = bf16[128,16,128]{0,2,1:T(8,128)(2,1)S(1)} async-done(((bf16[128,16,128]{0,2,1:T(8,128)(2,1)}), bf16[128,16,128]{0,2,1:T(8,128)(2,1)S(1)}, u32[]{:S(2)}, u32[]{:S(2)}) %all-to-all-start) | async-done | bytes 524320 | tf_op jit(solution)/shard_map/all_to_all | solution.py:113
  37.6 4.4 %all-to-all-start.1 = ((bf16[128,16,256]{2,0,1:T(8,128)(2,1)}), bf16[128,16,256]{2,0,1:T(8,128)(2,1)}, u32[]{:S(2)}, u32[]{:S(2)}) async-start(bf16[128,16,256]{2,0,1:T(8,128)(2,1)} %bitcast.190), calls=%async_computation.1 | async-start | bytes 2097152 | tf_op jit(solution)/shard_map/all_to_all | solution.py:114
  47.1 1.7 copy.139
  50.8 6.1 %all-to-all-done.1 = bf16[128,16,256]{2,0,1:T(8,128)(2,1)} async-done(((bf16[128,16,256]{2,0,1:T(8,128)(2,1)}), bf16[128,16,256]{2,0,1:T(8,128)(2,1)}, u32[]{:S(2)}, u32[]{:S(2)}) %all-to-all-start.1) | async-done | bytes 1048608 | tf_op jit(solution)/shard_map/all_to_all | solution.py:114
  58.4 2.1 divide_multiply_fusion
  64.9 1.9 fusion.14
  66.8 3.8 %fusion.11 = f32[16,2,64,128]{3,2,1,0:T(8,128)} fusion(f32[16,128,2]{1,2,0:T(2,128)S(1)} %copy.133, f32[16,128,128]{2,1,0:T(8,128)} %bitcast.191, f32[16,128,128]{2,1,0:T(8,128)} %bitcast.195, pred[128,128]{0,1:T(8,128)(4,1)S(1)} %iota_compare_fusion.1, bf16[16,128,2,64]{1,0,3,2:T(8,128)(2,1)} %copy-done.2), kind=kOutput, calls=%fused_computation.23 | convolution fusion | flops 203948032 | bytes 3702784 | tf_op jit(solution)/shard_map/clsh,cshp->clhp/dot_general | solution.py:42
  70.6 24.7 %while.13 = (s32[]{:T(128)}, f32[2,64,128]{2,1,0:T(8,128)S(1)}, bf16[16,2,64,128]{3,2,1,0:T(8,128)(2,1)}, f32[16,2]{1,0:T(8,128)S(1)}, f32[16,2,64,128]{3,2,1,0:T(8,128)}, /*index=5*/s32[]{:T(128)}, s32[]{:T(128)}) while((s32[]{:T(128)}, f32[2,64,128]{2,1,0:T(8,128)S(1)}, bf16[16,2,64,128]{3,2,1,0:T(8,128)(2,1)}, ...), condition=%wide.region_2.3_spmd.clone, body=%wide.region_1.2_spmd.clone.sunk | while | flops 65539 | bytes 295544 | solution.py:51
  95.3 3.6 %fusion.24 = f32[16,2,64,128]{3,2,1,0:T(8,128)} fusion(f32[16,2,64,128]{3,2,1,0:T(8,128)} %fusion.11, bf16[16,2,64,128]{3,2,1,0:T(8,128)(2,1)} %get-tuple-element.32, f32[16,128,2]{1,2,0:T(2,128)S(1)} %copy.142, f32[16,128,128]{2,1,0:T(8,128)} %bitcast.192), kind=kOutput, calls=%fused_computation.38 | convolution fusion | flops 67895296 | bytes 3686400 | tf_op jit(solution)/shard_map/clhn,chpn->clhp/dot_general | solution.py:52
  98.9 2.6 copy.143
  101.5 2.1 add_convert_fusion
  103.6 4.5 %all-to-all-start.3 = ((bf16[16,128,128]{2,1,0:T(8,128)(2,1)}), bf16[16,128,128]{2,1,0:T(8,128)(2,1)S(1)}, u32[]{:S(2)}, u32[]{:S(2)}) async-start(bf16[16,128,128]{2,1,0:T(8,128)(2,1)} %add_convert_fusion), calls=%async_computation.3 | async-start | bytes 1048576 | tf_op jit(solution)/shard_map/all_to_all | solution.py:144
  111.4 5.9 %all-to-all-done.3 = bf16[16,128,128]{2,1,0:T(8,128)(2,1)S(1)} async-done(((bf16[16,128,128]{2,1,0:T(8,128)(2,1)}), bf16[16,128,128]{2,1,0:T(8,128)(2,1)S(1)}, u32[]{:S(2)}, u32[]{:S(2)}) %all-to-all-start.3) | async-done | bytes 524320 | tf_op jit(solution)/shard_map/all_to_all | solution.py:144
  118.4 2.5 copy.144
  122.6 2.4 fusion.54
  125.0 4.9 %multiply_reduce_fusion.1 = (f32[128]{0:T(128)S(1)}, f32[128,2048]{1,0:T(8,128)S(1)}) fusion(bf16[128,2048]{0,1:T(8,128)(2,1)} %fusion.54, bf16[2048,2048]{1,0:T(8,128)(2,1)} %all-gather.2.cloned.1.call-done, bf16[1,128,2048]{2,1,0:T(8,128)(2,1)} %param.27), kind=kOutput, calls=%fused_computation.60 | convolution fusion | flops 1075314560 | bytes 10486272 | tf_op jit(solution)/shard_map/dot_general | solution.py:152
  130.9 7.2 %scatter_custom_fusion = bf16[512,2048]{1,0:T(8,128)(2,1)} fusion(s32[256]{0:T(256)S(1)} %bitcast.208, bf16[128,2048]{1,0:T(8,128)(2,1)} %multiply_convert_fusion, s32[1024]{0:T(1024)S(1)} %pad_clamp_fusion.1, bf16[]{:T(256)} %constant.85.clone.1), kind=kCustom, calls=%fused_computation.56 | custom fusion | bytes 2097664 | tf_op jit(solution)/shard_map/scatter | solution.py:179
  138.1 4.1 %reshape.285 = bf16[128,4,2048]{2,1,0:T(4,128)(2,1)} reshape(bf16[512,2048]{1,0:T(8,128)(2,1)} %scatter_custom_fusion) | data formatting | bytes 4194304 | tf_op jit(solution)/shard_map/reshape | solution.py:180
  142.2 39.3 %all_to_all.58 = bf16[128,4,2048]{2,1,0:T(4,128)(2,1)S(1)} all-to-all(bf16[128,4,2048]{2,1,0:T(4,128)(2,1)} %reshape.285), channel_id=1, replica_groups=mesh['sp'=16,'dp'=8] {'sp','dp'}, dimensions={0} | all-to-all | bytes 4194304 | tf_op jit(solution)/shard_map/all_to_all | solution.py:182
  182.8 3.4 %fusion.27 = f32[128,1,4,512]{3,0,2,1:T(8,128)} fusion(bf16[1,2048,512]{2,1,0:T(8,128)(2,1)S(1)} %copy-done.14, bf16[128,4,2048]{2,1,0:T(4,128)(2,1)S(1)} %all_to_all.58), kind=kOutput, calls=%fused_computation.39 | convolution fusion | flops 1073741824 | bytes 5242880 | tf_op jit(solution)/shard_map/aenc,ecf->aenf/dot_general | solution.py:59
  186.2 7.5 %convolution_convert_fusion = bf16[128,4,2048]{2,0,1:T(8,128)(2,1)} fusion(bf16[1,512,2048]{2,1,0:T(8,128)(2,1)S(1)} %copy-done, bf16[1,2048,512]{2,1,0:T(8,128)(2,1)} %param.46, bf16[128,4,2048]{2,1,0:T(4,128)(2,1)} %copy-done.3, f32[128,1,4,512]{3,0,2,1:T(8,128)} %fusion.27), kind=kOutput, calls=%fused_computation.9 | convolution fusion | flops 2150105088 | bytes 9437184 | tf_op jit(solution)/shard_map/aenf,efc->aenc/dot_general | solution.py:62
  193.7 4.5 %copy.155 = bf16[128,4,2048]{2,1,0:T(4,128)(2,1)} copy(bf16[128,4,2048]{2,0,1:T(8,128)(2,1)} %convolution_convert_fusion) | data formatting | bytes 4194304 | tf_op jit(solution)/shard_map/convert_element_type | solution.py:62
  198.3 5.6 %all-to-all-start.5 = ((bf16[128,4,2048]{2,1,0:T(4,128)(2,1)}), bf16[128,4,2048]{2,1,0:T(4,128)(2,1)}, u32[]{:S(2)}, u32[]{:S(2)}) async-start(bf16[128,4,2048]{2,1,0:T(4,128)(2,1)} %copy.155), calls=%async_computation.5 | async-start | bytes 4194304 | tf_op jit(solution)/shard_map/all_to_all | solution.py:187
  204.0 2.2 fusion.108
  206.2 27.9 %all-to-all-done.5 = bf16[128,4,2048]{2,1,0:T(4,128)(2,1)} async-done(((bf16[128,4,2048]{2,1,0:T(4,128)(2,1)}), bf16[128,4,2048]{2,1,0:T(4,128)(2,1)}, u32[]{:S(2)}, u32[]{:S(2)}) %all-to-all-start.5) | async-done | bytes 2097184 | tf_op jit(solution)/shard_map/all_to_all | solution.py:187
  234.1 4.0 %reshape.290 = bf16[512,2048]{1,0:T(8,128)(2,1)} reshape(bf16[128,4,2048]{2,1,0:T(4,128)(2,1)} %all-to-all-done.5) | data formatting | bytes 4194304 | tf_op jit(solution)/shard_map/reshape | solution.py:188
  238.1 5.2 %gather_fusion.1 = bf16[256,2048]{1,0:T(8,128)(2,1)} fusion(bf16[512,2048]{1,0:T(8,128)(2,1)} %reshape.290, s32[1024]{0:T(1024)S(1)} %pad_clamp_fusion), kind=kCustom, calls=%fused_computation.2 | custom fusion | bytes 2098176 | tf_op jit(solution)/shard_map/gather | solution.py:188
  243.3 3.4 %reshape.300 = f32[128,2,2048]{2,1,0:T(2,128)} reshape(bf16[256,2048]{1,0:T(8,128)(2,1)} %gather_fusion.1) | data formatting | bytes 3145728 | tf_op jit(solution)/shard_map/convert_element_type | solution.py:190
  246.7 5.7 %multiply_reduce_fusion = f32[128,2048]{1,0:T(8,128)} fusion(f32[128,2,2048]{2,1,0:T(2,128)} %reshape.300, f32[128,2]{1,0:T(8,128)S(1)} %copy.156), kind=kLoop, calls=%fused_computation.24 | loop fusion | flops 786432 | bytes 3146752 | tf_op jit(solution)/shard_map/reduce_sum | solution.py:189
  252.4 4.3 %fusion.5 = bf16[1,128,2048]{2,1,0:T(8,128)(2,1)} fusion(f32[128,2048]{1,0:T(8,128)} %multiply_reduce_fusion, f32[128,2048]{1,0:T(8,128)S(1)} %get-tuple-element.98, bf16[512,2048]{1,0:T(8,128)(2,1)} %param.44, bf16[128,2048]{1,0:T(8,128)(2,1)} %multiply_convert_fusion, bf16[2048,512]{1,0:T(8,128)(2,1)} %param.43, f32[128,512]{1,0:T(8,128)S(1)} %fusion.108), kind=kOutput, calls=%fused_computation.16 | convolution fusion | flops 538050560 | bytes 7602176 | tf_op jit(solution)/shard_map/dot_general | solution.py:168
  (153 shorter events, 57.7 us)
Async XLA Ops:
  6.5 179.7 %copy-start = (bf16[1,512,2048]{2,1,0:T(8,128)(2,1)S(1)}, bf16[1,512,2048]{2,1,0:T(8,128)(2,1)}, u32[]{:S(2)}) copy-start(bf16[1,512,2048]{2,1,0:T(8,128)(2,1)} %param.47) | copy-start | bytes 6291460
  6.5 20.9 %copy-start.13 = (s32[16]{0:T(128)S(1)}, s32[16]{0:T(128)}, u32[]{:S(2)}) copy-start(s32[16]{0:T(128)} %constant.120) | copy-start | bytes 196
  6.5 13.1 %copy-start.6 = (bf16[1,128,2048]{2,1,0:T(8,128)(2,1)S(1)}, bf16[1,128,2048]{2,1,0:T(8,128)(2,1)}, u32[]{:S(2)}) copy-start(bf16[1,128,2048]{2,1,0:T(8,128)(2,1)} %param.28) | copy-start | bytes 1572868
  6.5 20.9 %copy-start.8 = (bf16[1,128,1024]{2,1,0:T(8,128)(2,1)S(1)}, bf16[1,128,1024]{2,1,0:T(8,128)(2,1)}, u32[]{:S(2)}) copy-start(bf16[1,128,1024]{2,1,0:T(8,128)(2,1)} %param.30) | copy-start | bytes 786436
  6.5 15.2 %all-to-all-start.2 = ((bf16[128,16,2]{0,2,1:T(2,128)(2,1)}), bf16[128,16,2]{0,2,1:T(2,128)(2,1)S(1)}, u32[]{:S(2)}, u32[]{:S(2)}) async-start(bf16[128,16,2]{0,2,1:T(2,128)(2,1)} %bitcast.206), calls=%async_computation.2 | async-start | bytes 16384 | tf_op jit(solution)/shard_map/all_to_all | solution.py:115
  15.4 109.6 %all-gather.2.cloned.1.call-start = ((), (), s32[]{:S(2)}) async-start(), calls=%async_computation.6 | async-start | bytes 9437184 | tf_op jit(solution)/shard_map/all_gather | solution.py:154
  21.8 9.2 %copy-start.15 = (f32[32]{0:T(128)S(1)}, f32[32]{0:T(128)}, u32[]{:S(2)}) copy-start(f32[32]{0:T(128)} %param.37) | copy-start | bytes 388
  21.8 9.3 %copy-start.16 = (f32[32]{0:T(128)S(1)}, f32[32]{0:T(128)}, u32[]{:S(2)}) copy-start(f32[32]{0:T(128)} %param.36) | copy-start | bytes 388
  21.8 9.3 %copy-start.17 = (f32[32]{0:T(128)S(1)}, f32[32]{0:T(128)}, u32[]{:S(2)}) copy-start(f32[32]{0:T(128)} %param.38) | copy-start | bytes 388
  21.8 15.8 %all-to-all-start = ((bf16[128,16,128]{0,2,1:T(8,128)(2,1)}), bf16[128,16,128]{0,2,1:T(8,128)(2,1)S(1)}, u32[]{:S(2)}, u32[]{:S(2)}) async-start(bf16[128,16,128]{0,2,1:T(8,128)(2,1)} %bitcast.1), calls=%async_computation | async-start | bytes 1048576 | tf_op jit(solution)/shard_map/all_to_all | solution.py:113
  27.8 5.1 %copy-start.11 = (s32[1,128,2]{1,2,0:T(2,128)S(1)}, s32[1,128,2]{1,2,0:T(2,128)}, u32[]{:S(2)}) copy-start(s32[1,128,2]{1,2,0:T(2,128)} %param.48) | copy-start | bytes 3076
  37.6 4.5 %copy-start.4 = (bf16[128,16,128]{0,2,1:T(8,128)(2,1)}, bf16[128,16,128]{0,2,1:T(8,128)(2,1)S(1)}, u32[]{:S(2)}) copy-start(bf16[128,16,128]{0,2,1:T(8,128)(2,1)S(1)} %all-to-all-done) | copy-start | bytes 1572868
  37.6 19.3 %all-to-all-start.1 = ((bf16[128,16,256]{2,0,1:T(8,128)(2,1)}), bf16[128,16,256]{2,0,1:T(8,128)(2,1)}, u32[]{:S(2)}, u32[]{:S(2)}) async-start(bf16[128,16,256]{2,0,1:T(8,128)(2,1)} %bitcast.190), calls=%async_computation.1 | async-start | bytes 2097152 | tf_op jit(solution)/shard_map/all_to_all | solution.py:114
  47.1 3.5 %copy-start.5 = (bf16[128,16,128]{0,2,1:T(8,128)(2,1)S(1)}, bf16[128,16,128]{0,2,1:T(8,128)(2,1)}, u32[]{:S(2)}) copy-start(bf16[128,16,128]{0,2,1:T(8,128)(2,1)} %copy-done.4) | copy-start | bytes 1572868
  63.3 1.6 copy-start.1
  64.9 1.9 copy-start.2
  103.6 7.3 %copy-start.7 = (s32[128,8,32]{0,1,2:T(8,128)S(1)}, s32[128,8,32]{0,1,2:T(8,128)}, u32[]{:S(2)}) copy-start(s32[128,8,32]{0,1,2:T(8,128)} %broadcast_add_fusion) | copy-start | bytes 393220
  103.6 13.6 %all-to-all-start.3 = ((bf16[16,128,128]{2,1,0:T(8,128)(2,1)}), bf16[16,128,128]{2,1,0:T(8,128)(2,1)S(1)}, u32[]{:S(2)}, u32[]{:S(2)}) async-start(bf16[16,128,128]{2,1,0:T(8,128)(2,1)} %add_convert_fusion), calls=%async_computation.3 | async-start | bytes 1048576 | tf_op jit(solution)/shard_map/all_to_all | solution.py:144
  118.4 4.2 %copy-start.9 = (f32[2048]{0:T(1024)S(1)}, f32[2048]{0:T(1024)}, u32[]{:S(2)}) copy-start(f32[2048]{0:T(1024)} %param.39) | copy-start | bytes 24580
  125.0 5.0 %copy-start.10 = (f32[2048]{0:T(1024)S(1)}, f32[2048]{0:T(1024)}, u32[]{:S(2)}) copy-start(f32[2048]{0:T(1024)} %param.41) | copy-start | bytes 24580
  142.2 40.6 %copy-start.14 = (bf16[1,2048,512]{2,1,0:T(8,128)(2,1)S(1)}, bf16[1,2048,512]{2,1,0:T(8,128)(2,1)}, u32[]{:S(2)}) copy-start(bf16[1,2048,512]{2,1,0:T(8,128)(2,1)} %param.45) | copy-start | bytes 6291460
  181.5 1.3 copy-start.3
  198.3 5.6 %copy-start.12 = (f32[1,128,2]{1,2,0:T(2,128)S(1)}, f32[1,128,2]{1,2,0:T(2,128)}, u32[]{:S(2)}) copy-start(f32[1,128,2]{1,2,0:T(2,128)} %param.49) | copy-start | bytes 3076
  198.3 35.9 %all-to-all-start.5 = ((bf16[128,4,2048]{2,1,0:T(4,128)(2,1)}), bf16[128,4,2048]{2,1,0:T(4,128)(2,1)}, u32[]{:S(2)}, u32[]{:S(2)}) async-start(bf16[128,4,2048]{2,1,0:T(4,128)(2,1)} %copy.155), calls=%async_computation.5 | async-start | bytes 4194304 | tf_op jit(solution)/shard_map/all_to_all | solution.py:187
Sparse Core Ops, SparseCore 0:
  17.9 51.8 all-gather.1
where the time goes:
time: 266 us; the launch traced here: 264 us
  local copies, waits for them, and re-layouts  55.9 us (21%)
  other arithmetic  47.6 us (18%)
  waiting for transfers between devices  46.3 us (17%)
  blocking collectives  39.3 us (15%)
  matrix products  31.6 us (12%)
  starting transfers between devices  29 us (11%)
  between operations  13.7 us (5%)
    all_to_all x1, blocking collectives, body(): lax.all_to_all(outgoing, ('sp', 'dp'), split_axis=0, concat_axis=0, tiled...  39.3 us
    all_to_all x1, waiting for transfers between devices, body(): lax.all_to_all(done, ('sp', 'dp'), split_axis=0, concat_axis=0, tiled=True)  27.9 us
    add x16, other arithmetic, advance(): return (carry * factor[:, None, None] + fresh, carry)  14.6 us
    dynamic_update_slice x16, other arithmetic, block_scan(): last, before = lax.scan(advance, init, (states, totals))  9.94 us
    all_to_all x1, starting transfers between devices, body(): lax.all_to_all(outgoing[2], 'sp', split_axis=1, concat_axis=0, tiled=True)  8.86 us
    dot_general x1, matrix products, serve_experts(): jnp.einsum('aenf,efc->aenc', hidden, down_w, preferred_element_type=jnp.f...  7.52 us
    unnamed x44, local copies, waits for them, and re-layouts  7.39 us
    scatter x1, local copies, waits for them, and re-layouts, body(): jnp.zeros((experts * slots, D), jnp.bfloat16).at[target]  7.19 us
  transfers between devices with their start and end apart: 6, of which 5 were waited for; matrix products, arithmetic and copies ran while one was open for 30% of the time, Pallas kernels for 0%

commit v1 on v0

v1 whole, which is shorter than its diff:
```python
import jax
import jax.numpy as jnp
from jax import lax
from jax.experimental import pallas as pl
from jax.experimental.pallas import tpu as pltpu
from jax.sharding import PartitionSpec as P

D = 2048
HEADS = 32
HEAD_DIM = 64
GROUPS = 8
STATE = 128
TOK = 128
EPS = 1e-06
BF = jnp.bfloat16
F32 = jnp.float32
PER = HEADS // GROUPS
GW = PER * HEAD_DIM
HALF = D // 2
ROWS = 1024
ST_ROWS = 144


def full():
    return pl.BlockSpec(memory_space=pltpu.VMEM)


def smem():
    return pl.BlockSpec(memory_space=pltpu.SMEM)


def call(kernel, outs, n_in, name, scratch=(), smem_in=(), flops=10**6, nbytes=10**6):
    return pl.pallas_call(
        kernel,
        out_shape=tuple(jax.ShapeDtypeStruct(s, d) for s, d in outs),
        in_specs=[smem() if i in smem_in else full() for i in range(n_in)],
        out_specs=tuple(full() for _ in outs),
        scratch_shapes=list(scratch),
        name=name,
        cost_estimate=pl.CostEstimate(flops=flops, bytes_accessed=nbytes, transcendentals=0),
    )


def silu(v):
    return v / (1.0 + jnp.exp(-v))


def tap(pad, halo, rows, weight):
    pad[0:8, :] = halo.astype(F32)
    pad[8 : 8 + TOK, :] = rows.astype(F32)
    w = weight.astype(F32)
    total = pad[5 : 5 + TOK, :] * w[0:1, :]
    for k in range(1, 4):
        total = total + pad[5 + k : 5 + k + TOK, :] * w[k : k + 1, :]
    return silu(total)


def spread(cols, g):
    lane = lax.broadcasted_iota(jnp.int32, (TOK, 128), 1)
    out = []
    for i in range(0, PER, 2):
        h = g * PER + i
        out.append(jnp.where(lane < HEAD_DIM, cols[:, h : h + 1], cols[:, h + 1 : h + 2]))
    return jnp.concatenate(out, axis=1)


def states_kernel(
    x, b, hx, hb, step_in, cw, cbw, bias, dlog, st, v_out, xs_out, b_out, ec_out, padx, padb
):
    s = step_in[...].astype(F32) + bias[...]
    step = jnp.maximum(s, 0.0) + jnp.log(1.0 + jnp.exp(-jnp.abs(s)))
    logs = step * (-jnp.exp(dlog[...]))
    r = lax.broadcasted_iota(jnp.int32, (TOK, TOK), 0)
    c = lax.broadcasted_iota(jnp.int32, (TOK, TOK), 1)
    tri = (c <= r).astype(F32)
    cum = jnp.dot(tri, logs, precision=lax.Precision.HIGHEST, preferred_element_type=F32)
    ec_out[...] = jnp.exp(cum)
    grow = step * jnp.exp(-cum)
    tot = cum[TOK - 1 : TOK, :]
    etot = jnp.exp(tot)
    sub = lax.broadcasted_iota(jnp.int32, (16, 128), 0)
    for g in range(GROUPS):
        xc = slice(g * GW, (g + 1) * GW)
        bc = slice(g * STATE, (g + 1) * STATE)
        xs = tap(padx.at[g % 2], hx[:, xc], x[:, xc], cw[:, xc])
        bm = tap(padb.at[g % 2], hb[:, bc], b[:, bc], cbw[:, bc]).astype(BF)
        v = (xs * spread(grow, g)).astype(BF)
        xs_out[:, xc] = xs
        v_out[:, xc] = v
        b_out[:, bc] = bm
        fresh = lax.dot_general(v, bm, (((0,), (0,)), ((), ())), preferred_element_type=F32)
        for i in range(2):
            h = g * PER + 2 * i
            o = g * 2 + i
            for j in range(2):
                k = (2 * i + j) * HEAD_DIM
                st[o, j * HEAD_DIM : (j + 1) * HEAD_DIM, :] = (
                    fresh[k : k + HEAD_DIM, :] * etot[0:1, h + j : h + j + 1]
                ).astype(BF)
            tail = jnp.zeros((16, 128), F32)
            for j in range(2):
                rest = jnp.broadcast_to(tot[0:1, h + j : h + j + 1], (16, 128))
                for q in range(3):
                    part = rest.astype(BF).astype(F32)
                    tail = jnp.where(sub == 3 * j + q, part, tail)
                    rest = rest - part
            st[o, 2 * HEAD_DIM : ST_ROWS, :] = tail.astype(BF)


def inner_kernel(c, hc, ccw, v, bm, xs, ec, skip, a_out, c_out, padc):
    r = lax.broadcasted_iota(jnp.int32, (TOK, TOK), 0)
    s = lax.broadcasted_iota(jnp.int32, (TOK, TOK), 1)
    lower = s <= r
    cols = ec[...]
    sk = jnp.broadcast_to(skip[...], (TOK, HEADS))
    for g in range(GROUPS):
        xc = slice(g * GW, (g + 1) * GW)
        bc = slice(g * STATE, (g + 1) * STATE)
        cm = tap(padc.at[g % 2], hc[:, bc], c[:, bc], ccw[:, bc]).astype(BF)
        c_out[:, bc] = cm
        cb = lax.dot_general(cm, bm[:, bc], (((1,), (1,)), ((), ())), preferred_element_type=F32)
        cb = jnp.where(lower, cb, 0.0).astype(BF)
        u = jnp.dot(cb, v[:, xc], preferred_element_type=F32)
        a_out[:, xc] = u * spread(cols, g) + xs[:, xc] * spread(sk, g)


def carry_kernel(got, out):
    row = lax.broadcasted_iota(jnp.int32, (2 * HEAD_DIM, 128), 0)
    carry = jnp.zeros((2 * HEAD_DIM, 128), F32)
    count = got.shape[0]
    for i in range(count):
        out[i] = carry.astype(BF)
        if i + 1 < count:
            tail = got[i, 2 * HEAD_DIM : ST_ROWS, :].astype(F32)
            fa = jnp.exp(tail[0:1] + tail[1:2] + tail[2:3])
            fb = jnp.exp(tail[3:4] + tail[4:5] + tail[5:6])
            factor = jnp.where(row < HEAD_DIM, fa, fb)
            carry = carry * factor + got[i, 0 : 2 * HEAD_DIM, :].astype(F32)


def routes_kernel(routes, rw, d_out, hi_out, lo_out):
    e = lax.broadcasted_iota(jnp.int32, (TOK, 128), 1)
    r = lax.broadcasted_iota(jnp.int32, (TOK, TOK), 0)
    s = lax.broadcasted_iota(jnp.int32, (TOK, TOK), 1)
    tri = (s < r).astype(BF)
    ids = routes[...]
    hot = [(ids[:, k : k + 1] == e).astype(F32) for k in range(2)]
    before0 = jnp.dot(tri, hot[0].astype(BF), preferred_element_type=F32)
    before1 = jnp.dot(tri, hot[1].astype(BF), preferred_element_type=F32)
    before1 = before1 + jnp.sum(hot[0], axis=0, keepdims=True)
    pos = [
        jnp.sum(before0 * hot[0], axis=1, keepdims=True).astype(jnp.int32),
        jnp.sum(before1 * hot[1], axis=1, keepdims=True).astype(jnp.int32),
    ]
    lane = lax.broadcasted_iota(jnp.int32, (TOK, ROWS), 1)
    w = rw[...]
    for h in range(2):
        mask = [lane == ids[:, k : k + 1] * 8 + pos[k] + 4 * h for k in range(2)]
        disp = jnp.where(mask[0] | mask[1], 1.0, 0.0)
        d_out[:, h * TOK : (h + 1) * TOK] = disp.T.astype(BF)
        comb = jnp.where(mask[0], w[:, 0:1], 0.0) + jnp.where(mask[1], w[:, 1:2], 0.0)
        hi = comb.astype(BF)
        hi_out[h * TOK : (h + 1) * TOK, :] = hi
        lo_out[h * TOK : (h + 1) * TOK, :] = (comb - hi.astype(F32)).astype(BF)


def mix_kernel(
    place, a, cm, ec, pref, gate, gain, resid, fgain, disp,
    w0, w1, w2, w3, w4, w5, w6, w7, mixed_out, ein_out, send, norm
):
    cols = ec[...]
    for g in range(GROUPS):
        xc = slice(g * GW, (g + 1) * GW)
        bc = slice(g * STATE, (g + 1) * STATE)
        outer = lax.dot_general(
            cm[:, bc], pref[g], (((1,), (1,)), ((), ())), preferred_element_type=F32
        )
        y = (a[:, xc] + outer * spread(cols, g)).astype(BF).astype(F32)
        y = y * silu(gate[:, xc].astype(F32))
        y = y * lax.rsqrt(jnp.mean(y * y, axis=1, keepdims=True) + EPS)
        norm[g] = (y * gain[:, xc]).astype(BF)
    proj = resid[...].astype(F32)
    for k, w in enumerate((w0, w1, w2, w3, w4, w5, w6, w7)):
        proj = proj + jnp.dot(norm[place[k]], w[...], preferred_element_type=F32)
    mixed = proj.astype(BF)
    mixed_out[...] = mixed
    m = mixed.astype(F32)
    ein = (m * lax.rsqrt(jnp.mean(m * m, axis=1, keepdims=True) + EPS) * fgain[...]).astype(BF)
    ein_out[...] = ein
    stack = jnp.concatenate([ein[:, :HALF], ein[:, HALF:]], axis=0)
    send[...] = jnp.dot(disp[...], stack, preferred_element_type=F32).astype(BF)


def shared_kernel(ein, mixed, sg, su, sd, out):
    x = ein[...]
    gate = jnp.dot(x, sg[...], preferred_element_type=F32)
    up = jnp.dot(x, su[...], preferred_element_type=F32)
    hidden = (silu(gate) * up).astype(BF)
    out[...] = mixed[...].astype(F32) + jnp.dot(hidden, sd[...], preferred_element_type=F32)


def expert_kernel(got, wg, wu, wd, out, xbuf):
    n = 256
    sub = lax.broadcasted_iota(jnp.int32, (ROWS // 16, 8, n), 1)
    for q in range(HALF // n):
        t = got[:, q * n : (q + 1) * n].astype(F32).reshape(ROWS // 16, 2, 8, n)
        r0, r1 = t[:, 0], t[:, 1]
        x0 = jnp.where(sub < 4, r0, pltpu.roll(r1, 4, 1))
        x1 = jnp.where(sub < 4, pltpu.roll(r0, 4, 1), r1)
        xbuf[:, q * n : (q + 1) * n] = x0.reshape(ROWS // 2, n).astype(BF)
        xbuf[:, HALF + q * n : HALF + (q + 1) * n] = x1.reshape(ROWS // 2, n).astype(BF)
    x = xbuf[...]
    gate = jnp.dot(x, wg[...], preferred_element_type=F32)
    up = jnp.dot(x, wu[...], preferred_element_type=F32)
    hidden = (silu(gate) * up).astype(BF)
    for q in range(HALF // n):
        y0 = jnp.dot(hidden, wd[:, q * n : (q + 1) * n], preferred_element_type=F32)
        y1 = jnp.dot(hidden, wd[:, HALF + q * n : HALF + (q + 1) * n], preferred_element_type=F32)
        y0 = y0.reshape(ROWS // 16, 8, n)
        y1 = y1.reshape(ROWS // 16, 8, n)
        o0 = jnp.where(sub < 4, y0, pltpu.roll(y1, 4, 1))
        o1 = jnp.where(sub < 4, pltpu.roll(y0, 4, 1), y1)
        out[:, q * n : (q + 1) * n] = jnp.stack([o0, o1], axis=1).reshape(ROWS, n).astype(BF)


def combine_kernel(got, hi, lo, base, out):
    g = got[...]
    y = jnp.dot(hi[...], g, preferred_element_type=F32) + jnp.dot(
        lo[...], g, preferred_element_type=F32
    )
    out[:, :HALF] = (base[:, :HALF] + y[:TOK]).astype(BF)
    out[:, HALF:] = (base[:, HALF:] + y[TOK:]).astype(BF)


def body(
    residual,
    head_input,
    gate_input,
    b_input,
    c_input,
    step_input,
    conv_weight,
    conv_b_weight,
    conv_c_weight,
    step_bias,
    decay_log,
    skip,
    norm_gain,
    out_weight,
    ffn_gain,
    shared_gate,
    shared_up,
    shared_down,
    expert_gate,
    expert_up,
    expert_down,
    routes,
    route_weights,
):
    ways = lax.axis_size("sp")
    dps = lax.axis_size("dp")
    x, b, c = head_input[0], b_input[0], c_input[0]
    ends = jnp.concatenate([x[TOK - 8 :], b[TOK - 8 :], c[TOK - 8 :]], axis=1)
    halo = lax.ppermute(ends, "sp", [(i, i + 1) for i in range(ways - 1)])

    def along(v, k):
        return lax.ppermute(v, "dp", [(i, (i + k) % dps) for i in range(dps)])

    def swap(v):
        return lax.ppermute(v, "dp", [(i, i ^ 1) for i in range(dps)])

    own = [out_weight, along(out_weight, 2), along(out_weight, -2), along(out_weight, 4)]
    pieces = own + [swap(v) for v in own]
    me = lax.axis_index("dp")
    mine = [me, (me + dps - 2) % dps, (me + 2) % dps, (me + 4) % dps]
    place = jnp.stack(mine + [v ^ 1 for v in mine]).astype(jnp.int32)

    st, v, xs, bm, ec = call(
        states_kernel,
        [((ways, ST_ROWS, 128), BF), ((TOK, D), BF), ((TOK, D), F32), ((TOK, 1024), BF), ((TOK, HEADS), F32)],
        9,
        "states",
        scratch=[pltpu.VMEM((2, TOK + 8, GW), F32), pltpu.VMEM((2, TOK + 8, STATE), F32)],
    )(
        x, b, halo[:, :D], halo[:, D : D + 1024], step_input[0], conv_weight, conv_b_weight,
        step_bias[None], decay_log[None],
    )
    got = lax.all_to_all(st, "sp", split_axis=0, concat_axis=0, tiled=True)
    a, cm = call(
        inner_kernel,
        [((TOK, D), F32), ((TOK, 1024), BF)],
        8,
        "inner",
        scratch=[pltpu.VMEM((2, TOK + 8, STATE), F32)],
        flops=4 * 10**9,
    )(c, halo[:, D + 1024 :], conv_c_weight, v, bm, xs, ec, skip[None])
    disp, hi, lo = call(
        routes_kernel,
        [((ROWS, 2 * TOK), BF), ((2 * TOK, ROWS), BF), ((2 * TOK, ROWS), BF)],
        2,
        "routing",
        flops=2 * 10**9,
    )(routes[0], route_weights[0])
    (carried,) = call(carry_kernel, [((ways, 128, 128), BF)], 1, "carry")(got)
    pref = lax.all_to_all(carried, "sp", split_axis=0, concat_axis=0, tiled=True)
    mixed, ein, send = call(
        mix_kernel,
        [((TOK, D), BF), ((TOK, D), BF), ((ROWS, HALF), BF)],
        18,
        "mix",
        scratch=[pltpu.VMEM((GROUPS, TOK, GW), BF)],
        smem_in=(0,),
        flops=2 * 10**9,
    )(
        place, a, cm, ec, pref.reshape(GROUPS, GW, STATE), gate_input[0], norm_gain[None],
        residual[0], ffn_gain[None], disp, *pieces,
    )
    experts = ways * dps
    arrived = lax.all_to_all(
        send.reshape(experts, 8, HALF), ("sp", "dp"), split_axis=0, concat_axis=0, tiled=True
    )
    (base,) = call(shared_kernel, [((TOK, D), F32)], 5, "shared", flops=4 * 10**9)(
        ein, mixed, shared_gate, shared_up, shared_down
    )
    (done,) = call(
        expert_kernel,
        [((ROWS, HALF), BF)],
        4,
        "expert",
        scratch=[pltpu.VMEM((ROWS // 2, D), BF)],
        flops=3 * 10**9,
    )(arrived.reshape(ROWS, HALF), expert_gate[0], expert_up[0], expert_down[0])
    back = lax.all_to_all(
        done.reshape(experts, 8, HALF), ("sp", "dp"), split_axis=0, concat_axis=0, tiled=True
    )
    (out,) = call(combine_kernel, [((TOK, D), BF)], 4, "combine")(
        back.reshape(ROWS, HALF), hi, lo, base
    )
    return out[None]


def solution(mesh):
    rows = P("dp", "sp", None)
    one = P(("sp", "dp"), None, None)
    return jax.shard_map(
        body,
        mesh=mesh,
        in_specs=(
            (rows,) * 6 + (P(),) * 7 + (P("dp", None),) + (P(),) * 4 + (one,) * 3 + (rows, rows)
        ),
        out_specs=rows,
        check_vma=False,
    )
```

time: 266 us -> 171 us (0.64)
  other arithmetic: 47.6 us -> 0.01 us
  local copies, waits for them, and re-layouts: 55.9 us -> 9.26 us
  Pallas kernels: 0 us -> 40.2 us
  matrix products: 31.6 us -> 0 us
  between operations: 13.7 us -> 0.09 us
  starting transfers between devices: 29 us -> 33.9 us
  waiting for transfers between devices: 46.3 us -> 49.4 us
    pallas_call x0 -> x8, Pallas kernels: none -> 40.2 us  [the longest x1 8.79 us: body(): call(mix_kernel, [((TOK, D), BF), ((TOK, D), BF), ((ROWS, HALF), BF)], 18...]
    dot_general x8 -> x0, matrix products: 31.6 us -> none  [the longest x1 7.52 us: serve_experts(): jnp.einsum('aenf,efc->aenc', hidden, down_w, preferred_element_type=jnp.f...]
    ppermute x0 -> x8, waiting for transfers between devices: none -> 20.2 us  [the longest x3 20.2 us: along(): return lax.ppermute(v, 'dp', [(i, (i + k) % dps) for i in range(dps)])]
    all_to_all x5 -> x3, waiting for transfers between devices: 45.7 us -> 29.1 us  [the longest x1 25.3 us: body(): lax.all_to_all(done.reshape(experts, 8, HALF), ('sp', 'dp'), split_axis=0...]
    add x16 -> x0, other arithmetic: 14.6 us -> none  [advance(): return (carry * factor[:, None, None] + fresh, carry)]
    ppermute x0 -> x8, starting transfers between devices: none -> 13.3 us  [the longest x3 5.11 us: along(): return lax.ppermute(v, 'dp', [(i, (i + k) % dps) for i in range(dps)])]
    convert_element_type x4 -> x0, local copies, waits for them, and re-layouts: 11.7 us -> none  [the longest x1 4.52 us: serve_experts(): jnp.einsum('aenf,efc->aenc', hidden, down_w, preferred_element_type=jnp.f...]
    reshape x3 -> x0, local copies, waits for them, and re-layouts: 10.7 us -> none  [the longest x1 4.11 us: body(): outgoing = outgoing.reshape(experts, slots, D)]
  transfers between devices with their start and end apart: 6 -> 11, of which waited for: 5 -> 3; matrix products, arithmetic and copies ran while one was open for 30% -> 4% of each run, Pallas kernels for 0% -> 11%
where the time goes in v1:
time: 171 us; the launch traced here: 170 us
  waiting for transfers between devices  49.4 us (29%)
  Pallas kernels  40.2 us (24%)
  blocking collectives  37.3 us (22%)
  starting transfers between devices  33.9 us (20%)
  local copies, waits for them, and re-layouts  9.26 us (5%)
    all_to_all x1, blocking collectives, body(): lax.all_to_all(send.reshape(experts, 8, HALF), ('sp', 'dp'), split_axis=0...  37.3 us
    all_to_all x1, waiting for transfers between devices, body(): lax.all_to_all(done.reshape(experts, 8, HALF), ('sp', 'dp'), split_axis=0...  25.3 us
    ppermute x3, waiting for transfers between devices, along(): return lax.ppermute(v, 'dp', [(i, (i + k) % dps) for i in range(dps)])  20.2 us
    pallas_call x1, Pallas kernels, body(): call(mix_kernel, [((TOK, D), BF), ((TOK, D), BF), ((ROWS, HALF), BF)], 18...  8.79 us
    all_to_all x1, starting transfers between devices, body(): got = lax.all_to_all(st, 'sp', split_axis=0, concat_axis=0, tiled=True)  8.46 us
    pallas_call x1, Pallas kernels, body(): call(expert_kernel, [((ROWS, HALF), BF)], 4, 'expert', scratch=[pltpu.VME...  8.3 us
    all_to_all x1, starting transfers between devices, body(): lax.all_to_all(carried, 'sp', split_axis=0, concat_axis=0, tiled=True)  7.77 us
    unnamed x17, local copies, waits for them, and re-layouts  5.85 us
  transfers between devices with their start and end apart: 11, of which 3 were waited for; matrix products, arithmetic and copies ran while one was open for 4% of the time, Pallas kernels for 11%

profile of v1, /device:TPU:1, one launch (start us, length us, event | category | flops | bytes accessed | tf_op | source)
XLA Modules:
  0.0 170.1 jit_solution(12951046522764160324)
XLA Ops:
  0.0 3.6 %collective-permute-start.3 = (bf16[256,2048]{1,0:T(8,128)(2,1)}, bf16[256,2048]{1,0:T(8,128)(2,1)S(1)}, u32[]{:S(2)}, u32[]{:S(2)}) collective-permute-start(bf16[256,2048]{1,0:T(8,128)(2,1)} %w0.1), channel_id=1, source_target_pairs={{0,4},{1,5},{2,6},{3,7},{4,0},{5,1},{6,2},{7,3},{8,12},{9,13},{10,... | collective-permute-start | bytes 3145736 | tf_op jit(solution)/shard_map/ppermute | solution.py:267
  3.7 0.9 collective-permute-start.2
  5.1 0.8 slice_bitcast_fusion
  5.9 0.7 slice_bitcast_fusion.1
  6.6 3.2 %collective-permute-start = (bf16[8,4096]{1,0:T(8,128)(2,1)S(1)}, bf16[8,4096]{1,0:T(8,128)(2,1)S(1)}, u32[]{:S(2)}, u32[]{:S(2)}) collective-permute-start(bf16[8,4096]{1,0:T(8,128)(2,1)S(1)} %pad_maximum_fusion), channel_id=1, source_target_pairs={{0,8},{8,16},{16,24},{24,32},{32,40},{40,48},{48,56},{56,64},{64,7... | collective-permute-start | bytes 196616 | tf_op jit(solution)/shard_map/ppermute | solution.py:264
  9.8 1.4 copy.24
  11.2 0.6 slice.37.hx
  11.9 0.6 fusion
  12.5 4.8 %states.1 = (bf16[16,144,128]{2,1,0:T(8,128)(2,1)}, bf16[128,2048]{1,0:T(8,128)(2,1)}, f32[128,2048]{1,0:T(8,128)}, bf16[128,1024]{1,0:T(8,128)(2,1)}, f32[128,32]{1,0:T(8,128)}) custom-call(bf16[128,2048]{1,0:T(8,128)(2,1)} %bitcast.41, bf16[128,1024]{1,0:T(8,128)(2,1)} %bitcast.44, bf16[8,2048]{1,0:T(8,128)(2,1)} %slice.37.hx, ...), custom_call_target="tpu_custom_call" | custom-call | flops 1000000 | bytes 1000000 | tf_op jit(solution)/shard_map/states/pallas_call | solution.py:278
  17.3 8.5 %all-to-all-start = ((bf16[16,144,128]{2,1,0:T(8,128)(2,1)}), bf16[16,144,128]{2,1,0:T(8,128)(2,1)S(1)}, u32[]{:S(2)}, u32[]{:S(2)}) async-start(bf16[16,144,128]{2,1,0:T(8,128)(2,1)} %get-tuple-element.24), calls=%async_computation | async-start | bytes 1179648 | tf_op jit(solution)/shard_map/all_to_all | solution.py:288
  25.7 2.7 %collective-permute-start.4 = (bf16[256,2048]{1,0:T(8,128)(2,1)S(1)}, bf16[256,2048]{1,0:T(8,128)(2,1)}, u32[]{:S(2)}, u32[]{:S(2)}) collective-permute-start(bf16[256,2048]{1,0:T(8,128)(2,1)S(1)} %copy-done.3), channel_id=1, source_target_pairs={{0,1},{1,0},{2,3},{3,2},{4,5},{5,4},{6,7},{7,6},{8,9},{9,8},{10,11... | collective-permute-start | bytes 3145736 | tf_op jit(solution)/shard_map/ppermute | solution.py:270
  28.5 0.7 collective-permute-start.7
  29.2 20.2 %collective-permute-done.2.w2 = bf16[256,2048]{1,0:T(8,128)(2,1)} collective-permute-done((bf16[256,2048]{1,0:T(8,128)(2,1)}, bf16[256,2048]{1,0:T(8,128)(2,1)}, u32[]{:S(2)}, u32[]{:S(2)}) %collective-permute-start.2) | collective-permute-done | bytes 1048608 | tf_op jit(solution)/shard_map/ppermute | solution.py:267
  49.4 1.5 collective-permute-start.6
  50.9 0.7 copy.25
  51.7 0.7 copy.26
  52.4 0.7 stack.35.place
  53.1 0.9 copy-done.1
  53.9 2.0 %carry.1 = bf16[16,128,128]{2,1,0:T(8,128)(2,1)} custom-call(bf16[16,144,128]{2,1,0:T(8,128)(2,1)} %copy-done.1), custom_call_target="tpu_custom_call" | custom-call | flops 1000000 | bytes 1000000 | tf_op jit(solution)/shard_map/carry/pallas_call | solution.py:304
  56.0 7.8 %all-to-all-start.1 = ((bf16[16,128,128]{2,1,0:T(8,128)(2,1)}), bf16[16,128,128]{2,1,0:T(8,128)(2,1)S(1)}, u32[]{:S(2)}, u32[]{:S(2)}) async-start(bf16[16,128,128]{2,1,0:T(8,128)(2,1)} %carry.1), calls=%async_computation.1 | async-start | bytes 1048576 | tf_op jit(solution)/shard_map/all_to_all | solution.py:305
  63.7 2.8 %routing.1 = (bf16[1024,256]{1,0:T(8,128)(2,1)}, bf16[256,1024]{1,0:T(8,128)(2,1)}, bf16[256,1024]{1,0:T(8,128)(2,1)}) custom-call(s32[128,2]{1,0:T(8,128)} %bitcast.46, f32[128,2]{1,0:T(8,128)} %bitcast.47), custom_call_target="tpu_custom_call" | custom-call | flops 2000000000 | bytes 1000000 | tf_op jit(solution)/shard_map/routing/pallas_call | solution.py:297
  66.6 3.9 %inner.1 = (f32[128,2048]{1,0:T(8,128)}, bf16[128,1024]{1,0:T(8,128)(2,1)}) custom-call(bf16[128,1024]{1,0:T(8,128)(2,1)} %bitcast.50, bf16[8,1024]{1,0:T(8,128)(2,1)} %get-tuple-element.32.hc, bf16[4,1024]{1,0:T(4,128)(2,1)} %ccw.1, bf16[128,2048]{1,0:T(8,128)(2,1)} %get-tuple-element.18.v, bf16[128,1024]{1,0:T(8,128)(2,1)} %get-tuple-element.19.bm, ...), custom_call_target="tpu_custom_call" | custom-call | flops 4000000000 | bytes 1000000 | tf_op jit(solution)/shard_map/inner/pallas_call | solution.py:289
  70.5 3.8 %all-to-all-done.1 = bf16[16,128,128]{2,1,0:T(8,128)(2,1)S(1)} async-done(((bf16[16,128,128]{2,1,0:T(8,128)(2,1)}), bf16[16,128,128]{2,1,0:T(8,128)(2,1)S(1)}, u32[]{:S(2)}, u32[]{:S(2)}) %all-to-all-start.1) | async-done | bytes 524320 | tf_op jit(solution)/shard_map/all_to_all | solution.py:305
  74.3 0.8 copy-done.2
  75.1 8.8 %mix.1 = (bf16[128,2048]{1,0:T(8,128)(2,1)}, bf16[128,2048]{1,0:T(8,128)(2,1)}, bf16[1024,1024]{1,0:T(8,128)(2,1)}) custom-call(s32[8]{0:T(128)} %stack.35.place, f32[128,2048]{1,0:T(8,128)} %get-tuple-element.22.a, bf16[128,1024]{1,0:T(8,128)(2,1)} %get-tuple-element.23.cm, f32[128,32]{1,0:T(8,128)} %get-tuple-element.21.ec, bf16[8,256,128]{2,1,0:T(8,128)(2,1)} %bitcast.37, ...), custom_call_target="tpu_custom_call" | custom-call | flops 2000000000 | bytes 1000000 | tf_op jit(solution)/shard_map/mix/pallas_call | solution.py:306
  83.9 37.3 %all_to_all.20 = bf16[128,8,1024]{2,1,0:T(8,128)(2,1)} all-to-all(bf16[128,8,1024]{2,1,0:T(8,128)(2,1)} %bitcast.38), channel_id=1, replica_groups=mesh['sp'=16,'dp'=8] {'sp','dp'}, dimensions={0} | all-to-all | bytes 4194304 | tf_op jit(solution)/shard_map/all_to_all | solution.py:319
  121.2 8.3 %expert.1 = bf16[1024,1024]{1,0:T(8,128)(2,1)} custom-call(bf16[1024,1024]{1,0:T(8,128)(2,1)} %bitcast.40, bf16[2048,512]{1,0:T(8,128)(2,1)} %bitcast.53, bf16[2048,512]{1,0:T(8,128)(2,1)} %bitcast.54, bf16[512,2048]{1,0:T(8,128)(2,1)} %bitcast.55), custom_call_target="tpu_custom_call" | custom-call | flops 3000000000 | bytes 1000000 | tf_op jit(solution)/shard_map/expert/pallas_call | solution.py:325
  129.6 4.4 %all-to-all-start.3 = ((bf16[128,8,1024]{2,1,0:T(8,128)(2,1)}), bf16[128,8,1024]{2,1,0:T(8,128)(2,1)S(1)}, u32[]{:S(2)}, u32[]{:S(2)}) async-start(bf16[128,8,1024]{2,1,0:T(8,128)(2,1)} %bitcast.39), calls=%async_computation.3 | async-start | bytes 4194304 | tf_op jit(solution)/shard_map/all_to_all | solution.py:333
  134.0 5.3 %shared.1.base = f32[128,2048]{1,0:T(8,128)} custom-call(bf16[128,2048]{1,0:T(8,128)(2,1)} %get-tuple-element.29.ein, bf16[128,2048]{1,0:T(8,128)(2,1)} %get-tuple-element.30.mixed, bf16[2048,512]{1,0:T(8,128)(2,1)} %sg.1, bf16[2048,512]{1,0:T(8,128)(2,1)} %su.1, bf16[512,2048]{1,0:T(8,128)(2,1)} %sd.1), custom_call_target="tpu_custom_call" | custom-call | flops 4000000000 | bytes 1000000 | tf_op jit(solution)/shard_map/shared/pallas_call | solution.py:322
  139.2 25.3 %all-to-all-done.3 = bf16[128,8,1024]{2,1,0:T(8,128)(2,1)S(1)} async-done(((bf16[128,8,1024]{2,1,0:T(8,128)(2,1)}), bf16[128,8,1024]{2,1,0:T(8,128)(2,1)S(1)}, u32[]{:S(2)}, u32[]{:S(2)}) %all-to-all-start.3) | async-done | bytes 2097184 | tf_op jit(solution)/shard_map/all_to_all | solution.py:333
  164.6 1.3 copy-done
  165.9 4.2 %combine.1 = bf16[128,2048]{1,0:T(8,128)(2,1)} custom-call(bf16[1024,1024]{1,0:T(8,128)(2,1)} %bitcast.36, bf16[256,1024]{1,0:T(8,128)(2,1)} %get-tuple-element.27.hi, bf16[256,1024]{1,0:T(8,128)(2,1)} %get-tuple-element.28.lo, f32[128,2048]{1,0:T(8,128)} %shared.1.base), custom_call_target="tpu_custom_call" | custom-call | flops 1000000 | bytes 1000000 | tf_op jit(solution)/shard_map/combine/pallas_call | solution.py:336
  (22 shorter events, 0.7 us)
Async XLA Ops:
  0.0 25.7 %copy-start.3 = (bf16[256,2048]{1,0:T(8,128)(2,1)S(1)}, bf16[256,2048]{1,0:T(8,128)(2,1)}, u32[]{:S(2)}) copy-start(bf16[256,2048]{1,0:T(8,128)(2,1)} %w0.1) | copy-start | bytes 3145732
  0.0 50.9 %copy-start.5 = (s32[1,128,2]{1,2,0:T(2,128)S(1)}, s32[1,128,2]{1,2,0:T(2,128)}, u32[]{:S(2)}) copy-start(s32[1,128,2]{1,2,0:T(2,128)} %param.44) | copy-start | bytes 3076
  0.0 51.7 %copy-start.6 = (f32[1,128,2]{1,2,0:T(2,128)S(1)}, f32[1,128,2]{1,2,0:T(2,128)}, u32[]{:S(2)}) copy-start(f32[1,128,2]{1,2,0:T(2,128)} %param.45) | copy-start | bytes 3076
  0.0 28.5 %collective-permute-start.3 = (bf16[256,2048]{1,0:T(8,128)(2,1)}, bf16[256,2048]{1,0:T(8,128)(2,1)S(1)}, u32[]{:S(2)}, u32[]{:S(2)}) collective-permute-start(bf16[256,2048]{1,0:T(8,128)(2,1)} %w0.1), channel_id=1, source_target_pairs={{0,4},{1,5},{2,6},{3,7},{4,0},{5,1},{6,2},{7,3},{8,12},{9,13},{10,... | collective-permute-start | bytes 3145736 | tf_op jit(solution)/shard_map/ppermute | solution.py:267
  3.7 45.7 %collective-permute-start.2 = (bf16[256,2048]{1,0:T(8,128)(2,1)}, bf16[256,2048]{1,0:T(8,128)(2,1)}, u32[]{:S(2)}, u32[]{:S(2)}) collective-permute-start(bf16[256,2048]{1,0:T(8,128)(2,1)} %w0.1), channel_id=1, source_target_pairs={{0,6},{1,7},{2,0},{3,1},{4,2},{5,3},{6,4},{7,5},{8,14},{9,15},{10,... | collective-permute-start | bytes 3145736 | tf_op jit(solution)/shard_map/ppermute | solution.py:267
  4.5 46.4 %collective-permute-start.1 = (bf16[256,2048]{1,0:T(8,128)(2,1)}, bf16[256,2048]{1,0:T(8,128)(2,1)}, u32[]{:S(2)}, u32[]{:S(2)}) collective-permute-start(bf16[256,2048]{1,0:T(8,128)(2,1)} %w0.1), channel_id=1, source_target_pairs={{0,2},{1,3},{2,4},{3,5},{4,6},{5,7},{6,0},{7,1},{8,10},{9,11},{10,... | collective-permute-start | bytes 3145736 | tf_op jit(solution)/shard_map/ppermute | solution.py:267
  6.6 4.6 %collective-permute-start = (bf16[8,4096]{1,0:T(8,128)(2,1)S(1)}, bf16[8,4096]{1,0:T(8,128)(2,1)S(1)}, u32[]{:S(2)}, u32[]{:S(2)}) collective-permute-start(bf16[8,4096]{1,0:T(8,128)(2,1)S(1)} %pad_maximum_fusion), channel_id=1, source_target_pairs={{0,8},{8,16},{16,24},{24,32},{32,40},{40,48},{48,56},{56,64},{64,7... | collective-permute-start | bytes 196616 | tf_op jit(solution)/shard_map/ppermute | solution.py:264
  17.3 35.8 %all-to-all-start = ((bf16[16,144,128]{2,1,0:T(8,128)(2,1)}), bf16[16,144,128]{2,1,0:T(8,128)(2,1)S(1)}, u32[]{:S(2)}, u32[]{:S(2)}) async-start(bf16[16,144,128]{2,1,0:T(8,128)(2,1)} %get-tuple-element.24), calls=%async_computation | async-start | bytes 1179648 | tf_op jit(solution)/shard_map/all_to_all | solution.py:288
  25.7 44.8 %collective-permute-start.4 = (bf16[256,2048]{1,0:T(8,128)(2,1)S(1)}, bf16[256,2048]{1,0:T(8,128)(2,1)}, u32[]{:S(2)}, u32[]{:S(2)}) collective-permute-start(bf16[256,2048]{1,0:T(8,128)(2,1)S(1)} %copy-done.3), channel_id=1, source_target_pairs={{0,1},{1,0},{2,3},{3,2},{4,5},{5,4},{6,7},{7,6},{8,9},{9,8},{10,11... | collective-permute-start | bytes 3145736 | tf_op jit(solution)/shard_map/ppermute | solution.py:270
  28.5 42.0 %copy-start.4 = (bf16[256,2048]{1,0:T(8,128)(2,1)}, bf16[256,2048]{1,0:T(8,128)(2,1)S(1)}, u32[]{:S(2)}) copy-start(bf16[256,2048]{1,0:T(8,128)(2,1)S(1)} %collective-permute-done.3.w3) | copy-start | bytes 3145732
  28.5 45.9 %collective-permute-start.7 = (bf16[256,2048]{1,0:T(8,128)(2,1)S(1)}, bf16[256,2048]{1,0:T(8,128)(2,1)}, u32[]{:S(2)}, u32[]{:S(2)}) collective-permute-start(bf16[256,2048]{1,0:T(8,128)(2,1)S(1)} %collective-permute-done.3.w3), channel_id=1, source_target_pairs={{0,1},{1,0},{2,3},{3,2},{4,5},{5,4},{6,7},{7,6},{8,9},{9,8},{10,11... | collective-permute-start | bytes 3145736 | tf_op jit(solution)/shard_map/ppermute | solution.py:270
  49.4 25.0 %collective-permute-start.6 = (bf16[256,2048]{1,0:T(8,128)(2,1)}, bf16[256,2048]{1,0:T(8,128)(2,1)}, u32[]{:S(2)}, u32[]{:S(2)}) collective-permute-start(bf16[256,2048]{1,0:T(8,128)(2,1)} %collective-permute-done.2.w2), channel_id=1, source_target_pairs={{0,1},{1,0},{2,3},{3,2},{4,5},{5,4},{6,7},{7,6},{8,9},{9,8},{10,11... | collective-permute-start | bytes 3145736 | tf_op jit(solution)/shard_map/ppermute | solution.py:270
  50.9 23.4 %collective-permute-start.5 = (bf16[256,2048]{1,0:T(8,128)(2,1)}, bf16[256,2048]{1,0:T(8,128)(2,1)}, u32[]{:S(2)}, u32[]{:S(2)}) collective-permute-start(bf16[256,2048]{1,0:T(8,128)(2,1)} %collective-permute-done.1.w1), channel_id=1, source_target_pairs={{0,1},{1,0},{2,3},{3,2},{4,5},{5,4},{6,7},{7,6},{8,9},{9,8},{10,11... | collective-permute-start | bytes 3145736 | tf_op jit(solution)/shard_map/ppermute | solution.py:270
  53.1 0.9 copy-start.1
  56.0 18.4 %all-to-all-start.1 = ((bf16[16,128,128]{2,1,0:T(8,128)(2,1)}), bf16[16,128,128]{2,1,0:T(8,128)(2,1)S(1)}, u32[]{:S(2)}, u32[]{:S(2)}) async-start(bf16[16,128,128]{2,1,0:T(8,128)(2,1)} %carry.1), calls=%async_computation.1 | async-start | bytes 1048576 | tf_op jit(solution)/shard_map/all_to_all | solution.py:305
  74.3 0.8 copy-start.2
  129.6 35.0 %all-to-all-start.3 = ((bf16[128,8,1024]{2,1,0:T(8,128)(2,1)}), bf16[128,8,1024]{2,1,0:T(8,128)(2,1)S(1)}, u32[]{:S(2)}, u32[]{:S(2)}) async-start(bf16[128,8,1024]{2,1,0:T(8,128)(2,1)} %bitcast.39), calls=%async_computation.3 | async-start | bytes 4194304 | tf_op jit(solution)/shard_map/all_to_all | solution.py:333
  164.6 1.3 copy-start

commit v2 on v1

--- a/solution.py
+++ b/solution.py
@@ -1,9 +1,12 @@
 import jax
 import jax.numpy as jnp
 from jax import lax
+from jax._src.core import MemorySpace
+from jax._src.state.primitives import with_memory_space_constraint
 from jax.experimental import pallas as pl
 from jax.experimental.pallas import tpu as pltpu
 from jax.sharding import PartitionSpec as P
+
 
 D = 2048
 HEADS = 32
@@ -29,16 +32,33 @@
     return pl.BlockSpec(memory_space=pltpu.SMEM)
 
 
-def call(kernel, outs, n_in, name, scratch=(), smem_in=(), flops=10**6, nbytes=10**6):
+def anywhere():
+    return pl.BlockSpec(memory_space=pl.ANY)
+
+
+def call(
+    kernel, outs, args, scratch=(), vmem=(), smem_in=(), raw=(), out_vmem=(), limit=12, flops=10**6
+):
+    placed = [
+        v
+        if i in smem_in
+        else pltpu.with_memory_space_constraint(v, pltpu.VMEM if i in vmem else pltpu.HBM)
+        for i, v in enumerate(args)
+    ]
     return pl.pallas_call(
         kernel,
-        out_shape=tuple(jax.ShapeDtypeStruct(s, d) for s, d in outs),
-        in_specs=[smem() if i in smem_in else full() for i in range(n_in)],
+        out_shape=tuple(
+            pltpu.VMEM(s, d) if i in out_vmem else pltpu.HBM(s, d)
+            for i, (s, d) in enumerate(outs)
+        ),
+        in_specs=[
+            smem() if i in smem_in else anywhere() if i in raw else full() for i in range(len(args))
+        ],
         out_specs=tuple(full() for _ in outs),
         scratch_shapes=list(scratch),
-        name=name,
-        cost_estimate=pl.CostEstimate(flops=flops, bytes_accessed=nbytes, transcendentals=0),
-    )
+        compiler_params=pltpu.CompilerParams(vmem_limit_bytes=limit << 20),
+        cost_estimate=pl.CostEstimate(flops=flops, bytes_accessed=10**6, transcendentals=0),
+    )(*placed)
 
 
 def silu(v):
@@ -65,9 +85,9 @@
 
 
 def states_kernel(
-    x, b, hx, hb, step_in, cw, cbw, bias, dlog, st, v_out, xs_out, b_out, ec_out, padx, padb
+    x, b, halo, step_in, cw, cbw, bias, dlog, st, v_out, xs_out, b_out, ec_out, padx, padb
 ):
-    s = step_in[...].astype(F32) + bias[...]
+    s = step_in[...].astype(F32).T + bias[...]
     step = jnp.maximum(s, 0.0) + jnp.log(1.0 + jnp.exp(-jnp.abs(s)))
     logs = step * (-jnp.exp(dlog[...]))
     r = lax.broadcasted_iota(jnp.int32, (TOK, TOK), 0)
@@ -82,8 +102,8 @@
     for g in range(GROUPS):
         xc = slice(g * GW, (g + 1) * GW)
         bc = slice(g * STATE, (g + 1) * STATE)
-        xs = tap(padx.at[g % 2], hx[:, xc], x[:, xc], cw[:, xc])
-        bm = tap(padb.at[g % 2], hb[:, bc], b[:, bc], cbw[:, bc]).astype(BF)
+        xs = tap(padx.at[g % 2], halo[:, xc], x[:, xc], cw[:, xc])
+        bm = tap(padb.at[g % 2], halo[:, D + g * STATE : D + (g + 1) * STATE], b[:, bc], cbw[:, bc]).astype(BF)
         v = (xs * spread(grow, g)).astype(BF)
         xs_out[:, xc] = xs
         v_out[:, xc] = v
@@ -107,7 +127,7 @@
             st[o, 2 * HEAD_DIM : ST_ROWS, :] = tail.astype(BF)
 
 
-def inner_kernel(c, hc, ccw, v, bm, xs, ec, skip, a_out, c_out, padc):
+def inner_kernel(c, halo, ccw, v, bm, xs, ec, skip, a_out, c_out, padc):
     r = lax.broadcasted_iota(jnp.int32, (TOK, TOK), 0)
     s = lax.broadcasted_iota(jnp.int32, (TOK, TOK), 1)
     lower = s <= r
@@ -116,7 +136,7 @@
     for g in range(GROUPS):
         xc = slice(g * GW, (g + 1) * GW)
         bc = slice(g * STATE, (g + 1) * STATE)
-        cm = tap(padc.at[g % 2], hc[:, bc], c[:, bc], ccw[:, bc]).astype(BF)
+        cm = tap(padc.at[g % 2], halo[:, D + 1024 + g * STATE : D + 1024 + (g + 1) * STATE], c[:, bc], ccw[:, bc]).astype(BF)
         c_out[:, bc] = cm
         cb = lax.dot_general(cm, bm[:, bc], (((1,), (1,)), ((), ())), preferred_element_type=F32)
         cb = jnp.where(lower, cb, 0.0).astype(BF)
@@ -143,7 +163,9 @@
     r = lax.broadcasted_iota(jnp.int32, (TOK, TOK), 0)
     s = lax.broadcasted_iota(jnp.int32, (TOK, TOK), 1)
     tri = (s < r).astype(BF)
-    ids = routes[...]
+    both = jnp.concatenate([routes[...].astype(F32), rw[...], jnp.zeros((4, TOK), F32)], axis=0).T
+    ids = both[:, 0:2].astype(jnp.int32)
+    w = both[:, 2:4]
     hot = [(ids[:, k : k + 1] == e).astype(F32) for k in range(2)]
     before0 = jnp.dot(tri, hot[0].astype(BF), preferred_element_type=F32)
     before1 = jnp.dot(tri, hot[1].astype(BF), preferred_element_type=F32)
@@ -153,7 +175,6 @@
         jnp.sum(before1 * hot[1], axis=1, keepdims=True).astype(jnp.int32),
     ]
     lane = lax.broadcasted_iota(jnp.int32, (TOK, ROWS), 1)
-    w = rw[...]
     for h in range(2):
         mask = [lane == ids[:, k : k + 1] * 8 + pos[k] + 4 * h for k in range(2)]
         disp = jnp.where(mask[0] | mask[1], 1.0, 0.0)
@@ -166,8 +187,16 @@
 
 def mix_kernel(
     place, a, cm, ec, pref, gate, gain, resid, fgain, disp,
-    w0, w1, w2, w3, w4, w5, w6, w7, mixed_out, ein_out, send, norm
+    w0, w1, w2, w3, w4, w5, w6, w7, w8, w9, mixed_out, ein_out, send, norm,
+    wide, half, sems
 ):
+    loads = []
+    for k, w in enumerate((w0, w1, w2, w5, w6, w7)):
+        loads.append(pltpu.make_async_copy(w, wide.at[k], sems.at[k]))
+    for k, w in enumerate((w3, w4, w8, w9)):
+        loads.append(pltpu.make_async_copy(w, half.at[k], sems.at[6 + k]))
+    for load in loads:
+        load.start()
     cols = ec[...]
     for g in range(GROUPS):
         xc = slice(g * GW, (g + 1) * GW)
@@ -180,8 +209,13 @@
         y = y * lax.rsqrt(jnp.mean(y * y, axis=1, keepdims=True) + EPS)
         norm[g] = (y * gain[:, xc]).astype(BF)
     proj = resid[...].astype(F32)
-    for k, w in enumerate((w0, w1, w2, w3, w4, w5, w6, w7)):
-        proj = proj + jnp.dot(norm[place[k]], w[...], preferred_element_type=F32)
+    for k in range(6):
+        loads[k].wait()
+        proj = proj + jnp.dot(norm[place[k]], wide[k], preferred_element_type=F32)
+    for k in range(4):
+        loads[6 + k].wait()
+        row = norm[place[6 + k // 2]][:, (k % 2) * 128 : (k % 2) * 128 + 128]
+        proj = proj + jnp.dot(row, half[k], preferred_element_type=F32)
     mixed = proj.astype(BF)
     mixed_out[...] = mixed
     m = mixed.astype(F32)
@@ -199,7 +233,11 @@
     out[...] = mixed[...].astype(F32) + jnp.dot(hidden, sd[...], preferred_element_type=F32)
 
 
-def expert_kernel(got, wg, wu, wd, out, xbuf):
+def expert_kernel(got, wg_in, wu_in, wd_in, out, xbuf, wg, wu, wd, sems):
+    pairs = ((wg_in, wg), (wu_in, wu), (wd_in, wd))
+    loads = [pltpu.make_async_copy(v, w, sems.at[k]) for k, (v, w) in enumerate(pairs)]
+    for load in loads:
+        load.start()
     n = 256
     sub = lax.broadcasted_iota(jnp.int32, (ROWS // 16, 8, n), 1)
     for q in range(HALF // n):
@@ -210,9 +248,12 @@
         xbuf[:, q * n : (q + 1) * n] = x0.reshape(ROWS // 2, n).astype(BF)
         xbuf[:, HALF + q * n : HALF + (q + 1) * n] = x1.reshape(ROWS // 2, n).astype(BF)
     x = xbuf[...]
+    loads[0].wait()
     gate = jnp.dot(x, wg[...], preferred_element_type=F32)
+    loads[1].wait()
     up = jnp.dot(x, wu[...], preferred_element_type=F32)
     hidden = (silu(gate) * up).astype(BF)
+    loads[2].wait()
     for q in range(HALF // n):
         y0 = jnp.dot(hidden, wd[:, q * n : (q + 1) * n], preferred_element_type=F32)
         y1 = jnp.dot(hidden, wd[:, HALF + q * n : HALF + (q + 1) * n], preferred_element_type=F32)
@@ -232,33 +273,23 @@
     out[:, HALF:] = (base[:, HALF:] + y[TOK:]).astype(BF)
 
 
-def body(
-    residual,
-    head_input,
-    gate_input,
-    b_input,
-    c_input,
-    step_input,
-    conv_weight,
-    conv_b_weight,
-    conv_c_weight,
-    step_bias,
-    decay_log,
-    skip,
-    norm_gain,
-    out_weight,
-    ffn_gain,
-    shared_gate,
-    shared_up,
-    shared_down,
-    expert_gate,
-    expert_up,
-    expert_down,
-    routes,
-    route_weights,
+def plain(v):
+    return with_memory_space_constraint(v, MemorySpace.Device)
+
+
+def exchange(v, axis):
+    return lax.all_to_all(plain(v), axis, split_axis=0, concat_axis=0, tiled=True)
+
+
+def layer(
+    residual, head_input, gate_input, b_input, c_input, step_input, conv_weight,
+    conv_b_weight, conv_c_weight, step_bias, decay_log, skip, norm_gain, out_weight,
+    ffn_gain, shared_gate, shared_up, shared_down, expert_gate, expert_up, expert_down,
+    routes, route_weights,
 ):
     ways = lax.axis_size("sp")
     dps = lax.axis_size("dp")
+    experts = ways * dps
     x, b, c = head_input[0], b_input[0], c_input[0]
     ends = jnp.concatenate([x[TOK - 8 :], b[TOK - 8 :], c[TOK - 8 :]], axis=1)
     halo = lax.ppermute(ends, "sp", [(i, i + 1) for i in range(ways - 1)])
@@ -269,81 +300,95 @@
     def swap(v):
         return lax.ppermute(v, "dp", [(i, i ^ 1) for i in range(dps)])
 
-    own = [out_weight, along(out_weight, 2), along(out_weight, -2), along(out_weight, 4)]
-    pieces = own + [swap(v) for v in own]
+    left = along(out_weight, 2)
+    right = along(out_weight, -2)
+    far = [along(left[:128], 2), along(right[128:], -2)]
+    pieces = [out_weight, left, right, *far, swap(out_weight), swap(left)]
+    pieces += [swap(right), swap(far[0]), swap(far[1])]
     me = lax.axis_index("dp")
-    mine = [me, (me + dps - 2) % dps, (me + 2) % dps, (me + 4) % dps]
-    place = jnp.stack(mine + [v ^ 1 for v in mine]).astype(jnp.int32)
+    near = [me, (me + dps - 2) % dps, (me + 2) % dps]
+    far_at = (me + 4) % dps
+    place = jnp.stack(near + [v ^ 1 for v in near] + [far_at, far_at ^ 1]).astype(jnp.int32)
 
     st, v, xs, bm, ec = call(
         states_kernel,
         [((ways, ST_ROWS, 128), BF), ((TOK, D), BF), ((TOK, D), F32), ((TOK, 1024), BF), ((TOK, HEADS), F32)],
-        9,
-        "states",
+        (x, b, halo, step_input[0].T, conv_weight, conv_b_weight, step_bias[None], decay_log[None]),
+        vmem=(2,),
         scratch=[pltpu.VMEM((2, TOK + 8, GW), F32), pltpu.VMEM((2, TOK + 8, STATE), F32)],
-    )(
-        x, b, halo[:, :D], halo[:, D : D + 1024], step_input[0], conv_weight, conv_b_weight,
-        step_bias[None], decay_log[None],
-    )
-    got = lax.all_to_all(st, "sp", split_axis=0, concat_axis=0, tiled=True)
+    )
+    got = exchange(st, "sp")
     a, cm = call(
         inner_kernel,
         [((TOK, D), F32), ((TOK, 1024), BF)],
-        8,
-        "inner",
+        (c, halo, conv_c_weight, v, bm, xs, ec, skip[None]),
         scratch=[pltpu.VMEM((2, TOK + 8, STATE), F32)],
         flops=4 * 10**9,
-    )(c, halo[:, D + 1024 :], conv_c_weight, v, bm, xs, ec, skip[None])
+    )
     disp, hi, lo = call(
         routes_kernel,
         [((ROWS, 2 * TOK), BF), ((2 * TOK, ROWS), BF), ((2 * TOK, ROWS), BF)],
-        2,
-        "routing",
+        (routes[0].T, route_weights[0].T),
         flops=2 * 10**9,
-    )(routes[0], route_weights[0])
-    (carried,) = call(carry_kernel, [((ways, 128, 128), BF)], 1, "carry")(got)
-    pref = lax.all_to_all(carried, "sp", split_axis=0, concat_axis=0, tiled=True)
+    )
+    (carried,) = call(carry_kernel, [((ways, 128, 128), BF)], (got,), vmem=(0,))
+    pref = exchange(carried, "sp")
     mixed, ein, send = call(
         mix_kernel,
         [((TOK, D), BF), ((TOK, D), BF), ((ROWS, HALF), BF)],
-        18,
-        "mix",
-        scratch=[pltpu.VMEM((GROUPS, TOK, GW), BF)],
+        (
+            place, a, cm, ec, pref.reshape(GROUPS, GW, STATE), gate_input[0], norm_gain[None],
+            residual[0], ffn_gain[None], disp, *pieces,
+        ),
+        scratch=[
+            pltpu.VMEM((GROUPS, TOK, GW), BF),
+            pltpu.VMEM((6, 256, D), BF),
+            pltpu.VMEM((4, 128, D), BF),
+            pltpu.SemaphoreType.DMA((10,)),
+        ],
         smem_in=(0,),
+        vmem=(4,),
+        raw=range(10, 20),
+        limit=32,
         flops=2 * 10**9,
-    )(
-        place, a, cm, ec, pref.reshape(GROUPS, GW, STATE), gate_input[0], norm_gain[None],
-        residual[0], ffn_gain[None], disp, *pieces,
-    )
-    experts = ways * dps
-    arrived = lax.all_to_all(
-        send.reshape(experts, 8, HALF), ("sp", "dp"), split_axis=0, concat_axis=0, tiled=True
-    )
-    (base,) = call(shared_kernel, [((TOK, D), F32)], 5, "shared", flops=4 * 10**9)(
-        ein, mixed, shared_gate, shared_up, shared_down
+    )
+    arrived = exchange(plain(send).reshape(experts, 8, HALF), ("sp", "dp"))
+    (base,) = call(
+        shared_kernel,
+        [((TOK, D), F32)],
+        (ein, mixed, shared_gate, shared_up, shared_down),
+        limit=20,
+        flops=4 * 10**9,
     )
     (done,) = call(
         expert_kernel,
         [((ROWS, HALF), BF)],
-        4,
-        "expert",
-        scratch=[pltpu.VMEM((ROWS // 2, D), BF)],
+        (arrived.reshape(ROWS, HALF), expert_gate[0], expert_up[0], expert_down[0]),
+        scratch=[
+            pltpu.VMEM((ROWS // 2, D), BF),
+            pltpu.VMEM((D, 512), BF),
+            pltpu.VMEM((D, 512), BF),
+            pltpu.VMEM((512, D), BF),
+            pltpu.SemaphoreType.DMA((3,)),
+        ],
+        vmem=(0,),
+        raw=(1, 2, 3),
+        out_vmem=(0,),
+        limit=32,
         flops=3 * 10**9,
-    )(arrived.reshape(ROWS, HALF), expert_gate[0], expert_up[0], expert_down[0])
-    back = lax.all_to_all(
-        done.reshape(experts, 8, HALF), ("sp", "dp"), split_axis=0, concat_axis=0, tiled=True
-    )
-    (out,) = call(combine_kernel, [((TOK, D), BF)], 4, "combine")(
-        back.reshape(ROWS, HALF), hi, lo, base
-    )
-    return out[None]
+    )
+    back = exchange(plain(done).reshape(experts, 8, HALF), ("sp", "dp"))
+    (out,) = call(
+        combine_kernel, [((TOK, D), BF)], (back.reshape(ROWS, HALF), hi, lo, base), vmem=(0,)
+    )
+    return plain(out)[None]
 
 
 def solution(mesh):
     rows = P("dp", "sp", None)
     one = P(("sp", "dp"), None, None)
     return jax.shard_map(
-        body,
+        layer,
         mesh=mesh,
         in_specs=(
             (rows,) * 6 + (P(),) * 7 + (P("dp", None),) + (P(),) * 4 + (one,) * 3 + (rows, rows)

time: 171 us -> 147 us (0.86)
  waiting for transfers between devices: 49.4 us -> 31.2 us
  local copies, waits for them, and re-layouts: 9.26 us -> 4.81 us
  Pallas kernels: 40.2 us -> 36.1 us
  starting transfers between devices: 33.9 us -> 35.7 us
    ppermute x3 -> x4, waiting for transfers between devices: 20.2 us -> 4.36 us  [along(): return lax.ppermute(v, 'dp', [(i, (i + k) % dps) for i in range(dps)])]
    unnamed x17 -> x10, local copies, waits for them, and re-layouts: 5.85 us -> 1.34 us
    pallas_call x8, Pallas kernels: 40.2 us -> 36.1 us  [call(): pl.pallas_call(kernel, out_shape=tuple((pltpu.VMEM(s, d) if i in out_vmem...]
    all_to_all x3, waiting for transfers between devices: 29.1 us -> 25.5 us  [exchange(): lax.all_to_all(plain(v), axis, split_axis=0, concat_axis=0, tiled=True)]
    ppermute x3 -> x4, starting transfers between devices: 5.11 us -> 6.61 us  [along(): return lax.ppermute(v, 'dp', [(i, (i + k) % dps) for i in range(dps)])]
    ppermute x4 -> x5, starting transfers between devices: 4.98 us -> 5.37 us  [swap(): return lax.ppermute(v, 'dp', [(i, i ^ 1) for i in range(dps)])]
  transfers between devices with their start and end apart: 11 -> 13, of which waited for: 3 -> 5; matrix products, arithmetic and copies ran while one was open for 4% -> 2% of each run, Pallas kernels for 11% -> 12%
where the time goes in v2:
time: 147 us; the launch traced here: 146 us
  blocking collectives  38.1 us (26%)
  Pallas kernels  36.1 us (25%)
  starting transfers between devices  35.7 us (24%)
  waiting for transfers between devices  31.2 us (21%)
  local copies, waits for them, and re-layouts  4.81 us (3%)
    all_to_all x1, blocking collectives, exchange(): lax.all_to_all(plain(v), axis, split_axis=0, concat_axis=0, tiled=True)  38.1 us
    pallas_call x8, Pallas kernels, call(): pl.pallas_call(kernel, out_shape=tuple((pltpu.VMEM(s, d) if i in out_vmem...  36.1 us
    all_to_all x3, waiting for transfers between devices, exchange(): lax.all_to_all(plain(v), axis, split_axis=0, concat_axis=0, tiled=True)  25.5 us
    all_to_all x3, starting transfers between devices, exchange(): lax.all_to_all(plain(v), axis, split_axis=0, concat_axis=0, tiled=True)  20.6 us
    ppermute x4, starting transfers between devices, along(): return lax.ppermute(v, 'dp', [(i, (i + k) % dps) for i in range(dps)])  6.61 us
    ppermute x5, starting transfers between devices, swap(): return lax.ppermute(v, 'dp', [(i, i ^ 1) for i in range(dps)])  5.37 us
    ppermute x4, waiting for transfers between devices, along(): return lax.ppermute(v, 'dp', [(i, (i + k) % dps) for i in range(dps)])  4.36 us
    ppermute x1, starting transfers between devices, layer(): halo = lax.ppermute(ends, 'sp', [(i, i + 1) for i in range(ways - 1)])  3.2 us
  transfers between devices with their start and end apart: 13, of which 5 were waited for; matrix products, arithmetic and copies ran while one was open for 2% of the time, Pallas kernels for 12%

profile of v2, /device:TPU:1, one launch (start us, length us, event | category | flops | bytes accessed | tf_op | source)
XLA Modules:
  0.0 146.1 jit_solution(13412552157032294900)
XLA Ops:
  0.0 3.3 %collective-permute-start.2 = (bf16[256,2048]{1,0:T(8,128)(2,1)}, bf16[256,2048]{1,0:T(8,128)(2,1)S(1)}, u32[]{:S(2)}, u32[]{:S(2)}) collective-permute-start(bf16[256,2048]{1,0:T(8,128)(2,1)} %w0.1), channel_id=1, source_target_pairs={{0,6},{1,7},{2,0},{3,1},{4,2},{5,3},{6,4},{7,5},{8,14},{9,15},{10,... | collective-permute-start | bytes 3145736 | tf_op jit(solution)/shard_map/ppermute | solution.py:298
  3.3 0.0 collective-permute-start.1
  3.3 0.7 slice_bitcast_fusion.1
  4.0 0.8 slice_bitcast_fusion
  4.8 3.2 %collective-permute-start = (bf16[8,4096]{1,0:T(8,128)(2,1)S(1)}, bf16[8,4096]{1,0:T(8,128)(2,1)S(1)}, u32[]{:S(2)}, u32[]{:S(2)}) collective-permute-start(bf16[8,4096]{1,0:T(8,128)(2,1)S(1)} %pad_maximum_fusion), channel_id=1, source_target_pairs={{0,8},{8,16},{16,24},{24,32},{32,40},{40,48},{48,56},{56,64},{64,7... | collective-permute-start | bytes 196616 | tf_op jit(solution)/shard_map/ppermute | solution.py:295
  8.0 1.3 collective-permute-done.halo
  9.3 4.9 %shard_map.217 = (bf16[16,144,128]{2,1,0:T(8,128)(2,1)}, bf16[128,2048]{1,0:T(8,128)(2,1)}, f32[128,2048]{1,0:T(8,128)}, bf16[128,1024]{1,0:T(8,128)(2,1)}, f32[128,32]{1,0:T(8,128)}) custom-call(bf16[128,2048]{1,0:T(8,128)(2,1)} %bitcast.47, bf16[128,1024]{1,0:T(8,128)(2,1)} %bitcast.50, bf16[8,4096]{1,0:T(8,128)(2,1)S(1)} %collective-permute-done.halo, ...), custom_call_target="tpu_custom_call" | custom-call | flops 1000000 | bytes 1000000 | tf_op jit(solution)/shard_map/pallas_call | solution.py:48
  14.2 8.6 %all-to-all-start = ((bf16[16,144,128]{2,1,0:T(8,128)(2,1)}), bf16[16,144,128]{2,1,0:T(8,128)(2,1)S(1)}, u32[]{:S(2)}, u32[]{:S(2)}) async-start(bf16[16,144,128]{2,1,0:T(8,128)(2,1)} %get-tuple-element.24), calls=%async_computation | async-start | bytes 1179648 | tf_op jit(solution)/shard_map/all_to_all | solution.py:281
  22.7 2.7 %collective-permute-done.2.w2 = bf16[256,2048]{1,0:T(8,128)(2,1)S(1)} collective-permute-done((bf16[256,2048]{1,0:T(8,128)(2,1)}, bf16[256,2048]{1,0:T(8,128)(2,1)S(1)}, u32[]{:S(2)}, u32[]{:S(2)}) %collective-permute-start.2) | collective-permute-done | bytes 1048608 | tf_op jit(solution)/shard_map/ppermute | solution.py:298
  25.5 1.0 slice.33
  26.4 3.3 %collective-permute-start.4 = (bf16[128,2048]{1,0:T(8,128)(2,1)}, bf16[128,2048]{1,0:T(8,128)(2,1)S(1)}, u32[]{:S(2)}, u32[]{:S(2)}) collective-permute-start(bf16[128,2048]{1,0:T(8,128)(2,1)} %slice.33), channel_id=1, source_target_pairs={{0,6},{1,7},{2,0},{3,1},{4,2},{5,3},{6,4},{7,5},{8,14},{9,15},{10,... | collective-permute-start | bytes 1572872 | tf_op jit(solution)/shard_map/ppermute | solution.py:298
  29.8 0.9 slice.32
  30.7 1.8 %collective-permute-start.5 = (bf16[256,2048]{1,0:T(8,128)(2,1)}, bf16[256,2048]{1,0:T(8,128)(2,1)}, u32[]{:S(2)}, u32[]{:S(2)}) collective-permute-start(bf16[256,2048]{1,0:T(8,128)(2,1)} %w0.1), channel_id=1, source_target_pairs={{0,1},{1,0},{2,3},{3,2},{4,5},{5,4},{6,7},{7,6},{8,9},{9,8},{10,11... | collective-permute-start | bytes 3145736 | tf_op jit(solution)/shard_map/ppermute | solution.py:301
  32.5 0.0 collective-permute-start.7
  32.5 0.5 collective-permute-start.6
  33.0 0.1 stack.35.place
  33.1 0.2 all-to-all-done.got
  33.3 1.0 shard_map.219
  34.2 7.6 %all-to-all-start.1 = ((bf16[16,128,128]{2,1,0:T(8,128)(2,1)}), bf16[16,128,128]{2,1,0:T(8,128)(2,1)S(1)}, u32[]{:S(2)}, u32[]{:S(2)}) async-start(bf16[16,128,128]{2,1,0:T(8,128)(2,1)} %shard_map.219), calls=%async_computation.1 | async-start | bytes 1048576 | tf_op jit(solution)/shard_map/all_to_all | solution.py:281
  41.8 0.4 collective-permute-start.9
  42.2 1.6 %collective-permute-done.3.w3 = bf16[128,2048]{1,0:T(8,128)(2,1)} collective-permute-done((bf16[128,2048]{1,0:T(8,128)(2,1)}, bf16[128,2048]{1,0:T(8,128)(2,1)}, u32[]{:S(2)}, u32[]{:S(2)}) %collective-permute-start.3) | collective-permute-done | bytes 524320 | tf_op jit(solution)/shard_map/ppermute | solution.py:298
  43.9 2.7 %collective-permute-start.8 = (bf16[128,2048]{1,0:T(8,128)(2,1)}, bf16[128,2048]{1,0:T(8,128)(2,1)}, u32[]{:S(2)}, u32[]{:S(2)}) collective-permute-start(bf16[128,2048]{1,0:T(8,128)(2,1)} %collective-permute-done.3.w3), channel_id=1, source_target_pairs={{0,1},{1,0},{2,3},{3,2},{4,5},{5,4},{6,7},{7,6},{8,9},{9,8},{10,11... | collective-permute-start | bytes 1572872 | tf_op jit(solution)/shard_map/ppermute | solution.py:301
  46.5 2.8 %shard_map.220 = (bf16[1024,256]{1,0:T(8,128)(2,1)}, bf16[256,1024]{1,0:T(8,128)(2,1)}, bf16[256,1024]{1,0:T(8,128)(2,1)}) custom-call(s32[2,128]{1,0:T(2,128)} %bitcast.60, f32[2,128]{1,0:T(2,128)} %bitcast.61), custom_call_target="tpu_custom_call" | custom-call | flops 2000000000 | bytes 1000000 | tf_op jit(solution)/shard_map/pallas_call | solution.py:48
  49.3 4.0 %shard_map.218 = (f32[128,2048]{1,0:T(8,128)}, bf16[128,1024]{1,0:T(8,128)(2,1)}) custom-call(bf16[128,1024]{1,0:T(8,128)(2,1)} %bitcast.54, bf16[8,4096]{1,0:T(8,128)(2,1)} %copy-done.1, bf16[4,1024]{1,0:T(4,128)(2,1)} %ccw.1, bf16[128,2048]{1,0:T(8,128)(2,1)} %get-tuple-element.18.v, bf16[128,1024]{1,0:T(8,128)(2,1)} %get-tuple-element.19.bm, ...), custom_call_target="tpu_custom_call" | custom-call | flops 4000000000 | bytes 1000000 | tf_op jit(solution)/shard_map/pallas_call | solution.py:48
  53.4 9.1 %shard_map.221 = (bf16[128,2048]{1,0:T(8,128)(2,1)}, bf16[128,2048]{1,0:T(8,128)(2,1)}, bf16[1024,1024]{1,0:T(8,128)(2,1)}) custom-call(s32[8]{0:T(128)S(1)} %stack.35.place, f32[128,2048]{1,0:T(8,128)} %get-tuple-element.22.a, bf16[128,1024]{1,0:T(8,128)(2,1)} %get-tuple-element.23.cm, f32[128,32]{1,0:T(8,128)} %get-tuple-element.21.ec, ...), custom_call_target="tpu_custom_call" | custom-call | flops 2000000000 | bytes 1000000 | tf_op jit(solution)/shard_map/pallas_call | solution.py:48
  62.5 38.1 %all_to_all.20 = bf16[128,8,1024]{2,1,0:T(8,128)(2,1)S(1)} all-to-all(bf16[128,8,1024]{2,1,0:T(8,128)(2,1)} %bitcast.46), channel_id=1, replica_groups=mesh['sp'=16,'dp'=8] {'sp','dp'}, dimensions={0} | all-to-all | bytes 4194304 | tf_op jit(solution)/shard_map/all_to_all | solution.py:281
  100.7 5.4 %shard_map.222 = bf16[1024,1024]{1,0:T(8,128)(2,1)S(1)} custom-call(bf16[1024,1024]{1,0:T(8,128)(2,1)S(1)} %bitcast.45, bf16[2048,512]{1,0:T(8,128)(2,1)} %bitcast.57, bf16[2048,512]{1,0:T(8,128)(2,1)} %bitcast.58, bf16[512,2048]{1,0:T(8,128)(2,1)} %bitcast.59), custom_call_target="tpu_custom_call" | custom-call | flops 3000000000 | bytes 1000000 | tf_op jit(solution)/shard_map/pallas_call | solution.py:48
  106.1 1.3 copy-done
  107.4 4.4 %all-to-all-start.3 = ((bf16[128,8,1024]{2,1,0:T(8,128)(2,1)}), bf16[128,8,1024]{2,1,0:T(8,128)(2,1)S(1)}, u32[]{:S(2)}, u32[]{:S(2)}) async-start(bf16[128,8,1024]{2,1,0:T(8,128)(2,1)} %bitcast.44), calls=%async_computation.3 | async-start | bytes 4194304 | tf_op jit(solution)/shard_map/all_to_all | solution.py:281
  111.9 5.3 %shard_map.223.base = f32[128,2048]{1,0:T(8,128)} custom-call(bf16[128,2048]{1,0:T(8,128)(2,1)} %get-tuple-element.29.ein, bf16[128,2048]{1,0:T(8,128)(2,1)} %get-tuple-element.30.mixed, bf16[2048,512]{1,0:T(8,128)(2,1)} %sg.1, bf16[2048,512]{1,0:T(8,128)(2,1)} %su.1, bf16[512,2048]{1,0:T(8,128)(2,1)} %sd.1), custom_call_target="tpu_custom_call" | custom-call | flops 4000000000 | bytes 1000000 | tf_op jit(solution)/shard_map/pallas_call | solution.py:48
  117.2 25.3 %all-to-all-done.3 = bf16[128,8,1024]{2,1,0:T(8,128)(2,1)S(1)} async-done(((bf16[128,8,1024]{2,1,0:T(8,128)(2,1)}), bf16[128,8,1024]{2,1,0:T(8,128)(2,1)S(1)}, u32[]{:S(2)}, u32[]{:S(2)}) %all-to-all-start.3) | async-done | bytes 2097184 | tf_op jit(solution)/shard_map/all_to_all | solution.py:281
  142.5 3.6 %shard_map.224 = bf16[128,2048]{1,0:T(8,128)(2,1)} custom-call(bf16[1024,1024]{1,0:T(8,128)(2,1)S(1)} %bitcast.42, bf16[256,1024]{1,0:T(8,128)(2,1)} %get-tuple-element.27.hi, bf16[256,1024]{1,0:T(8,128)(2,1)} %get-tuple-element.28.lo, f32[128,2048]{1,0:T(8,128)} %shard_map.223.base), custom_call_target="tpu_custom_call" | custom-call | flops 1000000 | bytes 1000000 | tf_op jit(solution)/shard_map/pallas_call | solution.py:48
  (19 shorter events, 0.0 us)
Async XLA Ops:
  0.0 25.5 %collective-permute-start.2 = (bf16[256,2048]{1,0:T(8,128)(2,1)}, bf16[256,2048]{1,0:T(8,128)(2,1)S(1)}, u32[]{:S(2)}, u32[]{:S(2)}) collective-permute-start(bf16[256,2048]{1,0:T(8,128)(2,1)} %w0.1), channel_id=1, source_target_pairs={{0,6},{1,7},{2,0},{3,1},{4,2},{5,3},{6,4},{7,5},{8,14},{9,15},{10,... | collective-permute-start | bytes 3145736 | tf_op jit(solution)/shard_map/ppermute | solution.py:298
  3.3 26.5 %collective-permute-start.1 = (bf16[256,2048]{1,0:T(8,128)(2,1)}, bf16[256,2048]{1,0:T(8,128)(2,1)S(1)}, u32[]{:S(2)}, u32[]{:S(2)}) collective-permute-start(bf16[256,2048]{1,0:T(8,128)(2,1)} %w0.1), channel_id=1, source_target_pairs={{0,2},{1,3},{2,4},{3,5},{4,6},{5,7},{6,0},{7,1},{8,10},{9,11},{10,... | collective-permute-start | bytes 3145736 | tf_op jit(solution)/shard_map/ppermute | solution.py:298
  4.8 4.5 %collective-permute-start = (bf16[8,4096]{1,0:T(8,128)(2,1)S(1)}, bf16[8,4096]{1,0:T(8,128)(2,1)S(1)}, u32[]{:S(2)}, u32[]{:S(2)}) collective-permute-start(bf16[8,4096]{1,0:T(8,128)(2,1)S(1)} %pad_maximum_fusion), channel_id=1, source_target_pairs={{0,8},{8,16},{16,24},{24,32},{32,40},{40,48},{48,56},{56,64},{64,7... | collective-permute-start | bytes 196616 | tf_op jit(solution)/shard_map/ppermute | solution.py:295
  9.3 23.7 %copy-start.1 = (bf16[8,4096]{1,0:T(8,128)(2,1)}, bf16[8,4096]{1,0:T(8,128)(2,1)S(1)}, u32[]{:S(2)}) copy-start(bf16[8,4096]{1,0:T(8,128)(2,1)S(1)} %collective-permute-done.halo) | copy-start | bytes 196612
  14.2 19.1 %all-to-all-start = ((bf16[16,144,128]{2,1,0:T(8,128)(2,1)}), bf16[16,144,128]{2,1,0:T(8,128)(2,1)S(1)}, u32[]{:S(2)}, u32[]{:S(2)}) async-start(bf16[16,144,128]{2,1,0:T(8,128)(2,1)} %get-tuple-element.24), calls=%async_computation | async-start | bytes 1179648 | tf_op jit(solution)/shard_map/all_to_all | solution.py:281
  25.5 8.7 %copy-start.2 = (bf16[256,2048]{1,0:T(8,128)(2,1)}, bf16[256,2048]{1,0:T(8,128)(2,1)S(1)}, u32[]{:S(2)}) copy-start(bf16[256,2048]{1,0:T(8,128)(2,1)S(1)} %collective-permute-done.2.w2) | copy-start | bytes 3145732
  26.4 15.4 %collective-permute-start.4 = (bf16[128,2048]{1,0:T(8,128)(2,1)}, bf16[128,2048]{1,0:T(8,128)(2,1)S(1)}, u32[]{:S(2)}, u32[]{:S(2)}) collective-permute-start(bf16[128,2048]{1,0:T(8,128)(2,1)} %slice.33), channel_id=1, source_target_pairs={{0,6},{1,7},{2,0},{3,1},{4,2},{5,3},{6,4},{7,5},{8,14},{9,15},{10,... | collective-permute-start | bytes 1572872 | tf_op jit(solution)/shard_map/ppermute | solution.py:298
  29.8 19.6 %copy-start.3 = (bf16[256,2048]{1,0:T(8,128)(2,1)}, bf16[256,2048]{1,0:T(8,128)(2,1)S(1)}, u32[]{:S(2)}) copy-start(bf16[256,2048]{1,0:T(8,128)(2,1)S(1)} %collective-permute-done.1.w1) | copy-start | bytes 3145732
  30.7 13.2 %collective-permute-start.3 = (bf16[128,2048]{1,0:T(8,128)(2,1)}, bf16[128,2048]{1,0:T(8,128)(2,1)}, u32[]{:S(2)}, u32[]{:S(2)}) collective-permute-start(bf16[128,2048]{1,0:T(8,128)(2,1)} %slice.32), channel_id=1, source_target_pairs={{0,2},{1,3},{2,4},{3,5},{4,6},{5,7},{6,0},{7,1},{8,10},{9,11},{10,... | collective-permute-start | bytes 1572872 | tf_op jit(solution)/shard_map/ppermute | solution.py:298
  30.7 22.7 %collective-permute-start.5 = (bf16[256,2048]{1,0:T(8,128)(2,1)}, bf16[256,2048]{1,0:T(8,128)(2,1)}, u32[]{:S(2)}, u32[]{:S(2)}) collective-permute-start(bf16[256,2048]{1,0:T(8,128)(2,1)} %w0.1), channel_id=1, source_target_pairs={{0,1},{1,0},{2,3},{3,2},{4,5},{5,4},{6,7},{7,6},{8,9},{9,8},{10,11... | collective-permute-start | bytes 3145736 | tf_op jit(solution)/shard_map/ppermute | solution.py:301
  32.5 20.9 %collective-permute-start.7 = (bf16[256,2048]{1,0:T(8,128)(2,1)S(1)}, bf16[256,2048]{1,0:T(8,128)(2,1)}, u32[]{:S(2)}, u32[]{:S(2)}) collective-permute-start(bf16[256,2048]{1,0:T(8,128)(2,1)S(1)} %collective-permute-done.2.w2), channel_id=1, source_target_pairs={{0,1},{1,0},{2,3},{3,2},{4,5},{5,4},{6,7},{7,6},{8,9},{9,8},{10,11... | collective-permute-start | bytes 3145736 | tf_op jit(solution)/shard_map/ppermute | solution.py:301
  32.5 20.9 %collective-permute-start.6 = (bf16[256,2048]{1,0:T(8,128)(2,1)S(1)}, bf16[256,2048]{1,0:T(8,128)(2,1)}, u32[]{:S(2)}, u32[]{:S(2)}) collective-permute-start(bf16[256,2048]{1,0:T(8,128)(2,1)S(1)} %collective-permute-done.1.w1), channel_id=1, source_target_pairs={{0,1},{1,0},{2,3},{3,2},{4,5},{5,4},{6,7},{7,6},{8,9},{9,8},{10,11... | collective-permute-start | bytes 3145736 | tf_op jit(solution)/shard_map/ppermute | solution.py:301
  34.2 19.1 %all-to-all-start.1 = ((bf16[16,128,128]{2,1,0:T(8,128)(2,1)}), bf16[16,128,128]{2,1,0:T(8,128)(2,1)S(1)}, u32[]{:S(2)}, u32[]{:S(2)}) async-start(bf16[16,128,128]{2,1,0:T(8,128)(2,1)} %shard_map.219), calls=%async_computation.1 | async-start | bytes 1048576 | tf_op jit(solution)/shard_map/all_to_all | solution.py:281
  41.8 7.5 %copy-start.4 = (bf16[128,2048]{1,0:T(8,128)(2,1)}, bf16[128,2048]{1,0:T(8,128)(2,1)S(1)}, u32[]{:S(2)}) copy-start(bf16[128,2048]{1,0:T(8,128)(2,1)S(1)} %collective-permute-done.4.w4) | copy-start | bytes 1572868
  41.8 11.5 %collective-permute-start.9 = (bf16[128,2048]{1,0:T(8,128)(2,1)S(1)}, bf16[128,2048]{1,0:T(8,128)(2,1)}, u32[]{:S(2)}, u32[]{:S(2)}) collective-permute-start(bf16[128,2048]{1,0:T(8,128)(2,1)S(1)} %collective-permute-done.4.w4), channel_id=1, source_target_pairs={{0,1},{1,0},{2,3},{3,2},{4,5},{5,4},{6,7},{7,6},{8,9},{9,8},{10,11... | collective-permute-start | bytes 1572872 | tf_op jit(solution)/shard_map/ppermute | solution.py:301
  43.9 9.5 %collective-permute-start.8 = (bf16[128,2048]{1,0:T(8,128)(2,1)}, bf16[128,2048]{1,0:T(8,128)(2,1)}, u32[]{:S(2)}, u32[]{:S(2)}) collective-permute-start(bf16[128,2048]{1,0:T(8,128)(2,1)} %collective-permute-done.3.w3), channel_id=1, source_target_pairs={{0,1},{1,0},{2,3},{3,2},{4,5},{5,4},{6,7},{7,6},{8,9},{9,8},{10,11... | collective-permute-start | bytes 1572872 | tf_op jit(solution)/shard_map/ppermute | solution.py:301
  106.1 1.3 copy-start
  107.4 35.0 %all-to-all-start.3 = ((bf16[128,8,1024]{2,1,0:T(8,128)(2,1)}), bf16[128,8,1024]{2,1,0:T(8,128)(2,1)S(1)}, u32[]{:S(2)}, u32[]{:S(2)}) async-start(bf16[128,8,1024]{2,1,0:T(8,128)(2,1)} %bitcast.44), calls=%async_computation.3 | async-start | bytes 4194304 | tf_op jit(solution)/shard_map/all_to_all | solution.py:281

commit v3 on v2

--- a/solution.py
+++ b/solution.py
@@ -21,7 +21,8 @@
 GW = PER * HEAD_DIM
 HALF = D // 2
 ROWS = 1024
-ST_ROWS = 144
+ST_ROWS = 160
+TOP = 16
 
 
 def full():
@@ -37,11 +38,12 @@
 
 
 def call(
-    kernel, outs, args, scratch=(), vmem=(), smem_in=(), raw=(), out_vmem=(), limit=12, flops=10**6
+    kernel, outs, args, scratch=(), vmem=(), smem_in=(), raw=(), free=(), out_vmem=(), limit=12,
+    flops=10**6,
 ):
     placed = [
         v
-        if i in smem_in
+        if i in smem_in or i in free
         else pltpu.with_memory_space_constraint(v, pltpu.VMEM if i in vmem else pltpu.HBM)
         for i, v in enumerate(args)
     ]
@@ -65,8 +67,8 @@
     return v / (1.0 + jnp.exp(-v))
 
 
-def tap(pad, halo, rows, weight):
-    pad[0:8, :] = halo.astype(F32)
+def tap(pad, rows, weight):
+    pad[0:8, :] = jnp.zeros((8, pad.shape[1]), F32)
     pad[8 : 8 + TOK, :] = rows.astype(F32)
     w = weight.astype(F32)
     total = pad[5 : 5 + TOK, :] * w[0:1, :]
@@ -75,8 +77,18 @@
     return silu(total)
 
 
+def tap_top(pad, halo, rows, weight):
+    pad[0:8, :] = halo.astype(F32)
+    pad[8 : 8 + TOP, :] = rows.astype(F32)
+    w = weight.astype(F32)
+    total = pad[5 : 5 + TOP, :] * w[0:1, :]
+    for k in range(1, 4):
+        total = total + pad[5 + k : 5 + k + TOP, :] * w[k : k + 1, :]
+    return silu(total)
+
+
 def spread(cols, g):
-    lane = lax.broadcasted_iota(jnp.int32, (TOK, 128), 1)
+    lane = lax.broadcasted_iota(jnp.int32, (cols.shape[0], 128), 1)
     out = []
     for i in range(0, PER, 2):
         h = g * PER + i
@@ -85,7 +97,7 @@
 
 
 def states_kernel(
-    x, b, halo, step_in, cw, cbw, bias, dlog, st, v_out, xs_out, b_out, ec_out, padx, padb
+    x, b, step_in, cw, cbw, bias, dlog, st, v_out, xs_out, b_out, ec_out, grow_out, padx, padb
 ):
     s = step_in[...].astype(F32).T + bias[...]
     step = jnp.maximum(s, 0.0) + jnp.log(1.0 + jnp.exp(-jnp.abs(s)))
@@ -96,19 +108,28 @@
     cum = jnp.dot(tri, logs, precision=lax.Precision.HIGHEST, preferred_element_type=F32)
     ec_out[...] = jnp.exp(cum)
     grow = step * jnp.exp(-cum)
+    grow_out[...] = grow
+    later = jnp.where(lax.broadcasted_iota(jnp.int32, (TOK, HEADS), 0) < 3, 0.0, grow)
     tot = cum[TOK - 1 : TOK, :]
     etot = jnp.exp(tot)
-    sub = lax.broadcasted_iota(jnp.int32, (16, 128), 0)
+    first = grow[0:8, :] * etot
+    sub = lax.broadcasted_iota(jnp.int32, (8, 128), 0)
+    low = lax.broadcasted_iota(jnp.int32, (8, 128), 1) < HEAD_DIM
     for g in range(GROUPS):
         xc = slice(g * GW, (g + 1) * GW)
         bc = slice(g * STATE, (g + 1) * STATE)
-        xs = tap(padx.at[g % 2], halo[:, xc], x[:, xc], cw[:, xc])
-        bm = tap(padb.at[g % 2], halo[:, D + g * STATE : D + (g + 1) * STATE], b[:, bc], cbw[:, bc]).astype(BF)
-        v = (xs * spread(grow, g)).astype(BF)
+        xs = tap(padx.at[g % 2], x[:, xc], cw[:, xc])
+        bm = tap(padb.at[g % 2], b[:, bc], cbw[:, bc]).astype(BF)
+        v = (xs * spread(later, g)).astype(BF)
         xs_out[:, xc] = xs
         v_out[:, xc] = v
         b_out[:, bc] = bm
         fresh = lax.dot_general(v, bm, (((0,), (0,)), ((), ())), preferred_element_type=F32)
+
+        def ends(rows):
+            return jnp.where(sub < 3, pltpu.roll(rows[TOK - 8 :], 3, 0), pltpu.roll(rows[:8], 3, 0))
+
+        b_ends = ends(b[:, bc].astype(F32))
         for i in range(2):
             h = g * PER + 2 * i
             o = g * 2 + i
@@ -117,45 +138,87 @@
                 st[o, j * HEAD_DIM : (j + 1) * HEAD_DIM, :] = (
                     fresh[k : k + HEAD_DIM, :] * etot[0:1, h + j : h + j + 1]
                 ).astype(BF)
-            tail = jnp.zeros((16, 128), F32)
+            tail = jnp.zeros((8, 128), F32)
             for j in range(2):
-                rest = jnp.broadcast_to(tot[0:1, h + j : h + j + 1], (16, 128))
+                rest = jnp.broadcast_to(tot[0:1, h + j : h + j + 1], (8, 128))
                 for q in range(3):
                     part = rest.astype(BF).astype(F32)
                     tail = jnp.where(sub == 3 * j + q, part, tail)
                     rest = rest - part
-            st[o, 2 * HEAD_DIM : ST_ROWS, :] = tail.astype(BF)
-
-
-def inner_kernel(c, halo, ccw, v, bm, xs, ec, skip, a_out, c_out, padc):
+            w = jnp.where(low, first[:, h : h + 1], first[:, h + 1 : h + 2])
+            w_hi = w.astype(BF).astype(F32)
+            w_both = jnp.where(sub < 3, w_hi, pltpu.roll(w - w_hi, 3, 0))
+            x_ends = ends(x[:, o * 128 : (o + 1) * 128].astype(F32))
+            st[o, 128:144, :] = jnp.concatenate([tail, w_both], axis=0).astype(BF)
+            st[o, 144:160, :] = jnp.concatenate([x_ends, b_ends], axis=0).astype(BF)
+
+
+def inner_kernel(
+    x, b, c, halo, cw, cbw, ccw, v_in, b_in, xs_in, ec, grow, skip, a_out, c_out, padx, padb, padc
+):
     r = lax.broadcasted_iota(jnp.int32, (TOK, TOK), 0)
     s = lax.broadcasted_iota(jnp.int32, (TOK, TOK), 1)
     lower = s <= r
     cols = ec[...]
+    top = grow[0:TOP, :]
     sk = jnp.broadcast_to(skip[...], (TOK, HEADS))
     for g in range(GROUPS):
         xc = slice(g * GW, (g + 1) * GW)
         bc = slice(g * STATE, (g + 1) * STATE)
-        cm = tap(padc.at[g % 2], halo[:, D + 1024 + g * STATE : D + 1024 + (g + 1) * STATE], c[:, bc], ccw[:, bc]).astype(BF)
+        bh = slice(D + g * STATE, D + (g + 1) * STATE)
+        ch = slice(D + 1024 + g * STATE, D + 1024 + (g + 1) * STATE)
+        xt = tap_top(padx.at[g % 2], halo[:, xc], x[0:TOP, xc], cw[:, xc])
+        bt = tap_top(padb.at[g % 2, 0], halo[:, bh], b[0:TOP, bc], cbw[:, bc]).astype(BF)
+        ct = tap_top(padb.at[g % 2, 1], halo[:, ch], c[0:TOP, bc], ccw[:, bc])
+        vt = (xt * spread(top, g)).astype(BF)
+        cm = tap(padc.at[g % 2], c[:, bc], ccw[:, bc])
+        cm = jnp.concatenate([ct, cm[TOP:]], axis=0).astype(BF)
         c_out[:, bc] = cm
-        cb = lax.dot_general(cm, bm[:, bc], (((1,), (1,)), ((), ())), preferred_element_type=F32)
+        bm = jnp.concatenate([bt, b_in[TOP:, bc]], axis=0)
+        v = jnp.concatenate([vt, v_in[TOP:, xc]], axis=0)
+        xs = jnp.concatenate([xt, xs_in[TOP:, xc]], axis=0)
+        cb = lax.dot_general(cm, bm, (((1,), (1,)), ((), ())), preferred_element_type=F32)
         cb = jnp.where(lower, cb, 0.0).astype(BF)
-        u = jnp.dot(cb, v[:, xc], preferred_element_type=F32)
-        a_out[:, xc] = u * spread(cols, g) + xs[:, xc] * spread(sk, g)
-
-
-def carry_kernel(got, out):
+        u = jnp.dot(cb, v, preferred_element_type=F32)
+        a_out[:, xc] = u * spread(cols, g) + xs * spread(sk, g)
+
+
+def carry_kernel(place, cw, cbw, got, out):
+    count = got.shape[0]
+    o = place[8]
+    sub = lax.broadcasted_iota(jnp.int32, (count, 8, 128), 1)
+
+    def starts(rows, weight):
+        rows = rows.astype(F32)
+        before = jnp.concatenate([jnp.zeros((1, 8, 128), F32), rows[:-1]], axis=0)
+        seq = jnp.where(sub < 3, before, rows)
+        w = weight.astype(F32)
+        total = seq * w[0:1, :][None]
+        for k in range(1, 4):
+            total = total + pltpu.roll(seq, 8 - k, 1) * w[k : k + 1, :][None]
+        return jnp.where(sub < 3, silu(total), 0.0)
+
+    tails = got[:, 128:144, :].astype(F32)
+    ends = got[:, 144:160, :].astype(F32)
+    w = tails[:, 8:16]
+    w = w + pltpu.roll(w, 5, 1)
+    xs = starts(ends[:, 0:8], cw[:, pl.ds(pl.multiple_of(o * 128, 128), 128)])
+    bm = starts(ends[:, 8:16], cbw[:, pl.ds(pl.multiple_of((o // 2) * 128, 128), 128)])
+    vt = jnp.where(sub < 3, xs * w, 0.0).reshape(count * 8, 128).T
+    bm = bm.reshape(count * 8, 128).astype(BF)
+    lane = lax.broadcasted_iota(jnp.int32, (128, 128), 1)
     row = lax.broadcasted_iota(jnp.int32, (2 * HEAD_DIM, 128), 0)
     carry = jnp.zeros((2 * HEAD_DIM, 128), F32)
-    count = got.shape[0]
     for i in range(count):
         out[i] = carry.astype(BF)
         if i + 1 < count:
-            tail = got[i, 2 * HEAD_DIM : ST_ROWS, :].astype(F32)
+            mine = jnp.where(lane // 8 == i, vt, 0.0).astype(BF)
+            extra = jnp.dot(mine, bm, preferred_element_type=F32)
+            tail = tails[i, 0:8]
             fa = jnp.exp(tail[0:1] + tail[1:2] + tail[2:3])
             fb = jnp.exp(tail[3:4] + tail[4:5] + tail[5:6])
             factor = jnp.where(row < HEAD_DIM, fa, fb)
-            carry = carry * factor + got[i, 0 : 2 * HEAD_DIM, :].astype(F32)
+            carry = carry * factor + (got[i, 0 : 2 * HEAD_DIM, :].astype(F32) + extra)
 
 
 def routes_kernel(routes, rw, d_out, hi_out, lo_out):
@@ -185,18 +248,7 @@
         lo_out[h * TOK : (h + 1) * TOK, :] = (comb - hi.astype(F32)).astype(BF)
 
 
-def mix_kernel(
-    place, a, cm, ec, pref, gate, gain, resid, fgain, disp,
-    w0, w1, w2, w3, w4, w5, w6, w7, w8, w9, mixed_out, ein_out, send, norm,
-    wide, half, sems
-):
-    loads = []
-    for k, w in enumerate((w0, w1, w2, w5, w6, w7)):
-        loads.append(pltpu.make_async_copy(w, wide.at[k], sems.at[k]))
-    for k, w in enumerate((w3, w4, w8, w9)):
-        loads.append(pltpu.make_async_copy(w, half.at[k], sems.at[6 + k]))
-    for load in loads:
-        load.start()
+def norm_kernel(a, cm, ec, pref, gate, gain, norm):
     cols = ec[...]
     for g in range(GROUPS):
         xc = slice(g * GW, (g + 1) * GW)
@@ -208,14 +260,22 @@
         y = y * silu(gate[:, xc].astype(F32))
         y = y * lax.rsqrt(jnp.mean(y * y, axis=1, keepdims=True) + EPS)
         norm[g] = (y * gain[:, xc]).astype(BF)
+
+
+def mix_kernel(
+    place, norm, resid, fgain, disp, w0, w1, w2, w3, w4, w5, w6, w7,
+    mixed_out, ein_out, send, wide, sems
+):
+    loads = [
+        pltpu.make_async_copy(w, wide.at[k], sems.at[k])
+        for k, w in enumerate((w0, w1, w2, w3, w4, w5, w6, w7))
+    ]
+    for load in loads:
+        load.start()
     proj = resid[...].astype(F32)
-    for k in range(6):
-        loads[k].wait()
+    for k, load in enumerate(loads):
+        load.wait()
         proj = proj + jnp.dot(norm[place[k]], wide[k], preferred_element_type=F32)
-    for k in range(4):
-        loads[6 + k].wait()
-        row = norm[place[6 + k // 2]][:, (k % 2) * 128 : (k % 2) * 128 + 128]
-        proj = proj + jnp.dot(row, half[k], preferred_element_type=F32)
     mixed = proj.astype(BF)
     mixed_out[...] = mixed
     m = mixed.astype(F32)
@@ -294,35 +354,48 @@
     ends = jnp.concatenate([x[TOK - 8 :], b[TOK - 8 :], c[TOK - 8 :]], axis=1)
     halo = lax.ppermute(ends, "sp", [(i, i + 1) for i in range(ways - 1)])
 
-    def along(v, k):
-        return lax.ppermute(v, "dp", [(i, (i + k) % dps) for i in range(dps)])
+    def ring(v):
+        return lax.ppermute(v, "dp", [(i, (i + (-2 if i % 2 else 2)) % dps) for i in range(dps)])
 
     def swap(v):
         return lax.ppermute(v, "dp", [(i, i ^ 1) for i in range(dps)])
 
-    left = along(out_weight, 2)
-    right = along(out_weight, -2)
-    far = [along(left[:128], 2), along(right[128:], -2)]
-    pieces = [out_weight, left, right, *far, swap(out_weight), swap(left)]
-    pieces += [swap(right), swap(far[0]), swap(far[1])]
+    partner = swap(out_weight)
+    near = ring(out_weight)
+    near2 = ring(partner)
+    far = ring(near)
+    pieces = [out_weight, partner, near, near2, swap(near), swap(near2)]
+    pieces += [far, swap(far)]
     me = lax.axis_index("dp")
-    near = [me, (me + dps - 2) % dps, (me + 2) % dps]
-    far_at = (me + 4) % dps
-    place = jnp.stack(near + [v ^ 1 for v in near] + [far_at, far_at ^ 1]).astype(jnp.int32)
-
-    st, v, xs, bm, ec = call(
+    odd = me & 1
+    at = (me + dps - 2 + 4 * odd) % dps
+    other = ((me ^ 1) + 2 + (dps - 4) * odd) % dps
+    place = jnp.stack(
+        [me, me ^ 1, at, at ^ 1, other, other ^ 1, me ^ 4, me ^ 5, lax.axis_index("sp")]
+    ).astype(jnp.int32)
+
+    st, v, xs, bm, ec, grow = call(
         states_kernel,
-        [((ways, ST_ROWS, 128), BF), ((TOK, D), BF), ((TOK, D), F32), ((TOK, 1024), BF), ((TOK, HEADS), F32)],
-        (x, b, halo, step_input[0].T, conv_weight, conv_b_weight, step_bias[None], decay_log[None]),
-        vmem=(2,),
+        [
+            ((ways, ST_ROWS, 128), BF), ((TOK, D), BF), ((TOK, D), F32), ((TOK, 1024), BF),
+            ((TOK, HEADS), F32), ((TOK, HEADS), F32),
+        ],
+        (x, b, step_input[0].T, conv_weight, conv_b_weight, step_bias[None], decay_log[None]),
         scratch=[pltpu.VMEM((2, TOK + 8, GW), F32), pltpu.VMEM((2, TOK + 8, STATE), F32)],
     )
     got = exchange(st, "sp")
     a, cm = call(
         inner_kernel,
         [((TOK, D), F32), ((TOK, 1024), BF)],
-        (c, halo, conv_c_weight, v, bm, xs, ec, skip[None]),
-        scratch=[pltpu.VMEM((2, TOK + 8, STATE), F32)],
+        (
+            x, b, c, halo, conv_weight, conv_b_weight, conv_c_weight, v, bm, xs, ec, grow,
+            skip[None],
+        ),
+        scratch=[
+            pltpu.VMEM((2, TOP + 8, GW), F32),
+            pltpu.VMEM((2, 2, TOP + 8, STATE), F32),
+            pltpu.VMEM((2, TOK + 8, STATE), F32),
+        ],
         flops=4 * 10**9,
     )
     disp, hi, lo = call(
@@ -331,24 +404,31 @@
         (routes[0].T, route_weights[0].T),
         flops=2 * 10**9,
     )
-    (carried,) = call(carry_kernel, [((ways, 128, 128), BF)], (got,), vmem=(0,))
+    (carried,) = call(
+        carry_kernel,
+        [((ways, 128, 128), BF)],
+        (place, conv_weight, conv_b_weight, got),
+        smem_in=(0,),
+        vmem=(3,),
+    )
     pref = exchange(carried, "sp")
+    (norm,) = call(
+        norm_kernel,
+        [((GROUPS, TOK, GW), BF)],
+        (a, cm, ec, pref.reshape(GROUPS, GW, STATE), gate_input[0], norm_gain[None]),
+        vmem=(3,),
+        out_vmem=(0,),
+        flops=10**9,
+    )
     mixed, ein, send = call(
         mix_kernel,
         [((TOK, D), BF), ((TOK, D), BF), ((ROWS, HALF), BF)],
-        (
-            place, a, cm, ec, pref.reshape(GROUPS, GW, STATE), gate_input[0], norm_gain[None],
-            residual[0], ffn_gain[None], disp, *pieces,
-        ),
-        scratch=[
-            pltpu.VMEM((GROUPS, TOK, GW), BF),
-            pltpu.VMEM((6, 256, D), BF),
-            pltpu.VMEM((4, 128, D), BF),
-            pltpu.SemaphoreType.DMA((10,)),
-        ],
+        (place, norm, residual[0], ffn_gain[None], disp, *pieces),
+        scratch=[pltpu.VMEM((8, 256, D), BF), pltpu.SemaphoreType.DMA((8,))],
         smem_in=(0,),
-        vmem=(4,),
-        raw=range(10, 20),
+        vmem=(1,),
+        raw=range(5, 13),
+        free=range(6, 13),
         limit=32,
         flops=2 * 10**9,
     )

time: 147 us -> 161 us (1.095)
  waiting for transfers between devices: 31.2 us -> 47.2 us
  blocking collectives: 38.1 us -> 36 us
  Pallas kernels: 36.1 us -> 37.9 us
    ppermute x4 -> x3, waiting for transfers between devices: 4.36 us -> 18.8 us  [ring(): lax.ppermute(v, 'dp', [(i, (i + (-2 if i % 2 else 2)) % dps) for i in ran...]
    all_to_all x3, waiting for transfers between devices: 25.5 us -> 28.4 us  [exchange(): lax.all_to_all(plain(v), axis, split_axis=0, concat_axis=0, tiled=True)]
    all_to_all x1, blocking collectives: 38.1 us -> 36 us  [exchange(): lax.all_to_all(plain(v), axis, split_axis=0, concat_axis=0, tiled=True)]
    slice x2 -> x0, local copies, waits for them, and re-layouts: 1.88 us -> none  [layer(): far = [along(left[:128], 2), along(right[128:], -2)]]
    pallas_call x8 -> x9, Pallas kernels: 36.1 us -> 37.9 us  [call(): pl.pallas_call(kernel, out_shape=tuple((pltpu.VMEM(s, d) if i in out_vmem...]
    ppermute x5 -> x4, starting transfers between devices: 5.37 us -> 4.99 us  [swap(): return lax.ppermute(v, 'dp', [(i, i ^ 1) for i in range(dps)])]
    ppermute x4 -> x3, starting transfers between devices: 6.61 us -> 6.32 us  [ring(): lax.ppermute(v, 'dp', [(i, (i + (-2 if i % 2 else 2)) % dps) for i in ran...]
  transfers between devices with their start and end apart: 13 -> 11, of which waited for: 5 -> 4; matrix products, arithmetic and copies ran while one was open for 2% -> 1% of each run, Pallas kernels for 12% -> 14%
where the time goes in v3:
time: 161 us; the launch traced here: 160 us
  waiting for transfers between devices  47.2 us (29%)
  Pallas kernels  37.9 us (24%)
  blocking collectives  36 us (22%)
  starting transfers between devices  34.3 us (21%)
  local copies, waits for them, and re-layouts  4.24 us (3%)
    pallas_call x9, Pallas kernels, call(): pl.pallas_call(kernel, out_shape=tuple((pltpu.VMEM(s, d) if i in out_vmem...  37.9 us
    all_to_all x1, blocking collectives, exchange(): lax.all_to_all(plain(v), axis, split_axis=0, concat_axis=0, tiled=True)  36 us
    all_to_all x3, waiting for transfers between devices, exchange(): lax.all_to_all(plain(v), axis, split_axis=0, concat_axis=0, tiled=True)  28.4 us
    all_to_all x3, starting transfers between devices, exchange(): lax.all_to_all(plain(v), axis, split_axis=0, concat_axis=0, tiled=True)  19.7 us
    ppermute x3, waiting for transfers between devices, ring(): lax.ppermute(v, 'dp', [(i, (i + (-2 if i % 2 else 2)) % dps) for i in ran...  18.8 us
    ppermute x3, starting transfers between devices, ring(): lax.ppermute(v, 'dp', [(i, (i + (-2 if i % 2 else 2)) % dps) for i in ran...  6.32 us
    ppermute x4, starting transfers between devices, swap(): return lax.ppermute(v, 'dp', [(i, i ^ 1) for i in range(dps)])  4.99 us
    ppermute x1, starting transfers between devices, layer(): halo = lax.ppermute(ends, 'sp', [(i, i + 1) for i in range(ways - 1)])  3.3 us
  transfers between devices with their start and end apart: 11, of which 4 were waited for; matrix products, arithmetic and copies ran while one was open for 1% of the time, Pallas kernels for 14%

profile of v3, /device:TPU:1, one launch (start us, length us, event | category | flops | bytes accessed | tf_op | source)
XLA Modules:
  0.0 159.8 jit_solution(4813735253216060883)
XLA Ops:
  0.0 3.3 %collective-permute-start.2 = (bf16[256,2048]{1,0:T(8,128)(2,1)}, bf16[256,2048]{1,0:T(8,128)(2,1)S(1)}, u32[]{:S(2)}, u32[]{:S(2)}) collective-permute-start(bf16[256,2048]{1,0:T(8,128)(2,1)} %w0.1), channel_id=1, source_target_pairs={{0,2},{1,7},{2,4},{3,1},{4,6},{5,3},{6,0},{7,5},{8,10},{9,15},{10,... | collective-permute-start | bytes 3145736 | tf_op jit(solution)/shard_map/ppermute | solution.py:358
  3.3 0.0 collective-permute-start.1
  3.3 12.1 %collective-permute-done.2.w2 = bf16[256,2048]{1,0:T(8,128)(2,1)S(1)} collective-permute-done((bf16[256,2048]{1,0:T(8,128)(2,1)}, bf16[256,2048]{1,0:T(8,128)(2,1)S(1)}, u32[]{:S(2)}, u32[]{:S(2)}) %collective-permute-start.2) | collective-permute-done | bytes 1048608 | tf_op jit(solution)/shard_map/ppermute | solution.py:358
  15.4 3.0 %collective-permute-start.6 = (bf16[256,2048]{1,0:T(8,128)(2,1)S(1)}, bf16[256,2048]{1,0:T(8,128)(2,1)}, u32[]{:S(2)}, u32[]{:S(2)}) collective-permute-start(bf16[256,2048]{1,0:T(8,128)(2,1)S(1)} %collective-permute-done.2.w2), channel_id=1, source_target_pairs={{0,2},{1,7},{2,4},{3,1},{4,6},{5,3},{6,0},{7,5},{8,10},{9,15},{10,... | collective-permute-start | bytes 3145736 | tf_op jit(solution)/shard_map/ppermute | solution.py:358
  18.4 0.0 collective-permute-start.3
  18.4 4.9 %shard_map.217 = (bf16[16,160,128]{2,1,0:T(8,128)(2,1)}, bf16[128,2048]{1,0:T(8,128)(2,1)}, f32[128,2048]{1,0:T(8,128)}, bf16[128,1024]{1,0:T(8,128)(2,1)}, f32[128,32]{1,0:T(8,128)}, /*index=5*/f32[128,32]{1,0:T(8,128)}) custom-call(bf16[128,2048]{1,0:T(8,128)(2,1)} %bitcast.48, bf16[128,1024]{1,0:T(8,128)(2,1)} %bitcast.51, bf16[32,128]{1,0:T(8,128)(2,1)} %bitcast.53, ...), custom_call_target="tpu_custom_call" | custom-call | flops 1000000 | bytes 1000000 | tf_op jit(solution)/shard_map/pallas_call | solution.py:50
  23.3 7.8 %all-to-all-start = ((bf16[16,160,128]{2,1,0:T(8,128)(2,1)}), bf16[16,160,128]{2,1,0:T(8,128)(2,1)S(1)}, u32[]{:S(2)}, u32[]{:S(2)}) async-start(bf16[16,160,128]{2,1,0:T(8,128)(2,1)} %get-tuple-element.26), calls=%async_computation | async-start | bytes 1310720 | tf_op jit(solution)/shard_map/all_to_all | solution.py:341
  31.1 0.7 slice_bitcast_fusion.2
  31.8 0.8 slice_bitcast_fusion
  32.5 0.7 slice_bitcast_fusion.1
  33.3 1.4 collective-permute-start.4
  34.6 0.0 collective-permute-start.7
  34.6 6.7 %collective-permute-done.3.w3 = bf16[256,2048]{1,0:T(8,128)(2,1)} collective-permute-done((bf16[256,2048]{1,0:T(8,128)(2,1)S(1)}, bf16[256,2048]{1,0:T(8,128)(2,1)}, u32[]{:S(2)}, u32[]{:S(2)}) %collective-permute-start.3) | collective-permute-done | bytes 1048608 | tf_op jit(solution)/shard_map/ppermute | solution.py:358
  41.3 3.6 %collective-permute-start.5 = (bf16[256,2048]{1,0:T(8,128)(2,1)}, bf16[256,2048]{1,0:T(8,128)(2,1)}, u32[]{:S(2)}, u32[]{:S(2)}) collective-permute-start(bf16[256,2048]{1,0:T(8,128)(2,1)} %collective-permute-done.3.w3), channel_id=1, source_target_pairs={{0,1},{1,0},{2,3},{3,2},{4,5},{5,4},{6,7},{7,6},{8,9},{9,8},{10,11... | collective-permute-start | bytes 3145736 | tf_op jit(solution)/shard_map/ppermute | solution.py:361
  45.0 3.3 %collective-permute-start = (bf16[8,4096]{1,0:T(8,128)(2,1)S(1)}, bf16[8,4096]{1,0:T(8,128)(2,1)S(1)}, u32[]{:S(2)}, u32[]{:S(2)}) collective-permute-start(bf16[8,4096]{1,0:T(8,128)(2,1)S(1)} %pad_maximum_fusion), channel_id=1, source_target_pairs={{0,8},{8,16},{16,24},{24,32},{32,40},{40,48},{48,56},{56,64},{64,7... | collective-permute-start | bytes 196616 | tf_op jit(solution)/shard_map/ppermute | solution.py:355
  48.3 0.1 stack.39.place
  48.4 0.0 all-to-all-done.got
  48.4 2.0 %shard_map.219 = bf16[16,128,128]{2,1,0:T(8,128)(2,1)} custom-call(s32[9]{0:T(128)S(1)} %stack.39.place, bf16[4,2048]{1,0:T(4,128)(2,1)} %cw.5, bf16[4,1024]{1,0:T(4,128)(2,1)} %cbw.5, bf16[16,160,128]{2,1,0:T(8,128)(2,1)S(1)} %all-to-all-done.got), custom_call_target="tpu_custom_call" | custom-call | flops 1000000 | bytes 1000000 | tf_op jit(solution)/shard_map/pallas_call | solution.py:50
  50.4 7.5 %all-to-all-start.1 = ((bf16[16,128,128]{2,1,0:T(8,128)(2,1)}), bf16[16,128,128]{2,1,0:T(8,128)(2,1)S(1)}, u32[]{:S(2)}, u32[]{:S(2)}) async-start(bf16[16,128,128]{2,1,0:T(8,128)(2,1)} %shard_map.219), calls=%async_computation.1 | async-start | bytes 1048576 | tf_op jit(solution)/shard_map/all_to_all | solution.py:341
  57.9 2.9 %shard_map.221 = (bf16[1024,256]{1,0:T(8,128)(2,1)}, bf16[256,1024]{1,0:T(8,128)(2,1)}, bf16[256,1024]{1,0:T(8,128)(2,1)}) custom-call(s32[2,128]{1,0:T(2,128)} %bitcast.63, f32[2,128]{1,0:T(2,128)} %bitcast.64), custom_call_target="tpu_custom_call" | custom-call | flops 2000000000 | bytes 1000000 | tf_op jit(solution)/shard_map/pallas_call | solution.py:50
  60.8 0.6 copy-done.1
  61.4 4.2 %shard_map.218 = (f32[128,2048]{1,0:T(8,128)}, bf16[128,1024]{1,0:T(8,128)(2,1)}) custom-call(bf16[128,2048]{1,0:T(8,128)(2,1)} %bitcast.49, bf16[128,1024]{1,0:T(8,128)(2,1)} %bitcast.52, bf16[128,1024]{1,0:T(8,128)(2,1)} %bitcast.55, bf16[8,4096]{1,0:T(8,128)(2,1)} %copy-done.1, bf16[4,2048]{1,0:T(4,128)(2,1)} %cw.5, bf16[4,1024]{1,0:T(4,128)(2,1)} %cbw.5, ...), custom_call_target="tpu_custom_call" | custom-call | flops 4000000000 | bytes 1000000 | tf_op jit(solution)/shard_map/pallas_call | solution.py:50
  65.6 3.1 %all-to-all-done.1 = bf16[16,128,128]{2,1,0:T(8,128)(2,1)S(1)} async-done(((bf16[16,128,128]{2,1,0:T(8,128)(2,1)}), bf16[16,128,128]{2,1,0:T(8,128)(2,1)S(1)}, u32[]{:S(2)}, u32[]{:S(2)}) %all-to-all-start.1) | async-done | bytes 524320 | tf_op jit(solution)/shard_map/all_to_all | solution.py:341
  68.7 3.0 %shard_map.220.norm = bf16[8,128,256]{2,1,0:T(8,128)(2,1)S(1)} custom-call(f32[128,2048]{1,0:T(8,128)} %get-tuple-element.24.a, bf16[128,1024]{1,0:T(8,128)(2,1)} %get-tuple-element.25.cm, f32[128,32]{1,0:T(8,128)} %get-tuple-element.22.ec, bf16[8,256,128]{2,1,0:T(8,128)(2,1)S(1)} %bitcast.46, bf16[128,2048]{1,0:T(8,128)(2,1)} %bitcast.61, f32[1,2048]{1,0:T(1,128)} %bitcast.62), custom_call_target="tpu_custom_call" | custom-call | flops 1000000000 | bytes 1000000 | tf_op jit(solution)/shard_map/pallas_call | solution.py:50
  71.7 6.7 %shard_map.222 = (bf16[128,2048]{1,0:T(8,128)(2,1)}, bf16[128,2048]{1,0:T(8,128)(2,1)}, bf16[1024,1024]{1,0:T(8,128)(2,1)}) custom-call(s32[9]{0:T(128)S(1)} %stack.39.place, bf16[8,128,256]{2,1,0:T(8,128)(2,1)S(1)} %shard_map.220.norm, bf16[128,2048]{1,0:T(8,128)(2,1)} %bitcast.50, f32[1,2048]{1,0:T(1,128)} %bitcast.54, ...), custom_call_target="tpu_custom_call" | custom-call | flops 2000000000 | bytes 1000000 | tf_op jit(solution)/shard_map/pallas_call | solution.py:50
  78.4 36.0 %all_to_all.20 = bf16[128,8,1024]{2,1,0:T(8,128)(2,1)S(1)} all-to-all(bf16[128,8,1024]{2,1,0:T(8,128)(2,1)} %bitcast.47), channel_id=1, replica_groups=mesh['sp'=16,'dp'=8] {'sp','dp'}, dimensions={0} | all-to-all | bytes 4194304 | tf_op jit(solution)/shard_map/all_to_all | solution.py:341
  114.4 5.4 %shard_map.223 = bf16[1024,1024]{1,0:T(8,128)(2,1)S(1)} custom-call(bf16[1024,1024]{1,0:T(8,128)(2,1)S(1)} %bitcast.45, bf16[2048,512]{1,0:T(8,128)(2,1)} %bitcast.58, bf16[2048,512]{1,0:T(8,128)(2,1)} %bitcast.59, bf16[512,2048]{1,0:T(8,128)(2,1)} %bitcast.60), custom_call_target="tpu_custom_call" | custom-call | flops 3000000000 | bytes 1000000 | tf_op jit(solution)/shard_map/pallas_call | solution.py:50
  119.8 1.3 copy-done
  121.2 4.4 %all-to-all-start.3 = ((bf16[128,8,1024]{2,1,0:T(8,128)(2,1)}), bf16[128,8,1024]{2,1,0:T(8,128)(2,1)S(1)}, u32[]{:S(2)}, u32[]{:S(2)}) async-start(bf16[128,8,1024]{2,1,0:T(8,128)(2,1)} %bitcast.44), calls=%async_computation.3 | async-start | bytes 4194304 | tf_op jit(solution)/shard_map/all_to_all | solution.py:341
  125.6 5.3 %shard_map.224.base = f32[128,2048]{1,0:T(8,128)} custom-call(bf16[128,2048]{1,0:T(8,128)(2,1)} %get-tuple-element.31.ein, bf16[128,2048]{1,0:T(8,128)(2,1)} %get-tuple-element.32.mixed, bf16[2048,512]{1,0:T(8,128)(2,1)} %sg.1, bf16[2048,512]{1,0:T(8,128)(2,1)} %su.1, bf16[512,2048]{1,0:T(8,128)(2,1)} %sd.1), custom_call_target="tpu_custom_call" | custom-call | flops 4000000000 | bytes 1000000 | tf_op jit(solution)/shard_map/pallas_call | solution.py:50
  130.8 25.3 %all-to-all-done.3 = bf16[128,8,1024]{2,1,0:T(8,128)(2,1)S(1)} async-done(((bf16[128,8,1024]{2,1,0:T(8,128)(2,1)}), bf16[128,8,1024]{2,1,0:T(8,128)(2,1)S(1)}, u32[]{:S(2)}, u32[]{:S(2)}) %all-to-all-start.3) | async-done | bytes 2097184 | tf_op jit(solution)/shard_map/all_to_all | solution.py:341
  156.2 3.6 %shard_map.225 = bf16[128,2048]{1,0:T(8,128)(2,1)} custom-call(bf16[1024,1024]{1,0:T(8,128)(2,1)S(1)} %bitcast.43, bf16[256,1024]{1,0:T(8,128)(2,1)} %get-tuple-element.29.hi, bf16[256,1024]{1,0:T(8,128)(2,1)} %get-tuple-element.30.lo, f32[128,2048]{1,0:T(8,128)} %shard_map.224.base), custom_call_target="tpu_custom_call" | custom-call | flops 1000000 | bytes 1000000 | tf_op jit(solution)/shard_map/pallas_call | solution.py:50
  (9 shorter events, 0.0 us)
Async XLA Ops:
  0.0 15.4 %collective-permute-start.2 = (bf16[256,2048]{1,0:T(8,128)(2,1)}, bf16[256,2048]{1,0:T(8,128)(2,1)S(1)}, u32[]{:S(2)}, u32[]{:S(2)}) collective-permute-start(bf16[256,2048]{1,0:T(8,128)(2,1)} %w0.1), channel_id=1, source_target_pairs={{0,2},{1,7},{2,4},{3,1},{4,6},{5,3},{6,0},{7,5},{8,10},{9,15},{10,... | collective-permute-start | bytes 3145736 | tf_op jit(solution)/shard_map/ppermute | solution.py:358
  3.3 15.1 %collective-permute-start.1 = (bf16[256,2048]{1,0:T(8,128)(2,1)}, bf16[256,2048]{1,0:T(8,128)(2,1)S(1)}, u32[]{:S(2)}, u32[]{:S(2)}) collective-permute-start(bf16[256,2048]{1,0:T(8,128)(2,1)} %w0.1), channel_id=1, source_target_pairs={{0,1},{1,0},{2,3},{3,2},{4,5},{5,4},{6,7},{7,6},{8,9},{9,8},{10,11... | collective-permute-start | bytes 3145736 | tf_op jit(solution)/shard_map/ppermute | solution.py:361
  15.4 19.3 %collective-permute-start.6 = (bf16[256,2048]{1,0:T(8,128)(2,1)S(1)}, bf16[256,2048]{1,0:T(8,128)(2,1)}, u32[]{:S(2)}, u32[]{:S(2)}) collective-permute-start(bf16[256,2048]{1,0:T(8,128)(2,1)S(1)} %collective-permute-done.2.w2), channel_id=1, source_target_pairs={{0,2},{1,7},{2,4},{3,1},{4,6},{5,3},{6,0},{7,5},{8,10},{9,15},{10,... | collective-permute-start | bytes 3145736 | tf_op jit(solution)/shard_map/ppermute | solution.py:358
  18.4 23.0 %collective-permute-start.3 = (bf16[256,2048]{1,0:T(8,128)(2,1)S(1)}, bf16[256,2048]{1,0:T(8,128)(2,1)}, u32[]{:S(2)}, u32[]{:S(2)}) collective-permute-start(bf16[256,2048]{1,0:T(8,128)(2,1)S(1)} %collective-permute-done.1.w1), channel_id=1, source_target_pairs={{0,2},{1,7},{2,4},{3,1},{4,6},{5,3},{6,0},{7,5},{8,10},{9,15},{10,... | collective-permute-start | bytes 3145736 | tf_op jit(solution)/shard_map/ppermute | solution.py:358
  23.3 25.1 %all-to-all-start = ((bf16[16,160,128]{2,1,0:T(8,128)(2,1)}), bf16[16,160,128]{2,1,0:T(8,128)(2,1)S(1)}, u32[]{:S(2)}, u32[]{:S(2)}) async-start(bf16[16,160,128]{2,1,0:T(8,128)(2,1)} %get-tuple-element.26), calls=%async_computation | async-start | bytes 1310720 | tf_op jit(solution)/shard_map/all_to_all | solution.py:341
  33.3 38.4 %collective-permute-start.4 = (bf16[256,2048]{1,0:T(8,128)(2,1)S(1)}, bf16[256,2048]{1,0:T(8,128)(2,1)}, u32[]{:S(2)}, u32[]{:S(2)}) collective-permute-start(bf16[256,2048]{1,0:T(8,128)(2,1)S(1)} %collective-permute-done.2.w2), channel_id=1, source_target_pairs={{0,1},{1,0},{2,3},{3,2},{4,5},{5,4},{6,7},{7,6},{8,9},{9,8},{10,11... | collective-permute-start | bytes 3145736 | tf_op jit(solution)/shard_map/ppermute | solution.py:361
  34.6 37.1 %collective-permute-start.7 = (bf16[256,2048]{1,0:T(8,128)(2,1)}, bf16[256,2048]{1,0:T(8,128)(2,1)}, u32[]{:S(2)}, u32[]{:S(2)}) collective-permute-start(bf16[256,2048]{1,0:T(8,128)(2,1)} %collective-permute-done.6.w6), channel_id=1, source_target_pairs={{0,1},{1,0},{2,3},{3,2},{4,5},{5,4},{6,7},{7,6},{8,9},{9,8},{10,11... | collective-permute-start | bytes 3145736 | tf_op jit(solution)/shard_map/ppermute | solution.py:361
  41.3 30.4 %collective-permute-start.5 = (bf16[256,2048]{1,0:T(8,128)(2,1)}, bf16[256,2048]{1,0:T(8,128)(2,1)}, u32[]{:S(2)}, u32[]{:S(2)}) collective-permute-start(bf16[256,2048]{1,0:T(8,128)(2,1)} %collective-permute-done.3.w3), channel_id=1, source_target_pairs={{0,1},{1,0},{2,3},{3,2},{4,5},{5,4},{6,7},{7,6},{8,9},{9,8},{10,11... | collective-permute-start | bytes 3145736 | tf_op jit(solution)/shard_map/ppermute | solution.py:361
  45.0 15.8 %collective-permute-start = (bf16[8,4096]{1,0:T(8,128)(2,1)S(1)}, bf16[8,4096]{1,0:T(8,128)(2,1)S(1)}, u32[]{:S(2)}, u32[]{:S(2)}) collective-permute-start(bf16[8,4096]{1,0:T(8,128)(2,1)S(1)} %pad_maximum_fusion), channel_id=1, source_target_pairs={{0,8},{8,16},{16,24},{24,32},{32,40},{40,48},{48,56},{56,64},{64,7... | collective-permute-start | bytes 196616 | tf_op jit(solution)/shard_map/ppermute | solution.py:355
  50.4 18.3 %all-to-all-start.1 = ((bf16[16,128,128]{2,1,0:T(8,128)(2,1)}), bf16[16,128,128]{2,1,0:T(8,128)(2,1)S(1)}, u32[]{:S(2)}, u32[]{:S(2)}) async-start(bf16[16,128,128]{2,1,0:T(8,128)(2,1)} %shard_map.219), calls=%async_computation.1 | async-start | bytes 1048576 | tf_op jit(solution)/shard_map/all_to_all | solution.py:341
  60.7 0.6 copy-start.1
  119.8 1.3 copy-start
  121.2 35.0 %all-to-all-start.3 = ((bf16[128,8,1024]{2,1,0:T(8,128)(2,1)}), bf16[128,8,1024]{2,1,0:T(8,128)(2,1)S(1)}, u32[]{:S(2)}, u32[]{:S(2)}) async-start(bf16[128,8,1024]{2,1,0:T(8,128)(2,1)} %bitcast.44), calls=%async_computation.3 | async-start | bytes 4194304 | tf_op jit(solution)/shard_map/all_to_all | solution.py:341

commit v4 on v3

--- a/solution.py
+++ b/solution.py
@@ -22,7 +22,6 @@
 HALF = D // 2
 ROWS = 1024
 ST_ROWS = 160
-TOP = 16
 
 
 def full():
@@ -38,7 +37,7 @@
 
 
 def call(
-    kernel, outs, args, scratch=(), vmem=(), smem_in=(), raw=(), free=(), out_vmem=(), limit=12,
+    kernel, outs, args, scratch=(), vmem=(), smem_in=(), raw=(), free=(), out_vmem=(), raw_out=(), limit=12,
     flops=10**6,
 ):
     placed = [
@@ -56,7 +55,7 @@
         in_specs=[
             smem() if i in smem_in else anywhere() if i in raw else full() for i in range(len(args))
         ],
-        out_specs=tuple(full() for _ in outs),
+        out_specs=tuple(anywhere() if i in raw_out else full() for i in range(len(outs))),
         scratch_shapes=list(scratch),
         compiler_params=pltpu.CompilerParams(vmem_limit_bytes=limit << 20),
         cost_estimate=pl.CostEstimate(flops=flops, bytes_accessed=10**6, transcendentals=0),
@@ -67,23 +66,13 @@
     return v / (1.0 + jnp.exp(-v))
 
 
-def tap(pad, rows, weight):
-    pad[0:8, :] = jnp.zeros((8, pad.shape[1]), F32)
+def tap(pad, halo, rows, weight):
+    pad[0:8, :] = jnp.zeros((8, pad.shape[1]), F32) if halo is None else halo.astype(F32)
     pad[8 : 8 + TOK, :] = rows.astype(F32)
     w = weight.astype(F32)
     total = pad[5 : 5 + TOK, :] * w[0:1, :]
     for k in range(1, 4):
         total = total + pad[5 + k : 5 + k + TOK, :] * w[k : k + 1, :]
-    return silu(total)
-
-
-def tap_top(pad, halo, rows, weight):
-    pad[0:8, :] = halo.astype(F32)
-    pad[8 : 8 + TOP, :] = rows.astype(F32)
-    w = weight.astype(F32)
-    total = pad[5 : 5 + TOP, :] * w[0:1, :]
-    for k in range(1, 4):
-        total = total + pad[5 + k : 5 + k + TOP, :] * w[k : k + 1, :]
     return silu(total)
 
 
@@ -97,8 +86,10 @@
 
 
 def states_kernel(
-    x, b, step_in, cw, cbw, bias, dlog, st, v_out, xs_out, b_out, ec_out, grow_out, padx, padb
+    x, b, c, step_in, cw, cbw, bias, dlog, st, ec_out, grow_out, ends_out, padx, padb, last, sem
 ):
+    load = pltpu.make_async_copy(c.at[pl.ds(TOK - 8, 8), :], last, sem)
+    load.start()
     s = step_in[...].astype(F32).T + bias[...]
     step = jnp.maximum(s, 0.0) + jnp.log(1.0 + jnp.exp(-jnp.abs(s)))
     logs = step * (-jnp.exp(dlog[...]))
@@ -118,12 +109,9 @@
     for g in range(GROUPS):
         xc = slice(g * GW, (g + 1) * GW)
         bc = slice(g * STATE, (g + 1) * STATE)
-        xs = tap(padx.at[g % 2], x[:, xc], cw[:, xc])
-        bm = tap(padb.at[g % 2], b[:, bc], cbw[:, bc]).astype(BF)
+        xs = tap(padx.at[g % 2], None, x[:, xc], cw[:, xc])
+        bm = tap(padb.at[g % 2], None, b[:, bc], cbw[:, bc]).astype(BF)
         v = (xs * spread(later, g)).astype(BF)
-        xs_out[:, xc] = xs
-        v_out[:, xc] = v
-        b_out[:, bc] = bm
         fresh = lax.dot_general(v, bm, (((0,), (0,)), ((), ())), preferred_element_type=F32)
 
         def ends(rows):
@@ -151,32 +139,29 @@
             x_ends = ends(x[:, o * 128 : (o + 1) * 128].astype(F32))
             st[o, 128:144, :] = jnp.concatenate([tail, w_both], axis=0).astype(BF)
             st[o, 144:160, :] = jnp.concatenate([x_ends, b_ends], axis=0).astype(BF)
-
-
-def inner_kernel(
-    x, b, c, halo, cw, cbw, ccw, v_in, b_in, xs_in, ec, grow, skip, a_out, c_out, padx, padb, padc
-):
+    ends_out[:, 0:D] = x[TOK - 8 :, :]
+    ends_out[:, D : D + 1024] = b[TOK - 8 :, :]
+    load.wait()
+    ends_out[:, D + 1024 :] = last[...]
+
+
+def inner_kernel(x, b, c, halo, cw, cbw, ccw, ec, grow, skip, a_out, c_out, padx, padb):
     r = lax.broadcasted_iota(jnp.int32, (TOK, TOK), 0)
     s = lax.broadcasted_iota(jnp.int32, (TOK, TOK), 1)
     lower = s <= r
     cols = ec[...]
-    top = grow[0:TOP, :]
+    rows = grow[...]
     sk = jnp.broadcast_to(skip[...], (TOK, HEADS))
     for g in range(GROUPS):
         xc = slice(g * GW, (g + 1) * GW)
         bc = slice(g * STATE, (g + 1) * STATE)
         bh = slice(D + g * STATE, D + (g + 1) * STATE)
         ch = slice(D + 1024 + g * STATE, D + 1024 + (g + 1) * STATE)
-        xt = tap_top(padx.at[g % 2], halo[:, xc], x[0:TOP, xc], cw[:, xc])
-        bt = tap_top(padb.at[g % 2, 0], halo[:, bh], b[0:TOP, bc], cbw[:, bc]).astype(BF)
-        ct = tap_top(padb.at[g % 2, 1], halo[:, ch], c[0:TOP, bc], ccw[:, bc])
-        vt = (xt * spread(top, g)).astype(BF)
-        cm = tap(padc.at[g % 2], c[:, bc], ccw[:, bc])
-        cm = jnp.concatenate([ct, cm[TOP:]], axis=0).astype(BF)
+        xs = tap(padx.at[g % 2], halo[:, xc], x[:, xc], cw[:, xc])
+        bm = tap(padb.at[g % 2, 0], halo[:, bh], b[:, bc], cbw[:, bc]).astype(BF)
+        cm = tap(padb.at[g % 2, 1], halo[:, ch], c[:, bc], ccw[:, bc]).astype(BF)
         c_out[:, bc] = cm
-        bm = jnp.concatenate([bt, b_in[TOP:, bc]], axis=0)
-        v = jnp.concatenate([vt, v_in[TOP:, xc]], axis=0)
-        xs = jnp.concatenate([xt, xs_in[TOP:, xc]], axis=0)
+        v = (xs * spread(rows, g)).astype(BF)
         cb = lax.dot_general(cm, bm, (((1,), (1,)), ((), ())), preferred_element_type=F32)
         cb = jnp.where(lower, cb, 0.0).astype(BF)
         u = jnp.dot(cb, v, preferred_element_type=F32)
@@ -221,14 +206,13 @@
             carry = carry * factor + (got[i, 0 : 2 * HEAD_DIM, :].astype(F32) + extra)
 
 
-def routes_kernel(routes, rw, d_out, hi_out, lo_out):
+def slots(routes, rw):
+    both = jnp.concatenate([routes[...].astype(F32), rw[...], jnp.zeros((4, TOK), F32)], axis=0).T
+    ids = both[:, 0:2].astype(jnp.int32)
     e = lax.broadcasted_iota(jnp.int32, (TOK, 128), 1)
     r = lax.broadcasted_iota(jnp.int32, (TOK, TOK), 0)
     s = lax.broadcasted_iota(jnp.int32, (TOK, TOK), 1)
     tri = (s < r).astype(BF)
-    both = jnp.concatenate([routes[...].astype(F32), rw[...], jnp.zeros((4, TOK), F32)], axis=0).T
-    ids = both[:, 0:2].astype(jnp.int32)
-    w = both[:, 2:4]
     hot = [(ids[:, k : k + 1] == e).astype(F32) for k in range(2)]
     before0 = jnp.dot(tri, hot[0].astype(BF), preferred_element_type=F32)
     before1 = jnp.dot(tri, hot[1].astype(BF), preferred_element_type=F32)
@@ -237,18 +221,39 @@
         jnp.sum(before0 * hot[0], axis=1, keepdims=True).astype(jnp.int32),
         jnp.sum(before1 * hot[1], axis=1, keepdims=True).astype(jnp.int32),
     ]
+    return [ids[:, k : k + 1] * 8 + pos[k] for k in range(2)], both[:, 2:4]
+
+
+def routes_kernel(routes, rw, d_out):
+    at, _ = slots(routes, rw)
     lane = lax.broadcasted_iota(jnp.int32, (TOK, ROWS), 1)
     for h in range(2):
-        mask = [lane == ids[:, k : k + 1] * 8 + pos[k] + 4 * h for k in range(2)]
-        disp = jnp.where(mask[0] | mask[1], 1.0, 0.0)
-        d_out[:, h * TOK : (h + 1) * TOK] = disp.T.astype(BF)
-        comb = jnp.where(mask[0], w[:, 0:1], 0.0) + jnp.where(mask[1], w[:, 1:2], 0.0)
-        hi = comb.astype(BF)
-        hi_out[h * TOK : (h + 1) * TOK, :] = hi
-        lo_out[h * TOK : (h + 1) * TOK, :] = (comb - hi.astype(F32)).astype(BF)
-
-
-def norm_kernel(a, cm, ec, pref, gate, gain, norm):
+        hit = (lane == at[0] + 4 * h) | (lane == at[1] + 4 * h)
+        d_out[:, h * TOK : (h + 1) * TOK] = jnp.where(hit, 1.0, 0.0).T.astype(BF)
+
+
+def weights_kernel(routes, rw, w_out):
+    at, w = slots(routes, rw)
+    lane = lax.broadcasted_iota(jnp.int32, (TOK, ROWS), 1)
+    for h in range(2):
+        comb = jnp.where(lane == at[0] + 4 * h, w[:, 0:1], 0.0)
+        comb = comb + jnp.where(lane == at[1] + 4 * h, w[:, 1:2], 0.0)
+        w_out[h * TOK : (h + 1) * TOK, :] = comb.astype(BF)
+
+
+def mix_kernel(
+    place, a, cm, ec, pref, gate, gain, fgain, resid_in, disp_in,
+    w0, w1, w2, w3, w4, w5, w6, w7, mixed_out, ein_out, send_out,
+    norm, wide, resid, disp, mixed_buf, ein_buf, send, sems, out_sems
+):
+    loads = [
+        pltpu.make_async_copy(w, wide.at[k], sems.at[k])
+        for k, w in enumerate((w0, w1, w2, w3, w4, w5, w6, w7))
+    ]
+    loads.append(pltpu.make_async_copy(resid_in, resid, sems.at[8]))
+    loads.append(pltpu.make_async_copy(disp_in, disp, sems.at[9]))
+    for load in loads:
+        load.start()
     cols = ec[...]
     for g in range(GROUPS):
         xc = slice(g * GW, (g + 1) * GW)
@@ -260,29 +265,29 @@
         y = y * silu(gate[:, xc].astype(F32))
         y = y * lax.rsqrt(jnp.mean(y * y, axis=1, keepdims=True) + EPS)
         norm[g] = (y * gain[:, xc]).astype(BF)
-
-
-def mix_kernel(
-    place, norm, resid, fgain, disp, w0, w1, w2, w3, w4, w5, w6, w7,
-    mixed_out, ein_out, send, wide, sems
-):
-    loads = [
-        pltpu.make_async_copy(w, wide.at[k], sems.at[k])
-        for k, w in enumerate((w0, w1, w2, w3, w4, w5, w6, w7))
-    ]
     for load in loads:
-        load.start()
+        load.wait()
     proj = resid[...].astype(F32)
-    for k, load in enumerate(loads):
-        load.wait()
+    for k in range(8):
         proj = proj + jnp.dot(norm[place[k]], wide[k], preferred_element_type=F32)
     mixed = proj.astype(BF)
-    mixed_out[...] = mixed
+    mixed_buf[...] = mixed
+    stores = [pltpu.make_async_copy(mixed_buf, mixed_out, out_sems.at[0])]
+    stores[0].start()
     m = mixed.astype(F32)
     ein = (m * lax.rsqrt(jnp.mean(m * m, axis=1, keepdims=True) + EPS) * fgain[...]).astype(BF)
-    ein_out[...] = ein
+    ein_buf[...] = ein
+    stores.append(pltpu.make_async_copy(ein_buf, ein_out, out_sems.at[1]))
+    stores[1].start()
     stack = jnp.concatenate([ein[:, :HALF], ein[:, HALF:]], axis=0)
-    send[...] = jnp.dot(disp[...], stack, preferred_element_type=F32).astype(BF)
+    for q in range(4):
+        part = pl.ds(q * 256, 256)
+        send[part, :] = jnp.dot(disp[part, :], stack, preferred_element_type=F32).astype(BF)
+        store = pltpu.make_async_copy(send.at[part, :], send_out.at[part, :], out_sems.at[2 + q])
+        store.start()
+        stores.append(store)
+    for store in stores:
+        store.wait()
 
 
 def shared_kernel(ein, mixed, sg, su, sd, out):
@@ -324,11 +329,8 @@
         out[:, q * n : (q + 1) * n] = jnp.stack([o0, o1], axis=1).reshape(ROWS, n).astype(BF)
 
 
-def combine_kernel(got, hi, lo, base, out):
-    g = got[...]
-    y = jnp.dot(hi[...], g, preferred_element_type=F32) + jnp.dot(
-        lo[...], g, preferred_element_type=F32
-    )
+def combine_kernel(got, w, base, out):
+    y = jnp.dot(w[...], got[...], preferred_element_type=F32)
     out[:, :HALF] = (base[:, :HALF] + y[:TOK]).astype(BF)
     out[:, HALF:] = (base[:, HALF:] + y[TOK:]).astype(BF)
 
@@ -351,8 +353,6 @@
     dps = lax.axis_size("dp")
     experts = ways * dps
     x, b, c = head_input[0], b_input[0], c_input[0]
-    ends = jnp.concatenate([x[TOK - 8 :], b[TOK - 8 :], c[TOK - 8 :]], axis=1)
-    halo = lax.ppermute(ends, "sp", [(i, i + 1) for i in range(ways - 1)])
 
     def ring(v):
         return lax.ppermute(v, "dp", [(i, (i + (-2 if i % 2 else 2)) % dps) for i in range(dps)])
@@ -374,36 +374,31 @@
         [me, me ^ 1, at, at ^ 1, other, other ^ 1, me ^ 4, me ^ 5, lax.axis_index("sp")]
     ).astype(jnp.int32)
 
-    st, v, xs, bm, ec, grow = call(
+    st, ec, grow, ends = call(
         states_kernel,
-        [
-            ((ways, ST_ROWS, 128), BF), ((TOK, D), BF), ((TOK, D), F32), ((TOK, 1024), BF),
-            ((TOK, HEADS), F32), ((TOK, HEADS), F32),
+        [((ways, ST_ROWS, 128), BF), ((TOK, HEADS), F32), ((TOK, HEADS), F32), ((8, 4096), BF)],
+        (x, b, c, step_input[0].T, conv_weight, conv_b_weight, step_bias[None], decay_log[None]),
+        raw=(2,),
+        scratch=[
+            pltpu.VMEM((2, TOK + 8, GW), F32),
+            pltpu.VMEM((2, TOK + 8, STATE), F32),
+            pltpu.VMEM((8, 1024), BF),
+            pltpu.SemaphoreType.DMA,
         ],
-        (x, b, step_input[0].T, conv_weight, conv_b_weight, step_bias[None], decay_log[None]),
-        scratch=[pltpu.VMEM((2, TOK + 8, GW), F32), pltpu.VMEM((2, TOK + 8, STATE), F32)],
     )
     got = exchange(st, "sp")
+    halo = lax.ppermute(plain(ends), "sp", [(i, i + 1) for i in range(ways - 1)])
     a, cm = call(
         inner_kernel,
         [((TOK, D), F32), ((TOK, 1024), BF)],
-        (
-            x, b, c, halo, conv_weight, conv_b_weight, conv_c_weight, v, bm, xs, ec, grow,
-            skip[None],
-        ),
-        scratch=[
-            pltpu.VMEM((2, TOP + 8, GW), F32),
-            pltpu.VMEM((2, 2, TOP + 8, STATE), F32),
-            pltpu.VMEM((2, TOK + 8, STATE), F32),
-        ],
+        (x, b, c, halo, conv_weight, conv_b_weight, conv_c_weight, ec, grow, skip[None]),
+        free=(3,),
+        scratch=[pltpu.VMEM((2, TOK + 8, GW), F32), pltpu.VMEM((2, 2, TOK + 8, STATE), F32)],
         flops=4 * 10**9,
     )
-    disp, hi, lo = call(
-        routes_kernel,
-        [((ROWS, 2 * TOK), BF), ((2 * TOK, ROWS), BF), ((2 * TOK, ROWS), BF)],
-        (routes[0].T, route_weights[0].T),
-        flops=2 * 10**9,
-    )
+    ways_in = (routes[0].T, route_weights[0].T)
+    (disp,) = call(routes_kernel, [((ROWS, 2 * TOK), BF)], ways_in, flops=2 * 10**9)
+    (comb,) = call(weights_kernel, [((2 * TOK, ROWS), BF)], ways_in, flops=2 * 10**9)
     (carried,) = call(
         carry_kernel,
         [((ways, 128, 128), BF)],
@@ -412,24 +407,30 @@
         vmem=(3,),
     )
     pref = exchange(carried, "sp")
-    (norm,) = call(
-        norm_kernel,
-        [((GROUPS, TOK, GW), BF)],
-        (a, cm, ec, pref.reshape(GROUPS, GW, STATE), gate_input[0], norm_gain[None]),
-        vmem=(3,),
-        out_vmem=(0,),
-        flops=10**9,
-    )
     mixed, ein, send = call(
         mix_kernel,
         [((TOK, D), BF), ((TOK, D), BF), ((ROWS, HALF), BF)],
-        (place, norm, residual[0], ffn_gain[None], disp, *pieces),
-        scratch=[pltpu.VMEM((8, 256, D), BF), pltpu.SemaphoreType.DMA((8,))],
+        (
+            place, a, cm, ec, pref.reshape(GROUPS, GW, STATE), gate_input[0], norm_gain[None],
+            ffn_gain[None], residual[0], disp, *pieces,
+        ),
+        scratch=[
+            pltpu.VMEM((GROUPS, TOK, GW), BF),
+            pltpu.VMEM((8, 256, D), BF),
+            pltpu.VMEM((TOK, D), BF),
+            pltpu.VMEM((ROWS, 2 * TOK), BF),
+            pltpu.VMEM((TOK, D), BF),
+            pltpu.VMEM((TOK, D), BF),
+            pltpu.VMEM((ROWS, HALF), BF),
+            pltpu.SemaphoreType.DMA((10,)),
+            pltpu.SemaphoreType.DMA((6,)),
+        ],
         smem_in=(0,),
-        vmem=(1,),
-        raw=range(5, 13),
-        free=range(6, 13),
-        limit=32,
+        vmem=(4,),
+        raw=range(8, 18),
+        free=range(11, 18),
+        raw_out=(0, 1, 2),
+        limit=36,
         flops=2 * 10**9,
     )
     arrived = exchange(plain(send).reshape(experts, 8, HALF), ("sp", "dp"))
@@ -459,7 +460,7 @@
     )
     back = exchange(plain(done).reshape(experts, 8, HALF), ("sp", "dp"))
     (out,) = call(
-        combine_kernel, [((TOK, D), BF)], (back.reshape(ROWS, HALF), hi, lo, base), vmem=(0,)
+        combine_kernel, [((TOK, D), BF)], (back.reshape(ROWS, HALF), comb, base), vmem=(0,)
     )
     return plain(out)[None]
 

time: 161 us -> 159 us (0.988)
  local copies, waits for them, and re-layouts: 4.24 us -> 1.42 us
    slice x3 -> x0, local copies, waits for them, and re-layouts: 2.2 us -> none  [layer(): ends = jnp.concatenate([x[TOK - 8:], b[TOK - 8:], c[TOK - 8:]], axis=1)]
  transfers between devices with their start and end apart: 11 -> 11, of which waited for: 4 -> 4; matrix products, arithmetic and copies ran while one was open for 1% -> 0% of each run, Pallas kernels for 14% -> 13%
where the time goes in v4:
time: 159 us; the launch traced here: 158 us
  waiting for transfers between devices  46.8 us (29%)
  Pallas kernels  38.1 us (24%)
  blocking collectives  36.1 us (23%)
  starting transfers between devices  35.8 us (23%)
    pallas_call x9, Pallas kernels, call(): pl.pallas_call(kernel, out_shape=tuple((pltpu.VMEM(s, d) if i in out_vmem...  38.1 us
    all_to_all x1, blocking collectives, exchange(): lax.all_to_all(plain(v), axis, split_axis=0, concat_axis=0, tiled=True)  36.1 us
    all_to_all x3, waiting for transfers between devices, exchange(): lax.all_to_all(plain(v), axis, split_axis=0, concat_axis=0, tiled=True)  27.1 us
    ppermute x3, waiting for transfers between devices, ring(): lax.ppermute(v, 'dp', [(i, (i + (-2 if i % 2 else 2)) % dps) for i in ran...  19.7 us
    all_to_all x3, starting transfers between devices, exchange(): lax.all_to_all(plain(v), axis, split_axis=0, concat_axis=0, tiled=True)  19.7 us
    ppermute x4, starting transfers between devices, swap(): return lax.ppermute(v, 'dp', [(i, i ^ 1) for i in range(dps)])  6.49 us
    ppermute x3, starting transfers between devices, ring(): lax.ppermute(v, 'dp', [(i, (i + (-2 if i % 2 else 2)) % dps) for i in ran...  6.32 us
    ppermute x1, starting transfers between devices, layer(): lax.ppermute(plain(ends), 'sp', [(i, i + 1) for i in range(ways - 1)])  3.3 us
  transfers between devices with their start and end apart: 11, of which 4 were waited for; matrix products, arithmetic and copies ran while one was open for 0% of the time, Pallas kernels for 13%

profile of v4, /device:TPU:1, one launch (start us, length us, event | category | flops | bytes accessed | tf_op | source)
XLA Modules:
  0.0 158.4 jit_solution(6545711409321939819)
XLA Ops:
  0.0 3.3 %collective-permute-start.2 = (bf16[256,2048]{1,0:T(8,128)(2,1)}, bf16[256,2048]{1,0:T(8,128)(2,1)S(1)}, u32[]{:S(2)}, u32[]{:S(2)}) collective-permute-start(bf16[256,2048]{1,0:T(8,128)(2,1)} %w0.1), channel_id=1, source_target_pairs={{0,2},{1,7},{2,4},{3,1},{4,6},{5,3},{6,0},{7,5},{8,10},{9,15},{10,... | collective-permute-start | bytes 3145736 | tf_op jit(solution)/shard_map/ppermute | solution.py:358
  3.3 0.0 collective-permute-start.1
  3.3 12.1 %collective-permute-done.2.w2 = bf16[256,2048]{1,0:T(8,128)(2,1)S(1)} collective-permute-done((bf16[256,2048]{1,0:T(8,128)(2,1)}, bf16[256,2048]{1,0:T(8,128)(2,1)S(1)}, u32[]{:S(2)}, u32[]{:S(2)}) %collective-permute-start.2) | collective-permute-done | bytes 1048608 | tf_op jit(solution)/shard_map/ppermute | solution.py:358
  15.4 3.0 %collective-permute-start.6 = (bf16[256,2048]{1,0:T(8,128)(2,1)S(1)}, bf16[256,2048]{1,0:T(8,128)(2,1)}, u32[]{:S(2)}, u32[]{:S(2)}) collective-permute-start(bf16[256,2048]{1,0:T(8,128)(2,1)S(1)} %collective-permute-done.2.w2), channel_id=1, source_target_pairs={{0,2},{1,7},{2,4},{3,1},{4,6},{5,3},{6,0},{7,5},{8,10},{9,15},{10,... | collective-permute-start | bytes 3145736 | tf_op jit(solution)/shard_map/ppermute | solution.py:358
  18.4 0.0 collective-permute-done.1.w1
  18.4 0.0 collective-permute-start.3
  18.4 4.6 %shard_map.217 = (bf16[16,160,128]{2,1,0:T(8,128)(2,1)}, f32[128,32]{1,0:T(8,128)}, f32[128,32]{1,0:T(8,128)}, bf16[8,4096]{1,0:T(8,128)(2,1)}) custom-call(bf16[128,2048]{1,0:T(8,128)(2,1)} %bitcast.44, bf16[128,1024]{1,0:T(8,128)(2,1)} %bitcast.46, bf16[128,1024]{1,0:T(8,128)(2,1)} %bitcast.48, bf16[32,128]{1,0:T(8,128)(2,1)} %bitcast.50, ...), custom_call_target="tpu_custom_call" | custom-call | flops 1000000 | bytes 1000000 | tf_op jit(solution)/shard_map/pallas_call | solution.py:49
  23.0 7.8 %all-to-all-start = ((bf16[16,160,128]{2,1,0:T(8,128)(2,1)}), bf16[16,160,128]{2,1,0:T(8,128)(2,1)S(1)}, u32[]{:S(2)}, u32[]{:S(2)}) async-start(bf16[16,160,128]{2,1,0:T(8,128)(2,1)} %get-tuple-element.19), calls=%async_computation | async-start | bytes 1310720 | tf_op jit(solution)/shard_map/all_to_all | solution.py:343
  30.8 1.5 collective-permute-start.4
  32.3 0.0 collective-permute-done.6.w6
  32.3 1.4 collective-permute-start.7
  33.7 7.6 %collective-permute-done.3.w3 = bf16[256,2048]{1,0:T(8,128)(2,1)} collective-permute-done((bf16[256,2048]{1,0:T(8,128)(2,1)S(1)}, bf16[256,2048]{1,0:T(8,128)(2,1)}, u32[]{:S(2)}, u32[]{:S(2)}) %collective-permute-start.3) | collective-permute-done | bytes 1048608 | tf_op jit(solution)/shard_map/ppermute | solution.py:358
  41.3 3.6 %collective-permute-start.5 = (bf16[256,2048]{1,0:T(8,128)(2,1)}, bf16[256,2048]{1,0:T(8,128)(2,1)}, u32[]{:S(2)}, u32[]{:S(2)}) collective-permute-start(bf16[256,2048]{1,0:T(8,128)(2,1)} %collective-permute-done.3.w3), channel_id=1, source_target_pairs={{0,1},{1,0},{2,3},{3,2},{4,5},{5,4},{6,7},{7,6},{8,9},{9,8},{10,11... | collective-permute-start | bytes 3145736 | tf_op jit(solution)/shard_map/ppermute | solution.py:361
  45.0 3.3 %collective-permute-start = (bf16[8,4096]{1,0:T(8,128)(2,1)}, bf16[8,4096]{1,0:T(8,128)(2,1)S(1)}, u32[]{:S(2)}, u32[]{:S(2)}) collective-permute-start(bf16[8,4096]{1,0:T(8,128)(2,1)} %get-tuple-element.14), channel_id=1, source_target_pairs={{0,8},{8,16},{16,24},{24,32},{32,40},{40,48},{48,56},{56,64},{64,7... | collective-permute-start | bytes 196616 | tf_op jit(solution)/shard_map/ppermute | solution.py:390
  48.3 0.1 stack.39.place
  48.4 0.0 all-to-all-done.got
  48.4 2.0 %shard_map.219 = bf16[16,128,128]{2,1,0:T(8,128)(2,1)} custom-call(s32[9]{0:T(128)S(1)} %stack.39.place, bf16[4,2048]{1,0:T(4,128)(2,1)} %cw.5, bf16[4,1024]{1,0:T(4,128)(2,1)} %cbw.5, bf16[16,160,128]{2,1,0:T(8,128)(2,1)S(1)} %all-to-all-done.got), custom_call_target="tpu_custom_call" | custom-call | flops 1000000 | bytes 1000000 | tf_op jit(solution)/shard_map/pallas_call | solution.py:49
  50.4 7.5 %all-to-all-start.1 = ((bf16[16,128,128]{2,1,0:T(8,128)(2,1)}), bf16[16,128,128]{2,1,0:T(8,128)(2,1)S(1)}, u32[]{:S(2)}, u32[]{:S(2)}) async-start(bf16[16,128,128]{2,1,0:T(8,128)(2,1)} %shard_map.219), calls=%async_computation.1 | async-start | bytes 1048576 | tf_op jit(solution)/shard_map/all_to_all | solution.py:343
  57.9 2.4 %shard_map.220.disp_in = bf16[1024,256]{1,0:T(8,128)(2,1)} custom-call(s32[2,128]{1,0:T(2,128)} %bitcast.58, f32[2,128]{1,0:T(2,128)} %bitcast.60), custom_call_target="tpu_custom_call" | custom-call | flops 2000000000 | bytes 1000000 | tf_op jit(solution)/shard_map/pallas_call | solution.py:49
  60.2 0.0 collective-permute-done.halo
  60.2 4.4 %shard_map.218 = (f32[128,2048]{1,0:T(8,128)}, bf16[128,1024]{1,0:T(8,128)(2,1)}) custom-call(bf16[128,2048]{1,0:T(8,128)(2,1)} %bitcast.45, bf16[128,1024]{1,0:T(8,128)(2,1)} %bitcast.47, bf16[128,1024]{1,0:T(8,128)(2,1)} %bitcast.49, bf16[8,4096]{1,0:T(8,128)(2,1)S(1)} %collective-permute-done.halo, bf16[4,2048]{1,0:T(4,128)(2,1)} %cw.5, ...), custom_call_target="tpu_custom_call" | custom-call | flops 4000000000 | bytes 1000000 | tf_op jit(solution)/shard_map/pallas_call | solution.py:49
  64.6 4.0 %all-to-all-done.1 = bf16[16,128,128]{2,1,0:T(8,128)(2,1)S(1)} async-done(((bf16[16,128,128]{2,1,0:T(8,128)(2,1)}), bf16[16,128,128]{2,1,0:T(8,128)(2,1)S(1)}, u32[]{:S(2)}, u32[]{:S(2)}) %all-to-all-start.1) | async-done | bytes 524320 | tf_op jit(solution)/shard_map/all_to_all | solution.py:343
  68.7 0.0 collective-permute-done.4.w4
  68.7 8.8 %shard_map.221 = (bf16[128,2048]{1,0:T(8,128)(2,1)}, bf16[128,2048]{1,0:T(8,128)(2,1)}, bf16[1024,1024]{1,0:T(8,128)(2,1)}) custom-call(s32[9]{0:T(128)S(1)} %stack.39.place, f32[128,2048]{1,0:T(8,128)} %get-tuple-element.17.a, bf16[128,1024]{1,0:T(8,128)(2,1)} %get-tuple-element.18.cm, f32[128,32]{1,0:T(8,128)} %get-tuple-element.15.ec, ...), custom_call_target="tpu_custom_call" | custom-call | flops 2000000000 | bytes 1000000 | tf_op jit(solution)/shard_map/pallas_call | solution.py:49
  77.5 36.1 %all_to_all.20 = bf16[128,8,1024]{2,1,0:T(8,128)(2,1)S(1)} all-to-all(bf16[128,8,1024]{2,1,0:T(8,128)(2,1)} %bitcast.41), channel_id=1, replica_groups=mesh['sp'=16,'dp'=8] {'sp','dp'}, dimensions={0} | all-to-all | bytes 4194304 | tf_op jit(solution)/shard_map/all_to_all | solution.py:343
  113.7 5.4 %shard_map.222 = bf16[1024,1024]{1,0:T(8,128)(2,1)S(1)} custom-call(bf16[1024,1024]{1,0:T(8,128)(2,1)S(1)} %bitcast.40, bf16[2048,512]{1,0:T(8,128)(2,1)} %bitcast.55, bf16[2048,512]{1,0:T(8,128)(2,1)} %bitcast.56, bf16[512,2048]{1,0:T(8,128)(2,1)} %bitcast.57), custom_call_target="tpu_custom_call" | custom-call | flops 3000000000 | bytes 1000000 | tf_op jit(solution)/shard_map/pallas_call | solution.py:49
  119.1 1.3 copy-done
  120.5 4.4 %all-to-all-start.3 = ((bf16[128,8,1024]{2,1,0:T(8,128)(2,1)}), bf16[128,8,1024]{2,1,0:T(8,128)(2,1)S(1)}, u32[]{:S(2)}, u32[]{:S(2)}) async-start(bf16[128,8,1024]{2,1,0:T(8,128)(2,1)} %bitcast.39), calls=%async_computation.3 | async-start | bytes 4194304 | tf_op jit(solution)/shard_map/all_to_all | solution.py:343
  124.9 2.3 %shard_map.223.w = bf16[256,1024]{1,0:T(8,128)(2,1)} custom-call(s32[2,128]{1,0:T(2,128)} %bitcast.59, f32[2,128]{1,0:T(2,128)} %bitcast.61), custom_call_target="tpu_custom_call" | custom-call | flops 2000000000 | bytes 1000000 | tf_op jit(solution)/shard_map/pallas_call | solution.py:49
  127.1 5.3 %shard_map.224.base = f32[128,2048]{1,0:T(8,128)} custom-call(bf16[128,2048]{1,0:T(8,128)(2,1)} %get-tuple-element.21.ein, bf16[128,2048]{1,0:T(8,128)(2,1)} %get-tuple-element.22.mixed, bf16[2048,512]{1,0:T(8,128)(2,1)} %sg.1, bf16[2048,512]{1,0:T(8,128)(2,1)} %su.1, bf16[512,2048]{1,0:T(8,128)(2,1)} %sd.1), custom_call_target="tpu_custom_call" | custom-call | flops 4000000000 | bytes 1000000 | tf_op jit(solution)/shard_map/pallas_call | solution.py:49
  132.4 23.1 %all-to-all-done.3 = bf16[128,8,1024]{2,1,0:T(8,128)(2,1)S(1)} async-done(((bf16[128,8,1024]{2,1,0:T(8,128)(2,1)}), bf16[128,8,1024]{2,1,0:T(8,128)(2,1)S(1)}, u32[]{:S(2)}, u32[]{:S(2)}) %all-to-all-start.3) | async-done | bytes 2097184 | tf_op jit(solution)/shard_map/all_to_all | solution.py:343
  155.5 2.9 %shard_map.225 = bf16[128,2048]{1,0:T(8,128)(2,1)} custom-call(bf16[1024,1024]{1,0:T(8,128)(2,1)S(1)} %bitcast.37, bf16[256,1024]{1,0:T(8,128)(2,1)} %shard_map.223.w, f32[128,2048]{1,0:T(8,128)} %shard_map.224.base), custom_call_target="tpu_custom_call" | custom-call | flops 1000000 | bytes 1000000 | tf_op jit(solution)/shard_map/pallas_call | solution.py:49
  (3 shorter events, 0.0 us)
Async XLA Ops:
  0.0 15.4 %collective-permute-start.2 = (bf16[256,2048]{1,0:T(8,128)(2,1)}, bf16[256,2048]{1,0:T(8,128)(2,1)S(1)}, u32[]{:S(2)}, u32[]{:S(2)}) collective-permute-start(bf16[256,2048]{1,0:T(8,128)(2,1)} %w0.1), channel_id=1, source_target_pairs={{0,2},{1,7},{2,4},{3,1},{4,6},{5,3},{6,0},{7,5},{8,10},{9,15},{10,... | collective-permute-start | bytes 3145736 | tf_op jit(solution)/shard_map/ppermute | solution.py:358
  3.3 15.1 %collective-permute-start.1 = (bf16[256,2048]{1,0:T(8,128)(2,1)}, bf16[256,2048]{1,0:T(8,128)(2,1)S(1)}, u32[]{:S(2)}, u32[]{:S(2)}) collective-permute-start(bf16[256,2048]{1,0:T(8,128)(2,1)} %w0.1), channel_id=1, source_target_pairs={{0,1},{1,0},{2,3},{3,2},{4,5},{5,4},{6,7},{7,6},{8,9},{9,8},{10,11... | collective-permute-start | bytes 3145736 | tf_op jit(solution)/shard_map/ppermute | solution.py:361
  15.4 16.9 %collective-permute-start.6 = (bf16[256,2048]{1,0:T(8,128)(2,1)S(1)}, bf16[256,2048]{1,0:T(8,128)(2,1)}, u32[]{:S(2)}, u32[]{:S(2)}) collective-permute-start(bf16[256,2048]{1,0:T(8,128)(2,1)S(1)} %collective-permute-done.2.w2), channel_id=1, source_target_pairs={{0,2},{1,7},{2,4},{3,1},{4,6},{5,3},{6,0},{7,5},{8,10},{9,15},{10,... | collective-permute-start | bytes 3145736 | tf_op jit(solution)/shard_map/ppermute | solution.py:358
  18.4 23.0 %collective-permute-start.3 = (bf16[256,2048]{1,0:T(8,128)(2,1)S(1)}, bf16[256,2048]{1,0:T(8,128)(2,1)}, u32[]{:S(2)}, u32[]{:S(2)}) collective-permute-start(bf16[256,2048]{1,0:T(8,128)(2,1)S(1)} %collective-permute-done.1.w1), channel_id=1, source_target_pairs={{0,2},{1,7},{2,4},{3,1},{4,6},{5,3},{6,0},{7,5},{8,10},{9,15},{10,... | collective-permute-start | bytes 3145736 | tf_op jit(solution)/shard_map/ppermute | solution.py:358
  23.0 25.3 %all-to-all-start = ((bf16[16,160,128]{2,1,0:T(8,128)(2,1)}), bf16[16,160,128]{2,1,0:T(8,128)(2,1)S(1)}, u32[]{:S(2)}, u32[]{:S(2)}) async-start(bf16[16,160,128]{2,1,0:T(8,128)(2,1)} %get-tuple-element.19), calls=%async_computation | async-start | bytes 1310720 | tf_op jit(solution)/shard_map/all_to_all | solution.py:343
  30.8 37.9 %collective-permute-start.4 = (bf16[256,2048]{1,0:T(8,128)(2,1)S(1)}, bf16[256,2048]{1,0:T(8,128)(2,1)}, u32[]{:S(2)}, u32[]{:S(2)}) collective-permute-start(bf16[256,2048]{1,0:T(8,128)(2,1)S(1)} %collective-permute-done.2.w2), channel_id=1, source_target_pairs={{0,1},{1,0},{2,3},{3,2},{4,5},{5,4},{6,7},{7,6},{8,9},{9,8},{10,11... | collective-permute-start | bytes 3145736 | tf_op jit(solution)/shard_map/ppermute | solution.py:361
  32.3 36.4 %collective-permute-start.7 = (bf16[256,2048]{1,0:T(8,128)(2,1)}, bf16[256,2048]{1,0:T(8,128)(2,1)}, u32[]{:S(2)}, u32[]{:S(2)}) collective-permute-start(bf16[256,2048]{1,0:T(8,128)(2,1)} %collective-permute-done.6.w6), channel_id=1, source_target_pairs={{0,1},{1,0},{2,3},{3,2},{4,5},{5,4},{6,7},{7,6},{8,9},{9,8},{10,11... | collective-permute-start | bytes 3145736 | tf_op jit(solution)/shard_map/ppermute | solution.py:361
  41.3 27.3 %collective-permute-start.5 = (bf16[256,2048]{1,0:T(8,128)(2,1)}, bf16[256,2048]{1,0:T(8,128)(2,1)}, u32[]{:S(2)}, u32[]{:S(2)}) collective-permute-start(bf16[256,2048]{1,0:T(8,128)(2,1)} %collective-permute-done.3.w3), channel_id=1, source_target_pairs={{0,1},{1,0},{2,3},{3,2},{4,5},{5,4},{6,7},{7,6},{8,9},{9,8},{10,11... | collective-permute-start | bytes 3145736 | tf_op jit(solution)/shard_map/ppermute | solution.py:361
  45.0 15.3 %collective-permute-start = (bf16[8,4096]{1,0:T(8,128)(2,1)}, bf16[8,4096]{1,0:T(8,128)(2,1)S(1)}, u32[]{:S(2)}, u32[]{:S(2)}) collective-permute-start(bf16[8,4096]{1,0:T(8,128)(2,1)} %get-tuple-element.14), channel_id=1, source_target_pairs={{0,8},{8,16},{16,24},{24,32},{32,40},{40,48},{48,56},{56,64},{64,7... | collective-permute-start | bytes 196616 | tf_op jit(solution)/shard_map/ppermute | solution.py:390
  50.4 18.3 %all-to-all-start.1 = ((bf16[16,128,128]{2,1,0:T(8,128)(2,1)}), bf16[16,128,128]{2,1,0:T(8,128)(2,1)S(1)}, u32[]{:S(2)}, u32[]{:S(2)}) async-start(bf16[16,128,128]{2,1,0:T(8,128)(2,1)} %shard_map.219), calls=%async_computation.1 | async-start | bytes 1048576 | tf_op jit(solution)/shard_map/all_to_all | solution.py:343
  119.1 1.3 copy-start
  120.5 35.0 %all-to-all-start.3 = ((bf16[128,8,1024]{2,1,0:T(8,128)(2,1)}), bf16[128,8,1024]{2,1,0:T(8,128)(2,1)S(1)}, u32[]{:S(2)}, u32[]{:S(2)}) async-start(bf16[128,8,1024]{2,1,0:T(8,128)(2,1)} %bitcast.39), calls=%async_computation.3 | async-start | bytes 4194304 | tf_op jit(solution)/shard_map/all_to_all | solution.py:343

commit v5 on v4

--- a/solution.py
+++ b/solution.py
@@ -67,13 +67,17 @@
 
 
 def tap(pad, halo, rows, weight):
-    pad[0:8, :] = jnp.zeros((8, pad.shape[1]), F32) if halo is None else halo.astype(F32)
-    pad[8 : 8 + TOK, :] = rows.astype(F32)
-    w = weight.astype(F32)
-    total = pad[5 : 5 + TOK, :] * w[0:1, :]
-    for k in range(1, 4):
-        total = total + pad[5 + k : 5 + k + TOK, :] * w[k : k + 1, :]
-    return silu(total)
+    out = []
+    for i in range(rows.shape[1] // 128):
+        cols = slice(i * 128, (i + 1) * 128)
+        pad[i, 0:8, :] = jnp.zeros((8, 128), F32) if halo is None else halo[:, cols].astype(F32)
+        pad[i, 8 : 8 + TOK, :] = rows[:, cols].astype(F32)
+        w = weight[:, cols].astype(F32)
+        total = pad[i, 5 : 5 + TOK, :] * w[0:1, :]
+        for k in range(1, 4):
+            total = total + pad[i, 5 + k : 5 + k + TOK, :] * w[k : k + 1, :]
+        out.append(silu(total))
+    return jnp.concatenate(out, axis=1) if len(out) > 1 else out[0]
 
 
 def spread(cols, g):
@@ -109,8 +113,8 @@
     for g in range(GROUPS):
         xc = slice(g * GW, (g + 1) * GW)
         bc = slice(g * STATE, (g + 1) * STATE)
-        xs = tap(padx.at[g % 2], None, x[:, xc], cw[:, xc])
-        bm = tap(padb.at[g % 2], None, b[:, bc], cbw[:, bc]).astype(BF)
+        xs = tap(padx.at[g], None, x[:, xc], cw[:, xc])
+        bm = tap(padb.at[g], None, b[:, bc], cbw[:, bc]).astype(BF)
         v = (xs * spread(later, g)).astype(BF)
         fresh = lax.dot_general(v, bm, (((0,), (0,)), ((), ())), preferred_element_type=F32)
 
@@ -145,7 +149,7 @@
     ends_out[:, D + 1024 :] = last[...]
 
 
-def inner_kernel(x, b, c, halo, cw, cbw, ccw, ec, grow, skip, a_out, c_out, padx, padb):
+def inner_kernel(x, b, c, halo, cw, cbw, ccw, ec, grow, skip, a_out, c_out, padx, padb, padc):
     r = lax.broadcasted_iota(jnp.int32, (TOK, TOK), 0)
     s = lax.broadcasted_iota(jnp.int32, (TOK, TOK), 1)
     lower = s <= r
@@ -157,9 +161,9 @@
         bc = slice(g * STATE, (g + 1) * STATE)
         bh = slice(D + g * STATE, D + (g + 1) * STATE)
         ch = slice(D + 1024 + g * STATE, D + 1024 + (g + 1) * STATE)
-        xs = tap(padx.at[g % 2], halo[:, xc], x[:, xc], cw[:, xc])
-        bm = tap(padb.at[g % 2, 0], halo[:, bh], b[:, bc], cbw[:, bc]).astype(BF)
-        cm = tap(padb.at[g % 2, 1], halo[:, ch], c[:, bc], ccw[:, bc]).astype(BF)
+        xs = tap(padx.at[g], halo[:, xc], x[:, xc], cw[:, xc])
+        bm = tap(padb.at[g], halo[:, bh], b[:, bc], cbw[:, bc]).astype(BF)
+        cm = tap(padc.at[g], halo[:, ch], c[:, bc], ccw[:, bc]).astype(BF)
         c_out[:, bc] = cm
         v = (xs * spread(rows, g)).astype(BF)
         cb = lax.dot_general(cm, bm, (((1,), (1,)), ((), ())), preferred_element_type=F32)
@@ -241,17 +245,15 @@
         w_out[h * TOK : (h + 1) * TOK, :] = comb.astype(BF)
 
 
-def mix_kernel(
-    place, a, cm, ec, pref, gate, gain, fgain, resid_in, disp_in,
-    w0, w1, w2, w3, w4, w5, w6, w7, mixed_out, ein_out, send_out,
-    norm, wide, resid, disp, mixed_buf, ein_buf, send, sems, out_sems
+def norm_kernel(
+    place, a, cm, ec, pref, gate, gain, resid_in, w0, w1, w2, w3, w4, w5, proj, rest,
+    norm, wide, picked, resid, sems
 ):
     loads = [
-        pltpu.make_async_copy(w, wide.at[k], sems.at[k])
-        for k, w in enumerate((w0, w1, w2, w3, w4, w5, w6, w7))
+        pltpu.make_async_copy(w, wide.at[pl.ds(k * GW, GW), :], sems.at[k])
+        for k, w in enumerate((w0, w1, w2, w3, w4, w5))
     ]
-    loads.append(pltpu.make_async_copy(resid_in, resid, sems.at[8]))
-    loads.append(pltpu.make_async_copy(disp_in, disp, sems.at[9]))
+    loads.append(pltpu.make_async_copy(resid_in, resid, sems.at[6]))
     for load in loads:
         load.start()
     cols = ec[...]
@@ -265,11 +267,31 @@
         y = y * silu(gate[:, xc].astype(F32))
         y = y * lax.rsqrt(jnp.mean(y * y, axis=1, keepdims=True) + EPS)
         norm[g] = (y * gain[:, xc]).astype(BF)
+    for k in range(6):
+        picked[:, k * GW : (k + 1) * GW] = norm[place[k]]
+    for k in range(2):
+        rest[:, k * GW : (k + 1) * GW] = norm[place[6 + k]]
     for load in loads:
         load.wait()
-    proj = resid[...].astype(F32)
-    for k in range(8):
-        proj = proj + jnp.dot(norm[place[k]], wide[k], preferred_element_type=F32)
+    proj[...] = resid[...].astype(F32) + jnp.dot(
+        picked[...], wide[...], preferred_element_type=F32
+    )
+
+
+def mix_kernel(
+    proj_in, rest, fgain, disp_in, w6, w7, mixed_out, ein_out, send_out,
+    wide, disp, mixed_buf, ein_buf, send, sems, out_sems
+):
+    loads = [
+        pltpu.make_async_copy(w, wide.at[pl.ds(k * GW, GW), :], sems.at[k])
+        for k, w in enumerate((w6, w7))
+    ]
+    loads.append(pltpu.make_async_copy(disp_in, disp, sems.at[2]))
+    for load in loads:
+        load.start()
+    for load in loads[:2]:
+        load.wait()
+    proj = proj_in[...] + jnp.dot(rest[...], wide[...], preferred_element_type=F32)
     mixed = proj.astype(BF)
     mixed_buf[...] = mixed
     stores = [pltpu.make_async_copy(mixed_buf, mixed_out, out_sems.at[0])]
@@ -280,6 +302,7 @@
     stores.append(pltpu.make_async_copy(ein_buf, ein_out, out_sems.at[1]))
     stores[1].start()
     stack = jnp.concatenate([ein[:, :HALF], ein[:, HALF:]], axis=0)
+    loads[2].wait()
     for q in range(4):
         part = pl.ds(q * 256, 256)
         send[part, :] = jnp.dot(disp[part, :], stack, preferred_element_type=F32).astype(BF)
@@ -380,8 +403,8 @@
         (x, b, c, step_input[0].T, conv_weight, conv_b_weight, step_bias[None], decay_log[None]),
         raw=(2,),
         scratch=[
-            pltpu.VMEM((2, TOK + 8, GW), F32),
-            pltpu.VMEM((2, TOK + 8, STATE), F32),
+            pltpu.VMEM((GROUPS, 2, TOK + 8, 128), F32),
+            pltpu.VMEM((GROUPS, 1, TOK + 8, 128), F32),
             pltpu.VMEM((8, 1024), BF),
             pltpu.SemaphoreType.DMA,
         ],
@@ -393,7 +416,11 @@
         [((TOK, D), F32), ((TOK, 1024), BF)],
         (x, b, c, halo, conv_weight, conv_b_weight, conv_c_weight, ec, grow, skip[None]),
         free=(3,),
-        scratch=[pltpu.VMEM((2, TOK + 8, GW), F32), pltpu.VMEM((2, 2, TOK + 8, STATE), F32)],
+        scratch=[
+            pltpu.VMEM((GROUPS, 2, TOK + 8, 128), F32),
+            pltpu.VMEM((GROUPS, 1, TOK + 8, 128), F32),
+            pltpu.VMEM((GROUPS, 1, TOK + 8, 128), F32),
+        ],
         flops=4 * 10**9,
     )
     ways_in = (routes[0].T, route_weights[0].T)
@@ -407,30 +434,46 @@
         vmem=(3,),
     )
     pref = exchange(carried, "sp")
+    proj, rest = call(
+        norm_kernel,
+        [((TOK, D), F32), ((TOK, 2 * GW), BF)],
+        (
+            place, a, cm, ec, pref.reshape(GROUPS, GW, STATE), gate_input[0], norm_gain[None],
+            residual[0], *pieces[:6],
+        ),
+        scratch=[
+            pltpu.VMEM((GROUPS, TOK, GW), BF),
+            pltpu.VMEM((6 * GW, D), BF),
+            pltpu.VMEM((TOK, 6 * GW), BF),
+            pltpu.VMEM((TOK, D), BF),
+            pltpu.SemaphoreType.DMA((7,)),
+        ],
+        smem_in=(0,),
+        vmem=(4,),
+        raw=range(7, 14),
+        free=range(9, 14),
+        out_vmem=(0, 1),
+        limit=32,
+        flops=2 * 10**9,
+    )
     mixed, ein, send = call(
         mix_kernel,
         [((TOK, D), BF), ((TOK, D), BF), ((ROWS, HALF), BF)],
-        (
-            place, a, cm, ec, pref.reshape(GROUPS, GW, STATE), gate_input[0], norm_gain[None],
-            ffn_gain[None], residual[0], disp, *pieces,
-        ),
+        (proj, rest, ffn_gain[None], disp, *pieces[6:]),
         scratch=[
-            pltpu.VMEM((GROUPS, TOK, GW), BF),
-            pltpu.VMEM((8, 256, D), BF),
-            pltpu.VMEM((TOK, D), BF),
+            pltpu.VMEM((2 * GW, D), BF),
             pltpu.VMEM((ROWS, 2 * TOK), BF),
             pltpu.VMEM((TOK, D), BF),
             pltpu.VMEM((TOK, D), BF),
             pltpu.VMEM((ROWS, HALF), BF),
-            pltpu.SemaphoreType.DMA((10,)),
+            pltpu.SemaphoreType.DMA((3,)),
             pltpu.SemaphoreType.DMA((6,)),
         ],
-        smem_in=(0,),
-        vmem=(4,),
-        raw=range(8, 18),
-        free=range(11, 18),
+        vmem=(0, 1),
+        raw=range(3, 6),
+        free=range(4, 6),
         raw_out=(0, 1, 2),
-        limit=36,
+        limit=28,
         flops=2 * 10**9,
     )
     arrived = exchange(plain(send).reshape(experts, 8, HALF), ("sp", "dp"))

time: 159 us -> 156 us (0.981)
  waiting for transfers between devices: 46.8 us -> 44.5 us
  starting transfers between devices: 35.8 us -> 33.9 us
    ppermute x3, waiting for transfers between devices: 19.7 us -> 16 us  [ring(): lax.ppermute(v, 'dp', [(i, (i + (-2 if i % 2 else 2)) % dps) for i in ran...]
    ppermute x4, starting transfers between devices: 6.49 us -> 3.74 us  [swap(): return lax.ppermute(v, 'dp', [(i, i ^ 1) for i in range(dps)])]
    ppermute x3, starting transfers between devices: 6.32 us -> 8.09 us  [ring(): lax.ppermute(v, 'dp', [(i, (i + (-2 if i % 2 else 2)) % dps) for i in ran...]
    pallas_call x9 -> x10, Pallas kernels: 38.1 us -> 39.3 us  [call(): pl.pallas_call(kernel, out_shape=tuple((pltpu.VMEM(s, d) if i in out_vmem...]
  transfers between devices with their start and end apart: 11 -> 11, of which waited for: 4 -> 5; matrix products, arithmetic and copies ran while one was open for 0% -> 0% of each run, Pallas kernels for 13% -> 17%
where the time goes in v5:
time: 156 us; the launch traced here: 155 us
  waiting for transfers between devices  44.5 us (29%)
  Pallas kernels  39.3 us (25%)
  blocking collectives  36 us (23%)
  starting transfers between devices  33.9 us (22%)
    pallas_call x10, Pallas kernels, call(): pl.pallas_call(kernel, out_shape=tuple((pltpu.VMEM(s, d) if i in out_vmem...  39.3 us
    all_to_all x1, blocking collectives, exchange(): lax.all_to_all(plain(v), axis, split_axis=0, concat_axis=0, tiled=True)  36 us
    all_to_all x3, waiting for transfers between devices, exchange(): lax.all_to_all(plain(v), axis, split_axis=0, concat_axis=0, tiled=True)  28.5 us
    all_to_all x3, starting transfers between devices, exchange(): lax.all_to_all(plain(v), axis, split_axis=0, concat_axis=0, tiled=True)  18.7 us
    ppermute x3, waiting for transfers between devices, ring(): lax.ppermute(v, 'dp', [(i, (i + (-2 if i % 2 else 2)) % dps) for i in ran...  16 us
    ppermute x3, starting transfers between devices, ring(): lax.ppermute(v, 'dp', [(i, (i + (-2 if i % 2 else 2)) % dps) for i in ran...  8.09 us
    ppermute x4, starting transfers between devices, swap(): return lax.ppermute(v, 'dp', [(i, i ^ 1) for i in range(dps)])  3.74 us
    ppermute x1, starting transfers between devices, layer(): lax.ppermute(plain(ends), 'sp', [(i, i + 1) for i in range(ways - 1)])  3.3 us
  transfers between devices with their start and end apart: 11, of which 5 were waited for; matrix products, arithmetic and copies ran while one was open for 0% of the time, Pallas kernels for 17%

profile of v5, /device:TPU:1, one launch (start us, length us, event | category | flops | bytes accessed | tf_op | source)
XLA Modules:
  0.0 155.1 jit_solution(8000729261127435694)
XLA Ops:
  0.0 1.4 collective-permute-start.1
  1.4 2.6 %collective-permute-start.2 = (bf16[256,2048]{1,0:T(8,128)(2,1)}, bf16[256,2048]{1,0:T(8,128)(2,1)S(1)}, u32[]{:S(2)}, u32[]{:S(2)}) collective-permute-start(bf16[256,2048]{1,0:T(8,128)(2,1)} %w0.1), channel_id=1, source_target_pairs={{0,2},{1,7},{2,4},{3,1},{4,6},{5,3},{6,0},{7,5},{8,10},{9,15},{10,... | collective-permute-start | bytes 3145736 | tf_op jit(solution)/shard_map/ppermute | solution.py:381
  4.0 2.5 %collective-permute-start.3 = (bf16[256,2048]{1,0:T(8,128)(2,1)S(1)}, bf16[256,2048]{1,0:T(8,128)(2,1)}, u32[]{:S(2)}, u32[]{:S(2)}) collective-permute-start(bf16[256,2048]{1,0:T(8,128)(2,1)S(1)} %collective-permute-done.1.w1), channel_id=1, source_target_pairs={{0,2},{1,7},{2,4},{3,1},{4,6},{5,3},{6,0},{7,5},{8,10},{9,15},{10,... | collective-permute-start | bytes 3145736 | tf_op jit(solution)/shard_map/ppermute | solution.py:381
  6.5 9.6 %collective-permute-done.2.w2 = bf16[256,2048]{1,0:T(8,128)(2,1)S(1)} collective-permute-done((bf16[256,2048]{1,0:T(8,128)(2,1)}, bf16[256,2048]{1,0:T(8,128)(2,1)S(1)}, u32[]{:S(2)}, u32[]{:S(2)}) %collective-permute-start.2) | collective-permute-done | bytes 1048608 | tf_op jit(solution)/shard_map/ppermute | solution.py:381
  16.0 3.0 %collective-permute-start.6 = (bf16[256,2048]{1,0:T(8,128)(2,1)S(1)}, bf16[256,2048]{1,0:T(8,128)(2,1)}, u32[]{:S(2)}, u32[]{:S(2)}) collective-permute-start(bf16[256,2048]{1,0:T(8,128)(2,1)S(1)} %collective-permute-done.2.w2), channel_id=1, source_target_pairs={{0,2},{1,7},{2,4},{3,1},{4,6},{5,3},{6,0},{7,5},{8,10},{9,15},{10,... | collective-permute-start | bytes 3145736 | tf_op jit(solution)/shard_map/ppermute | solution.py:381
  19.0 4.5 %shard_map.217 = (bf16[16,160,128]{2,1,0:T(8,128)(2,1)}, f32[128,32]{1,0:T(8,128)}, f32[128,32]{1,0:T(8,128)}, bf16[8,4096]{1,0:T(8,128)(2,1)}) custom-call(bf16[128,2048]{1,0:T(8,128)(2,1)} %bitcast.42, bf16[128,1024]{1,0:T(8,128)(2,1)} %bitcast.46, bf16[128,1024]{1,0:T(8,128)(2,1)} %bitcast.48, bf16[32,128]{1,0:T(8,128)(2,1)} %bitcast.50, ...), custom_call_target="tpu_custom_call" | custom-call | flops 1000000 | bytes 1000000 | tf_op jit(solution)/shard_map/pallas_call | solution.py:49
  23.6 7.8 %all-to-all-start = ((bf16[16,160,128]{2,1,0:T(8,128)(2,1)}), bf16[16,160,128]{2,1,0:T(8,128)(2,1)S(1)}, u32[]{:S(2)}, u32[]{:S(2)}) async-start(bf16[16,160,128]{2,1,0:T(8,128)(2,1)} %get-tuple-element.21), calls=%async_computation | async-start | bytes 1310720 | tf_op jit(solution)/shard_map/all_to_all | solution.py:366
  31.4 0.1 collective-permute-start.4
  31.5 0.0 collective-permute-done.3.w3
  31.5 0.5 collective-permute-start.5
  32.0 6.4 %collective-permute-done.6.w6 = bf16[256,2048]{1,0:T(8,128)(2,1)} collective-permute-done((bf16[256,2048]{1,0:T(8,128)(2,1)S(1)}, bf16[256,2048]{1,0:T(8,128)(2,1)}, u32[]{:S(2)}, u32[]{:S(2)}) %collective-permute-start.6) | collective-permute-done | bytes 1048608 | tf_op jit(solution)/shard_map/ppermute | solution.py:381
  38.4 1.8 %collective-permute-start.7 = (bf16[256,2048]{1,0:T(8,128)(2,1)}, bf16[256,2048]{1,0:T(8,128)(2,1)}, u32[]{:S(2)}, u32[]{:S(2)}) collective-permute-start(bf16[256,2048]{1,0:T(8,128)(2,1)} %collective-permute-done.6.w6), channel_id=1, source_target_pairs={{0,1},{1,0},{2,3},{3,2},{4,5},{5,4},{6,7},{7,6},{8,9},{9,8},{10,11... | collective-permute-start | bytes 3145736 | tf_op jit(solution)/shard_map/ppermute | solution.py:384
  40.2 3.3 %collective-permute-start = (bf16[8,4096]{1,0:T(8,128)(2,1)}, bf16[8,4096]{1,0:T(8,128)(2,1)S(1)}, u32[]{:S(2)}, u32[]{:S(2)}) collective-permute-start(bf16[8,4096]{1,0:T(8,128)(2,1)} %get-tuple-element.16), channel_id=1, source_target_pairs={{0,8},{8,16},{16,24},{24,32},{32,40},{40,48},{48,56},{56,64},{64,7... | collective-permute-start | bytes 196616 | tf_op jit(solution)/shard_map/ppermute | solution.py:413
  43.5 0.1 stack.39.place
  43.6 1.0 all-to-all-done.got
  44.6 2.0 %shard_map.219 = bf16[16,128,128]{2,1,0:T(8,128)(2,1)} custom-call(s32[9]{0:T(128)S(1)} %stack.39.place, bf16[4,2048]{1,0:T(4,128)(2,1)} %cw.5, bf16[4,1024]{1,0:T(4,128)(2,1)} %cbw.5, bf16[16,160,128]{2,1,0:T(8,128)(2,1)S(1)} %all-to-all-done.got), custom_call_target="tpu_custom_call" | custom-call | flops 1000000 | bytes 1000000 | tf_op jit(solution)/shard_map/pallas_call | solution.py:49
  46.6 6.5 %all-to-all-start.1 = ((bf16[16,128,128]{2,1,0:T(8,128)(2,1)}), bf16[16,128,128]{2,1,0:T(8,128)(2,1)S(1)}, u32[]{:S(2)}, u32[]{:S(2)}) async-start(bf16[16,128,128]{2,1,0:T(8,128)(2,1)} %shard_map.219), calls=%async_computation.1 | async-start | bytes 1048576 | tf_op jit(solution)/shard_map/all_to_all | solution.py:366
  53.1 2.4 %shard_map.221.disp_in = bf16[1024,256]{1,0:T(8,128)(2,1)} custom-call(s32[2,128]{1,0:T(2,128)} %bitcast.58, f32[2,128]{1,0:T(2,128)} %bitcast.60), custom_call_target="tpu_custom_call" | custom-call | flops 2000000000 | bytes 1000000 | tf_op jit(solution)/shard_map/pallas_call | solution.py:49
  55.4 4.0 %shard_map.218 = (f32[128,2048]{1,0:T(8,128)}, bf16[128,1024]{1,0:T(8,128)(2,1)}) custom-call(bf16[128,2048]{1,0:T(8,128)(2,1)} %bitcast.43, bf16[128,1024]{1,0:T(8,128)(2,1)} %bitcast.47, bf16[128,1024]{1,0:T(8,128)(2,1)} %bitcast.49, bf16[8,4096]{1,0:T(8,128)(2,1)S(1)} %collective-permute-done.halo, bf16[4,2048]{1,0:T(4,128)(2,1)} %cw.5, ...), custom_call_target="tpu_custom_call" | custom-call | flops 4000000000 | bytes 1000000 | tf_op jit(solution)/shard_map/pallas_call | solution.py:49
  59.5 4.4 %all-to-all-done.1 = bf16[16,128,128]{2,1,0:T(8,128)(2,1)S(1)} async-done(((bf16[16,128,128]{2,1,0:T(8,128)(2,1)}), bf16[16,128,128]{2,1,0:T(8,128)(2,1)S(1)}, u32[]{:S(2)}, u32[]{:S(2)}) %all-to-all-start.1) | async-done | bytes 524320 | tf_op jit(solution)/shard_map/all_to_all | solution.py:366
  63.9 0.0 collective-permute-done.4.w4
  63.9 0.0 collective-permute-done.5.w5
  63.9 5.9 %shard_map.220 = (f32[128,2048]{1,0:T(8,128)S(1)}, bf16[128,512]{1,0:T(8,128)(2,1)S(1)}) custom-call(s32[9]{0:T(128)S(1)} %stack.39.place, f32[128,2048]{1,0:T(8,128)} %get-tuple-element.19.a, bf16[128,1024]{1,0:T(8,128)(2,1)} %get-tuple-element.20.cm, f32[128,32]{1,0:T(8,128)} %get-tuple-element.17.ec, bf16[8,256,128]{2,1,0:T(8,128)(2,1)S(1)} %bitcast.40, ...), custom_call_target="tpu_custom_call" | custom-call | flops 2000000000 | bytes 1000000 | tf_op jit(solution)/shard_map/pallas_call | solution.py:49
  69.8 4.6 %shard_map.222 = (bf16[128,2048]{1,0:T(8,128)(2,1)}, bf16[128,2048]{1,0:T(8,128)(2,1)}, bf16[1024,1024]{1,0:T(8,128)(2,1)}) custom-call(f32[128,2048]{1,0:T(8,128)S(1)} %get-tuple-element.22.proj_in, bf16[128,512]{1,0:T(8,128)(2,1)S(1)} %get-tuple-element.23.rest, f32[1,2048]{1,0:T(1,128)} %bitcast.57, bf16[1024,256]{1,0:T(8,128)(2,1)} %shard_map.221.disp_in, ...), custom_call_target="tpu_custom_call" | custom-call | flops 2000000000 | bytes 1000000 | tf_op jit(solution)/shard_map/pallas_call | solution.py:49
  74.4 36.0 %all_to_all.20 = bf16[128,8,1024]{2,1,0:T(8,128)(2,1)S(1)} all-to-all(bf16[128,8,1024]{2,1,0:T(8,128)(2,1)} %bitcast.41), channel_id=1, replica_groups=mesh['sp'=16,'dp'=8] {'sp','dp'}, dimensions={0} | all-to-all | bytes 4194304 | tf_op jit(solution)/shard_map/all_to_all | solution.py:366
  110.4 5.4 %shard_map.223 = bf16[1024,1024]{1,0:T(8,128)(2,1)S(1)} custom-call(bf16[1024,1024]{1,0:T(8,128)(2,1)S(1)} %bitcast.39, bf16[2048,512]{1,0:T(8,128)(2,1)} %bitcast.54, bf16[2048,512]{1,0:T(8,128)(2,1)} %bitcast.55, bf16[512,2048]{1,0:T(8,128)(2,1)} %bitcast.56), custom_call_target="tpu_custom_call" | custom-call | flops 3000000000 | bytes 1000000 | tf_op jit(solution)/shard_map/pallas_call | solution.py:49
  115.9 1.3 copy-done
  117.2 4.4 %all-to-all-start.3 = ((bf16[128,8,1024]{2,1,0:T(8,128)(2,1)}), bf16[128,8,1024]{2,1,0:T(8,128)(2,1)S(1)}, u32[]{:S(2)}, u32[]{:S(2)}) async-start(bf16[128,8,1024]{2,1,0:T(8,128)(2,1)} %bitcast.38), calls=%async_computation.3 | async-start | bytes 4194304 | tf_op jit(solution)/shard_map/all_to_all | solution.py:366
  121.6 2.3 %shard_map.224.w = bf16[256,1024]{1,0:T(8,128)(2,1)} custom-call(s32[2,128]{1,0:T(2,128)} %bitcast.59, f32[2,128]{1,0:T(2,128)} %bitcast.61), custom_call_target="tpu_custom_call" | custom-call | flops 2000000000 | bytes 1000000 | tf_op jit(solution)/shard_map/pallas_call | solution.py:49
  123.9 5.3 %shard_map.225.base = f32[128,2048]{1,0:T(8,128)} custom-call(bf16[128,2048]{1,0:T(8,128)(2,1)} %get-tuple-element.25.ein, bf16[128,2048]{1,0:T(8,128)(2,1)} %get-tuple-element.26.mixed, bf16[2048,512]{1,0:T(8,128)(2,1)} %sg.1, bf16[2048,512]{1,0:T(8,128)(2,1)} %su.1, bf16[512,2048]{1,0:T(8,128)(2,1)} %sd.1), custom_call_target="tpu_custom_call" | custom-call | flops 4000000000 | bytes 1000000 | tf_op jit(solution)/shard_map/pallas_call | solution.py:49
  129.2 23.1 %all-to-all-done.3 = bf16[128,8,1024]{2,1,0:T(8,128)(2,1)S(1)} async-done(((bf16[128,8,1024]{2,1,0:T(8,128)(2,1)}), bf16[128,8,1024]{2,1,0:T(8,128)(2,1)S(1)}, u32[]{:S(2)}, u32[]{:S(2)}) %all-to-all-start.3) | async-done | bytes 2097184 | tf_op jit(solution)/shard_map/all_to_all | solution.py:366
  152.2 2.9 %shard_map.226 = bf16[128,2048]{1,0:T(8,128)(2,1)} custom-call(bf16[1024,1024]{1,0:T(8,128)(2,1)S(1)} %bitcast.37, bf16[256,1024]{1,0:T(8,128)(2,1)} %shard_map.224.w, f32[128,2048]{1,0:T(8,128)} %shard_map.225.base), custom_call_target="tpu_custom_call" | custom-call | flops 1000000 | bytes 1000000 | tf_op jit(solution)/shard_map/pallas_call | solution.py:49
  (4 shorter events, 0.0 us)
Async XLA Ops:
  0.0 4.0 %collective-permute-start.1 = (bf16[256,2048]{1,0:T(8,128)(2,1)}, bf16[256,2048]{1,0:T(8,128)(2,1)S(1)}, u32[]{:S(2)}, u32[]{:S(2)}) collective-permute-start(bf16[256,2048]{1,0:T(8,128)(2,1)} %w0.1), channel_id=1, source_target_pairs={{0,1},{1,0},{2,3},{3,2},{4,5},{5,4},{6,7},{7,6},{8,9},{9,8},{10,11... | collective-permute-start | bytes 3145736 | tf_op jit(solution)/shard_map/ppermute | solution.py:384
  1.4 14.7 %collective-permute-start.2 = (bf16[256,2048]{1,0:T(8,128)(2,1)}, bf16[256,2048]{1,0:T(8,128)(2,1)S(1)}, u32[]{:S(2)}, u32[]{:S(2)}) collective-permute-start(bf16[256,2048]{1,0:T(8,128)(2,1)} %w0.1), channel_id=1, source_target_pairs={{0,2},{1,7},{2,4},{3,1},{4,6},{5,3},{6,0},{7,5},{8,10},{9,15},{10,... | collective-permute-start | bytes 3145736 | tf_op jit(solution)/shard_map/ppermute | solution.py:381
  4.0 27.5 %collective-permute-start.3 = (bf16[256,2048]{1,0:T(8,128)(2,1)S(1)}, bf16[256,2048]{1,0:T(8,128)(2,1)}, u32[]{:S(2)}, u32[]{:S(2)}) collective-permute-start(bf16[256,2048]{1,0:T(8,128)(2,1)S(1)} %collective-permute-done.1.w1), channel_id=1, source_target_pairs={{0,2},{1,7},{2,4},{3,1},{4,6},{5,3},{6,0},{7,5},{8,10},{9,15},{10,... | collective-permute-start | bytes 3145736 | tf_op jit(solution)/shard_map/ppermute | solution.py:381
  16.0 22.4 %collective-permute-start.6 = (bf16[256,2048]{1,0:T(8,128)(2,1)S(1)}, bf16[256,2048]{1,0:T(8,128)(2,1)}, u32[]{:S(2)}, u32[]{:S(2)}) collective-permute-start(bf16[256,2048]{1,0:T(8,128)(2,1)S(1)} %collective-permute-done.2.w2), channel_id=1, source_target_pairs={{0,2},{1,7},{2,4},{3,1},{4,6},{5,3},{6,0},{7,5},{8,10},{9,15},{10,... | collective-permute-start | bytes 3145736 | tf_op jit(solution)/shard_map/ppermute | solution.py:381
  23.6 21.0 %all-to-all-start = ((bf16[16,160,128]{2,1,0:T(8,128)(2,1)}), bf16[16,160,128]{2,1,0:T(8,128)(2,1)S(1)}, u32[]{:S(2)}, u32[]{:S(2)}) async-start(bf16[16,160,128]{2,1,0:T(8,128)(2,1)} %get-tuple-element.21), calls=%async_computation | async-start | bytes 1310720 | tf_op jit(solution)/shard_map/all_to_all | solution.py:366
  31.4 32.5 %collective-permute-start.4 = (bf16[256,2048]{1,0:T(8,128)(2,1)S(1)}, bf16[256,2048]{1,0:T(8,128)(2,1)}, u32[]{:S(2)}, u32[]{:S(2)}) collective-permute-start(bf16[256,2048]{1,0:T(8,128)(2,1)S(1)} %collective-permute-done.2.w2), channel_id=1, source_target_pairs={{0,1},{1,0},{2,3},{3,2},{4,5},{5,4},{6,7},{7,6},{8,9},{9,8},{10,11... | collective-permute-start | bytes 3145736 | tf_op jit(solution)/shard_map/ppermute | solution.py:384
  31.5 32.4 %collective-permute-start.5 = (bf16[256,2048]{1,0:T(8,128)(2,1)}, bf16[256,2048]{1,0:T(8,128)(2,1)}, u32[]{:S(2)}, u32[]{:S(2)}) collective-permute-start(bf16[256,2048]{1,0:T(8,128)(2,1)} %collective-permute-done.3.w3), channel_id=1, source_target_pairs={{0,1},{1,0},{2,3},{3,2},{4,5},{5,4},{6,7},{7,6},{8,9},{9,8},{10,11... | collective-permute-start | bytes 3145736 | tf_op jit(solution)/shard_map/ppermute | solution.py:384
  38.4 31.4 %collective-permute-start.7 = (bf16[256,2048]{1,0:T(8,128)(2,1)}, bf16[256,2048]{1,0:T(8,128)(2,1)}, u32[]{:S(2)}, u32[]{:S(2)}) collective-permute-start(bf16[256,2048]{1,0:T(8,128)(2,1)} %collective-permute-done.6.w6), channel_id=1, source_target_pairs={{0,1},{1,0},{2,3},{3,2},{4,5},{5,4},{6,7},{7,6},{8,9},{9,8},{10,11... | collective-permute-start | bytes 3145736 | tf_op jit(solution)/shard_map/ppermute | solution.py:384
  40.2 15.3 %collective-permute-start = (bf16[8,4096]{1,0:T(8,128)(2,1)}, bf16[8,4096]{1,0:T(8,128)(2,1)S(1)}, u32[]{:S(2)}, u32[]{:S(2)}) collective-permute-start(bf16[8,4096]{1,0:T(8,128)(2,1)} %get-tuple-element.16), channel_id=1, source_target_pairs={{0,8},{8,16},{16,24},{24,32},{32,40},{40,48},{48,56},{56,64},{64,7... | collective-permute-start | bytes 196616 | tf_op jit(solution)/shard_map/ppermute | solution.py:413
  46.6 17.3 %all-to-all-start.1 = ((bf16[16,128,128]{2,1,0:T(8,128)(2,1)}), bf16[16,128,128]{2,1,0:T(8,128)(2,1)S(1)}, u32[]{:S(2)}, u32[]{:S(2)}) async-start(bf16[16,128,128]{2,1,0:T(8,128)(2,1)} %shard_map.219), calls=%async_computation.1 | async-start | bytes 1048576 | tf_op jit(solution)/shard_map/all_to_all | solution.py:366
  115.9 1.3 copy-start
  117.2 35.0 %all-to-all-start.3 = ((bf16[128,8,1024]{2,1,0:T(8,128)(2,1)}), bf16[128,8,1024]{2,1,0:T(8,128)(2,1)S(1)}, u32[]{:S(2)}, u32[]{:S(2)}) async-start(bf16[128,8,1024]{2,1,0:T(8,128)(2,1)} %bitcast.38), calls=%async_computation.3 | async-start | bytes 4194304 | tf_op jit(solution)/shard_map/all_to_all | solution.py:366

commit v6 on v5

--- a/solution.py
+++ b/solution.py
@@ -89,11 +89,37 @@
     return jnp.concatenate(out, axis=1)
 
 
+def begin(pairs, sems):
+    copies = [pltpu.make_async_copy(v, w, sems.at[k]) for k, (v, w) in enumerate(pairs)]
+    for copy in copies:
+        copy.start()
+    return copies
+
+
+def group(g):
+    return slice(g * GW, (g + 1) * GW), slice(g * STATE, (g + 1) * STATE)
+
+
+def part(g, width):
+    return pl.ds(g * width, width)
+
+
 def states_kernel(
-    x, b, c, step_in, cw, cbw, bias, dlog, st, ec_out, grow_out, ends_out, padx, padb, last, sem
+    step_in, cw, cbw, bias, dlog, x_in, b_in, c_in, st_out, ec_out, grow_out, ends_out,
+    padx, padb, x, b, st, ec, grow_buf, ends_buf, sems, out_sems
 ):
-    load = pltpu.make_async_copy(c.at[pl.ds(TOK - 8, 8), :], last, sem)
-    load.start()
+    pairs = []
+    for g in range(GROUPS):
+        pairs.append((x_in.at[:, part(g, GW)], x.at[:, part(g, GW)]))
+        pairs.append((b_in.at[:, part(g, STATE)], b.at[:, part(g, STATE)]))
+    pairs.append((c_in.at[pl.ds(TOK - 8, 8), :], ends_buf.at[:, pl.ds(D + 1024, 1024)]))
+    loads = begin(pairs, sems)
+    stores = []
+
+    def store(v, w):
+        stores.append(pltpu.make_async_copy(v, w, out_sems.at[len(stores)]))
+        stores[-1].start()
+
     s = step_in[...].astype(F32).T + bias[...]
     step = jnp.maximum(s, 0.0) + jnp.log(1.0 + jnp.exp(-jnp.abs(s)))
     logs = step * (-jnp.exp(dlog[...]))
@@ -101,9 +127,11 @@
     c = lax.broadcasted_iota(jnp.int32, (TOK, TOK), 1)
     tri = (c <= r).astype(F32)
     cum = jnp.dot(tri, logs, precision=lax.Precision.HIGHEST, preferred_element_type=F32)
-    ec_out[...] = jnp.exp(cum)
+    ec[...] = jnp.exp(cum)
+    store(ec, ec_out)
     grow = step * jnp.exp(-cum)
-    grow_out[...] = grow
+    grow_buf[...] = grow
+    store(grow_buf, grow_out)
     later = jnp.where(lax.broadcasted_iota(jnp.int32, (TOK, HEADS), 0) < 3, 0.0, grow)
     tot = cum[TOK - 1 : TOK, :]
     etot = jnp.exp(tot)
@@ -111,17 +139,23 @@
     sub = lax.broadcasted_iota(jnp.int32, (8, 128), 0)
     low = lax.broadcasted_iota(jnp.int32, (8, 128), 1) < HEAD_DIM
     for g in range(GROUPS):
-        xc = slice(g * GW, (g + 1) * GW)
-        bc = slice(g * STATE, (g + 1) * STATE)
+        xc, bc = group(g)
+        loads[2 * g].wait()
+        loads[2 * g + 1].wait()
         xs = tap(padx.at[g], None, x[:, xc], cw[:, xc])
         bm = tap(padb.at[g], None, b[:, bc], cbw[:, bc]).astype(BF)
         v = (xs * spread(later, g)).astype(BF)
         fresh = lax.dot_general(v, bm, (((0,), (0,)), ((), ())), preferred_element_type=F32)
 
-        def ends(rows):
-            return jnp.where(sub < 3, pltpu.roll(rows[TOK - 8 :], 3, 0), pltpu.roll(rows[:8], 3, 0))
-
-        b_ends = ends(b[:, bc].astype(F32))
+        def ends(rows, taps):
+            out = jnp.where(sub < 3, pltpu.roll(rows[TOK - 8 :], 3, 0), pltpu.roll(rows[:8], 3, 0))
+            return with_taps(out, taps)
+
+        def with_taps(rows, taps):
+            taps = taps.astype(F32)
+            return jnp.where(sub == 6, taps[0:1], jnp.where(sub == 7, taps[1:2], rows))
+
+        b_taps = cbw[:, bc]
         for i in range(2):
             h = g * PER + 2 * i
             o = g * 2 + i
@@ -134,22 +168,45 @@
             for j in range(2):
                 rest = jnp.broadcast_to(tot[0:1, h + j : h + j + 1], (8, 128))
                 for q in range(3):
-                    part = rest.astype(BF).astype(F32)
-                    tail = jnp.where(sub == 3 * j + q, part, tail)
-                    rest = rest - part
+                    piece = rest.astype(BF).astype(F32)
+                    tail = jnp.where(sub == 3 * j + q, piece, tail)
+                    rest = rest - piece
             w = jnp.where(low, first[:, h : h + 1], first[:, h + 1 : h + 2])
             w_hi = w.astype(BF).astype(F32)
             w_both = jnp.where(sub < 3, w_hi, pltpu.roll(w - w_hi, 3, 0))
-            x_ends = ends(x[:, o * 128 : (o + 1) * 128].astype(F32))
+            oc = slice(o * 128, (o + 1) * 128)
+            tail = with_taps(tail, cw[0:2, oc])
+            w_both = with_taps(w_both, cw[2:4, oc])
+            x_ends = ends(x[:, oc].astype(F32), b_taps[0:2])
+            b_ends = ends(b[:, bc].astype(F32), b_taps[2:4])
             st[o, 128:144, :] = jnp.concatenate([tail, w_both], axis=0).astype(BF)
             st[o, 144:160, :] = jnp.concatenate([x_ends, b_ends], axis=0).astype(BF)
-    ends_out[:, 0:D] = x[TOK - 8 :, :]
-    ends_out[:, D : D + 1024] = b[TOK - 8 :, :]
-    load.wait()
-    ends_out[:, D + 1024 :] = last[...]
-
-
-def inner_kernel(x, b, c, halo, cw, cbw, ccw, ec, grow, skip, a_out, c_out, padx, padb, padc):
+        store(st.at[part(g, 2)], st_out.at[part(g, 2)])
+    ends_buf[:, 0:D] = x[TOK - 8 :, :]
+    ends_buf[:, D : D + 1024] = b[TOK - 8 :, :]
+    loads[-1].wait()
+    store(ends_buf, ends_out)
+    for copy in stores:
+        copy.wait()
+
+
+def inner_kernel(
+    halo, cw, cbw, ccw, ec, grow, skip, routes, rw, x_in, b_in, c_in, a_out, c_out, d_out,
+    padx, padb, padc, x, b, c, a_buf, cm_buf, disp, sems, out_sems
+):
+    pairs = []
+    for g in range(GROUPS):
+        pairs.append((x_in.at[:, part(g, GW)], x.at[:, part(g, GW)]))
+        pairs.append((b_in.at[:, part(g, STATE)], b.at[:, part(g, STATE)]))
+        pairs.append((c_in.at[:, part(g, STATE)], c.at[:, part(g, STATE)]))
+    loads = begin(pairs, sems)
+    at, _ = slots(routes, rw)
+    lane = lax.broadcasted_iota(jnp.int32, (TOK, ROWS), 1)
+    for h in range(2):
+        hit = (lane == at[0] + 4 * h) | (lane == at[1] + 4 * h)
+        disp[:, h * TOK : (h + 1) * TOK] = jnp.where(hit, 1.0, 0.0).T.astype(BF)
+    stores = [pltpu.make_async_copy(disp, d_out, out_sems.at[0])]
+    stores[0].start()
     r = lax.broadcasted_iota(jnp.int32, (TOK, TOK), 0)
     s = lax.broadcasted_iota(jnp.int32, (TOK, TOK), 1)
     lower = s <= r
@@ -157,49 +214,64 @@
     rows = grow[...]
     sk = jnp.broadcast_to(skip[...], (TOK, HEADS))
     for g in range(GROUPS):
-        xc = slice(g * GW, (g + 1) * GW)
-        bc = slice(g * STATE, (g + 1) * STATE)
+        xc, bc = group(g)
         bh = slice(D + g * STATE, D + (g + 1) * STATE)
         ch = slice(D + 1024 + g * STATE, D + 1024 + (g + 1) * STATE)
+        for k in range(3):
+            loads[3 * g + k].wait()
         xs = tap(padx.at[g], halo[:, xc], x[:, xc], cw[:, xc])
         bm = tap(padb.at[g], halo[:, bh], b[:, bc], cbw[:, bc]).astype(BF)
         cm = tap(padc.at[g], halo[:, ch], c[:, bc], ccw[:, bc]).astype(BF)
-        c_out[:, bc] = cm
+        cm_buf[:, bc] = cm
         v = (xs * spread(rows, g)).astype(BF)
         cb = lax.dot_general(cm, bm, (((1,), (1,)), ((), ())), preferred_element_type=F32)
         cb = jnp.where(lower, cb, 0.0).astype(BF)
         u = jnp.dot(cb, v, preferred_element_type=F32)
-        a_out[:, xc] = u * spread(cols, g) + xs * spread(sk, g)
-
-
-def carry_kernel(place, cw, cbw, got, out):
+        a_buf[:, xc] = u * spread(cols, g) + xs * spread(sk, g)
+        stores.append(
+            pltpu.make_async_copy(
+                a_buf.at[:, part(g, GW)], a_out.at[:, part(g, GW)], out_sems.at[1 + g]
+            )
+        )
+        stores[-1].start()
+    stores.append(pltpu.make_async_copy(cm_buf, c_out, out_sems.at[1 + GROUPS]))
+    stores[-1].start()
+    for copy in stores:
+        copy.wait()
+
+
+def carry_kernel(got, out, buf, sems):
     count = got.shape[0]
-    o = place[8]
     sub = lax.broadcasted_iota(jnp.int32, (count, 8, 128), 1)
 
-    def starts(rows, weight):
-        rows = rows.astype(F32)
+    def starts(rows, w):
         before = jnp.concatenate([jnp.zeros((1, 8, 128), F32), rows[:-1]], axis=0)
         seq = jnp.where(sub < 3, before, rows)
-        w = weight.astype(F32)
-        total = seq * w[0:1, :][None]
+        total = seq * w[0]
         for k in range(1, 4):
-            total = total + pltpu.roll(seq, 8 - k, 1) * w[k : k + 1, :][None]
+            total = total + pltpu.roll(seq, 8 - k, 1) * w[k]
         return jnp.where(sub < 3, silu(total), 0.0)
 
     tails = got[:, 128:144, :].astype(F32)
     ends = got[:, 144:160, :].astype(F32)
     w = tails[:, 8:16]
     w = w + pltpu.roll(w, 5, 1)
-    xs = starts(ends[:, 0:8], cw[:, pl.ds(pl.multiple_of(o * 128, 128), 128)])
-    bm = starts(ends[:, 8:16], cbw[:, pl.ds(pl.multiple_of((o // 2) * 128, 128), 128)])
+    x_taps = [tails[0:1, k : k + 1] for k in (6, 7, 14, 15)]
+    b_taps = [ends[0:1, k : k + 1] for k in (6, 7, 14, 15)]
+    xs = starts(ends[:, 0:8], x_taps)
+    bm = starts(ends[:, 8:16], b_taps)
     vt = jnp.where(sub < 3, xs * w, 0.0).reshape(count * 8, 128).T
     bm = bm.reshape(count * 8, 128).astype(BF)
     lane = lax.broadcasted_iota(jnp.int32, (128, 128), 1)
     row = lax.broadcasted_iota(jnp.int32, (2 * HEAD_DIM, 128), 0)
     carry = jnp.zeros((2 * HEAD_DIM, 128), F32)
+    stores = []
     for i in range(count):
-        out[i] = carry.astype(BF)
+        buf[i] = carry.astype(BF)
+        if i % 4 == 3:
+            rows = pl.ds(i - 3, 4)
+            stores.append(pltpu.make_async_copy(buf.at[rows], out.at[rows], sems.at[i // 4]))
+            stores[-1].start()
         if i + 1 < count:
             mine = jnp.where(lane // 8 == i, vt, 0.0).astype(BF)
             extra = jnp.dot(mine, bm, preferred_element_type=F32)
@@ -208,6 +280,8 @@
             fb = jnp.exp(tail[3:4] + tail[4:5] + tail[5:6])
             factor = jnp.where(row < HEAD_DIM, fa, fb)
             carry = carry * factor + (got[i, 0 : 2 * HEAD_DIM, :].astype(F32) + extra)
+    for copy in stores:
+        copy.wait()
 
 
 def slots(routes, rw):
@@ -228,14 +302,6 @@
     return [ids[:, k : k + 1] * 8 + pos[k] for k in range(2)], both[:, 2:4]
 
 
-def routes_kernel(routes, rw, d_out):
-    at, _ = slots(routes, rw)
-    lane = lax.broadcasted_iota(jnp.int32, (TOK, ROWS), 1)
-    for h in range(2):
-        hit = (lane == at[0] + 4 * h) | (lane == at[1] + 4 * h)
-        d_out[:, h * TOK : (h + 1) * TOK] = jnp.where(hit, 1.0, 0.0).T.astype(BF)
-
-
 def weights_kernel(routes, rw, w_out):
     at, w = slots(routes, rw)
     lane = lax.broadcasted_iota(jnp.int32, (TOK, ROWS), 1)
@@ -246,20 +312,25 @@
 
 
 def norm_kernel(
-    place, a, cm, ec, pref, gate, gain, resid_in, w0, w1, w2, w3, w4, w5, proj, rest,
-    norm, wide, picked, resid, sems
+    place, pref, ec_in, a_in, cm_in, gate_in, gain_in, resid_in, w0, w1, w2, w3, w4, w5, proj, rest,
+    norm, wide, picked, ec, a, cm, gate, gain, resid, sems
 ):
-    loads = [
-        pltpu.make_async_copy(w, wide.at[pl.ds(k * GW, GW), :], sems.at[k])
-        for k, w in enumerate((w0, w1, w2, w3, w4, w5))
-    ]
-    loads.append(pltpu.make_async_copy(resid_in, resid, sems.at[6]))
-    for load in loads:
-        load.start()
+    pairs = [(ec_in, ec), (cm_in, cm), (gain_in, gain)]
+    for q in range(4):
+        pairs.append((a_in.at[:, part(q, 512)], a.at[:, part(q, 512)]))
+        pairs.append((gate_in.at[:, part(q, 512)], gate.at[:, part(q, 512)]))
+    for k, w in enumerate((w0, w1, w2, w3, w4, w5)):
+        pairs.append((w, wide.at[part(k, GW), :]))
+    pairs.append((resid_in, resid))
+    loads = begin(pairs, sems)
+    for load in loads[:3]:
+        load.wait()
     cols = ec[...]
     for g in range(GROUPS):
-        xc = slice(g * GW, (g + 1) * GW)
-        bc = slice(g * STATE, (g + 1) * STATE)
+        xc, bc = group(g)
+        if g % 2 == 0:
+            loads[3 + g].wait()
+            loads[4 + g].wait()
         outer = lax.dot_general(
             cm[:, bc], pref[g], (((1,), (1,)), ((), ())), preferred_element_type=F32
         )
@@ -271,7 +342,7 @@
         picked[:, k * GW : (k + 1) * GW] = norm[place[k]]
     for k in range(2):
         rest[:, k * GW : (k + 1) * GW] = norm[place[6 + k]]
-    for load in loads:
+    for load in loads[11:]:
         load.wait()
     proj[...] = resid[...].astype(F32) + jnp.dot(
         picked[...], wide[...], preferred_element_type=F32
@@ -279,19 +350,15 @@
 
 
 def mix_kernel(
-    proj_in, rest, fgain, disp_in, w6, w7, mixed_out, ein_out, send_out,
-    wide, disp, mixed_buf, ein_buf, send, sems, out_sems
+    proj_in, rest, fgain_in, disp_in, w6, w7, mixed_out, ein_out, send_out,
+    wide, fgain, disp, mixed_buf, ein_buf, send, sems, out_sems
 ):
-    loads = [
-        pltpu.make_async_copy(w, wide.at[pl.ds(k * GW, GW), :], sems.at[k])
-        for k, w in enumerate((w6, w7))
-    ]
-    loads.append(pltpu.make_async_copy(disp_in, disp, sems.at[2]))
-    for load in loads:
-        load.start()
+    pairs = [(w6, wide.at[part(0, GW), :]), (w7, wide.at[part(1, GW), :])]
+    loads = begin(pairs + [(fgain_in, fgain), (disp_in, disp)], sems)
     for load in loads[:2]:
         load.wait()
     proj = proj_in[...] + jnp.dot(rest[...], wide[...], preferred_element_type=F32)
+    loads[2].wait()
     mixed = proj.astype(BF)
     mixed_buf[...] = mixed
     stores = [pltpu.make_async_copy(mixed_buf, mixed_out, out_sems.at[0])]
@@ -302,11 +369,11 @@
     stores.append(pltpu.make_async_copy(ein_buf, ein_out, out_sems.at[1]))
     stores[1].start()
     stack = jnp.concatenate([ein[:, :HALF], ein[:, HALF:]], axis=0)
-    loads[2].wait()
+    loads[3].wait()
     for q in range(4):
-        part = pl.ds(q * 256, 256)
-        send[part, :] = jnp.dot(disp[part, :], stack, preferred_element_type=F32).astype(BF)
-        store = pltpu.make_async_copy(send.at[part, :], send_out.at[part, :], out_sems.at[2 + q])
+        rows = part(q, 256)
+        send[rows, :] = jnp.dot(disp[rows, :], stack, preferred_element_type=F32).astype(BF)
+        store = pltpu.make_async_copy(send.at[rows, :], send_out.at[rows, :], out_sems.at[2 + q])
         store.start()
         stores.append(store)
     for store in stores:
@@ -352,10 +419,20 @@
         out[:, q * n : (q + 1) * n] = jnp.stack([o0, o1], axis=1).reshape(ROWS, n).astype(BF)
 
 
-def combine_kernel(got, w, base, out):
-    y = jnp.dot(w[...], got[...], preferred_element_type=F32)
-    out[:, :HALF] = (base[:, :HALF] + y[:TOK]).astype(BF)
-    out[:, HALF:] = (base[:, HALF:] + y[TOK:]).astype(BF)
+def combine_kernel(got, w_in, base_in, out_ref, w, base, out, sems, out_sems):
+    loads = begin([(w_in, w), (base_in, base)], sems)
+    loads[0].wait()
+    stores = []
+    for h in range(2):
+        cols = part(h, HALF)
+        y = jnp.dot(w[part(h, TOK), :], got[...], preferred_element_type=F32)
+        if h == 0:
+            loads[1].wait()
+        out[:, cols] = (base[:, cols] + y).astype(BF)
+        stores.append(pltpu.make_async_copy(out.at[:, cols], out_ref.at[:, cols], out_sems.at[h]))
+        stores[h].start()
+    for copy in stores:
+        copy.wait()
 
 
 def plain(v):
@@ -394,63 +471,88 @@
     at = (me + dps - 2 + 4 * odd) % dps
     other = ((me ^ 1) + 2 + (dps - 4) * odd) % dps
     place = jnp.stack(
-        [me, me ^ 1, at, at ^ 1, other, other ^ 1, me ^ 4, me ^ 5, lax.axis_index("sp")]
+        [me, me ^ 1, at, at ^ 1, other, other ^ 1, me ^ 4, me ^ 5]
     ).astype(jnp.int32)
 
     st, ec, grow, ends = call(
         states_kernel,
         [((ways, ST_ROWS, 128), BF), ((TOK, HEADS), F32), ((TOK, HEADS), F32), ((8, 4096), BF)],
-        (x, b, c, step_input[0].T, conv_weight, conv_b_weight, step_bias[None], decay_log[None]),
-        raw=(2,),
+        (step_input[0].T, conv_weight, conv_b_weight, step_bias[None], decay_log[None], x, b, c),
+        raw=(5, 6, 7),
+        raw_out=range(4),
         scratch=[
             pltpu.VMEM((GROUPS, 2, TOK + 8, 128), F32),
             pltpu.VMEM((GROUPS, 1, TOK + 8, 128), F32),
-            pltpu.VMEM((8, 1024), BF),
-            pltpu.SemaphoreType.DMA,
+            pltpu.VMEM((TOK, D), BF),
+            pltpu.VMEM((TOK, 1024), BF),
+            pltpu.VMEM((ways, ST_ROWS, 128), BF),
+            pltpu.VMEM((TOK, HEADS), F32),
+            pltpu.VMEM((TOK, HEADS), F32),
+            pltpu.VMEM((8, 4096), BF),
+            pltpu.SemaphoreType.DMA((17,)),
+            pltpu.SemaphoreType.DMA((11,)),
         ],
     )
     got = exchange(st, "sp")
     halo = lax.ppermute(plain(ends), "sp", [(i, i + 1) for i in range(ways - 1)])
-    a, cm = call(
+    ways_in = (routes[0].T, route_weights[0].T)
+    a, cm, disp = call(
         inner_kernel,
-        [((TOK, D), F32), ((TOK, 1024), BF)],
-        (x, b, c, halo, conv_weight, conv_b_weight, conv_c_weight, ec, grow, skip[None]),
-        free=(3,),
+        [((TOK, D), F32), ((TOK, 1024), BF), ((ROWS, 2 * TOK), BF)],
+        (
+            halo, conv_weight, conv_b_weight, conv_c_weight, ec, grow, skip[None], *ways_in,
+            x, b, c,
+        ),
+        free=(0,),
+        raw=(9, 10, 11),
+        raw_out=range(3),
         scratch=[
             pltpu.VMEM((GROUPS, 2, TOK + 8, 128), F32),
             pltpu.VMEM((GROUPS, 1, TOK + 8, 128), F32),
             pltpu.VMEM((GROUPS, 1, TOK + 8, 128), F32),
+            pltpu.VMEM((TOK, D), BF),
+            pltpu.VMEM((TOK, 1024), BF),
+            pltpu.VMEM((TOK, 1024), BF),
+            pltpu.VMEM((TOK, D), F32),
+            pltpu.VMEM((TOK, 1024), BF),
+            pltpu.VMEM((ROWS, 2 * TOK), BF),
+            pltpu.SemaphoreType.DMA((24,)),
+            pltpu.SemaphoreType.DMA((10,)),
         ],
         flops=4 * 10**9,
     )
-    ways_in = (routes[0].T, route_weights[0].T)
-    (disp,) = call(routes_kernel, [((ROWS, 2 * TOK), BF)], ways_in, flops=2 * 10**9)
     (comb,) = call(weights_kernel, [((2 * TOK, ROWS), BF)], ways_in, flops=2 * 10**9)
     (carried,) = call(
         carry_kernel,
         [((ways, 128, 128), BF)],
-        (place, conv_weight, conv_b_weight, got),
-        smem_in=(0,),
-        vmem=(3,),
+        (got,),
+        vmem=(0,),
+        raw_out=(0,),
+        scratch=[pltpu.VMEM((ways, 128, 128), BF), pltpu.SemaphoreType.DMA((4,))],
     )
     pref = exchange(carried, "sp")
     proj, rest = call(
         norm_kernel,
         [((TOK, D), F32), ((TOK, 2 * GW), BF)],
         (
-            place, a, cm, ec, pref.reshape(GROUPS, GW, STATE), gate_input[0], norm_gain[None],
+            place, pref.reshape(GROUPS, GW, STATE), ec, a, cm, gate_input[0], norm_gain[None],
             residual[0], *pieces[:6],
         ),
         scratch=[
             pltpu.VMEM((GROUPS, TOK, GW), BF),
             pltpu.VMEM((6 * GW, D), BF),
             pltpu.VMEM((TOK, 6 * GW), BF),
+            pltpu.VMEM((TOK, HEADS), F32),
+            pltpu.VMEM((TOK, D), F32),
+            pltpu.VMEM((TOK, 1024), BF),
             pltpu.VMEM((TOK, D), BF),
-            pltpu.SemaphoreType.DMA((7,)),
+            pltpu.VMEM((1, D), F32),
+            pltpu.VMEM((TOK, D), BF),
+            pltpu.SemaphoreType.DMA((18,)),
         ],
         smem_in=(0,),
-        vmem=(4,),
-        raw=range(7, 14),
+        vmem=(1,),
+        raw=range(2, 14),
         free=range(9, 14),
         out_vmem=(0, 1),
         limit=32,
@@ -462,15 +564,16 @@
         (proj, rest, ffn_gain[None], disp, *pieces[6:]),
         scratch=[
             pltpu.VMEM((2 * GW, D), BF),
+            pltpu.VMEM((1, D), F32),
             pltpu.VMEM((ROWS, 2 * TOK), BF),
             pltpu.VMEM((TOK, D), BF),
             pltpu.VMEM((TOK, D), BF),
             pltpu.VMEM((ROWS, HALF), BF),
-            pltpu.SemaphoreType.DMA((3,)),
+            pltpu.SemaphoreType.DMA((4,)),
             pltpu.SemaphoreType.DMA((6,)),
         ],
         vmem=(0, 1),
-        raw=range(3, 6),
+        raw=range(2, 6),
         free=range(4, 6),
         raw_out=(0, 1, 2),
         limit=28,
@@ -503,7 +606,19 @@
     )
     back = exchange(plain(done).reshape(experts, 8, HALF), ("sp", "dp"))
     (out,) = call(
-        combine_kernel, [((TOK, D), BF)], (back.reshape(ROWS, HALF), comb, base), vmem=(0,)
+        combine_kernel,
+        [((TOK, D), BF)],
+        (back.reshape(ROWS, HALF), comb, base),
+        vmem=(0,),
+        raw=(1, 2),
+        raw_out=(0,),
+        scratch=[
+            pltpu.VMEM((2 * TOK, ROWS), BF),
+            pltpu.VMEM((TOK, D), F32),
+            pltpu.VMEM((TOK, D), BF),
+            pltpu.SemaphoreType.DMA((2,)),
+            pltpu.SemaphoreType.DMA((2,)),
+        ],
     )
     return plain(out)[None]
 

time: 156 us -> 157 us (level)
  blocking collectives: 36 us -> 39.3 us
  starting transfers between devices: 33.9 us -> 31.1 us
  waiting for transfers between devices: 44.5 us -> 47.1 us
  Pallas kernels: 39.3 us -> 36.8 us
    ppermute x1, waiting for transfers between devices: 0.01 us -> 3.6 us  [layer(): lax.ppermute(plain(ends), 'sp', [(i, i + 1) for i in range(ways - 1)])]
    all_to_all x1, blocking collectives: 36 us -> 39.3 us  [exchange(): lax.all_to_all(plain(v), axis, split_axis=0, concat_axis=0, tiled=True)]
    all_to_all x3, starting transfers between devices: 18.7 us -> 15.9 us  [exchange(): lax.all_to_all(plain(v), axis, split_axis=0, concat_axis=0, tiled=True)]
    pallas_call x10 -> x9, Pallas kernels: 39.3 us -> 36.8 us  [call(): pl.pallas_call(kernel, out_shape=tuple((pltpu.VMEM(s, d) if i in out_vmem...]
  transfers between devices with their start and end apart: 11 -> 11, of which waited for: 5 -> 5; matrix products, arithmetic and copies ran while one was open for 0% -> 0% of each run, Pallas kernels for 17% -> 16%
where the time goes in v6:
time: 157 us; the launch traced here: 156 us
  waiting for transfers between devices  47.1 us (30%)
  blocking collectives  39.3 us (25%)
  Pallas kernels  36.8 us (23%)
  starting transfers between devices  31.1 us (20%)
    all_to_all x1, blocking collectives, exchange(): lax.all_to_all(plain(v), axis, split_axis=0, concat_axis=0, tiled=True)  39.3 us
    pallas_call x9, Pallas kernels, call(): pl.pallas_call(kernel, out_shape=tuple((pltpu.VMEM(s, d) if i in out_vmem...  36.8 us
    all_to_all x3, waiting for transfers between devices, exchange(): lax.all_to_all(plain(v), axis, split_axis=0, concat_axis=0, tiled=True)  28.4 us
    all_to_all x3, starting transfers between devices, exchange(): lax.all_to_all(plain(v), axis, split_axis=0, concat_axis=0, tiled=True)  15.9 us
    ppermute x3, waiting for transfers between devices, ring(): lax.ppermute(v, 'dp', [(i, (i + (-2 if i % 2 else 2)) % dps) for i in ran...  15.1 us
    ppermute x3, starting transfers between devices, ring(): lax.ppermute(v, 'dp', [(i, (i + (-2 if i % 2 else 2)) % dps) for i in ran...  8.09 us
    ppermute x4, starting transfers between devices, swap(): return lax.ppermute(v, 'dp', [(i, i ^ 1) for i in range(dps)])  3.74 us
    ppermute x1, waiting for transfers between devices, layer(): lax.ppermute(plain(ends), 'sp', [(i, i + 1) for i in range(ways - 1)])  3.6 us
  transfers between devices with their start and end apart: 11, of which 5 were waited for; matrix products, arithmetic and copies ran while one was open for 0% of the time, Pallas kernels for 16%

profile of v6, /device:TPU:1, one launch (start us, length us, event | category | flops | bytes accessed | tf_op | source)
XLA Modules:
  0.0 156.1 jit_solution(8970858485643196002)
XLA Ops:
  0.0 1.4 collective-permute-start.1
  1.4 2.6 %collective-permute-start.2 = (bf16[256,2048]{1,0:T(8,128)(2,1)}, bf16[256,2048]{1,0:T(8,128)(2,1)S(1)}, u32[]{:S(2)}, u32[]{:S(2)}) collective-permute-start(bf16[256,2048]{1,0:T(8,128)(2,1)} %w0.1), channel_id=1, source_target_pairs={{0,2},{1,7},{2,4},{3,1},{4,6},{5,3},{6,0},{7,5},{8,10},{9,15},{10,... | collective-permute-start | bytes 3145736 | tf_op jit(solution)/shard_map/ppermute | solution.py:458
  4.0 0.0 collective-permute-done.1.w1
  4.0 2.5 %collective-permute-start.3 = (bf16[256,2048]{1,0:T(8,128)(2,1)S(1)}, bf16[256,2048]{1,0:T(8,128)(2,1)}, u32[]{:S(2)}, u32[]{:S(2)}) collective-permute-start(bf16[256,2048]{1,0:T(8,128)(2,1)S(1)} %collective-permute-done.1.w1), channel_id=1, source_target_pairs={{0,2},{1,7},{2,4},{3,1},{4,6},{5,3},{6,0},{7,5},{8,10},{9,15},{10,... | collective-permute-start | bytes 3145736 | tf_op jit(solution)/shard_map/ppermute | solution.py:458
  6.5 9.6 %collective-permute-done.2.w2 = bf16[256,2048]{1,0:T(8,128)(2,1)S(1)} collective-permute-done((bf16[256,2048]{1,0:T(8,128)(2,1)}, bf16[256,2048]{1,0:T(8,128)(2,1)S(1)}, u32[]{:S(2)}, u32[]{:S(2)}) %collective-permute-start.2) | collective-permute-done | bytes 1048608 | tf_op jit(solution)/shard_map/ppermute | solution.py:458
  16.0 3.0 %collective-permute-start.6 = (bf16[256,2048]{1,0:T(8,128)(2,1)S(1)}, bf16[256,2048]{1,0:T(8,128)(2,1)}, u32[]{:S(2)}, u32[]{:S(2)}) collective-permute-start(bf16[256,2048]{1,0:T(8,128)(2,1)S(1)} %collective-permute-done.2.w2), channel_id=1, source_target_pairs={{0,2},{1,7},{2,4},{3,1},{4,6},{5,3},{6,0},{7,5},{8,10},{9,15},{10,... | collective-permute-start | bytes 3145736 | tf_op jit(solution)/shard_map/ppermute | solution.py:458
  19.0 5.3 %shard_map.217 = (bf16[16,160,128]{2,1,0:T(8,128)(2,1)}, f32[128,32]{1,0:T(8,128)}, f32[128,32]{1,0:T(8,128)}, bf16[8,4096]{1,0:T(8,128)(2,1)}) custom-call(bf16[32,128]{1,0:T(8,128)(2,1)} %bitcast.49, bf16[4,2048]{1,0:T(4,128)(2,1)} %cw.3, bf16[4,1024]{1,0:T(4,128)(2,1)} %cbw.3, f32[1,32]{1,0:T(1,128)} %bitcast.51, f32[1,32]{1,0:T(1,128)} %bitcast.52, ...), custom_call_target="tpu_custom_call" | custom-call | flops 1000000 | bytes 1000000 | tf_op jit(solution)/shard_map/pallas_call | solution.py:49
  24.4 7.9 %all-to-all-start = ((bf16[16,160,128]{2,1,0:T(8,128)(2,1)}), bf16[16,160,128]{2,1,0:T(8,128)(2,1)S(1)}, u32[]{:S(2)}, u32[]{:S(2)}) async-start(bf16[16,160,128]{2,1,0:T(8,128)(2,1)} %get-tuple-element.17), calls=%async_computation | async-start | bytes 1310720 | tf_op jit(solution)/shard_map/all_to_all | solution.py:443
  32.3 0.1 collective-permute-start.4
  32.4 0.0 collective-permute-done.3.w3
  32.4 0.5 collective-permute-start.5
  32.9 5.5 %collective-permute-done.6.w6 = bf16[256,2048]{1,0:T(8,128)(2,1)} collective-permute-done((bf16[256,2048]{1,0:T(8,128)(2,1)S(1)}, bf16[256,2048]{1,0:T(8,128)(2,1)}, u32[]{:S(2)}, u32[]{:S(2)}) %collective-permute-start.6) | collective-permute-done | bytes 1048608 | tf_op jit(solution)/shard_map/ppermute | solution.py:458
  38.4 1.8 %collective-permute-start.7 = (bf16[256,2048]{1,0:T(8,128)(2,1)}, bf16[256,2048]{1,0:T(8,128)(2,1)}, u32[]{:S(2)}, u32[]{:S(2)}) collective-permute-start(bf16[256,2048]{1,0:T(8,128)(2,1)} %collective-permute-done.6.w6), channel_id=1, source_target_pairs={{0,1},{1,0},{2,3},{3,2},{4,5},{5,4},{6,7},{7,6},{8,9},{9,8},{10,11... | collective-permute-start | bytes 3145736 | tf_op jit(solution)/shard_map/ppermute | solution.py:461
  40.2 5.3 %all-to-all-done.got = bf16[16,160,128]{2,1,0:T(8,128)(2,1)S(1)} async-done(((bf16[16,160,128]{2,1,0:T(8,128)(2,1)}), bf16[16,160,128]{2,1,0:T(8,128)(2,1)S(1)}, u32[]{:S(2)}, u32[]{:S(2)}) %all-to-all-start) | async-done | bytes 655392 | tf_op jit(solution)/shard_map/all_to_all | solution.py:443
  45.5 1.2 shard_map.218
  46.7 3.6 %all-to-all-start.1 = ((bf16[16,128,128]{2,1,0:T(8,128)(2,1)}), bf16[16,128,128]{2,1,0:T(8,128)(2,1)S(1)}, u32[]{:S(2)}, u32[]{:S(2)}) async-start(bf16[16,128,128]{2,1,0:T(8,128)(2,1)} %shard_map.218), calls=%async_computation.1 | async-start | bytes 1048576 | tf_op jit(solution)/shard_map/all_to_all | solution.py:443
  50.3 3.3 %collective-permute-start = (bf16[8,4096]{1,0:T(8,128)(2,1)S(1)}, bf16[8,4096]{1,0:T(8,128)(2,1)S(1)}, u32[]{:S(2)}, u32[]{:S(2)}) collective-permute-start(bf16[8,4096]{1,0:T(8,128)(2,1)S(1)} %copy-done.1), channel_id=1, source_target_pairs={{0,8},{8,16},{16,24},{24,32},{32,40},{40,48},{48,56},{56,64},{64,7... | collective-permute-start | bytes 196616 | tf_op jit(solution)/shard_map/ppermute | solution.py:497
  53.6 0.1 stack.35.place
  53.7 3.6 %collective-permute-done.halo = bf16[8,4096]{1,0:T(8,128)(2,1)S(1)} collective-permute-done((bf16[8,4096]{1,0:T(8,128)(2,1)S(1)}, bf16[8,4096]{1,0:T(8,128)(2,1)S(1)}, u32[]{:S(2)}, u32[]{:S(2)}) %collective-permute-start) | collective-permute-done | bytes 65568 | tf_op jit(solution)/shard_map/ppermute | solution.py:497
  57.3 5.7 %shard_map.219 = (f32[128,2048]{1,0:T(8,128)}, bf16[128,1024]{1,0:T(8,128)(2,1)}, bf16[1024,256]{1,0:T(8,128)(2,1)}) custom-call(bf16[8,4096]{1,0:T(8,128)(2,1)S(1)} %collective-permute-done.halo, bf16[4,2048]{1,0:T(4,128)(2,1)} %cw.3, bf16[4,1024]{1,0:T(4,128)(2,1)} %cbw.3, bf16[4,1024]{1,0:T(4,128)(2,1)} %ccw.1, f32[128,32]{1,0:T(8,128)} %get-tuple-element.18.ec.ec_in, ...), custom_call_target="tpu_custom_call" | custom-call | flops 4000000000 | bytes 1000000 | tf_op jit(solution)/shard_map/pallas_call | solution.py:49
  63.1 0.0 collective-permute-done.4.w4
  63.1 0.0 collective-permute-done.5.w5
  63.1 4.8 %shard_map.220 = (f32[128,2048]{1,0:T(8,128)S(1)}, bf16[128,512]{1,0:T(8,128)(2,1)S(1)}) custom-call(s32[8]{0:T(128)S(1)} %stack.35.place, bf16[8,256,128]{2,1,0:T(8,128)(2,1)S(1)} %bitcast.39, f32[128,32]{1,0:T(8,128)} %get-tuple-element.18.ec.ec_in, f32[128,2048]{1,0:T(8,128)} %get-tuple-element.21.a_in, bf16[128,1024]{1,0:T(8,128)(2,1)} %get-tuple-element.22.cm_in, ...), custom_call_target="tpu_custom_call" | custom-call | flops 2000000000 | bytes 1000000 | tf_op jit(solution)/shard_map/pallas_call | solution.py:49
  67.9 4.1 %shard_map.221 = (bf16[128,2048]{1,0:T(8,128)(2,1)}, bf16[128,2048]{1,0:T(8,128)(2,1)}, bf16[1024,1024]{1,0:T(8,128)(2,1)}) custom-call(f32[128,2048]{1,0:T(8,128)S(1)} %get-tuple-element.23.proj_in, bf16[128,512]{1,0:T(8,128)(2,1)S(1)} %get-tuple-element.24.rest, f32[1,2048]{1,0:T(1,128)} %bitcast.56, bf16[1024,256]{1,0:T(8,128)(2,1)} %get-tuple-element.25.disp_in, ...), custom_call_target="tpu_custom_call" | custom-call | flops 2000000000 | bytes 1000000 | tf_op jit(solution)/shard_map/pallas_call | solution.py:49
  72.0 39.3 %all_to_all.20 = bf16[128,8,1024]{2,1,0:T(8,128)(2,1)S(1)} all-to-all(bf16[128,8,1024]{2,1,0:T(8,128)(2,1)} %bitcast.40), channel_id=1, replica_groups=mesh['sp'=16,'dp'=8] {'sp','dp'}, dimensions={0} | all-to-all | bytes 4194304 | tf_op jit(solution)/shard_map/all_to_all | solution.py:443
  111.4 5.5 %shard_map.222 = bf16[1024,1024]{1,0:T(8,128)(2,1)S(1)} custom-call(bf16[1024,1024]{1,0:T(8,128)(2,1)S(1)} %bitcast.38, bf16[2048,512]{1,0:T(8,128)(2,1)} %bitcast.53, bf16[2048,512]{1,0:T(8,128)(2,1)} %bitcast.54, bf16[512,2048]{1,0:T(8,128)(2,1)} %bitcast.55), custom_call_target="tpu_custom_call" | custom-call | flops 3000000000 | bytes 1000000 | tf_op jit(solution)/shard_map/pallas_call | solution.py:49
  116.8 1.3 copy-done
  118.2 4.4 %all-to-all-start.3 = ((bf16[128,8,1024]{2,1,0:T(8,128)(2,1)}), bf16[128,8,1024]{2,1,0:T(8,128)(2,1)S(1)}, u32[]{:S(2)}, u32[]{:S(2)}) async-start(bf16[128,8,1024]{2,1,0:T(8,128)(2,1)} %bitcast.37), calls=%async_computation.3 | async-start | bytes 4194304 | tf_op jit(solution)/shard_map/all_to_all | solution.py:443
  122.6 2.3 %shard_map.223.w_in = bf16[256,1024]{1,0:T(8,128)(2,1)} custom-call(s32[2,128]{1,0:T(2,128)} %bitcast.58, f32[2,128]{1,0:T(2,128)} %bitcast.60), custom_call_target="tpu_custom_call" | custom-call | flops 2000000000 | bytes 1000000 | tf_op jit(solution)/shard_map/pallas_call | solution.py:49
  124.8 5.3 %shard_map.224.base_in = f32[128,2048]{1,0:T(8,128)} custom-call(bf16[128,2048]{1,0:T(8,128)(2,1)} %get-tuple-element.27.ein, bf16[128,2048]{1,0:T(8,128)(2,1)} %get-tuple-element.28.mixed, bf16[2048,512]{1,0:T(8,128)(2,1)} %sg.1, bf16[2048,512]{1,0:T(8,128)(2,1)} %su.1, bf16[512,2048]{1,0:T(8,128)(2,1)} %sd.1), custom_call_target="tpu_custom_call" | custom-call | flops 4000000000 | bytes 1000000 | tf_op jit(solution)/shard_map/pallas_call | solution.py:49
  130.1 23.1 %all-to-all-done.3 = bf16[128,8,1024]{2,1,0:T(8,128)(2,1)S(1)} async-done(((bf16[128,8,1024]{2,1,0:T(8,128)(2,1)}), bf16[128,8,1024]{2,1,0:T(8,128)(2,1)S(1)}, u32[]{:S(2)}, u32[]{:S(2)}) %all-to-all-start.3) | async-done | bytes 2097184 | tf_op jit(solution)/shard_map/all_to_all | solution.py:443
  153.2 2.7 %shard_map.225 = bf16[128,2048]{1,0:T(8,128)(2,1)} custom-call(bf16[1024,1024]{1,0:T(8,128)(2,1)S(1)} %bitcast.36, bf16[256,1024]{1,0:T(8,128)(2,1)} %shard_map.223.w_in, f32[128,2048]{1,0:T(8,128)} %shard_map.224.base_in), custom_call_target="tpu_custom_call" | custom-call | flops 1000000 | bytes 1000000 | tf_op jit(solution)/shard_map/pallas_call | solution.py:49
  (5 shorter events, 0.0 us)
Async XLA Ops:
  0.0 4.0 %collective-permute-start.1 = (bf16[256,2048]{1,0:T(8,128)(2,1)}, bf16[256,2048]{1,0:T(8,128)(2,1)S(1)}, u32[]{:S(2)}, u32[]{:S(2)}) collective-permute-start(bf16[256,2048]{1,0:T(8,128)(2,1)} %w0.1), channel_id=1, source_target_pairs={{0,1},{1,0},{2,3},{3,2},{4,5},{5,4},{6,7},{7,6},{8,9},{9,8},{10,11... | collective-permute-start | bytes 3145736 | tf_op jit(solution)/shard_map/ppermute | solution.py:461
  1.4 14.7 %collective-permute-start.2 = (bf16[256,2048]{1,0:T(8,128)(2,1)}, bf16[256,2048]{1,0:T(8,128)(2,1)S(1)}, u32[]{:S(2)}, u32[]{:S(2)}) collective-permute-start(bf16[256,2048]{1,0:T(8,128)(2,1)} %w0.1), channel_id=1, source_target_pairs={{0,2},{1,7},{2,4},{3,1},{4,6},{5,3},{6,0},{7,5},{8,10},{9,15},{10,... | collective-permute-start | bytes 3145736 | tf_op jit(solution)/shard_map/ppermute | solution.py:458
  4.0 28.4 %collective-permute-start.3 = (bf16[256,2048]{1,0:T(8,128)(2,1)S(1)}, bf16[256,2048]{1,0:T(8,128)(2,1)}, u32[]{:S(2)}, u32[]{:S(2)}) collective-permute-start(bf16[256,2048]{1,0:T(8,128)(2,1)S(1)} %collective-permute-done.1.w1), channel_id=1, source_target_pairs={{0,2},{1,7},{2,4},{3,1},{4,6},{5,3},{6,0},{7,5},{8,10},{9,15},{10,... | collective-permute-start | bytes 3145736 | tf_op jit(solution)/shard_map/ppermute | solution.py:458
  16.0 22.4 %collective-permute-start.6 = (bf16[256,2048]{1,0:T(8,128)(2,1)S(1)}, bf16[256,2048]{1,0:T(8,128)(2,1)}, u32[]{:S(2)}, u32[]{:S(2)}) collective-permute-start(bf16[256,2048]{1,0:T(8,128)(2,1)S(1)} %collective-permute-done.2.w2), channel_id=1, source_target_pairs={{0,2},{1,7},{2,4},{3,1},{4,6},{5,3},{6,0},{7,5},{8,10},{9,15},{10,... | collective-permute-start | bytes 3145736 | tf_op jit(solution)/shard_map/ppermute | solution.py:458
  24.4 25.9 %copy-start.1 = (bf16[8,4096]{1,0:T(8,128)(2,1)S(1)}, bf16[8,4096]{1,0:T(8,128)(2,1)}, u32[]{:S(2)}) copy-start(bf16[8,4096]{1,0:T(8,128)(2,1)} %get-tuple-element.19) | copy-start | bytes 196612
  24.4 21.1 %all-to-all-start = ((bf16[16,160,128]{2,1,0:T(8,128)(2,1)}), bf16[16,160,128]{2,1,0:T(8,128)(2,1)S(1)}, u32[]{:S(2)}, u32[]{:S(2)}) async-start(bf16[16,160,128]{2,1,0:T(8,128)(2,1)} %get-tuple-element.17), calls=%async_computation | async-start | bytes 1310720 | tf_op jit(solution)/shard_map/all_to_all | solution.py:443
  32.3 30.8 %collective-permute-start.4 = (bf16[256,2048]{1,0:T(8,128)(2,1)S(1)}, bf16[256,2048]{1,0:T(8,128)(2,1)}, u32[]{:S(2)}, u32[]{:S(2)}) collective-permute-start(bf16[256,2048]{1,0:T(8,128)(2,1)S(1)} %collective-permute-done.2.w2), channel_id=1, source_target_pairs={{0,1},{1,0},{2,3},{3,2},{4,5},{5,4},{6,7},{7,6},{8,9},{9,8},{10,11... | collective-permute-start | bytes 3145736 | tf_op jit(solution)/shard_map/ppermute | solution.py:461
  32.4 30.7 %collective-permute-start.5 = (bf16[256,2048]{1,0:T(8,128)(2,1)}, bf16[256,2048]{1,0:T(8,128)(2,1)}, u32[]{:S(2)}, u32[]{:S(2)}) collective-permute-start(bf16[256,2048]{1,0:T(8,128)(2,1)} %collective-permute-done.3.w3), channel_id=1, source_target_pairs={{0,1},{1,0},{2,3},{3,2},{4,5},{5,4},{6,7},{7,6},{8,9},{9,8},{10,11... | collective-permute-start | bytes 3145736 | tf_op jit(solution)/shard_map/ppermute | solution.py:461
  38.4 29.5 %collective-permute-start.7 = (bf16[256,2048]{1,0:T(8,128)(2,1)}, bf16[256,2048]{1,0:T(8,128)(2,1)}, u32[]{:S(2)}, u32[]{:S(2)}) collective-permute-start(bf16[256,2048]{1,0:T(8,128)(2,1)} %collective-permute-done.6.w6), channel_id=1, source_target_pairs={{0,1},{1,0},{2,3},{3,2},{4,5},{5,4},{6,7},{7,6},{8,9},{9,8},{10,11... | collective-permute-start | bytes 3145736 | tf_op jit(solution)/shard_map/ppermute | solution.py:461
  46.7 16.4 %all-to-all-start.1 = ((bf16[16,128,128]{2,1,0:T(8,128)(2,1)}), bf16[16,128,128]{2,1,0:T(8,128)(2,1)S(1)}, u32[]{:S(2)}, u32[]{:S(2)}) async-start(bf16[16,128,128]{2,1,0:T(8,128)(2,1)} %shard_map.218), calls=%async_computation.1 | async-start | bytes 1048576 | tf_op jit(solution)/shard_map/all_to_all | solution.py:443
  50.3 7.1 %collective-permute-start = (bf16[8,4096]{1,0:T(8,128)(2,1)S(1)}, bf16[8,4096]{1,0:T(8,128)(2,1)S(1)}, u32[]{:S(2)}, u32[]{:S(2)}) collective-permute-start(bf16[8,4096]{1,0:T(8,128)(2,1)S(1)} %copy-done.1), channel_id=1, source_target_pairs={{0,8},{8,16},{16,24},{24,32},{32,40},{40,48},{48,56},{56,64},{64,7... | collective-permute-start | bytes 196616 | tf_op jit(solution)/shard_map/ppermute | solution.py:497
  116.8 1.3 copy-start
  118.2 35.0 %all-to-all-start.3 = ((bf16[128,8,1024]{2,1,0:T(8,128)(2,1)}), bf16[128,8,1024]{2,1,0:T(8,128)(2,1)S(1)}, u32[]{:S(2)}, u32[]{:S(2)}) async-start(bf16[128,8,1024]{2,1,0:T(8,128)(2,1)} %bitcast.37), calls=%async_computation.3 | async-start | bytes 4194304 | tf_op jit(solution)/shard_map/all_to_all | solution.py:443

commit v7 on v6

--- a/solution.py
+++ b/solution.py
@@ -105,21 +105,12 @@
 
 
 def states_kernel(
-    step_in, cw, cbw, bias, dlog, x_in, b_in, c_in, st_out, ec_out, grow_out, ends_out,
-    padx, padb, x, b, st, ec, grow_buf, ends_buf, sems, out_sems
+    step_in, cw, cbw, bias, dlog, x, b, c, st, ec, grow_out, ends_out, padx, padb, sem
 ):
-    pairs = []
-    for g in range(GROUPS):
-        pairs.append((x_in.at[:, part(g, GW)], x.at[:, part(g, GW)]))
-        pairs.append((b_in.at[:, part(g, STATE)], b.at[:, part(g, STATE)]))
-    pairs.append((c_in.at[pl.ds(TOK - 8, 8), :], ends_buf.at[:, pl.ds(D + 1024, 1024)]))
-    loads = begin(pairs, sems)
-    stores = []
-
-    def store(v, w):
-        stores.append(pltpu.make_async_copy(v, w, out_sems.at[len(stores)]))
-        stores[-1].start()
-
+    load = pltpu.make_async_copy(
+        c.at[pl.ds(TOK - 8, 8), :], ends_out.at[:, pl.ds(D + 1024, 1024)], sem
+    )
+    load.start()
     s = step_in[...].astype(F32).T + bias[...]
     step = jnp.maximum(s, 0.0) + jnp.log(1.0 + jnp.exp(-jnp.abs(s)))
     logs = step * (-jnp.exp(dlog[...]))
@@ -128,10 +119,8 @@
     tri = (c <= r).astype(F32)
     cum = jnp.dot(tri, logs, precision=lax.Precision.HIGHEST, preferred_element_type=F32)
     ec[...] = jnp.exp(cum)
-    store(ec, ec_out)
     grow = step * jnp.exp(-cum)
-    grow_buf[...] = grow
-    store(grow_buf, grow_out)
+    grow_out[...] = grow
     later = jnp.where(lax.broadcasted_iota(jnp.int32, (TOK, HEADS), 0) < 3, 0.0, grow)
     tot = cum[TOK - 1 : TOK, :]
     etot = jnp.exp(tot)
@@ -140,8 +129,6 @@
     low = lax.broadcasted_iota(jnp.int32, (8, 128), 1) < HEAD_DIM
     for g in range(GROUPS):
         xc, bc = group(g)
-        loads[2 * g].wait()
-        loads[2 * g + 1].wait()
         xs = tap(padx.at[g], None, x[:, xc], cw[:, xc])
         bm = tap(padb.at[g], None, b[:, bc], cbw[:, bc]).astype(BF)
         v = (xs * spread(later, g)).astype(BF)
@@ -181,32 +168,12 @@
             b_ends = ends(b[:, bc].astype(F32), b_taps[2:4])
             st[o, 128:144, :] = jnp.concatenate([tail, w_both], axis=0).astype(BF)
             st[o, 144:160, :] = jnp.concatenate([x_ends, b_ends], axis=0).astype(BF)
-        store(st.at[part(g, 2)], st_out.at[part(g, 2)])
-    ends_buf[:, 0:D] = x[TOK - 8 :, :]
-    ends_buf[:, D : D + 1024] = b[TOK - 8 :, :]
-    loads[-1].wait()
-    store(ends_buf, ends_out)
-    for copy in stores:
-        copy.wait()
-
-
-def inner_kernel(
-    halo, cw, cbw, ccw, ec, grow, skip, routes, rw, x_in, b_in, c_in, a_out, c_out, d_out,
-    padx, padb, padc, x, b, c, a_buf, cm_buf, disp, sems, out_sems
-):
-    pairs = []
-    for g in range(GROUPS):
-        pairs.append((x_in.at[:, part(g, GW)], x.at[:, part(g, GW)]))
-        pairs.append((b_in.at[:, part(g, STATE)], b.at[:, part(g, STATE)]))
-        pairs.append((c_in.at[:, part(g, STATE)], c.at[:, part(g, STATE)]))
-    loads = begin(pairs, sems)
-    at, _ = slots(routes, rw)
-    lane = lax.broadcasted_iota(jnp.int32, (TOK, ROWS), 1)
-    for h in range(2):
-        hit = (lane == at[0] + 4 * h) | (lane == at[1] + 4 * h)
-        disp[:, h * TOK : (h + 1) * TOK] = jnp.where(hit, 1.0, 0.0).T.astype(BF)
-    stores = [pltpu.make_async_copy(disp, d_out, out_sems.at[0])]
-    stores[0].start()
+    ends_out[:, 0:D] = x[TOK - 8 :, :]
+    ends_out[:, D : D + 1024] = b[TOK - 8 :, :]
+    load.wait()
+
+
+def inner_kernel(x, b, c, halo, cw, cbw, ccw, ec, grow, skip, a_out, c_out, padx, padb, padc):
     r = lax.broadcasted_iota(jnp.int32, (TOK, TOK), 0)
     s = lax.broadcasted_iota(jnp.int32, (TOK, TOK), 1)
     lower = s <= r
@@ -214,30 +181,19 @@
     rows = grow[...]
     sk = jnp.broadcast_to(skip[...], (TOK, HEADS))
     for g in range(GROUPS):
-        xc, bc = group(g)
+        xc = slice(g * GW, (g + 1) * GW)
+        bc = slice(g * STATE, (g + 1) * STATE)
         bh = slice(D + g * STATE, D + (g + 1) * STATE)
         ch = slice(D + 1024 + g * STATE, D + 1024 + (g + 1) * STATE)
-        for k in range(3):
-            loads[3 * g + k].wait()
         xs = tap(padx.at[g], halo[:, xc], x[:, xc], cw[:, xc])
         bm = tap(padb.at[g], halo[:, bh], b[:, bc], cbw[:, bc]).astype(BF)
         cm = tap(padc.at[g], halo[:, ch], c[:, bc], ccw[:, bc]).astype(BF)
-        cm_buf[:, bc] = cm
+        c_out[:, bc] = cm
         v = (xs * spread(rows, g)).astype(BF)
         cb = lax.dot_general(cm, bm, (((1,), (1,)), ((), ())), preferred_element_type=F32)
         cb = jnp.where(lower, cb, 0.0).astype(BF)
         u = jnp.dot(cb, v, preferred_element_type=F32)
-        a_buf[:, xc] = u * spread(cols, g) + xs * spread(sk, g)
-        stores.append(
-            pltpu.make_async_copy(
-                a_buf.at[:, part(g, GW)], a_out.at[:, part(g, GW)], out_sems.at[1 + g]
-            )
-        )
-        stores[-1].start()
-    stores.append(pltpu.make_async_copy(cm_buf, c_out, out_sems.at[1 + GROUPS]))
-    stores[-1].start()
-    for copy in stores:
-        copy.wait()
+        a_out[:, xc] = u * spread(cols, g) + xs * spread(sk, g)
 
 
 def carry_kernel(got, out, buf, sems):
@@ -302,6 +258,14 @@
     return [ids[:, k : k + 1] * 8 + pos[k] for k in range(2)], both[:, 2:4]
 
 
+def routes_kernel(routes, rw, d_out):
+    at, _ = slots(routes, rw)
+    lane = lax.broadcasted_iota(jnp.int32, (TOK, ROWS), 1)
+    for h in range(2):
+        hit = (lane == at[0] + 4 * h) | (lane == at[1] + 4 * h)
+        d_out[:, h * TOK : (h + 1) * TOK] = jnp.where(hit, 1.0, 0.0).T.astype(BF)
+
+
 def weights_kernel(routes, rw, w_out):
     at, w = slots(routes, rw)
     lane = lax.broadcasted_iota(jnp.int32, (TOK, ROWS), 1)
@@ -312,7 +276,7 @@
 
 
 def norm_kernel(
-    place, pref, ec_in, a_in, cm_in, gate_in, gain_in, resid_in, w0, w1, w2, w3, w4, w5, proj, rest,
+    pref, ec_in, a_in, cm_in, gate_in, gain_in, resid_in, w0, w1, w2, w3, w4, w5, proj, rest,
     norm, wide, picked, ec, a, cm, gate, gain, resid, sems
 ):
     pairs = [(ec_in, ec), (cm_in, cm), (gain_in, gain)]
@@ -338,6 +302,11 @@
         y = y * silu(gate[:, xc].astype(F32))
         y = y * lax.rsqrt(jnp.mean(y * y, axis=1, keepdims=True) + EPS)
         norm[g] = (y * gain[:, xc]).astype(BF)
+    me = lax.axis_index("dp")
+    odd = me & 1
+    at = (me + 6 + 4 * odd) & 7
+    other = ((me ^ 1) + 6 - 4 * odd + 4) & 7
+    place = [me, me ^ 1, at, at ^ 1, other, other ^ 1, me ^ 4, me ^ 5]
     for k in range(6):
         picked[:, k * GW : (k + 1) * GW] = norm[place[k]]
     for k in range(2):
@@ -466,61 +435,33 @@
     far = ring(near)
     pieces = [out_weight, partner, near, near2, swap(near), swap(near2)]
     pieces += [far, swap(far)]
-    me = lax.axis_index("dp")
-    odd = me & 1
-    at = (me + dps - 2 + 4 * odd) % dps
-    other = ((me ^ 1) + 2 + (dps - 4) * odd) % dps
-    place = jnp.stack(
-        [me, me ^ 1, at, at ^ 1, other, other ^ 1, me ^ 4, me ^ 5]
-    ).astype(jnp.int32)
-
     st, ec, grow, ends = call(
         states_kernel,
         [((ways, ST_ROWS, 128), BF), ((TOK, HEADS), F32), ((TOK, HEADS), F32), ((8, 4096), BF)],
         (step_input[0].T, conv_weight, conv_b_weight, step_bias[None], decay_log[None], x, b, c),
-        raw=(5, 6, 7),
-        raw_out=range(4),
+        raw=(7,),
         scratch=[
             pltpu.VMEM((GROUPS, 2, TOK + 8, 128), F32),
             pltpu.VMEM((GROUPS, 1, TOK + 8, 128), F32),
-            pltpu.VMEM((TOK, D), BF),
-            pltpu.VMEM((TOK, 1024), BF),
-            pltpu.VMEM((ways, ST_ROWS, 128), BF),
-            pltpu.VMEM((TOK, HEADS), F32),
-            pltpu.VMEM((TOK, HEADS), F32),
-            pltpu.VMEM((8, 4096), BF),
-            pltpu.SemaphoreType.DMA((17,)),
-            pltpu.SemaphoreType.DMA((11,)),
+            pltpu.SemaphoreType.DMA,
         ],
     )
     got = exchange(st, "sp")
     halo = lax.ppermute(plain(ends), "sp", [(i, i + 1) for i in range(ways - 1)])
-    ways_in = (routes[0].T, route_weights[0].T)
-    a, cm, disp = call(
+    a, cm = call(
         inner_kernel,
-        [((TOK, D), F32), ((TOK, 1024), BF), ((ROWS, 2 * TOK), BF)],
-        (
-            halo, conv_weight, conv_b_weight, conv_c_weight, ec, grow, skip[None], *ways_in,
-            x, b, c,
-        ),
-        free=(0,),
-        raw=(9, 10, 11),
-        raw_out=range(3),
+        [((TOK, D), F32), ((TOK, 1024), BF)],
+        (x, b, c, halo, conv_weight, conv_b_weight, conv_c_weight, ec, grow, skip[None]),
+        free=(3,),
         scratch=[
             pltpu.VMEM((GROUPS, 2, TOK + 8, 128), F32),
             pltpu.VMEM((GROUPS, 1, TOK + 8, 128), F32),
             pltpu.VMEM((GROUPS, 1, TOK + 8, 128), F32),
-            pltpu.VMEM((TOK, D), BF),
-            pltpu.VMEM((TOK, 1024), BF),
-            pltpu.VMEM((TOK, 1024), BF),
-            pltpu.VMEM((TOK, D), F32),
-            pltpu.VMEM((TOK, 1024), BF),
-            pltpu.VMEM((ROWS, 2 * TOK), BF),
-            pltpu.SemaphoreType.DMA((24,)),
-            pltpu.SemaphoreType.DMA((10,)),
         ],
         flops=4 * 10**9,
     )
+    ways_in = (routes[0].T, route_weights[0].T)
+    (disp,) = call(routes_kernel, [((ROWS, 2 * TOK), BF)], ways_in, flops=2 * 10**9)
     (comb,) = call(weights_kernel, [((2 * TOK, ROWS), BF)], ways_in, flops=2 * 10**9)
     (carried,) = call(
         carry_kernel,
@@ -535,7 +476,7 @@
         norm_kernel,
         [((TOK, D), F32), ((TOK, 2 * GW), BF)],
         (
-            place, pref.reshape(GROUPS, GW, STATE), ec, a, cm, gate_input[0], norm_gain[None],
+            pref.reshape(GROUPS, GW, STATE), ec, a, cm, gate_input[0], norm_gain[None],
             residual[0], *pieces[:6],
         ),
         scratch=[
@@ -550,10 +491,9 @@
             pltpu.VMEM((TOK, D), BF),
             pltpu.SemaphoreType.DMA((18,)),
         ],
-        smem_in=(0,),
-        vmem=(1,),
-        raw=range(2, 14),
-        free=range(9, 14),
+        vmem=(0,),
+        raw=range(1, 13),
+        free=range(8, 13),
         out_vmem=(0, 1),
         limit=32,
         flops=2 * 10**9,

time: 157 us -> 153 us (0.975)
  blocking collectives: 39.3 us -> 36 us
  starting transfers between devices: 31.1 us -> 33.7 us
  waiting for transfers between devices: 47.1 us -> 44.6 us
    ppermute x1, waiting for transfers between devices: 3.6 us -> 0.01 us  [layer(): lax.ppermute(plain(ends), 'sp', [(i, i + 1) for i in range(ways - 1)])]
    all_to_all x1, blocking collectives: 39.3 us -> 36 us  [exchange(): lax.all_to_all(plain(v), axis, split_axis=0, concat_axis=0, tiled=True)]
    all_to_all x3, starting transfers between devices: 15.9 us -> 18.5 us  [exchange(): lax.all_to_all(plain(v), axis, split_axis=0, concat_axis=0, tiled=True)]
    pallas_call x9 -> x10, Pallas kernels: 36.8 us -> 36.2 us  [call(): pl.pallas_call(kernel, out_shape=tuple((pltpu.VMEM(s, d) if i in out_vmem...]
where the time goes in v7:
time: 153 us; the launch traced here: 152 us
  waiting for transfers between devices  44.6 us (29%)
  Pallas kernels  36.2 us (24%)
  blocking collectives  36 us (24%)
  starting transfers between devices  33.7 us (22%)
    pallas_call x10, Pallas kernels, call(): pl.pallas_call(kernel, out_shape=tuple((pltpu.VMEM(s, d) if i in out_vmem...  36.2 us
    all_to_all x1, blocking collectives, exchange(): lax.all_to_all(plain(v), axis, split_axis=0, concat_axis=0, tiled=True)  36 us
    all_to_all x3, waiting for transfers between devices, exchange(): lax.all_to_all(plain(v), axis, split_axis=0, concat_axis=0, tiled=True)  28.6 us
    all_to_all x3, starting transfers between devices, exchange(): lax.all_to_all(plain(v), axis, split_axis=0, concat_axis=0, tiled=True)  18.5 us
    ppermute x3, waiting for transfers between devices, ring(): lax.ppermute(v, 'dp', [(i, (i + (-2 if i % 2 else 2)) % dps) for i in ran...  16 us
    ppermute x3, starting transfers between devices, ring(): lax.ppermute(v, 'dp', [(i, (i + (-2 if i % 2 else 2)) % dps) for i in ran...  8.09 us
    ppermute x4, starting transfers between devices, swap(): return lax.ppermute(v, 'dp', [(i, i ^ 1) for i in range(dps)])  3.74 us
    ppermute x1, starting transfers between devices, layer(): lax.ppermute(plain(ends), 'sp', [(i, i + 1) for i in range(ways - 1)])  3.3 us
  transfers between devices with their start and end apart: 11, of which 5 were waited for; matrix products, arithmetic and copies ran while one was open for 0% of the time, Pallas kernels for 16%

profile of v7, /device:TPU:1, one launch (start us, length us, event | category | flops | bytes accessed | tf_op | source)
XLA Modules:
  0.0 152.0 jit_solution(10793801493106696467)
XLA Ops:
  0.0 1.4 collective-permute-start.1
  1.4 2.6 %collective-permute-start.2 = (bf16[256,2048]{1,0:T(8,128)(2,1)}, bf16[256,2048]{1,0:T(8,128)(2,1)S(1)}, u32[]{:S(2)}, u32[]{:S(2)}) collective-permute-start(bf16[256,2048]{1,0:T(8,128)(2,1)} %w0.1), channel_id=1, source_target_pairs={{0,2},{1,7},{2,4},{3,1},{4,6},{5,3},{6,0},{7,5},{8,10},{9,15},{10,... | collective-permute-start | bytes 3145736 | tf_op jit(solution)/shard_map/ppermute | solution.py:427
  4.0 0.0 collective-permute-done.1.w1
  4.0 2.5 %collective-permute-start.3 = (bf16[256,2048]{1,0:T(8,128)(2,1)S(1)}, bf16[256,2048]{1,0:T(8,128)(2,1)}, u32[]{:S(2)}, u32[]{:S(2)}) collective-permute-start(bf16[256,2048]{1,0:T(8,128)(2,1)S(1)} %collective-permute-done.1.w1), channel_id=1, source_target_pairs={{0,2},{1,7},{2,4},{3,1},{4,6},{5,3},{6,0},{7,5},{8,10},{9,15},{10,... | collective-permute-start | bytes 3145736 | tf_op jit(solution)/shard_map/ppermute | solution.py:427
  6.5 9.6 %collective-permute-done.2.w2 = bf16[256,2048]{1,0:T(8,128)(2,1)S(1)} collective-permute-done((bf16[256,2048]{1,0:T(8,128)(2,1)}, bf16[256,2048]{1,0:T(8,128)(2,1)S(1)}, u32[]{:S(2)}, u32[]{:S(2)}) %collective-permute-start.2) | collective-permute-done | bytes 1048608 | tf_op jit(solution)/shard_map/ppermute | solution.py:427
  16.0 3.0 %collective-permute-start.6 = (bf16[256,2048]{1,0:T(8,128)(2,1)S(1)}, bf16[256,2048]{1,0:T(8,128)(2,1)}, u32[]{:S(2)}, u32[]{:S(2)}) collective-permute-start(bf16[256,2048]{1,0:T(8,128)(2,1)S(1)} %collective-permute-done.2.w2), channel_id=1, source_target_pairs={{0,2},{1,7},{2,4},{3,1},{4,6},{5,3},{6,0},{7,5},{8,10},{9,15},{10,... | collective-permute-start | bytes 3145736 | tf_op jit(solution)/shard_map/ppermute | solution.py:427
  19.0 4.6 %shard_map.217 = (bf16[16,160,128]{2,1,0:T(8,128)(2,1)}, f32[128,32]{1,0:T(8,128)}, f32[128,32]{1,0:T(8,128)}, bf16[8,4096]{1,0:T(8,128)(2,1)}) custom-call(bf16[32,128]{1,0:T(8,128)(2,1)} %bitcast.41, bf16[4,2048]{1,0:T(4,128)(2,1)} %cw.3, bf16[4,1024]{1,0:T(4,128)(2,1)} %cbw.3, f32[1,32]{1,0:T(1,128)} %bitcast.43, f32[1,32]{1,0:T(1,128)} %bitcast.44, ...), custom_call_target="tpu_custom_call" | custom-call | flops 1000000 | bytes 1000000 | tf_op jit(solution)/shard_map/pallas_call | solution.py:49
  23.6 7.8 %all-to-all-start = ((bf16[16,160,128]{2,1,0:T(8,128)(2,1)}), bf16[16,160,128]{2,1,0:T(8,128)(2,1)S(1)}, u32[]{:S(2)}, u32[]{:S(2)}) async-start(bf16[16,160,128]{2,1,0:T(8,128)(2,1)} %get-tuple-element.16), calls=%async_computation | async-start | bytes 1310720 | tf_op jit(solution)/shard_map/all_to_all | solution.py:412
  31.4 0.1 collective-permute-start.4
  31.5 0.0 collective-permute-done.3.w3
  31.5 0.5 collective-permute-start.5
  32.0 6.4 %collective-permute-done.6.w6 = bf16[256,2048]{1,0:T(8,128)(2,1)} collective-permute-done((bf16[256,2048]{1,0:T(8,128)(2,1)S(1)}, bf16[256,2048]{1,0:T(8,128)(2,1)}, u32[]{:S(2)}, u32[]{:S(2)}) %collective-permute-start.6) | collective-permute-done | bytes 1048608 | tf_op jit(solution)/shard_map/ppermute | solution.py:427
  38.4 1.8 %collective-permute-start.7 = (bf16[256,2048]{1,0:T(8,128)(2,1)}, bf16[256,2048]{1,0:T(8,128)(2,1)}, u32[]{:S(2)}, u32[]{:S(2)}) collective-permute-start(bf16[256,2048]{1,0:T(8,128)(2,1)} %collective-permute-done.6.w6), channel_id=1, source_target_pairs={{0,1},{1,0},{2,3},{3,2},{4,5},{5,4},{6,7},{7,6},{8,9},{9,8},{10,11... | collective-permute-start | bytes 3145736 | tf_op jit(solution)/shard_map/ppermute | solution.py:430
  40.2 3.3 %collective-permute-start = (bf16[8,4096]{1,0:T(8,128)(2,1)}, bf16[8,4096]{1,0:T(8,128)(2,1)S(1)}, u32[]{:S(2)}, u32[]{:S(2)}) collective-permute-start(bf16[8,4096]{1,0:T(8,128)(2,1)} %get-tuple-element.18), channel_id=1, source_target_pairs={{0,8},{8,16},{16,24},{24,32},{32,40},{40,48},{48,56},{56,64},{64,7... | collective-permute-start | bytes 196616 | tf_op jit(solution)/shard_map/ppermute | solution.py:450
  43.5 1.1 all-to-all-done.got
  44.6 1.2 shard_map.218
  45.8 6.4 %all-to-all-start.1 = ((bf16[16,128,128]{2,1,0:T(8,128)(2,1)}), bf16[16,128,128]{2,1,0:T(8,128)(2,1)S(1)}, u32[]{:S(2)}, u32[]{:S(2)}) async-start(bf16[16,128,128]{2,1,0:T(8,128)(2,1)} %shard_map.218), calls=%async_computation.1 | async-start | bytes 1048576 | tf_op jit(solution)/shard_map/all_to_all | solution.py:412
  52.2 2.4 %shard_map.221.disp_in = bf16[1024,256]{1,0:T(8,128)(2,1)} custom-call(s32[2,128]{1,0:T(2,128)} %bitcast.49, f32[2,128]{1,0:T(2,128)} %bitcast.51), custom_call_target="tpu_custom_call" | custom-call | flops 2000000000 | bytes 1000000 | tf_op jit(solution)/shard_map/pallas_call | solution.py:49
  54.5 0.0 collective-permute-done.halo
  54.5 4.0 %shard_map.219 = (f32[128,2048]{1,0:T(8,128)}, bf16[128,1024]{1,0:T(8,128)(2,1)}) custom-call(bf16[128,2048]{1,0:T(8,128)(2,1)} %bitcast.34, bf16[128,1024]{1,0:T(8,128)(2,1)} %bitcast.38, bf16[128,1024]{1,0:T(8,128)(2,1)} %bitcast.40, bf16[8,4096]{1,0:T(8,128)(2,1)S(1)} %collective-permute-done.halo, bf16[4,2048]{1,0:T(4,128)(2,1)} %cw.3, ...), custom_call_target="tpu_custom_call" | custom-call | flops 4000000000 | bytes 1000000 | tf_op jit(solution)/shard_map/pallas_call | solution.py:49
  58.6 4.4 %all-to-all-done.1 = bf16[16,128,128]{2,1,0:T(8,128)(2,1)S(1)} async-done(((bf16[16,128,128]{2,1,0:T(8,128)(2,1)}), bf16[16,128,128]{2,1,0:T(8,128)(2,1)S(1)}, u32[]{:S(2)}, u32[]{:S(2)}) %all-to-all-start.1) | async-done | bytes 524320 | tf_op jit(solution)/shard_map/all_to_all | solution.py:412
  63.0 0.0 collective-permute-done.4.w4
  63.0 4.3 %shard_map.220 = (f32[128,2048]{1,0:T(8,128)S(1)}, bf16[128,512]{1,0:T(8,128)(2,1)S(1)}) custom-call(bf16[8,256,128]{2,1,0:T(8,128)(2,1)S(1)} %bitcast.31, f32[128,32]{1,0:T(8,128)} %get-tuple-element.17.ec.ec_in, f32[128,2048]{1,0:T(8,128)} %get-tuple-element.20.a_in, bf16[128,1024]{1,0:T(8,128)(2,1)} %get-tuple-element.21.cm_in, ...), custom_call_target="tpu_custom_call" | custom-call | flops 2000000000 | bytes 1000000 | tf_op jit(solution)/shard_map/pallas_call | solution.py:49
  67.3 4.1 %shard_map.222 = (bf16[128,2048]{1,0:T(8,128)(2,1)}, bf16[128,2048]{1,0:T(8,128)(2,1)}, bf16[1024,1024]{1,0:T(8,128)(2,1)}) custom-call(f32[128,2048]{1,0:T(8,128)S(1)} %get-tuple-element.22.proj_in, bf16[128,512]{1,0:T(8,128)(2,1)S(1)} %get-tuple-element.23.rest, f32[1,2048]{1,0:T(1,128)} %bitcast.48, bf16[1024,256]{1,0:T(8,128)(2,1)} %shard_map.221.disp_in, ...), custom_call_target="tpu_custom_call" | custom-call | flops 2000000000 | bytes 1000000 | tf_op jit(solution)/shard_map/pallas_call | solution.py:49
  71.4 36.0 %all_to_all.20 = bf16[128,8,1024]{2,1,0:T(8,128)(2,1)S(1)} all-to-all(bf16[128,8,1024]{2,1,0:T(8,128)(2,1)} %bitcast.32), channel_id=1, replica_groups=mesh['sp'=16,'dp'=8] {'sp','dp'}, dimensions={0} | all-to-all | bytes 4194304 | tf_op jit(solution)/shard_map/all_to_all | solution.py:412
  107.3 5.5 %shard_map.223 = bf16[1024,1024]{1,0:T(8,128)(2,1)S(1)} custom-call(bf16[1024,1024]{1,0:T(8,128)(2,1)S(1)} %bitcast.30, bf16[2048,512]{1,0:T(8,128)(2,1)} %bitcast.45, bf16[2048,512]{1,0:T(8,128)(2,1)} %bitcast.46, bf16[512,2048]{1,0:T(8,128)(2,1)} %bitcast.47), custom_call_target="tpu_custom_call" | custom-call | flops 3000000000 | bytes 1000000 | tf_op jit(solution)/shard_map/pallas_call | solution.py:49
  112.8 1.3 copy-done
  114.2 4.4 %all-to-all-start.3 = ((bf16[128,8,1024]{2,1,0:T(8,128)(2,1)}), bf16[128,8,1024]{2,1,0:T(8,128)(2,1)S(1)}, u32[]{:S(2)}, u32[]{:S(2)}) async-start(bf16[128,8,1024]{2,1,0:T(8,128)(2,1)} %bitcast.29), calls=%async_computation.3 | async-start | bytes 4194304 | tf_op jit(solution)/shard_map/all_to_all | solution.py:412
  118.6 2.3 %shard_map.224.w_in = bf16[256,1024]{1,0:T(8,128)(2,1)} custom-call(s32[2,128]{1,0:T(2,128)} %bitcast.50, f32[2,128]{1,0:T(2,128)} %bitcast.52), custom_call_target="tpu_custom_call" | custom-call | flops 2000000000 | bytes 1000000 | tf_op jit(solution)/shard_map/pallas_call | solution.py:49
  120.8 5.3 %shard_map.225.base_in = f32[128,2048]{1,0:T(8,128)} custom-call(bf16[128,2048]{1,0:T(8,128)(2,1)} %get-tuple-element.25.ein, bf16[128,2048]{1,0:T(8,128)(2,1)} %get-tuple-element.26.mixed, bf16[2048,512]{1,0:T(8,128)(2,1)} %sg.1, bf16[2048,512]{1,0:T(8,128)(2,1)} %su.1, bf16[512,2048]{1,0:T(8,128)(2,1)} %sd.1), custom_call_target="tpu_custom_call" | custom-call | flops 4000000000 | bytes 1000000 | tf_op jit(solution)/shard_map/pallas_call | solution.py:49
  126.1 23.1 %all-to-all-done.3 = bf16[128,8,1024]{2,1,0:T(8,128)(2,1)S(1)} async-done(((bf16[128,8,1024]{2,1,0:T(8,128)(2,1)}), bf16[128,8,1024]{2,1,0:T(8,128)(2,1)S(1)}, u32[]{:S(2)}, u32[]{:S(2)}) %all-to-all-start.3) | async-done | bytes 2097184 | tf_op jit(solution)/shard_map/all_to_all | solution.py:412
  149.2 2.7 %shard_map.226 = bf16[128,2048]{1,0:T(8,128)(2,1)} custom-call(bf16[1024,1024]{1,0:T(8,128)(2,1)S(1)} %bitcast.28, bf16[256,1024]{1,0:T(8,128)(2,1)} %shard_map.224.w_in, f32[128,2048]{1,0:T(8,128)} %shard_map.225.base_in), custom_call_target="tpu_custom_call" | custom-call | flops 1000000 | bytes 1000000 | tf_op jit(solution)/shard_map/pallas_call | solution.py:49
  (3 shorter events, 0.0 us)
Async XLA Ops:
  0.0 4.0 %collective-permute-start.1 = (bf16[256,2048]{1,0:T(8,128)(2,1)}, bf16[256,2048]{1,0:T(8,128)(2,1)S(1)}, u32[]{:S(2)}, u32[]{:S(2)}) collective-permute-start(bf16[256,2048]{1,0:T(8,128)(2,1)} %w0.1), channel_id=1, source_target_pairs={{0,1},{1,0},{2,3},{3,2},{4,5},{5,4},{6,7},{7,6},{8,9},{9,8},{10,11... | collective-permute-start | bytes 3145736 | tf_op jit(solution)/shard_map/ppermute | solution.py:430
  1.4 14.7 %collective-permute-start.2 = (bf16[256,2048]{1,0:T(8,128)(2,1)}, bf16[256,2048]{1,0:T(8,128)(2,1)S(1)}, u32[]{:S(2)}, u32[]{:S(2)}) collective-permute-start(bf16[256,2048]{1,0:T(8,128)(2,1)} %w0.1), channel_id=1, source_target_pairs={{0,2},{1,7},{2,4},{3,1},{4,6},{5,3},{6,0},{7,5},{8,10},{9,15},{10,... | collective-permute-start | bytes 3145736 | tf_op jit(solution)/shard_map/ppermute | solution.py:427
  4.0 27.5 %collective-permute-start.3 = (bf16[256,2048]{1,0:T(8,128)(2,1)S(1)}, bf16[256,2048]{1,0:T(8,128)(2,1)}, u32[]{:S(2)}, u32[]{:S(2)}) collective-permute-start(bf16[256,2048]{1,0:T(8,128)(2,1)S(1)} %collective-permute-done.1.w1), channel_id=1, source_target_pairs={{0,2},{1,7},{2,4},{3,1},{4,6},{5,3},{6,0},{7,5},{8,10},{9,15},{10,... | collective-permute-start | bytes 3145736 | tf_op jit(solution)/shard_map/ppermute | solution.py:427
  16.0 22.4 %collective-permute-start.6 = (bf16[256,2048]{1,0:T(8,128)(2,1)S(1)}, bf16[256,2048]{1,0:T(8,128)(2,1)}, u32[]{:S(2)}, u32[]{:S(2)}) collective-permute-start(bf16[256,2048]{1,0:T(8,128)(2,1)S(1)} %collective-permute-done.2.w2), channel_id=1, source_target_pairs={{0,2},{1,7},{2,4},{3,1},{4,6},{5,3},{6,0},{7,5},{8,10},{9,15},{10,... | collective-permute-start | bytes 3145736 | tf_op jit(solution)/shard_map/ppermute | solution.py:427
  23.6 21.0 %all-to-all-start = ((bf16[16,160,128]{2,1,0:T(8,128)(2,1)}), bf16[16,160,128]{2,1,0:T(8,128)(2,1)S(1)}, u32[]{:S(2)}, u32[]{:S(2)}) async-start(bf16[16,160,128]{2,1,0:T(8,128)(2,1)} %get-tuple-element.16), calls=%async_computation | async-start | bytes 1310720 | tf_op jit(solution)/shard_map/all_to_all | solution.py:412
  31.4 31.6 %collective-permute-start.4 = (bf16[256,2048]{1,0:T(8,128)(2,1)S(1)}, bf16[256,2048]{1,0:T(8,128)(2,1)}, u32[]{:S(2)}, u32[]{:S(2)}) collective-permute-start(bf16[256,2048]{1,0:T(8,128)(2,1)S(1)} %collective-permute-done.2.w2), channel_id=1, source_target_pairs={{0,1},{1,0},{2,3},{3,2},{4,5},{5,4},{6,7},{7,6},{8,9},{9,8},{10,11... | collective-permute-start | bytes 3145736 | tf_op jit(solution)/shard_map/ppermute | solution.py:430
  31.5 31.5 %collective-permute-start.5 = (bf16[256,2048]{1,0:T(8,128)(2,1)}, bf16[256,2048]{1,0:T(8,128)(2,1)}, u32[]{:S(2)}, u32[]{:S(2)}) collective-permute-start(bf16[256,2048]{1,0:T(8,128)(2,1)} %collective-permute-done.3.w3), channel_id=1, source_target_pairs={{0,1},{1,0},{2,3},{3,2},{4,5},{5,4},{6,7},{7,6},{8,9},{9,8},{10,11... | collective-permute-start | bytes 3145736 | tf_op jit(solution)/shard_map/ppermute | solution.py:430
  38.4 28.9 %collective-permute-start.7 = (bf16[256,2048]{1,0:T(8,128)(2,1)}, bf16[256,2048]{1,0:T(8,128)(2,1)}, u32[]{:S(2)}, u32[]{:S(2)}) collective-permute-start(bf16[256,2048]{1,0:T(8,128)(2,1)} %collective-permute-done.6.w6), channel_id=1, source_target_pairs={{0,1},{1,0},{2,3},{3,2},{4,5},{5,4},{6,7},{7,6},{8,9},{9,8},{10,11... | collective-permute-start | bytes 3145736 | tf_op jit(solution)/shard_map/ppermute | solution.py:430
  40.2 14.3 %collective-permute-start = (bf16[8,4096]{1,0:T(8,128)(2,1)}, bf16[8,4096]{1,0:T(8,128)(2,1)S(1)}, u32[]{:S(2)}, u32[]{:S(2)}) collective-permute-start(bf16[8,4096]{1,0:T(8,128)(2,1)} %get-tuple-element.18), channel_id=1, source_target_pairs={{0,8},{8,16},{16,24},{24,32},{32,40},{40,48},{48,56},{56,64},{64,7... | collective-permute-start | bytes 196616 | tf_op jit(solution)/shard_map/ppermute | solution.py:450
  45.8 17.2 %all-to-all-start.1 = ((bf16[16,128,128]{2,1,0:T(8,128)(2,1)}), bf16[16,128,128]{2,1,0:T(8,128)(2,1)S(1)}, u32[]{:S(2)}, u32[]{:S(2)}) async-start(bf16[16,128,128]{2,1,0:T(8,128)(2,1)} %shard_map.218), calls=%async_computation.1 | async-start | bytes 1048576 | tf_op jit(solution)/shard_map/all_to_all | solution.py:412
  112.8 1.3 copy-start
  114.2 35.0 %all-to-all-start.3 = ((bf16[128,8,1024]{2,1,0:T(8,128)(2,1)}), bf16[128,8,1024]{2,1,0:T(8,128)(2,1)S(1)}, u32[]{:S(2)}, u32[]{:S(2)}) async-start(bf16[128,8,1024]{2,1,0:T(8,128)(2,1)} %bitcast.29), calls=%async_computation.3 | async-start | bytes 4194304 | tf_op jit(solution)/shard_map/all_to_all | solution.py:412

commit v8 on v7

--- a/solution.py
+++ b/solution.py
@@ -276,14 +276,14 @@
 
 
 def norm_kernel(
-    pref, ec_in, a_in, cm_in, gate_in, gain_in, resid_in, w0, w1, w2, w3, w4, w5, proj, rest,
+    pref, ec_in, a_in, cm_in, gate_in, gain_in, resid_in, w0, w1, w2, w3, w4, w5, w6, proj, rest,
     norm, wide, picked, ec, a, cm, gate, gain, resid, sems
 ):
     pairs = [(ec_in, ec), (cm_in, cm), (gain_in, gain)]
     for q in range(4):
         pairs.append((a_in.at[:, part(q, 512)], a.at[:, part(q, 512)]))
         pairs.append((gate_in.at[:, part(q, 512)], gate.at[:, part(q, 512)]))
-    for k, w in enumerate((w0, w1, w2, w3, w4, w5)):
+    for k, w in enumerate((w0, w1, w2, w3, w4, w5, w6)):
         pairs.append((w, wide.at[part(k, GW), :]))
     pairs.append((resid_in, resid))
     loads = begin(pairs, sems)
@@ -307,10 +307,9 @@
     at = (me + 6 + 4 * odd) & 7
     other = ((me ^ 1) + 6 - 4 * odd + 4) & 7
     place = [me, me ^ 1, at, at ^ 1, other, other ^ 1, me ^ 4, me ^ 5]
-    for k in range(6):
+    for k in range(7):
         picked[:, k * GW : (k + 1) * GW] = norm[place[k]]
-    for k in range(2):
-        rest[:, k * GW : (k + 1) * GW] = norm[place[6 + k]]
+    rest[...] = norm[place[7]]
     for load in loads[11:]:
         load.wait()
     proj[...] = resid[...].astype(F32) + jnp.dot(
@@ -319,15 +318,13 @@
 
 
 def mix_kernel(
-    proj_in, rest, fgain_in, disp_in, w6, w7, mixed_out, ein_out, send_out,
+    proj_in, rest, fgain_in, disp_in, w7, mixed_out, ein_out, send_out,
     wide, fgain, disp, mixed_buf, ein_buf, send, sems, out_sems
 ):
-    pairs = [(w6, wide.at[part(0, GW), :]), (w7, wide.at[part(1, GW), :])]
-    loads = begin(pairs + [(fgain_in, fgain), (disp_in, disp)], sems)
-    for load in loads[:2]:
-        load.wait()
+    loads = begin([(w7, wide), (fgain_in, fgain), (disp_in, disp)], sems)
+    loads[0].wait()
     proj = proj_in[...] + jnp.dot(rest[...], wide[...], preferred_element_type=F32)
-    loads[2].wait()
+    loads[1].wait()
     mixed = proj.astype(BF)
     mixed_buf[...] = mixed
     stores = [pltpu.make_async_copy(mixed_buf, mixed_out, out_sems.at[0])]
@@ -338,7 +335,7 @@
     stores.append(pltpu.make_async_copy(ein_buf, ein_out, out_sems.at[1]))
     stores[1].start()
     stack = jnp.concatenate([ein[:, :HALF], ein[:, HALF:]], axis=0)
-    loads[3].wait()
+    loads[2].wait()
     for q in range(4):
         rows = part(q, 256)
         send[rows, :] = jnp.dot(disp[rows, :], stack, preferred_element_type=F32).astype(BF)
@@ -474,26 +471,26 @@
     pref = exchange(carried, "sp")
     proj, rest = call(
         norm_kernel,
-        [((TOK, D), F32), ((TOK, 2 * GW), BF)],
+        [((TOK, D), F32), ((TOK, GW), BF)],
         (
             pref.reshape(GROUPS, GW, STATE), ec, a, cm, gate_input[0], norm_gain[None],
-            residual[0], *pieces[:6],
+            residual[0], *pieces[:7],
         ),
         scratch=[
             pltpu.VMEM((GROUPS, TOK, GW), BF),
-            pltpu.VMEM((6 * GW, D), BF),
-            pltpu.VMEM((TOK, 6 * GW), BF),
+            pltpu.VMEM((7 * GW, D), BF),
+            pltpu.VMEM((TOK, 7 * GW), BF),
             pltpu.VMEM((TOK, HEADS), F32),
             pltpu.VMEM((TOK, D), F32),
             pltpu.VMEM((TOK, 1024), BF),
             pltpu.VMEM((TOK, D), BF),
             pltpu.VMEM((1, D), F32),
             pltpu.VMEM((TOK, D), BF),
-            pltpu.SemaphoreType.DMA((18,)),
+            pltpu.SemaphoreType.DMA((19,)),
         ],
         vmem=(0,),
-        raw=range(1, 13),
-        free=range(8, 13),
+        raw=range(1, 14),
+        free=range(8, 14),
         out_vmem=(0, 1),
         limit=32,
         flops=2 * 10**9,
@@ -501,20 +498,20 @@
     mixed, ein, send = call(
         mix_kernel,
         [((TOK, D), BF), ((TOK, D), BF), ((ROWS, HALF), BF)],
-        (proj, rest, ffn_gain[None], disp, *pieces[6:]),
+        (proj, rest, ffn_gain[None], disp, *pieces[7:]),
         scratch=[
-            pltpu.VMEM((2 * GW, D), BF),
+            pltpu.VMEM((GW, D), BF),
             pltpu.VMEM((1, D), F32),
             pltpu.VMEM((ROWS, 2 * TOK), BF),
             pltpu.VMEM((TOK, D), BF),
             pltpu.VMEM((TOK, D), BF),
             pltpu.VMEM((ROWS, HALF), BF),
-            pltpu.SemaphoreType.DMA((4,)),
+            pltpu.SemaphoreType.DMA((3,)),
             pltpu.SemaphoreType.DMA((6,)),
         ],
         vmem=(0, 1),
-        raw=range(2, 6),
-        free=range(4, 6),
+        raw=range(2, 5),
+        free=(4,),
         raw_out=(0, 1, 2),
         limit=28,
         flops=2 * 10**9,

time: 153 us -> 152 us (level)
  no operation moved by 1% of the time
where the time goes in v8:
time: 152 us
  waiting for transfers between devices  44.6 us (29%)
  Pallas kernels  36 us (24%)
  blocking collectives  36 us (24%)
  starting transfers between devices  33.7 us (22%)
    all_to_all x1, blocking collectives, exchange(): lax.all_to_all(plain(v), axis, split_axis=0, concat_axis=0, tiled=True)  36 us
    pallas_call x10, Pallas kernels, call(): pl.pallas_call(kernel, out_shape=tuple((pltpu.VMEM(s, d) if i in out_vmem...  36 us
    all_to_all x3, waiting for transfers between devices, exchange(): lax.all_to_all(plain(v), axis, split_axis=0, concat_axis=0, tiled=True)  28.6 us
    all_to_all x3, starting transfers between devices, exchange(): lax.all_to_all(plain(v), axis, split_axis=0, concat_axis=0, tiled=True)  18.5 us
    ppermute x3, waiting for transfers between devices, ring(): lax.ppermute(v, 'dp', [(i, (i + (-2 if i % 2 else 2)) % dps) for i in ran...  16 us
    ppermute x3, starting transfers between devices, ring(): lax.ppermute(v, 'dp', [(i, (i + (-2 if i % 2 else 2)) % dps) for i in ran...  8.09 us
    ppermute x4, starting transfers between devices, swap(): return lax.ppermute(v, 'dp', [(i, i ^ 1) for i in range(dps)])  3.74 us
    ppermute x1, starting transfers between devices, layer(): lax.ppermute(plain(ends), 'sp', [(i, i + 1) for i in range(ways - 1)])  3.3 us
  transfers between devices with their start and end apart: 11, of which 5 were waited for; matrix products, arithmetic and copies ran while one was open for 0% of the time, Pallas kernels for 16%

profile of v8, /device:TPU:1, one launch (start us, length us, event | category | flops | bytes accessed | tf_op | source)
XLA Modules:
  0.0 151.8 jit_solution(11431748754931264903)
XLA Ops:
  0.0 1.4 collective-permute-start.1
  1.4 2.6 %collective-permute-start.2 = (bf16[256,2048]{1,0:T(8,128)(2,1)}, bf16[256,2048]{1,0:T(8,128)(2,1)S(1)}, u32[]{:S(2)}, u32[]{:S(2)}) collective-permute-start(bf16[256,2048]{1,0:T(8,128)(2,1)} %w0.1), channel_id=1, source_target_pairs={{0,2},{1,7},{2,4},{3,1},{4,6},{5,3},{6,0},{7,5},{8,10},{9,15},{10,... | collective-permute-start | bytes 3145736 | tf_op jit(solution)/shard_map/ppermute | solution.py:424
  4.0 0.0 collective-permute-done.1.w1
  4.0 2.5 %collective-permute-start.3 = (bf16[256,2048]{1,0:T(8,128)(2,1)S(1)}, bf16[256,2048]{1,0:T(8,128)(2,1)}, u32[]{:S(2)}, u32[]{:S(2)}) collective-permute-start(bf16[256,2048]{1,0:T(8,128)(2,1)S(1)} %collective-permute-done.1.w1), channel_id=1, source_target_pairs={{0,2},{1,7},{2,4},{3,1},{4,6},{5,3},{6,0},{7,5},{8,10},{9,15},{10,... | collective-permute-start | bytes 3145736 | tf_op jit(solution)/shard_map/ppermute | solution.py:424
  6.5 9.6 %collective-permute-done.2.w2 = bf16[256,2048]{1,0:T(8,128)(2,1)S(1)} collective-permute-done((bf16[256,2048]{1,0:T(8,128)(2,1)}, bf16[256,2048]{1,0:T(8,128)(2,1)S(1)}, u32[]{:S(2)}, u32[]{:S(2)}) %collective-permute-start.2) | collective-permute-done | bytes 1048608 | tf_op jit(solution)/shard_map/ppermute | solution.py:424
  16.0 3.0 %collective-permute-start.6 = (bf16[256,2048]{1,0:T(8,128)(2,1)S(1)}, bf16[256,2048]{1,0:T(8,128)(2,1)}, u32[]{:S(2)}, u32[]{:S(2)}) collective-permute-start(bf16[256,2048]{1,0:T(8,128)(2,1)S(1)} %collective-permute-done.2.w2), channel_id=1, source_target_pairs={{0,2},{1,7},{2,4},{3,1},{4,6},{5,3},{6,0},{7,5},{8,10},{9,15},{10,... | collective-permute-start | bytes 3145736 | tf_op jit(solution)/shard_map/ppermute | solution.py:424
  19.0 4.6 %shard_map.217 = (bf16[16,160,128]{2,1,0:T(8,128)(2,1)}, f32[128,32]{1,0:T(8,128)}, f32[128,32]{1,0:T(8,128)}, bf16[8,4096]{1,0:T(8,128)(2,1)}) custom-call(bf16[32,128]{1,0:T(8,128)(2,1)} %bitcast.41, bf16[4,2048]{1,0:T(4,128)(2,1)} %cw.3, bf16[4,1024]{1,0:T(4,128)(2,1)} %cbw.3, f32[1,32]{1,0:T(1,128)} %bitcast.43, f32[1,32]{1,0:T(1,128)} %bitcast.44, ...), custom_call_target="tpu_custom_call" | custom-call | flops 1000000 | bytes 1000000 | tf_op jit(solution)/shard_map/pallas_call | solution.py:49
  23.6 7.8 %all-to-all-start = ((bf16[16,160,128]{2,1,0:T(8,128)(2,1)}), bf16[16,160,128]{2,1,0:T(8,128)(2,1)S(1)}, u32[]{:S(2)}, u32[]{:S(2)}) async-start(bf16[16,160,128]{2,1,0:T(8,128)(2,1)} %get-tuple-element.16), calls=%async_computation | async-start | bytes 1310720 | tf_op jit(solution)/shard_map/all_to_all | solution.py:409
  31.4 0.1 collective-permute-start.4
  31.5 0.0 collective-permute-done.3.w3
  31.5 0.5 collective-permute-start.5
  32.0 6.4 %collective-permute-done.6.w6 = bf16[256,2048]{1,0:T(8,128)(2,1)} collective-permute-done((bf16[256,2048]{1,0:T(8,128)(2,1)S(1)}, bf16[256,2048]{1,0:T(8,128)(2,1)}, u32[]{:S(2)}, u32[]{:S(2)}) %collective-permute-start.6) | collective-permute-done | bytes 1048608 | tf_op jit(solution)/shard_map/ppermute | solution.py:424
  38.4 1.8 %collective-permute-start.7 = (bf16[256,2048]{1,0:T(8,128)(2,1)}, bf16[256,2048]{1,0:T(8,128)(2,1)}, u32[]{:S(2)}, u32[]{:S(2)}) collective-permute-start(bf16[256,2048]{1,0:T(8,128)(2,1)} %collective-permute-done.6.w6), channel_id=1, source_target_pairs={{0,1},{1,0},{2,3},{3,2},{4,5},{5,4},{6,7},{7,6},{8,9},{9,8},{10,11... | collective-permute-start | bytes 3145736 | tf_op jit(solution)/shard_map/ppermute | solution.py:427
  40.2 3.3 %collective-permute-start = (bf16[8,4096]{1,0:T(8,128)(2,1)}, bf16[8,4096]{1,0:T(8,128)(2,1)S(1)}, u32[]{:S(2)}, u32[]{:S(2)}) collective-permute-start(bf16[8,4096]{1,0:T(8,128)(2,1)} %get-tuple-element.18), channel_id=1, source_target_pairs={{0,8},{8,16},{16,24},{24,32},{32,40},{40,48},{48,56},{56,64},{64,7... | collective-permute-start | bytes 196616 | tf_op jit(solution)/shard_map/ppermute | solution.py:447
  43.5 1.1 all-to-all-done.got
  44.6 1.2 shard_map.218
  45.8 6.4 %all-to-all-start.1 = ((bf16[16,128,128]{2,1,0:T(8,128)(2,1)}), bf16[16,128,128]{2,1,0:T(8,128)(2,1)S(1)}, u32[]{:S(2)}, u32[]{:S(2)}) async-start(bf16[16,128,128]{2,1,0:T(8,128)(2,1)} %shard_map.218), calls=%async_computation.1 | async-start | bytes 1048576 | tf_op jit(solution)/shard_map/all_to_all | solution.py:409
  52.2 2.4 %shard_map.221.disp_in = bf16[1024,256]{1,0:T(8,128)(2,1)} custom-call(s32[2,128]{1,0:T(2,128)} %bitcast.49, f32[2,128]{1,0:T(2,128)} %bitcast.51), custom_call_target="tpu_custom_call" | custom-call | flops 2000000000 | bytes 1000000 | tf_op jit(solution)/shard_map/pallas_call | solution.py:49
  54.5 0.0 collective-permute-done.halo
  54.5 4.0 %shard_map.219 = (f32[128,2048]{1,0:T(8,128)}, bf16[128,1024]{1,0:T(8,128)(2,1)}) custom-call(bf16[128,2048]{1,0:T(8,128)(2,1)} %bitcast.36, bf16[128,1024]{1,0:T(8,128)(2,1)} %bitcast.38, bf16[128,1024]{1,0:T(8,128)(2,1)} %bitcast.40, bf16[8,4096]{1,0:T(8,128)(2,1)S(1)} %collective-permute-done.halo, bf16[4,2048]{1,0:T(4,128)(2,1)} %cw.3, ...), custom_call_target="tpu_custom_call" | custom-call | flops 4000000000 | bytes 1000000 | tf_op jit(solution)/shard_map/pallas_call | solution.py:49
  58.6 4.4 %all-to-all-done.1 = bf16[16,128,128]{2,1,0:T(8,128)(2,1)S(1)} async-done(((bf16[16,128,128]{2,1,0:T(8,128)(2,1)}), bf16[16,128,128]{2,1,0:T(8,128)(2,1)S(1)}, u32[]{:S(2)}, u32[]{:S(2)}) %all-to-all-start.1) | async-done | bytes 524320 | tf_op jit(solution)/shard_map/all_to_all | solution.py:409
  63.0 4.5 %shard_map.220 = (f32[128,2048]{1,0:T(8,128)S(1)}, bf16[128,256]{1,0:T(8,128)(2,1)S(1)}) custom-call(bf16[8,256,128]{2,1,0:T(8,128)(2,1)S(1)} %bitcast.29, f32[128,32]{1,0:T(8,128)} %get-tuple-element.17.ec.ec_in, f32[128,2048]{1,0:T(8,128)} %get-tuple-element.20.a_in, bf16[128,1024]{1,0:T(8,128)(2,1)} %get-tuple-element.21.cm_in, ...), custom_call_target="tpu_custom_call" | custom-call | flops 2000000000 | bytes 1000000 | tf_op jit(solution)/shard_map/pallas_call | solution.py:49
  67.5 0.0 collective-permute-done.7.w7
  67.5 3.6 %shard_map.222 = (bf16[128,2048]{1,0:T(8,128)(2,1)}, bf16[128,2048]{1,0:T(8,128)(2,1)}, bf16[1024,1024]{1,0:T(8,128)(2,1)}) custom-call(f32[128,2048]{1,0:T(8,128)S(1)} %get-tuple-element.22.proj_in, bf16[128,256]{1,0:T(8,128)(2,1)S(1)} %get-tuple-element.23.rest, f32[1,2048]{1,0:T(1,128)} %bitcast.48, bf16[1024,256]{1,0:T(8,128)(2,1)} %shard_map.221.disp_in, ...), custom_call_target="tpu_custom_call" | custom-call | flops 2000000000 | bytes 1000000 | tf_op jit(solution)/shard_map/pallas_call | solution.py:49
  71.2 36.0 %all_to_all.20 = bf16[128,8,1024]{2,1,0:T(8,128)(2,1)S(1)} all-to-all(bf16[128,8,1024]{2,1,0:T(8,128)(2,1)} %bitcast.32), channel_id=1, replica_groups=mesh['sp'=16,'dp'=8] {'sp','dp'}, dimensions={0} | all-to-all | bytes 4194304 | tf_op jit(solution)/shard_map/all_to_all | solution.py:409
  107.1 5.5 %shard_map.223 = bf16[1024,1024]{1,0:T(8,128)(2,1)S(1)} custom-call(bf16[1024,1024]{1,0:T(8,128)(2,1)S(1)} %bitcast.31, bf16[2048,512]{1,0:T(8,128)(2,1)} %bitcast.45, bf16[2048,512]{1,0:T(8,128)(2,1)} %bitcast.46, bf16[512,2048]{1,0:T(8,128)(2,1)} %bitcast.47), custom_call_target="tpu_custom_call" | custom-call | flops 3000000000 | bytes 1000000 | tf_op jit(solution)/shard_map/pallas_call | solution.py:49
  112.6 1.3 copy-done
  113.9 4.4 %all-to-all-start.3 = ((bf16[128,8,1024]{2,1,0:T(8,128)(2,1)}), bf16[128,8,1024]{2,1,0:T(8,128)(2,1)S(1)}, u32[]{:S(2)}, u32[]{:S(2)}) async-start(bf16[128,8,1024]{2,1,0:T(8,128)(2,1)} %bitcast.30), calls=%async_computation.3 | async-start | bytes 4194304 | tf_op jit(solution)/shard_map/all_to_all | solution.py:409
  118.3 2.3 %shard_map.224.w_in = bf16[256,1024]{1,0:T(8,128)(2,1)} custom-call(s32[2,128]{1,0:T(2,128)} %bitcast.50, f32[2,128]{1,0:T(2,128)} %bitcast.52), custom_call_target="tpu_custom_call" | custom-call | flops 2000000000 | bytes 1000000 | tf_op jit(solution)/shard_map/pallas_call | solution.py:49
  120.6 5.3 %shard_map.225.base_in = f32[128,2048]{1,0:T(8,128)} custom-call(bf16[128,2048]{1,0:T(8,128)(2,1)} %get-tuple-element.25.ein, bf16[128,2048]{1,0:T(8,128)(2,1)} %get-tuple-element.26.mixed, bf16[2048,512]{1,0:T(8,128)(2,1)} %sg.1, bf16[2048,512]{1,0:T(8,128)(2,1)} %su.1, bf16[512,2048]{1,0:T(8,128)(2,1)} %sd.1), custom_call_target="tpu_custom_call" | custom-call | flops 4000000000 | bytes 1000000 | tf_op jit(solution)/shard_map/pallas_call | solution.py:49
  125.9 23.1 %all-to-all-done.3 = bf16[128,8,1024]{2,1,0:T(8,128)(2,1)S(1)} async-done(((bf16[128,8,1024]{2,1,0:T(8,128)(2,1)}), bf16[128,8,1024]{2,1,0:T(8,128)(2,1)S(1)}, u32[]{:S(2)}, u32[]{:S(2)}) %all-to-all-start.3) | async-done | bytes 2097184 | tf_op jit(solution)/shard_map/all_to_all | solution.py:409
  148.9 2.7 %shard_map.226 = bf16[128,2048]{1,0:T(8,128)(2,1)} custom-call(bf16[1024,1024]{1,0:T(8,128)(2,1)S(1)} %bitcast.28, bf16[256,1024]{1,0:T(8,128)(2,1)} %shard_map.224.w_in, f32[128,2048]{1,0:T(8,128)} %shard_map.225.base_in), custom_call_target="tpu_custom_call" | custom-call | flops 1000000 | bytes 1000000 | tf_op jit(solution)/shard_map/pallas_call | solution.py:49
  (3 shorter events, 0.0 us)
Async XLA Ops:
  0.0 4.0 %collective-permute-start.1 = (bf16[256,2048]{1,0:T(8,128)(2,1)}, bf16[256,2048]{1,0:T(8,128)(2,1)S(1)}, u32[]{:S(2)}, u32[]{:S(2)}) collective-permute-start(bf16[256,2048]{1,0:T(8,128)(2,1)} %w0.1), channel_id=1, source_target_pairs={{0,1},{1,0},{2,3},{3,2},{4,5},{5,4},{6,7},{7,6},{8,9},{9,8},{10,11... | collective-permute-start | bytes 3145736 | tf_op jit(solution)/shard_map/ppermute | solution.py:427
  1.4 14.7 %collective-permute-start.2 = (bf16[256,2048]{1,0:T(8,128)(2,1)}, bf16[256,2048]{1,0:T(8,128)(2,1)S(1)}, u32[]{:S(2)}, u32[]{:S(2)}) collective-permute-start(bf16[256,2048]{1,0:T(8,128)(2,1)} %w0.1), channel_id=1, source_target_pairs={{0,2},{1,7},{2,4},{3,1},{4,6},{5,3},{6,0},{7,5},{8,10},{9,15},{10,... | collective-permute-start | bytes 3145736 | tf_op jit(solution)/shard_map/ppermute | solution.py:424
  4.0 27.5 %collective-permute-start.3 = (bf16[256,2048]{1,0:T(8,128)(2,1)S(1)}, bf16[256,2048]{1,0:T(8,128)(2,1)}, u32[]{:S(2)}, u32[]{:S(2)}) collective-permute-start(bf16[256,2048]{1,0:T(8,128)(2,1)S(1)} %collective-permute-done.1.w1), channel_id=1, source_target_pairs={{0,2},{1,7},{2,4},{3,1},{4,6},{5,3},{6,0},{7,5},{8,10},{9,15},{10,... | collective-permute-start | bytes 3145736 | tf_op jit(solution)/shard_map/ppermute | solution.py:424
  16.0 22.4 %collective-permute-start.6 = (bf16[256,2048]{1,0:T(8,128)(2,1)S(1)}, bf16[256,2048]{1,0:T(8,128)(2,1)}, u32[]{:S(2)}, u32[]{:S(2)}) collective-permute-start(bf16[256,2048]{1,0:T(8,128)(2,1)S(1)} %collective-permute-done.2.w2), channel_id=1, source_target_pairs={{0,2},{1,7},{2,4},{3,1},{4,6},{5,3},{6,0},{7,5},{8,10},{9,15},{10,... | collective-permute-start | bytes 3145736 | tf_op jit(solution)/shard_map/ppermute | solution.py:424
  23.6 21.0 %all-to-all-start = ((bf16[16,160,128]{2,1,0:T(8,128)(2,1)}), bf16[16,160,128]{2,1,0:T(8,128)(2,1)S(1)}, u32[]{:S(2)}, u32[]{:S(2)}) async-start(bf16[16,160,128]{2,1,0:T(8,128)(2,1)} %get-tuple-element.16), calls=%async_computation | async-start | bytes 1310720 | tf_op jit(solution)/shard_map/all_to_all | solution.py:409
  31.4 31.6 %collective-permute-start.4 = (bf16[256,2048]{1,0:T(8,128)(2,1)S(1)}, bf16[256,2048]{1,0:T(8,128)(2,1)}, u32[]{:S(2)}, u32[]{:S(2)}) collective-permute-start(bf16[256,2048]{1,0:T(8,128)(2,1)S(1)} %collective-permute-done.2.w2), channel_id=1, source_target_pairs={{0,1},{1,0},{2,3},{3,2},{4,5},{5,4},{6,7},{7,6},{8,9},{9,8},{10,11... | collective-permute-start | bytes 3145736 | tf_op jit(solution)/shard_map/ppermute | solution.py:427
  31.5 31.5 %collective-permute-start.5 = (bf16[256,2048]{1,0:T(8,128)(2,1)}, bf16[256,2048]{1,0:T(8,128)(2,1)}, u32[]{:S(2)}, u32[]{:S(2)}) collective-permute-start(bf16[256,2048]{1,0:T(8,128)(2,1)} %collective-permute-done.3.w3), channel_id=1, source_target_pairs={{0,1},{1,0},{2,3},{3,2},{4,5},{5,4},{6,7},{7,6},{8,9},{9,8},{10,11... | collective-permute-start | bytes 3145736 | tf_op jit(solution)/shard_map/ppermute | solution.py:427
  38.4 29.1 %collective-permute-start.7 = (bf16[256,2048]{1,0:T(8,128)(2,1)}, bf16[256,2048]{1,0:T(8,128)(2,1)}, u32[]{:S(2)}, u32[]{:S(2)}) collective-permute-start(bf16[256,2048]{1,0:T(8,128)(2,1)} %collective-permute-done.6.w6), channel_id=1, source_target_pairs={{0,1},{1,0},{2,3},{3,2},{4,5},{5,4},{6,7},{7,6},{8,9},{9,8},{10,11... | collective-permute-start | bytes 3145736 | tf_op jit(solution)/shard_map/ppermute | solution.py:427
  40.2 14.3 %collective-permute-start = (bf16[8,4096]{1,0:T(8,128)(2,1)}, bf16[8,4096]{1,0:T(8,128)(2,1)S(1)}, u32[]{:S(2)}, u32[]{:S(2)}) collective-permute-start(bf16[8,4096]{1,0:T(8,128)(2,1)} %get-tuple-element.18), channel_id=1, source_target_pairs={{0,8},{8,16},{16,24},{24,32},{32,40},{40,48},{48,56},{56,64},{64,7... | collective-permute-start | bytes 196616 | tf_op jit(solution)/shard_map/ppermute | solution.py:447
  45.8 17.2 %all-to-all-start.1 = ((bf16[16,128,128]{2,1,0:T(8,128)(2,1)}), bf16[16,128,128]{2,1,0:T(8,128)(2,1)S(1)}, u32[]{:S(2)}, u32[]{:S(2)}) async-start(bf16[16,128,128]{2,1,0:T(8,128)(2,1)} %shard_map.218), calls=%async_computation.1 | async-start | bytes 1048576 | tf_op jit(solution)/shard_map/all_to_all | solution.py:409
  112.6 1.3 copy-start
  113.9 35.0 %all-to-all-start.3 = ((bf16[128,8,1024]{2,1,0:T(8,128)(2,1)}), bf16[128,8,1024]{2,1,0:T(8,128)(2,1)S(1)}, u32[]{:S(2)}, u32[]{:S(2)}) async-start(bf16[128,8,1024]{2,1,0:T(8,128)(2,1)} %bitcast.30), calls=%async_computation.3 | async-start | bytes 4194304 | tf_op jit(solution)/shard_map/all_to_all | solution.py:409

commit v9 on v8

--- a/solution.py
+++ b/solution.py
@@ -105,12 +105,15 @@
 
 
 def states_kernel(
-    step_in, cw, cbw, bias, dlog, x, b, c, st, ec, grow_out, ends_out, padx, padb, sem
+    step_from, bias_in, dlog_in, x_in, b_in, cw_in, cbw_in, c_in, st, ec, grow_out, ends_out,
+    padx, padb, step_in, bias, dlog, x, b, cw, cbw, sems
 ):
-    load = pltpu.make_async_copy(
-        c.at[pl.ds(TOK - 8, 8), :], ends_out.at[:, pl.ds(D + 1024, 1024)], sem
-    )
-    load.start()
+    pairs = [(step_from, step_in), (bias_in, bias), (dlog_in, dlog)]
+    pairs += [(x_in, x), (b_in, b), (cw_in, cw), (cbw_in, cbw)]
+    pairs.append((c_in.at[pl.ds(TOK - 8, 8), :], ends_out.at[:, pl.ds(D + 1024, 1024)]))
+    loads = begin(pairs, sems)
+    for load in loads[:3]:
+        load.wait()
     s = step_in[...].astype(F32).T + bias[...]
     step = jnp.maximum(s, 0.0) + jnp.log(1.0 + jnp.exp(-jnp.abs(s)))
     logs = step * (-jnp.exp(dlog[...]))
@@ -127,6 +130,8 @@
     first = grow[0:8, :] * etot
     sub = lax.broadcasted_iota(jnp.int32, (8, 128), 0)
     low = lax.broadcasted_iota(jnp.int32, (8, 128), 1) < HEAD_DIM
+    for load in loads[3:]:
+        load.wait()
     for g in range(GROUPS):
         xc, bc = group(g)
         xs = tap(padx.at[g], None, x[:, xc], cw[:, xc])
@@ -170,7 +175,6 @@
             st[o, 144:160, :] = jnp.concatenate([x_ends, b_ends], axis=0).astype(BF)
     ends_out[:, 0:D] = x[TOK - 8 :, :]
     ends_out[:, D : D + 1024] = b[TOK - 8 :, :]
-    load.wait()
 
 
 def inner_kernel(x, b, c, halo, cw, cbw, ccw, ec, grow, skip, a_out, c_out, padx, padb, padc):
@@ -283,9 +287,9 @@
     for q in range(4):
         pairs.append((a_in.at[:, part(q, 512)], a.at[:, part(q, 512)]))
         pairs.append((gate_in.at[:, part(q, 512)], gate.at[:, part(q, 512)]))
+    pairs.append((resid_in, resid))
     for k, w in enumerate((w0, w1, w2, w3, w4, w5, w6)):
         pairs.append((w, wide.at[part(k, GW), :]))
-    pairs.append((resid_in, resid))
     loads = begin(pairs, sems)
     for load in loads[:3]:
         load.wait()
@@ -310,11 +314,15 @@
     for k in range(7):
         picked[:, k * GW : (k + 1) * GW] = norm[place[k]]
     rest[...] = norm[place[7]]
-    for load in loads[11:]:
+    for load in loads[11:16]:
         load.wait()
+    cut = 4 * GW
     proj[...] = resid[...].astype(F32) + jnp.dot(
-        picked[...], wide[...], preferred_element_type=F32
-    )
+        picked[:, :cut], wide[:cut, :], preferred_element_type=F32
+    )
+    for load in loads[16:]:
+        load.wait()
+    proj[...] += jnp.dot(picked[:, cut:], wide[cut:, :], preferred_element_type=F32)
 
 
 def mix_kernel(
@@ -354,27 +362,36 @@
     out[...] = mixed[...].astype(F32) + jnp.dot(hidden, sd[...], preferred_element_type=F32)
 
 
-def expert_kernel(got, wg_in, wu_in, wd_in, out, xbuf, wg, wu, wd, sems):
-    pairs = ((wg_in, wg), (wu_in, wu), (wd_in, wd))
-    loads = [pltpu.make_async_copy(v, w, sems.at[k]) for k, (v, w) in enumerate(pairs)]
-    for load in loads:
-        load.start()
+def expert_kernel(got, wg_in, wu_in, wd_in, out, xbuf, wg, wu, wd, gate, up, sems):
     n = 256
     sub = lax.broadcasted_iota(jnp.int32, (ROWS // 16, 8, n), 1)
-    for q in range(HALF // n):
+    pairs = []
+    for q in range(4):
+        for v, w in ((wg_in, wg), (wu_in, wu)):
+            for h in range(2):
+                pairs.append((v.at[part(4 * h + q, n), :], w.at[q, part(h, n), :]))
+    pairs.append((wd_in, wd))
+    loads = begin(pairs, sems)
+
+    def pack(q):
         t = got[:, q * n : (q + 1) * n].astype(F32).reshape(ROWS // 16, 2, 8, n)
         r0, r1 = t[:, 0], t[:, 1]
         x0 = jnp.where(sub < 4, r0, pltpu.roll(r1, 4, 1))
         x1 = jnp.where(sub < 4, pltpu.roll(r0, 4, 1), r1)
-        xbuf[:, q * n : (q + 1) * n] = x0.reshape(ROWS // 2, n).astype(BF)
-        xbuf[:, HALF + q * n : HALF + (q + 1) * n] = x1.reshape(ROWS // 2, n).astype(BF)
-    x = xbuf[...]
-    loads[0].wait()
-    gate = jnp.dot(x, wg[...], preferred_element_type=F32)
-    loads[1].wait()
-    up = jnp.dot(x, wu[...], preferred_element_type=F32)
-    hidden = (silu(gate) * up).astype(BF)
-    loads[2].wait()
+        xbuf[q, :, :n] = x0.reshape(ROWS // 2, n).astype(BF)
+        xbuf[q, :, n:] = x1.reshape(ROWS // 2, n).astype(BF)
+
+    pack(0)
+    for q in range(4):
+        for load in loads[4 * q : 4 * q + 4]:
+            load.wait()
+        if q < 3:
+            pack(q + 1)
+        for acc, w in ((gate, wg), (up, wu)):
+            y = jnp.dot(xbuf[q], w[q], preferred_element_type=F32)
+            acc[...] = y if q == 0 else acc[...] + y
+    loads[16].wait()
+    hidden = (silu(gate[...]) * up[...]).astype(BF)
     for q in range(HALF // n):
         y0 = jnp.dot(hidden, wd[:, q * n : (q + 1) * n], preferred_element_type=F32)
         y1 = jnp.dot(hidden, wd[:, HALF + q * n : HALF + (q + 1) * n], preferred_element_type=F32)
@@ -435,12 +452,19 @@
     st, ec, grow, ends = call(
         states_kernel,
         [((ways, ST_ROWS, 128), BF), ((TOK, HEADS), F32), ((TOK, HEADS), F32), ((8, 4096), BF)],
-        (step_input[0].T, conv_weight, conv_b_weight, step_bias[None], decay_log[None], x, b, c),
-        raw=(7,),
+        (step_input[0].T, step_bias[None], decay_log[None], x, b, conv_weight, conv_b_weight, c),
+        raw=range(8),
         scratch=[
             pltpu.VMEM((GROUPS, 2, TOK + 8, 128), F32),
             pltpu.VMEM((GROUPS, 1, TOK + 8, 128), F32),
-            pltpu.SemaphoreType.DMA,
+            pltpu.VMEM((HEADS, TOK), BF),
+            pltpu.VMEM((1, HEADS), F32),
+            pltpu.VMEM((1, HEADS), F32),
+            pltpu.VMEM((TOK, D), BF),
+            pltpu.VMEM((TOK, 1024), BF),
+            pltpu.VMEM((4, D), BF),
+            pltpu.VMEM((4, 1024), BF),
+            pltpu.SemaphoreType.DMA((8,)),
         ],
     )
     got = exchange(st, "sp")
@@ -529,11 +553,13 @@
         [((ROWS, HALF), BF)],
         (arrived.reshape(ROWS, HALF), expert_gate[0], expert_up[0], expert_down[0]),
         scratch=[
-            pltpu.VMEM((ROWS // 2, D), BF),
-            pltpu.VMEM((D, 512), BF),
-            pltpu.VMEM((D, 512), BF),
+            pltpu.VMEM((4, ROWS // 2, 512), BF),
+            pltpu.VMEM((4, 512, 512), BF),
+            pltpu.VMEM((4, 512, 512), BF),
             pltpu.VMEM((512, D), BF),
-            pltpu.SemaphoreType.DMA((3,)),
+            pltpu.VMEM((ROWS // 2, 512), F32),
+            pltpu.VMEM((ROWS // 2, 512), F32),
+            pltpu.SemaphoreType.DMA((17,)),
         ],
         vmem=(0,),
         raw=(1, 2, 3),

time: 152 us -> 153 us (level)
  transfers between devices with their start and end apart: 11 -> 11, of which waited for: 5 -> 5; matrix products, arithmetic and copies ran while one was open for 0% -> 0% of each run, Pallas kernels for 16% -> 15%
where the time goes in v9:
time: 153 us; the launch traced here: 152 us
  waiting for transfers between devices  44.6 us (29%)
  blocking collectives  36 us (24%)
  Pallas kernels  35.4 us (23%)
  starting transfers between devices  34.5 us (23%)
    all_to_all x1, blocking collectives, exchange(): lax.all_to_all(plain(v), axis, split_axis=0, concat_axis=0, tiled=True)  36 us
    pallas_call x10, Pallas kernels, call(): pl.pallas_call(kernel, out_shape=tuple((pltpu.VMEM(s, d) if i in out_vmem...  35.4 us
    all_to_all x3, waiting for transfers between devices, exchange(): lax.all_to_all(plain(v), axis, split_axis=0, concat_axis=0, tiled=True)  27.8 us
    all_to_all x3, starting transfers between devices, exchange(): lax.all_to_all(plain(v), axis, split_axis=0, concat_axis=0, tiled=True)  19.4 us
    ppermute x3, waiting for transfers between devices, ring(): lax.ppermute(v, 'dp', [(i, (i + (-2 if i % 2 else 2)) % dps) for i in ran...  16.8 us
    ppermute x3, starting transfers between devices, ring(): lax.ppermute(v, 'dp', [(i, (i + (-2 if i % 2 else 2)) % dps) for i in ran...  8.09 us
    ppermute x4, starting transfers between devices, swap(): return lax.ppermute(v, 'dp', [(i, i ^ 1) for i in range(dps)])  3.74 us
    ppermute x1, starting transfers between devices, layer(): lax.ppermute(plain(ends), 'sp', [(i, i + 1) for i in range(ways - 1)])  3.3 us
  transfers between devices with their start and end apart: 11, of which 5 were waited for; matrix products, arithmetic and copies ran while one was open for 0% of the time, Pallas kernels for 15%

profile of v9, /device:TPU:1, one launch (start us, length us, event | category | flops | bytes accessed | tf_op | source)
XLA Modules:
  0.0 152.1 jit_solution(4365535069810508661)
XLA Ops:
  0.0 1.4 collective-permute-start.1
  1.4 2.6 %collective-permute-start.2 = (bf16[256,2048]{1,0:T(8,128)(2,1)}, bf16[256,2048]{1,0:T(8,128)(2,1)S(1)}, u32[]{:S(2)}, u32[]{:S(2)}) collective-permute-start(bf16[256,2048]{1,0:T(8,128)(2,1)} %w0.1), channel_id=1, source_target_pairs={{0,2},{1,7},{2,4},{3,1},{4,6},{5,3},{6,0},{7,5},{8,10},{9,15},{10,... | collective-permute-start | bytes 3145736 | tf_op jit(solution)/shard_map/ppermute | solution.py:441
  4.0 0.0 collective-permute-done.1.w1
  4.0 2.5 %collective-permute-start.3 = (bf16[256,2048]{1,0:T(8,128)(2,1)S(1)}, bf16[256,2048]{1,0:T(8,128)(2,1)}, u32[]{:S(2)}, u32[]{:S(2)}) collective-permute-start(bf16[256,2048]{1,0:T(8,128)(2,1)S(1)} %collective-permute-done.1.w1), channel_id=1, source_target_pairs={{0,2},{1,7},{2,4},{3,1},{4,6},{5,3},{6,0},{7,5},{8,10},{9,15},{10,... | collective-permute-start | bytes 3145736 | tf_op jit(solution)/shard_map/ppermute | solution.py:441
  6.5 9.6 %collective-permute-done.2.w2 = bf16[256,2048]{1,0:T(8,128)(2,1)S(1)} collective-permute-done((bf16[256,2048]{1,0:T(8,128)(2,1)}, bf16[256,2048]{1,0:T(8,128)(2,1)S(1)}, u32[]{:S(2)}, u32[]{:S(2)}) %collective-permute-start.2) | collective-permute-done | bytes 1048608 | tf_op jit(solution)/shard_map/ppermute | solution.py:441
  16.0 3.0 %collective-permute-start.6 = (bf16[256,2048]{1,0:T(8,128)(2,1)S(1)}, bf16[256,2048]{1,0:T(8,128)(2,1)}, u32[]{:S(2)}, u32[]{:S(2)}) collective-permute-start(bf16[256,2048]{1,0:T(8,128)(2,1)S(1)} %collective-permute-done.2.w2), channel_id=1, source_target_pairs={{0,2},{1,7},{2,4},{3,1},{4,6},{5,3},{6,0},{7,5},{8,10},{9,15},{10,... | collective-permute-start | bytes 3145736 | tf_op jit(solution)/shard_map/ppermute | solution.py:441
  19.0 3.8 %shard_map.217 = (bf16[16,160,128]{2,1,0:T(8,128)(2,1)}, f32[128,32]{1,0:T(8,128)}, f32[128,32]{1,0:T(8,128)}, bf16[8,4096]{1,0:T(8,128)(2,1)}) custom-call(bf16[32,128]{1,0:T(8,128)(2,1)} %bitcast.41, f32[1,32]{1,0:T(1,128)} %bitcast.43, f32[1,32]{1,0:T(1,128)} %bitcast.44, bf16[128,2048]{1,0:T(8,128)(2,1)} %bitcast.35, bf16[128,1024]{1,0:T(8,128)(2,1)} %bitcast.37, ...), custom_call_target="tpu_custom_call" | custom-call | flops 1000000 | bytes 1000000 | tf_op jit(solution)/shard_map/pallas_call | solution.py:49
  22.8 7.8 %all-to-all-start = ((bf16[16,160,128]{2,1,0:T(8,128)(2,1)}), bf16[16,160,128]{2,1,0:T(8,128)(2,1)S(1)}, u32[]{:S(2)}, u32[]{:S(2)}) async-start(bf16[16,160,128]{2,1,0:T(8,128)(2,1)} %get-tuple-element.16), calls=%async_computation | async-start | bytes 1310720 | tf_op jit(solution)/shard_map/all_to_all | solution.py:426
  30.6 0.1 collective-permute-start.4
  30.7 0.0 collective-permute-done.3.w3
  30.7 0.5 collective-permute-start.5
  31.2 7.2 %collective-permute-done.6.w6 = bf16[256,2048]{1,0:T(8,128)(2,1)} collective-permute-done((bf16[256,2048]{1,0:T(8,128)(2,1)S(1)}, bf16[256,2048]{1,0:T(8,128)(2,1)}, u32[]{:S(2)}, u32[]{:S(2)}) %collective-permute-start.6) | collective-permute-done | bytes 1048608 | tf_op jit(solution)/shard_map/ppermute | solution.py:441
  38.4 1.8 %collective-permute-start.7 = (bf16[256,2048]{1,0:T(8,128)(2,1)}, bf16[256,2048]{1,0:T(8,128)(2,1)}, u32[]{:S(2)}, u32[]{:S(2)}) collective-permute-start(bf16[256,2048]{1,0:T(8,128)(2,1)} %collective-permute-done.6.w6), channel_id=1, source_target_pairs={{0,1},{1,0},{2,3},{3,2},{4,5},{5,4},{6,7},{7,6},{8,9},{9,8},{10,11... | collective-permute-start | bytes 3145736 | tf_op jit(solution)/shard_map/ppermute | solution.py:444
  40.2 3.3 %collective-permute-start = (bf16[8,4096]{1,0:T(8,128)(2,1)}, bf16[8,4096]{1,0:T(8,128)(2,1)S(1)}, u32[]{:S(2)}, u32[]{:S(2)}) collective-permute-start(bf16[8,4096]{1,0:T(8,128)(2,1)} %get-tuple-element.18), channel_id=1, source_target_pairs={{0,8},{8,16},{16,24},{24,32},{32,40},{40,48},{48,56},{56,64},{64,7... | collective-permute-start | bytes 196616 | tf_op jit(solution)/shard_map/ppermute | solution.py:471
  43.5 0.3 all-to-all-done.got
  43.8 1.2 shard_map.218
  45.0 7.2 %all-to-all-start.1 = ((bf16[16,128,128]{2,1,0:T(8,128)(2,1)}), bf16[16,128,128]{2,1,0:T(8,128)(2,1)S(1)}, u32[]{:S(2)}, u32[]{:S(2)}) async-start(bf16[16,128,128]{2,1,0:T(8,128)(2,1)} %shard_map.218), calls=%async_computation.1 | async-start | bytes 1048576 | tf_op jit(solution)/shard_map/all_to_all | solution.py:426
  52.2 2.4 %shard_map.221.disp_in = bf16[1024,256]{1,0:T(8,128)(2,1)} custom-call(s32[2,128]{1,0:T(2,128)} %bitcast.49, f32[2,128]{1,0:T(2,128)} %bitcast.51), custom_call_target="tpu_custom_call" | custom-call | flops 2000000000 | bytes 1000000 | tf_op jit(solution)/shard_map/pallas_call | solution.py:49
  54.5 0.0 collective-permute-done.halo
  54.5 4.0 %shard_map.219 = (f32[128,2048]{1,0:T(8,128)}, bf16[128,1024]{1,0:T(8,128)(2,1)}) custom-call(bf16[128,2048]{1,0:T(8,128)(2,1)} %bitcast.36, bf16[128,1024]{1,0:T(8,128)(2,1)} %bitcast.38, bf16[128,1024]{1,0:T(8,128)(2,1)} %bitcast.40, bf16[8,4096]{1,0:T(8,128)(2,1)S(1)} %collective-permute-done.halo, bf16[4,2048]{1,0:T(4,128)(2,1)} %cw.1, ...), custom_call_target="tpu_custom_call" | custom-call | flops 4000000000 | bytes 1000000 | tf_op jit(solution)/shard_map/pallas_call | solution.py:49
  58.6 4.4 %all-to-all-done.1 = bf16[16,128,128]{2,1,0:T(8,128)(2,1)S(1)} async-done(((bf16[16,128,128]{2,1,0:T(8,128)(2,1)}), bf16[16,128,128]{2,1,0:T(8,128)(2,1)S(1)}, u32[]{:S(2)}, u32[]{:S(2)}) %all-to-all-start.1) | async-done | bytes 524320 | tf_op jit(solution)/shard_map/all_to_all | solution.py:426
  63.0 0.0 collective-permute-done.4.w4
  63.0 4.5 %shard_map.220 = (f32[128,2048]{1,0:T(8,128)S(1)}, bf16[128,256]{1,0:T(8,128)(2,1)S(1)}) custom-call(bf16[8,256,128]{2,1,0:T(8,128)(2,1)S(1)} %bitcast.29, f32[128,32]{1,0:T(8,128)} %get-tuple-element.17.ec.ec_in, f32[128,2048]{1,0:T(8,128)} %get-tuple-element.20.a_in, bf16[128,1024]{1,0:T(8,128)(2,1)} %get-tuple-element.21.cm_in, ...), custom_call_target="tpu_custom_call" | custom-call | flops 2000000000 | bytes 1000000 | tf_op jit(solution)/shard_map/pallas_call | solution.py:49
  67.5 3.6 %shard_map.222 = (bf16[128,2048]{1,0:T(8,128)(2,1)}, bf16[128,2048]{1,0:T(8,128)(2,1)}, bf16[1024,1024]{1,0:T(8,128)(2,1)}) custom-call(f32[128,2048]{1,0:T(8,128)S(1)} %get-tuple-element.22.proj_in, bf16[128,256]{1,0:T(8,128)(2,1)S(1)} %get-tuple-element.23.rest, f32[1,2048]{1,0:T(1,128)} %bitcast.48, bf16[1024,256]{1,0:T(8,128)(2,1)} %shard_map.221.disp_in, ...), custom_call_target="tpu_custom_call" | custom-call | flops 2000000000 | bytes 1000000 | tf_op jit(solution)/shard_map/pallas_call | solution.py:49
  71.2 36.0 %all_to_all.20 = bf16[128,8,1024]{2,1,0:T(8,128)(2,1)S(1)} all-to-all(bf16[128,8,1024]{2,1,0:T(8,128)(2,1)} %bitcast.32), channel_id=1, replica_groups=mesh['sp'=16,'dp'=8] {'sp','dp'}, dimensions={0} | all-to-all | bytes 4194304 | tf_op jit(solution)/shard_map/all_to_all | solution.py:426
  107.2 5.7 %shard_map.223 = bf16[1024,1024]{1,0:T(8,128)(2,1)S(1)} custom-call(bf16[1024,1024]{1,0:T(8,128)(2,1)S(1)} %bitcast.31, bf16[2048,512]{1,0:T(8,128)(2,1)} %bitcast.45, bf16[2048,512]{1,0:T(8,128)(2,1)} %bitcast.46, bf16[512,2048]{1,0:T(8,128)(2,1)} %bitcast.47), custom_call_target="tpu_custom_call" | custom-call | flops 3000000000 | bytes 1000000 | tf_op jit(solution)/shard_map/pallas_call | solution.py:49
  112.9 1.3 copy-done
  114.2 4.4 %all-to-all-start.3 = ((bf16[128,8,1024]{2,1,0:T(8,128)(2,1)}), bf16[128,8,1024]{2,1,0:T(8,128)(2,1)S(1)}, u32[]{:S(2)}, u32[]{:S(2)}) async-start(bf16[128,8,1024]{2,1,0:T(8,128)(2,1)} %bitcast.30), calls=%async_computation.3 | async-start | bytes 4194304 | tf_op jit(solution)/shard_map/all_to_all | solution.py:426
  118.6 2.3 %shard_map.224.w_in = bf16[256,1024]{1,0:T(8,128)(2,1)} custom-call(s32[2,128]{1,0:T(2,128)} %bitcast.50, f32[2,128]{1,0:T(2,128)} %bitcast.52), custom_call_target="tpu_custom_call" | custom-call | flops 2000000000 | bytes 1000000 | tf_op jit(solution)/shard_map/pallas_call | solution.py:49
  120.9 5.3 %shard_map.225.base_in = f32[128,2048]{1,0:T(8,128)} custom-call(bf16[128,2048]{1,0:T(8,128)(2,1)} %get-tuple-element.25.ein, bf16[128,2048]{1,0:T(8,128)(2,1)} %get-tuple-element.26.mixed, bf16[2048,512]{1,0:T(8,128)(2,1)} %sg.1, bf16[2048,512]{1,0:T(8,128)(2,1)} %su.1, bf16[512,2048]{1,0:T(8,128)(2,1)} %sd.1), custom_call_target="tpu_custom_call" | custom-call | flops 4000000000 | bytes 1000000 | tf_op jit(solution)/shard_map/pallas_call | solution.py:49
  126.2 23.1 %all-to-all-done.3 = bf16[128,8,1024]{2,1,0:T(8,128)(2,1)S(1)} async-done(((bf16[128,8,1024]{2,1,0:T(8,128)(2,1)}), bf16[128,8,1024]{2,1,0:T(8,128)(2,1)S(1)}, u32[]{:S(2)}, u32[]{:S(2)}) %all-to-all-start.3) | async-done | bytes 2097184 | tf_op jit(solution)/shard_map/all_to_all | solution.py:426
  149.2 2.7 %shard_map.226 = bf16[128,2048]{1,0:T(8,128)(2,1)} custom-call(bf16[1024,1024]{1,0:T(8,128)(2,1)S(1)} %bitcast.28, bf16[256,1024]{1,0:T(8,128)(2,1)} %shard_map.224.w_in, f32[128,2048]{1,0:T(8,128)} %shard_map.225.base_in), custom_call_target="tpu_custom_call" | custom-call | flops 1000000 | bytes 1000000 | tf_op jit(solution)/shard_map/pallas_call | solution.py:49
  (3 shorter events, 0.0 us)
Async XLA Ops:
  0.0 4.0 %collective-permute-start.1 = (bf16[256,2048]{1,0:T(8,128)(2,1)}, bf16[256,2048]{1,0:T(8,128)(2,1)S(1)}, u32[]{:S(2)}, u32[]{:S(2)}) collective-permute-start(bf16[256,2048]{1,0:T(8,128)(2,1)} %w0.1), channel_id=1, source_target_pairs={{0,1},{1,0},{2,3},{3,2},{4,5},{5,4},{6,7},{7,6},{8,9},{9,8},{10,11... | collective-permute-start | bytes 3145736 | tf_op jit(solution)/shard_map/ppermute | solution.py:444
  1.4 14.7 %collective-permute-start.2 = (bf16[256,2048]{1,0:T(8,128)(2,1)}, bf16[256,2048]{1,0:T(8,128)(2,1)S(1)}, u32[]{:S(2)}, u32[]{:S(2)}) collective-permute-start(bf16[256,2048]{1,0:T(8,128)(2,1)} %w0.1), channel_id=1, source_target_pairs={{0,2},{1,7},{2,4},{3,1},{4,6},{5,3},{6,0},{7,5},{8,10},{9,15},{10,... | collective-permute-start | bytes 3145736 | tf_op jit(solution)/shard_map/ppermute | solution.py:441
  4.0 26.7 %collective-permute-start.3 = (bf16[256,2048]{1,0:T(8,128)(2,1)S(1)}, bf16[256,2048]{1,0:T(8,128)(2,1)}, u32[]{:S(2)}, u32[]{:S(2)}) collective-permute-start(bf16[256,2048]{1,0:T(8,128)(2,1)S(1)} %collective-permute-done.1.w1), channel_id=1, source_target_pairs={{0,2},{1,7},{2,4},{3,1},{4,6},{5,3},{6,0},{7,5},{8,10},{9,15},{10,... | collective-permute-start | bytes 3145736 | tf_op jit(solution)/shard_map/ppermute | solution.py:441
  16.0 22.4 %collective-permute-start.6 = (bf16[256,2048]{1,0:T(8,128)(2,1)S(1)}, bf16[256,2048]{1,0:T(8,128)(2,1)}, u32[]{:S(2)}, u32[]{:S(2)}) collective-permute-start(bf16[256,2048]{1,0:T(8,128)(2,1)S(1)} %collective-permute-done.2.w2), channel_id=1, source_target_pairs={{0,2},{1,7},{2,4},{3,1},{4,6},{5,3},{6,0},{7,5},{8,10},{9,15},{10,... | collective-permute-start | bytes 3145736 | tf_op jit(solution)/shard_map/ppermute | solution.py:441
  22.8 21.0 %all-to-all-start = ((bf16[16,160,128]{2,1,0:T(8,128)(2,1)}), bf16[16,160,128]{2,1,0:T(8,128)(2,1)S(1)}, u32[]{:S(2)}, u32[]{:S(2)}) async-start(bf16[16,160,128]{2,1,0:T(8,128)(2,1)} %get-tuple-element.16), calls=%async_computation | async-start | bytes 1310720 | tf_op jit(solution)/shard_map/all_to_all | solution.py:426
  30.6 32.4 %collective-permute-start.4 = (bf16[256,2048]{1,0:T(8,128)(2,1)S(1)}, bf16[256,2048]{1,0:T(8,128)(2,1)}, u32[]{:S(2)}, u32[]{:S(2)}) collective-permute-start(bf16[256,2048]{1,0:T(8,128)(2,1)S(1)} %collective-permute-done.2.w2), channel_id=1, source_target_pairs={{0,1},{1,0},{2,3},{3,2},{4,5},{5,4},{6,7},{7,6},{8,9},{9,8},{10,11... | collective-permute-start | bytes 3145736 | tf_op jit(solution)/shard_map/ppermute | solution.py:444
  30.7 32.3 %collective-permute-start.5 = (bf16[256,2048]{1,0:T(8,128)(2,1)}, bf16[256,2048]{1,0:T(8,128)(2,1)}, u32[]{:S(2)}, u32[]{:S(2)}) collective-permute-start(bf16[256,2048]{1,0:T(8,128)(2,1)} %collective-permute-done.3.w3), channel_id=1, source_target_pairs={{0,1},{1,0},{2,3},{3,2},{4,5},{5,4},{6,7},{7,6},{8,9},{9,8},{10,11... | collective-permute-start | bytes 3145736 | tf_op jit(solution)/shard_map/ppermute | solution.py:444
  38.4 29.1 %collective-permute-start.7 = (bf16[256,2048]{1,0:T(8,128)(2,1)}, bf16[256,2048]{1,0:T(8,128)(2,1)}, u32[]{:S(2)}, u32[]{:S(2)}) collective-permute-start(bf16[256,2048]{1,0:T(8,128)(2,1)} %collective-permute-done.6.w6), channel_id=1, source_target_pairs={{0,1},{1,0},{2,3},{3,2},{4,5},{5,4},{6,7},{7,6},{8,9},{9,8},{10,11... | collective-permute-start | bytes 3145736 | tf_op jit(solution)/shard_map/ppermute | solution.py:444
  40.2 14.3 %collective-permute-start = (bf16[8,4096]{1,0:T(8,128)(2,1)}, bf16[8,4096]{1,0:T(8,128)(2,1)S(1)}, u32[]{:S(2)}, u32[]{:S(2)}) collective-permute-start(bf16[8,4096]{1,0:T(8,128)(2,1)} %get-tuple-element.18), channel_id=1, source_target_pairs={{0,8},{8,16},{16,24},{24,32},{32,40},{40,48},{48,56},{56,64},{64,7... | collective-permute-start | bytes 196616 | tf_op jit(solution)/shard_map/ppermute | solution.py:471
  45.0 18.0 %all-to-all-start.1 = ((bf16[16,128,128]{2,1,0:T(8,128)(2,1)}), bf16[16,128,128]{2,1,0:T(8,128)(2,1)S(1)}, u32[]{:S(2)}, u32[]{:S(2)}) async-start(bf16[16,128,128]{2,1,0:T(8,128)(2,1)} %shard_map.218), calls=%async_computation.1 | async-start | bytes 1048576 | tf_op jit(solution)/shard_map/all_to_all | solution.py:426
  112.9 1.3 copy-start
  114.2 35.0 %all-to-all-start.3 = ((bf16[128,8,1024]{2,1,0:T(8,128)(2,1)}), bf16[128,8,1024]{2,1,0:T(8,128)(2,1)S(1)}, u32[]{:S(2)}, u32[]{:S(2)}) async-start(bf16[128,8,1024]{2,1,0:T(8,128)(2,1)} %bitcast.30), calls=%async_computation.3 | async-start | bytes 4194304 | tf_op jit(solution)/shard_map/all_to_all | solution.py:426

commit v10 on v8

--- a/solution.py
+++ b/solution.py
@@ -105,12 +105,15 @@
 
 
 def states_kernel(
-    step_in, cw, cbw, bias, dlog, x, b, c, st, ec, grow_out, ends_out, padx, padb, sem
+    step_from, bias_in, dlog_in, x_in, b_in, cw_in, cbw_in, c_in, st, ec, grow_out, ends_out,
+    padx, padb, step_in, bias, dlog, x, b, cw, cbw, sems
 ):
-    load = pltpu.make_async_copy(
-        c.at[pl.ds(TOK - 8, 8), :], ends_out.at[:, pl.ds(D + 1024, 1024)], sem
-    )
-    load.start()
+    pairs = [(step_from, step_in), (bias_in, bias), (dlog_in, dlog)]
+    pairs += [(x_in, x), (b_in, b), (cw_in, cw), (cbw_in, cbw)]
+    pairs.append((c_in.at[pl.ds(TOK - 8, 8), :], ends_out.at[:, pl.ds(D + 1024, 1024)]))
+    loads = begin(pairs, sems)
+    for load in loads[:3]:
+        load.wait()
     s = step_in[...].astype(F32).T + bias[...]
     step = jnp.maximum(s, 0.0) + jnp.log(1.0 + jnp.exp(-jnp.abs(s)))
     logs = step * (-jnp.exp(dlog[...]))
@@ -127,6 +130,8 @@
     first = grow[0:8, :] * etot
     sub = lax.broadcasted_iota(jnp.int32, (8, 128), 0)
     low = lax.broadcasted_iota(jnp.int32, (8, 128), 1) < HEAD_DIM
+    for load in loads[3:]:
+        load.wait()
     for g in range(GROUPS):
         xc, bc = group(g)
         xs = tap(padx.at[g], None, x[:, xc], cw[:, xc])
@@ -170,10 +175,17 @@
             st[o, 144:160, :] = jnp.concatenate([x_ends, b_ends], axis=0).astype(BF)
     ends_out[:, 0:D] = x[TOK - 8 :, :]
     ends_out[:, D : D + 1024] = b[TOK - 8 :, :]
-    load.wait()
-
-
-def inner_kernel(x, b, c, halo, cw, cbw, ccw, ec, grow, skip, a_out, c_out, padx, padb, padc):
+
+
+def inner_kernel(
+    x_in, b_in, c_in, halo_in, cw_in, cbw_in, ccw_in, ec_in, grow_in, skip_in, a_out, c_out,
+    padx, padb, padc, x, b, c, halo, cw, cbw, ccw, ec, grow, skip, a_buf, cm_buf, sems, out_sems
+):
+    pairs = [(x_in, x), (b_in, b), (c_in, c), (halo_in, halo), (cw_in, cw), (cbw_in, cbw)]
+    pairs += [(ccw_in, ccw), (ec_in, ec), (grow_in, grow), (skip_in, skip)]
+    for load in begin(pairs, sems):
+        load.wait()
+    stores = []
     r = lax.broadcasted_iota(jnp.int32, (TOK, TOK), 0)
     s = lax.broadcasted_iota(jnp.int32, (TOK, TOK), 1)
     lower = s <= r
@@ -188,12 +200,22 @@
         xs = tap(padx.at[g], halo[:, xc], x[:, xc], cw[:, xc])
         bm = tap(padb.at[g], halo[:, bh], b[:, bc], cbw[:, bc]).astype(BF)
         cm = tap(padc.at[g], halo[:, ch], c[:, bc], ccw[:, bc]).astype(BF)
-        c_out[:, bc] = cm
+        cm_buf[:, bc] = cm
         v = (xs * spread(rows, g)).astype(BF)
         cb = lax.dot_general(cm, bm, (((1,), (1,)), ((), ())), preferred_element_type=F32)
         cb = jnp.where(lower, cb, 0.0).astype(BF)
         u = jnp.dot(cb, v, preferred_element_type=F32)
-        a_out[:, xc] = u * spread(cols, g) + xs * spread(sk, g)
+        a_buf[:, xc] = u * spread(cols, g) + xs * spread(sk, g)
+        if g % 4 == 3:
+            cols4 = part(g // 4, D // 2)
+            stores.append(
+                pltpu.make_async_copy(a_buf.at[:, cols4], a_out.at[:, cols4], out_sems.at[g // 4])
+            )
+            stores[-1].start()
+    stores.append(pltpu.make_async_copy(cm_buf, c_out, out_sems.at[2]))
+    stores[-1].start()
+    for store in stores:
+        store.wait()
 
 
 def carry_kernel(got, out, buf, sems):
@@ -283,9 +305,9 @@
     for q in range(4):
         pairs.append((a_in.at[:, part(q, 512)], a.at[:, part(q, 512)]))
         pairs.append((gate_in.at[:, part(q, 512)], gate.at[:, part(q, 512)]))
+    pairs.append((resid_in, resid))
     for k, w in enumerate((w0, w1, w2, w3, w4, w5, w6)):
         pairs.append((w, wide.at[part(k, GW), :]))
-    pairs.append((resid_in, resid))
     loads = begin(pairs, sems)
     for load in loads[:3]:
         load.wait()
@@ -310,11 +332,15 @@
     for k in range(7):
         picked[:, k * GW : (k + 1) * GW] = norm[place[k]]
     rest[...] = norm[place[7]]
-    for load in loads[11:]:
+    for load in loads[11:16]:
         load.wait()
+    cut = 4 * GW
     proj[...] = resid[...].astype(F32) + jnp.dot(
-        picked[...], wide[...], preferred_element_type=F32
-    )
+        picked[:, :cut], wide[:cut, :], preferred_element_type=F32
+    )
+    for load in loads[16:]:
+        load.wait()
+    proj[...] += jnp.dot(picked[:, cut:], wide[cut:, :], preferred_element_type=F32)
 
 
 def mix_kernel(
@@ -435,12 +461,19 @@
     st, ec, grow, ends = call(
         states_kernel,
         [((ways, ST_ROWS, 128), BF), ((TOK, HEADS), F32), ((TOK, HEADS), F32), ((8, 4096), BF)],
-        (step_input[0].T, conv_weight, conv_b_weight, step_bias[None], decay_log[None], x, b, c),
-        raw=(7,),
+        (step_input[0].T, step_bias[None], decay_log[None], x, b, conv_weight, conv_b_weight, c),
+        raw=range(8),
         scratch=[
             pltpu.VMEM((GROUPS, 2, TOK + 8, 128), F32),
             pltpu.VMEM((GROUPS, 1, TOK + 8, 128), F32),
-            pltpu.SemaphoreType.DMA,
+            pltpu.VMEM((HEADS, TOK), BF),
+            pltpu.VMEM((1, HEADS), F32),
+            pltpu.VMEM((1, HEADS), F32),
+            pltpu.VMEM((TOK, D), BF),
+            pltpu.VMEM((TOK, 1024), BF),
+            pltpu.VMEM((4, D), BF),
+            pltpu.VMEM((4, 1024), BF),
+            pltpu.SemaphoreType.DMA((8,)),
         ],
     )
     got = exchange(st, "sp")
@@ -449,11 +482,27 @@
         inner_kernel,
         [((TOK, D), F32), ((TOK, 1024), BF)],
         (x, b, c, halo, conv_weight, conv_b_weight, conv_c_weight, ec, grow, skip[None]),
+        raw=range(10),
         free=(3,),
+        raw_out=(0, 1),
         scratch=[
             pltpu.VMEM((GROUPS, 2, TOK + 8, 128), F32),
             pltpu.VMEM((GROUPS, 1, TOK + 8, 128), F32),
             pltpu.VMEM((GROUPS, 1, TOK + 8, 128), F32),
+            pltpu.VMEM((TOK, D), BF),
+            pltpu.VMEM((TOK, 1024), BF),
+            pltpu.VMEM((TOK, 1024), BF),
+            pltpu.VMEM((8, 4096), BF),
+            pltpu.VMEM((4, D), BF),
+            pltpu.VMEM((4, 1024), BF),
+            pltpu.VMEM((4, 1024), BF),
+            pltpu.VMEM((TOK, HEADS), F32),
+            pltpu.VMEM((TOK, HEADS), F32),
+            pltpu.VMEM((1, HEADS), F32),
+            pltpu.VMEM((TOK, D), F32),
+            pltpu.VMEM((TOK, 1024), BF),
+            pltpu.SemaphoreType.DMA((10,)),
+            pltpu.SemaphoreType.DMA((3,)),
         ],
         flops=4 * 10**9,
     )

time: 152 us -> 152 us (level)
  transfers between devices with their start and end apart: 11 -> 11, of which waited for: 5 -> 5; matrix products, arithmetic and copies ran while one was open for 0% -> 0% of each run, Pallas kernels for 16% -> 15%
where the time goes in v10:
time: 152 us
  waiting for transfers between devices  44.6 us (29%)
  blocking collectives  36 us (24%)
  Pallas kernels  35.2 us (23%)
  starting transfers between devices  34.5 us (23%)
    all_to_all x1, blocking collectives, exchange(): lax.all_to_all(plain(v), axis, split_axis=0, concat_axis=0, tiled=True)  36 us
    pallas_call x10, Pallas kernels, call(): pl.pallas_call(kernel, out_shape=tuple((pltpu.VMEM(s, d) if i in out_vmem...  35.2 us
    all_to_all x3, waiting for transfers between devices, exchange(): lax.all_to_all(plain(v), axis, split_axis=0, concat_axis=0, tiled=True)  27.8 us
    all_to_all x3, starting transfers between devices, exchange(): lax.all_to_all(plain(v), axis, split_axis=0, concat_axis=0, tiled=True)  19.4 us
    ppermute x3, waiting for transfers between devices, ring(): lax.ppermute(v, 'dp', [(i, (i + (-2 if i % 2 else 2)) % dps) for i in ran...  16.8 us
    ppermute x3, starting transfers between devices, ring(): lax.ppermute(v, 'dp', [(i, (i + (-2 if i % 2 else 2)) % dps) for i in ran...  8.09 us
    ppermute x4, starting transfers between devices, swap(): return lax.ppermute(v, 'dp', [(i, i ^ 1) for i in range(dps)])  3.74 us
    ppermute x1, starting transfers between devices, layer(): lax.ppermute(plain(ends), 'sp', [(i, i + 1) for i in range(ways - 1)])  3.3 us
  transfers between devices with their start and end apart: 11, of which 5 were waited for; matrix products, arithmetic and copies ran while one was open for 0% of the time, Pallas kernels for 15%

profile of v10, /device:TPU:1, one launch (start us, length us, event | category | flops | bytes accessed | tf_op | source)
XLA Modules:
  0.0 151.9 jit_solution(17018728457622125063)
XLA Ops:
  0.0 1.4 collective-permute-start.1
  1.4 2.6 %collective-permute-start.2 = (bf16[256,2048]{1,0:T(8,128)(2,1)}, bf16[256,2048]{1,0:T(8,128)(2,1)S(1)}, u32[]{:S(2)}, u32[]{:S(2)}) collective-permute-start(bf16[256,2048]{1,0:T(8,128)(2,1)} %w0.1), channel_id=1, source_target_pairs={{0,2},{1,7},{2,4},{3,1},{4,6},{5,3},{6,0},{7,5},{8,10},{9,15},{10,... | collective-permute-start | bytes 3145736 | tf_op jit(solution)/shard_map/ppermute | solution.py:450
  4.0 0.0 collective-permute-done.1.w1
  4.0 2.5 %collective-permute-start.3 = (bf16[256,2048]{1,0:T(8,128)(2,1)S(1)}, bf16[256,2048]{1,0:T(8,128)(2,1)}, u32[]{:S(2)}, u32[]{:S(2)}) collective-permute-start(bf16[256,2048]{1,0:T(8,128)(2,1)S(1)} %collective-permute-done.1.w1), channel_id=1, source_target_pairs={{0,2},{1,7},{2,4},{3,1},{4,6},{5,3},{6,0},{7,5},{8,10},{9,15},{10,... | collective-permute-start | bytes 3145736 | tf_op jit(solution)/shard_map/ppermute | solution.py:450
  6.5 9.6 %collective-permute-done.2.w2 = bf16[256,2048]{1,0:T(8,128)(2,1)S(1)} collective-permute-done((bf16[256,2048]{1,0:T(8,128)(2,1)}, bf16[256,2048]{1,0:T(8,128)(2,1)S(1)}, u32[]{:S(2)}, u32[]{:S(2)}) %collective-permute-start.2) | collective-permute-done | bytes 1048608 | tf_op jit(solution)/shard_map/ppermute | solution.py:450
  16.0 3.0 %collective-permute-start.6 = (bf16[256,2048]{1,0:T(8,128)(2,1)S(1)}, bf16[256,2048]{1,0:T(8,128)(2,1)}, u32[]{:S(2)}, u32[]{:S(2)}) collective-permute-start(bf16[256,2048]{1,0:T(8,128)(2,1)S(1)} %collective-permute-done.2.w2), channel_id=1, source_target_pairs={{0,2},{1,7},{2,4},{3,1},{4,6},{5,3},{6,0},{7,5},{8,10},{9,15},{10,... | collective-permute-start | bytes 3145736 | tf_op jit(solution)/shard_map/ppermute | solution.py:450
  19.0 3.8 %shard_map.217 = (bf16[16,160,128]{2,1,0:T(8,128)(2,1)}, f32[128,32]{1,0:T(8,128)}, f32[128,32]{1,0:T(8,128)}, bf16[8,4096]{1,0:T(8,128)(2,1)}) custom-call(bf16[32,128]{1,0:T(8,128)(2,1)} %bitcast.41, f32[1,32]{1,0:T(1,128)} %bitcast.43, f32[1,32]{1,0:T(1,128)} %bitcast.44, bf16[128,2048]{1,0:T(8,128)(2,1)} %bitcast.35, bf16[128,1024]{1,0:T(8,128)(2,1)} %bitcast.37, ...), custom_call_target="tpu_custom_call" | custom-call | flops 1000000 | bytes 1000000 | tf_op jit(solution)/shard_map/pallas_call | solution.py:49
  22.8 7.8 %all-to-all-start = ((bf16[16,160,128]{2,1,0:T(8,128)(2,1)}), bf16[16,160,128]{2,1,0:T(8,128)(2,1)S(1)}, u32[]{:S(2)}, u32[]{:S(2)}) async-start(bf16[16,160,128]{2,1,0:T(8,128)(2,1)} %get-tuple-element.16), calls=%async_computation | async-start | bytes 1310720 | tf_op jit(solution)/shard_map/all_to_all | solution.py:435
  30.6 0.1 collective-permute-start.4
  30.7 0.0 collective-permute-done.3.w3
  30.7 0.5 collective-permute-start.5
  31.2 7.2 %collective-permute-done.6.w6 = bf16[256,2048]{1,0:T(8,128)(2,1)} collective-permute-done((bf16[256,2048]{1,0:T(8,128)(2,1)S(1)}, bf16[256,2048]{1,0:T(8,128)(2,1)}, u32[]{:S(2)}, u32[]{:S(2)}) %collective-permute-start.6) | collective-permute-done | bytes 1048608 | tf_op jit(solution)/shard_map/ppermute | solution.py:450
  38.4 1.8 %collective-permute-start.7 = (bf16[256,2048]{1,0:T(8,128)(2,1)}, bf16[256,2048]{1,0:T(8,128)(2,1)}, u32[]{:S(2)}, u32[]{:S(2)}) collective-permute-start(bf16[256,2048]{1,0:T(8,128)(2,1)} %collective-permute-done.6.w6), channel_id=1, source_target_pairs={{0,1},{1,0},{2,3},{3,2},{4,5},{5,4},{6,7},{7,6},{8,9},{9,8},{10,11... | collective-permute-start | bytes 3145736 | tf_op jit(solution)/shard_map/ppermute | solution.py:453
  40.2 3.3 %collective-permute-start = (bf16[8,4096]{1,0:T(8,128)(2,1)}, bf16[8,4096]{1,0:T(8,128)(2,1)S(1)}, u32[]{:S(2)}, u32[]{:S(2)}) collective-permute-start(bf16[8,4096]{1,0:T(8,128)(2,1)} %get-tuple-element.18), channel_id=1, source_target_pairs={{0,8},{8,16},{16,24},{24,32},{32,40},{40,48},{48,56},{56,64},{64,7... | collective-permute-start | bytes 196616 | tf_op jit(solution)/shard_map/ppermute | solution.py:480
  43.5 0.3 all-to-all-done.got
  43.8 1.2 shard_map.218
  45.0 7.2 %all-to-all-start.1 = ((bf16[16,128,128]{2,1,0:T(8,128)(2,1)}), bf16[16,128,128]{2,1,0:T(8,128)(2,1)S(1)}, u32[]{:S(2)}, u32[]{:S(2)}) async-start(bf16[16,128,128]{2,1,0:T(8,128)(2,1)} %shard_map.218), calls=%async_computation.1 | async-start | bytes 1048576 | tf_op jit(solution)/shard_map/all_to_all | solution.py:435
  52.2 2.4 %shard_map.221.disp_in = bf16[1024,256]{1,0:T(8,128)(2,1)} custom-call(s32[2,128]{1,0:T(2,128)} %bitcast.49, f32[2,128]{1,0:T(2,128)} %bitcast.51), custom_call_target="tpu_custom_call" | custom-call | flops 2000000000 | bytes 1000000 | tf_op jit(solution)/shard_map/pallas_call | solution.py:49
  54.5 0.0 collective-permute-done.halo_in
  54.5 4.0 %shard_map.219 = (f32[128,2048]{1,0:T(8,128)}, bf16[128,1024]{1,0:T(8,128)(2,1)}) custom-call(bf16[128,2048]{1,0:T(8,128)(2,1)} %bitcast.36, bf16[128,1024]{1,0:T(8,128)(2,1)} %bitcast.38, bf16[128,1024]{1,0:T(8,128)(2,1)} %bitcast.40, bf16[8,4096]{1,0:T(8,128)(2,1)S(1)} %collective-permute-done.halo_in, bf16[4,2048]{1,0:T(4,128)(2,1)} %cw_in.3, ...), custom_call_target="tpu_custom_call" | custom-call | flops 4000000000 | bytes 1000000 | tf_op jit(solution)/shard_map/pallas_call | solution.py:49
  58.5 4.5 %all-to-all-done.1 = bf16[16,128,128]{2,1,0:T(8,128)(2,1)S(1)} async-done(((bf16[16,128,128]{2,1,0:T(8,128)(2,1)}), bf16[16,128,128]{2,1,0:T(8,128)(2,1)S(1)}, u32[]{:S(2)}, u32[]{:S(2)}) %all-to-all-start.1) | async-done | bytes 524320 | tf_op jit(solution)/shard_map/all_to_all | solution.py:435
  63.0 0.0 collective-permute-done.4.w4
  63.0 4.5 %shard_map.220 = (f32[128,2048]{1,0:T(8,128)S(1)}, bf16[128,256]{1,0:T(8,128)(2,1)S(1)}) custom-call(bf16[8,256,128]{2,1,0:T(8,128)(2,1)S(1)} %bitcast.29, f32[128,32]{1,0:T(8,128)} %get-tuple-element.17.ec_in, f32[128,2048]{1,0:T(8,128)} %get-tuple-element.20.a_in, bf16[128,1024]{1,0:T(8,128)(2,1)} %get-tuple-element.21.cm_in, bf16[128,2048]{1,0:T(8,128)(2,1)} %bitcast.33, ...), custom_call_target="tpu_custom_call" | custom-call | flops 2000000000 | bytes 1000000 | tf_op jit(solution)/shard_map/pallas_call | solution.py:49
  67.5 3.6 %shard_map.222 = (bf16[128,2048]{1,0:T(8,128)(2,1)}, bf16[128,2048]{1,0:T(8,128)(2,1)}, bf16[1024,1024]{1,0:T(8,128)(2,1)}) custom-call(f32[128,2048]{1,0:T(8,128)S(1)} %get-tuple-element.22.proj_in, bf16[128,256]{1,0:T(8,128)(2,1)S(1)} %get-tuple-element.23.rest, f32[1,2048]{1,0:T(1,128)} %bitcast.48, bf16[1024,256]{1,0:T(8,128)(2,1)} %shard_map.221.disp_in, ...), custom_call_target="tpu_custom_call" | custom-call | flops 2000000000 | bytes 1000000 | tf_op jit(solution)/shard_map/pallas_call | solution.py:49
  71.2 36.0 %all_to_all.20 = bf16[128,8,1024]{2,1,0:T(8,128)(2,1)S(1)} all-to-all(bf16[128,8,1024]{2,1,0:T(8,128)(2,1)} %bitcast.32), channel_id=1, replica_groups=mesh['sp'=16,'dp'=8] {'sp','dp'}, dimensions={0} | all-to-all | bytes 4194304 | tf_op jit(solution)/shard_map/all_to_all | solution.py:435
  107.2 5.4 %shard_map.223 = bf16[1024,1024]{1,0:T(8,128)(2,1)S(1)} custom-call(bf16[1024,1024]{1,0:T(8,128)(2,1)S(1)} %bitcast.31, bf16[2048,512]{1,0:T(8,128)(2,1)} %bitcast.45, bf16[2048,512]{1,0:T(8,128)(2,1)} %bitcast.46, bf16[512,2048]{1,0:T(8,128)(2,1)} %bitcast.47), custom_call_target="tpu_custom_call" | custom-call | flops 3000000000 | bytes 1000000 | tf_op jit(solution)/shard_map/pallas_call | solution.py:49
  112.6 1.3 copy-done
  114.0 4.4 %all-to-all-start.3 = ((bf16[128,8,1024]{2,1,0:T(8,128)(2,1)}), bf16[128,8,1024]{2,1,0:T(8,128)(2,1)S(1)}, u32[]{:S(2)}, u32[]{:S(2)}) async-start(bf16[128,8,1024]{2,1,0:T(8,128)(2,1)} %bitcast.30), calls=%async_computation.3 | async-start | bytes 4194304 | tf_op jit(solution)/shard_map/all_to_all | solution.py:435
  118.4 2.3 %shard_map.224.w_in = bf16[256,1024]{1,0:T(8,128)(2,1)} custom-call(s32[2,128]{1,0:T(2,128)} %bitcast.50, f32[2,128]{1,0:T(2,128)} %bitcast.52), custom_call_target="tpu_custom_call" | custom-call | flops 2000000000 | bytes 1000000 | tf_op jit(solution)/shard_map/pallas_call | solution.py:49
  120.7 5.3 %shard_map.225.base_in = f32[128,2048]{1,0:T(8,128)} custom-call(bf16[128,2048]{1,0:T(8,128)(2,1)} %get-tuple-element.25.ein, bf16[128,2048]{1,0:T(8,128)(2,1)} %get-tuple-element.26.mixed, bf16[2048,512]{1,0:T(8,128)(2,1)} %sg.1, bf16[2048,512]{1,0:T(8,128)(2,1)} %su.1, bf16[512,2048]{1,0:T(8,128)(2,1)} %sd.1), custom_call_target="tpu_custom_call" | custom-call | flops 4000000000 | bytes 1000000 | tf_op jit(solution)/shard_map/pallas_call | solution.py:49
  125.9 23.1 %all-to-all-done.3 = bf16[128,8,1024]{2,1,0:T(8,128)(2,1)S(1)} async-done(((bf16[128,8,1024]{2,1,0:T(8,128)(2,1)}), bf16[128,8,1024]{2,1,0:T(8,128)(2,1)S(1)}, u32[]{:S(2)}, u32[]{:S(2)}) %all-to-all-start.3) | async-done | bytes 2097184 | tf_op jit(solution)/shard_map/all_to_all | solution.py:435
  149.0 2.7 %shard_map.226 = bf16[128,2048]{1,0:T(8,128)(2,1)} custom-call(bf16[1024,1024]{1,0:T(8,128)(2,1)S(1)} %bitcast.28, bf16[256,1024]{1,0:T(8,128)(2,1)} %shard_map.224.w_in, f32[128,2048]{1,0:T(8,128)} %shard_map.225.base_in), custom_call_target="tpu_custom_call" | custom-call | flops 1000000 | bytes 1000000 | tf_op jit(solution)/shard_map/pallas_call | solution.py:49
  (3 shorter events, 0.0 us)
Async XLA Ops:
  0.0 4.0 %collective-permute-start.1 = (bf16[256,2048]{1,0:T(8,128)(2,1)}, bf16[256,2048]{1,0:T(8,128)(2,1)S(1)}, u32[]{:S(2)}, u32[]{:S(2)}) collective-permute-start(bf16[256,2048]{1,0:T(8,128)(2,1)} %w0.1), channel_id=1, source_target_pairs={{0,1},{1,0},{2,3},{3,2},{4,5},{5,4},{6,7},{7,6},{8,9},{9,8},{10,11... | collective-permute-start | bytes 3145736 | tf_op jit(solution)/shard_map/ppermute | solution.py:453
  1.4 14.7 %collective-permute-start.2 = (bf16[256,2048]{1,0:T(8,128)(2,1)}, bf16[256,2048]{1,0:T(8,128)(2,1)S(1)}, u32[]{:S(2)}, u32[]{:S(2)}) collective-permute-start(bf16[256,2048]{1,0:T(8,128)(2,1)} %w0.1), channel_id=1, source_target_pairs={{0,2},{1,7},{2,4},{3,1},{4,6},{5,3},{6,0},{7,5},{8,10},{9,15},{10,... | collective-permute-start | bytes 3145736 | tf_op jit(solution)/shard_map/ppermute | solution.py:450
  4.0 26.7 %collective-permute-start.3 = (bf16[256,2048]{1,0:T(8,128)(2,1)S(1)}, bf16[256,2048]{1,0:T(8,128)(2,1)}, u32[]{:S(2)}, u32[]{:S(2)}) collective-permute-start(bf16[256,2048]{1,0:T(8,128)(2,1)S(1)} %collective-permute-done.1.w1), channel_id=1, source_target_pairs={{0,2},{1,7},{2,4},{3,1},{4,6},{5,3},{6,0},{7,5},{8,10},{9,15},{10,... | collective-permute-start | bytes 3145736 | tf_op jit(solution)/shard_map/ppermute | solution.py:450
  16.0 22.4 %collective-permute-start.6 = (bf16[256,2048]{1,0:T(8,128)(2,1)S(1)}, bf16[256,2048]{1,0:T(8,128)(2,1)}, u32[]{:S(2)}, u32[]{:S(2)}) collective-permute-start(bf16[256,2048]{1,0:T(8,128)(2,1)S(1)} %collective-permute-done.2.w2), channel_id=1, source_target_pairs={{0,2},{1,7},{2,4},{3,1},{4,6},{5,3},{6,0},{7,5},{8,10},{9,15},{10,... | collective-permute-start | bytes 3145736 | tf_op jit(solution)/shard_map/ppermute | solution.py:450
  22.8 21.0 %all-to-all-start = ((bf16[16,160,128]{2,1,0:T(8,128)(2,1)}), bf16[16,160,128]{2,1,0:T(8,128)(2,1)S(1)}, u32[]{:S(2)}, u32[]{:S(2)}) async-start(bf16[16,160,128]{2,1,0:T(8,128)(2,1)} %get-tuple-element.16), calls=%async_computation | async-start | bytes 1310720 | tf_op jit(solution)/shard_map/all_to_all | solution.py:435
  30.6 32.4 %collective-permute-start.4 = (bf16[256,2048]{1,0:T(8,128)(2,1)S(1)}, bf16[256,2048]{1,0:T(8,128)(2,1)}, u32[]{:S(2)}, u32[]{:S(2)}) collective-permute-start(bf16[256,2048]{1,0:T(8,128)(2,1)S(1)} %collective-permute-done.2.w2), channel_id=1, source_target_pairs={{0,1},{1,0},{2,3},{3,2},{4,5},{5,4},{6,7},{7,6},{8,9},{9,8},{10,11... | collective-permute-start | bytes 3145736 | tf_op jit(solution)/shard_map/ppermute | solution.py:453
  30.7 32.3 %collective-permute-start.5 = (bf16[256,2048]{1,0:T(8,128)(2,1)}, bf16[256,2048]{1,0:T(8,128)(2,1)}, u32[]{:S(2)}, u32[]{:S(2)}) collective-permute-start(bf16[256,2048]{1,0:T(8,128)(2,1)} %collective-permute-done.3.w3), channel_id=1, source_target_pairs={{0,1},{1,0},{2,3},{3,2},{4,5},{5,4},{6,7},{7,6},{8,9},{9,8},{10,11... | collective-permute-start | bytes 3145736 | tf_op jit(solution)/shard_map/ppermute | solution.py:453
  38.4 29.1 %collective-permute-start.7 = (bf16[256,2048]{1,0:T(8,128)(2,1)}, bf16[256,2048]{1,0:T(8,128)(2,1)}, u32[]{:S(2)}, u32[]{:S(2)}) collective-permute-start(bf16[256,2048]{1,0:T(8,128)(2,1)} %collective-permute-done.6.w6), channel_id=1, source_target_pairs={{0,1},{1,0},{2,3},{3,2},{4,5},{5,4},{6,7},{7,6},{8,9},{9,8},{10,11... | collective-permute-start | bytes 3145736 | tf_op jit(solution)/shard_map/ppermute | solution.py:453
  40.2 14.3 %collective-permute-start = (bf16[8,4096]{1,0:T(8,128)(2,1)}, bf16[8,4096]{1,0:T(8,128)(2,1)S(1)}, u32[]{:S(2)}, u32[]{:S(2)}) collective-permute-start(bf16[8,4096]{1,0:T(8,128)(2,1)} %get-tuple-element.18), channel_id=1, source_target_pairs={{0,8},{8,16},{16,24},{24,32},{32,40},{40,48},{48,56},{56,64},{64,7... | collective-permute-start | bytes 196616 | tf_op jit(solution)/shard_map/ppermute | solution.py:480
  45.0 18.0 %all-to-all-start.1 = ((bf16[16,128,128]{2,1,0:T(8,128)(2,1)}), bf16[16,128,128]{2,1,0:T(8,128)(2,1)S(1)}, u32[]{:S(2)}, u32[]{:S(2)}) async-start(bf16[16,128,128]{2,1,0:T(8,128)(2,1)} %shard_map.218), calls=%async_computation.1 | async-start | bytes 1048576 | tf_op jit(solution)/shard_map/all_to_all | solution.py:435
  112.6 1.3 copy-start
  114.0 35.0 %all-to-all-start.3 = ((bf16[128,8,1024]{2,1,0:T(8,128)(2,1)}), bf16[128,8,1024]{2,1,0:T(8,128)(2,1)S(1)}, u32[]{:S(2)}, u32[]{:S(2)}) async-start(bf16[128,8,1024]{2,1,0:T(8,128)(2,1)} %bitcast.30), calls=%async_computation.3 | async-start | bytes 4194304 | tf_op jit(solution)/shard_map/all_to_all | solution.py:435

commit v11 on v10

--- a/solution.py
+++ b/solution.py
@@ -298,14 +298,13 @@
 
 
 def norm_kernel(
-    pref, ec_in, a_in, cm_in, gate_in, gain_in, resid_in, w0, w1, w2, w3, w4, w5, w6, proj, rest,
-    norm, wide, picked, ec, a, cm, gate, gain, resid, sems
+    pref, ec_in, a_in, cm_in, gate_in, gain_in, w0, w1, w2, w3, w4, w5, w6, proj, rest,
+    norm, wide, picked, ec, a, cm, gate, gain, sems
 ):
     pairs = [(ec_in, ec), (cm_in, cm), (gain_in, gain)]
     for q in range(4):
         pairs.append((a_in.at[:, part(q, 512)], a.at[:, part(q, 512)]))
         pairs.append((gate_in.at[:, part(q, 512)], gate.at[:, part(q, 512)]))
-    pairs.append((resid_in, resid))
     for k, w in enumerate((w0, w1, w2, w3, w4, w5, w6)):
         pairs.append((w, wide.at[part(k, GW), :]))
     loads = begin(pairs, sems)
@@ -332,25 +331,23 @@
     for k in range(7):
         picked[:, k * GW : (k + 1) * GW] = norm[place[k]]
     rest[...] = norm[place[7]]
-    for load in loads[11:16]:
-        load.wait()
-    cut = 4 * GW
-    proj[...] = resid[...].astype(F32) + jnp.dot(
-        picked[:, :cut], wide[:cut, :], preferred_element_type=F32
-    )
-    for load in loads[16:]:
-        load.wait()
-    proj[...] += jnp.dot(picked[:, cut:], wide[cut:, :], preferred_element_type=F32)
+    for first, last in ((0, 4), (4, 6), (6, 7)):
+        for load in loads[11 + first : 11 + last]:
+            load.wait()
+        rows = slice(first * GW, last * GW)
+        y = jnp.dot(picked[:, rows], wide[rows, :], preferred_element_type=F32)
+        proj[...] = y if first == 0 else proj[...] + y
 
 
 def mix_kernel(
-    proj_in, rest, fgain_in, disp_in, w7, mixed_out, ein_out, send_out,
-    wide, fgain, disp, mixed_buf, ein_buf, send, sems, out_sems
+    proj_in, rest, fgain_in, resid_in, disp_in, w7, mixed_out, ein_out, send_out,
+    wide, fgain, resid, disp, mixed_buf, ein_buf, send, sems, out_sems
 ):
-    loads = begin([(w7, wide), (fgain_in, fgain), (disp_in, disp)], sems)
+    loads = begin([(w7, wide), (resid_in, resid), (fgain_in, fgain), (disp_in, disp)], sems)
     loads[0].wait()
-    proj = proj_in[...] + jnp.dot(rest[...], wide[...], preferred_element_type=F32)
     loads[1].wait()
+    proj = resid[...].astype(F32) + proj_in[...] + jnp.dot(rest[...], wide[...], preferred_element_type=F32)
+    loads[2].wait()
     mixed = proj.astype(BF)
     mixed_buf[...] = mixed
     stores = [pltpu.make_async_copy(mixed_buf, mixed_out, out_sems.at[0])]
@@ -361,7 +358,7 @@
     stores.append(pltpu.make_async_copy(ein_buf, ein_out, out_sems.at[1]))
     stores[1].start()
     stack = jnp.concatenate([ein[:, :HALF], ein[:, HALF:]], axis=0)
-    loads[2].wait()
+    loads[3].wait()
     for q in range(4):
         rows = part(q, 256)
         send[rows, :] = jnp.dot(disp[rows, :], stack, preferred_element_type=F32).astype(BF)
@@ -523,7 +520,7 @@
         [((TOK, D), F32), ((TOK, GW), BF)],
         (
             pref.reshape(GROUPS, GW, STATE), ec, a, cm, gate_input[0], norm_gain[None],
-            residual[0], *pieces[:7],
+            *pieces[:7],
         ),
         scratch=[
             pltpu.VMEM((GROUPS, TOK, GW), BF),
@@ -534,12 +531,11 @@
             pltpu.VMEM((TOK, 1024), BF),
             pltpu.VMEM((TOK, D), BF),
             pltpu.VMEM((1, D), F32),
-            pltpu.VMEM((TOK, D), BF),
-            pltpu.SemaphoreType.DMA((19,)),
+            pltpu.SemaphoreType.DMA((18,)),
         ],
         vmem=(0,),
-        raw=range(1, 14),
-        free=range(8, 14),
+        raw=range(1, 13),
+        free=range(7, 13),
         out_vmem=(0, 1),
         limit=32,
         flops=2 * 10**9,
@@ -547,20 +543,21 @@
     mixed, ein, send = call(
         mix_kernel,
         [((TOK, D), BF), ((TOK, D), BF), ((ROWS, HALF), BF)],
-        (proj, rest, ffn_gain[None], disp, *pieces[7:]),
+        (proj, rest, ffn_gain[None], residual[0], disp, *pieces[7:]),
         scratch=[
             pltpu.VMEM((GW, D), BF),
             pltpu.VMEM((1, D), F32),
+            pltpu.VMEM((TOK, D), BF),
             pltpu.VMEM((ROWS, 2 * TOK), BF),
             pltpu.VMEM((TOK, D), BF),
             pltpu.VMEM((TOK, D), BF),
             pltpu.VMEM((ROWS, HALF), BF),
-            pltpu.SemaphoreType.DMA((3,)),
+            pltpu.SemaphoreType.DMA((4,)),
             pltpu.SemaphoreType.DMA((6,)),
         ],
         vmem=(0, 1),
-        raw=range(2, 5),
-        free=(4,),
+        raw=range(2, 6),
+        free=(5,),
         raw_out=(0, 1, 2),
         limit=28,
         flops=2 * 10**9,

time: 152 us -> 153 us (level)
  no operation moved by 1% of the time
where the time goes in v11:
time: 153 us; the launch traced here: 152 us
  waiting for transfers between devices  44.6 us (29%)
  blocking collectives  36 us (24%)
  Pallas kernels  35.3 us (23%)
  starting transfers between devices  34.5 us (23%)
    all_to_all x1, blocking collectives, exchange(): lax.all_to_all(plain(v), axis, split_axis=0, concat_axis=0, tiled=True)  36 us
    pallas_call x10, Pallas kernels, call(): pl.pallas_call(kernel, out_shape=tuple((pltpu.VMEM(s, d) if i in out_vmem...  35.3 us
    all_to_all x3, waiting for transfers between devices, exchange(): lax.all_to_all(plain(v), axis, split_axis=0, concat_axis=0, tiled=True)  27.9 us
    all_to_all x3, starting transfers between devices, exchange(): lax.all_to_all(plain(v), axis, split_axis=0, concat_axis=0, tiled=True)  19.4 us
    ppermute x3, waiting for transfers between devices, ring(): lax.ppermute(v, 'dp', [(i, (i + (-2 if i % 2 else 2)) % dps) for i in ran...  16.8 us
    ppermute x3, starting transfers between devices, ring(): lax.ppermute(v, 'dp', [(i, (i + (-2 if i % 2 else 2)) % dps) for i in ran...  8.09 us
    ppermute x4, starting transfers between devices, swap(): return lax.ppermute(v, 'dp', [(i, i ^ 1) for i in range(dps)])  3.74 us
    ppermute x1, starting transfers between devices, layer(): lax.ppermute(plain(ends), 'sp', [(i, i + 1) for i in range(ways - 1)])  3.3 us
  transfers between devices with their start and end apart: 11, of which 5 were waited for; matrix products, arithmetic and copies ran while one was open for 0% of the time, Pallas kernels for 15%

profile of v11, /device:TPU:1, one launch (start us, length us, event | category | flops | bytes accessed | tf_op | source)
XLA Modules:
  0.0 152.0 jit_solution(4938861777633460307)
XLA Ops:
  0.0 1.4 collective-permute-start.1
  1.4 2.6 %collective-permute-start.2 = (bf16[256,2048]{1,0:T(8,128)(2,1)}, bf16[256,2048]{1,0:T(8,128)(2,1)S(1)}, u32[]{:S(2)}, u32[]{:S(2)}) collective-permute-start(bf16[256,2048]{1,0:T(8,128)(2,1)} %w0.1), channel_id=1, source_target_pairs={{0,2},{1,7},{2,4},{3,1},{4,6},{5,3},{6,0},{7,5},{8,10},{9,15},{10,... | collective-permute-start | bytes 3145736 | tf_op jit(solution)/shard_map/ppermute | solution.py:447
  4.0 0.0 collective-permute-done.1.w1
  4.0 2.5 %collective-permute-start.3 = (bf16[256,2048]{1,0:T(8,128)(2,1)S(1)}, bf16[256,2048]{1,0:T(8,128)(2,1)}, u32[]{:S(2)}, u32[]{:S(2)}) collective-permute-start(bf16[256,2048]{1,0:T(8,128)(2,1)S(1)} %collective-permute-done.1.w1), channel_id=1, source_target_pairs={{0,2},{1,7},{2,4},{3,1},{4,6},{5,3},{6,0},{7,5},{8,10},{9,15},{10,... | collective-permute-start | bytes 3145736 | tf_op jit(solution)/shard_map/ppermute | solution.py:447
  6.5 9.6 %collective-permute-done.2.w2 = bf16[256,2048]{1,0:T(8,128)(2,1)S(1)} collective-permute-done((bf16[256,2048]{1,0:T(8,128)(2,1)}, bf16[256,2048]{1,0:T(8,128)(2,1)S(1)}, u32[]{:S(2)}, u32[]{:S(2)}) %collective-permute-start.2) | collective-permute-done | bytes 1048608 | tf_op jit(solution)/shard_map/ppermute | solution.py:447
  16.0 3.0 %collective-permute-start.6 = (bf16[256,2048]{1,0:T(8,128)(2,1)S(1)}, bf16[256,2048]{1,0:T(8,128)(2,1)}, u32[]{:S(2)}, u32[]{:S(2)}) collective-permute-start(bf16[256,2048]{1,0:T(8,128)(2,1)S(1)} %collective-permute-done.2.w2), channel_id=1, source_target_pairs={{0,2},{1,7},{2,4},{3,1},{4,6},{5,3},{6,0},{7,5},{8,10},{9,15},{10,... | collective-permute-start | bytes 3145736 | tf_op jit(solution)/shard_map/ppermute | solution.py:447
  19.0 3.8 %shard_map.217 = (bf16[16,160,128]{2,1,0:T(8,128)(2,1)}, f32[128,32]{1,0:T(8,128)}, f32[128,32]{1,0:T(8,128)}, bf16[8,4096]{1,0:T(8,128)(2,1)}) custom-call(bf16[32,128]{1,0:T(8,128)(2,1)} %bitcast.40, f32[1,32]{1,0:T(1,128)} %bitcast.42, f32[1,32]{1,0:T(1,128)} %bitcast.43, bf16[128,2048]{1,0:T(8,128)(2,1)} %bitcast.34, bf16[128,1024]{1,0:T(8,128)(2,1)} %bitcast.36, ...), custom_call_target="tpu_custom_call" | custom-call | flops 1000000 | bytes 1000000 | tf_op jit(solution)/shard_map/pallas_call | solution.py:49
  22.8 7.8 %all-to-all-start = ((bf16[16,160,128]{2,1,0:T(8,128)(2,1)}), bf16[16,160,128]{2,1,0:T(8,128)(2,1)S(1)}, u32[]{:S(2)}, u32[]{:S(2)}) async-start(bf16[16,160,128]{2,1,0:T(8,128)(2,1)} %get-tuple-element.16), calls=%async_computation | async-start | bytes 1310720 | tf_op jit(solution)/shard_map/all_to_all | solution.py:432
  30.6 0.1 collective-permute-start.4
  30.7 0.0 collective-permute-done.3.w3
  30.7 0.5 collective-permute-start.5
  31.2 7.2 %collective-permute-done.6.w6 = bf16[256,2048]{1,0:T(8,128)(2,1)} collective-permute-done((bf16[256,2048]{1,0:T(8,128)(2,1)S(1)}, bf16[256,2048]{1,0:T(8,128)(2,1)}, u32[]{:S(2)}, u32[]{:S(2)}) %collective-permute-start.6) | collective-permute-done | bytes 1048608 | tf_op jit(solution)/shard_map/ppermute | solution.py:447
  38.4 1.8 %collective-permute-start.7 = (bf16[256,2048]{1,0:T(8,128)(2,1)}, bf16[256,2048]{1,0:T(8,128)(2,1)}, u32[]{:S(2)}, u32[]{:S(2)}) collective-permute-start(bf16[256,2048]{1,0:T(8,128)(2,1)} %collective-permute-done.6.w6), channel_id=1, source_target_pairs={{0,1},{1,0},{2,3},{3,2},{4,5},{5,4},{6,7},{7,6},{8,9},{9,8},{10,11... | collective-permute-start | bytes 3145736 | tf_op jit(solution)/shard_map/ppermute | solution.py:450
  40.2 3.3 %collective-permute-start = (bf16[8,4096]{1,0:T(8,128)(2,1)}, bf16[8,4096]{1,0:T(8,128)(2,1)S(1)}, u32[]{:S(2)}, u32[]{:S(2)}) collective-permute-start(bf16[8,4096]{1,0:T(8,128)(2,1)} %get-tuple-element.18), channel_id=1, source_target_pairs={{0,8},{8,16},{16,24},{24,32},{32,40},{40,48},{48,56},{56,64},{64,7... | collective-permute-start | bytes 196616 | tf_op jit(solution)/shard_map/ppermute | solution.py:477
  43.5 0.3 all-to-all-done.got
  43.8 1.2 shard_map.218
  45.0 7.2 %all-to-all-start.1 = ((bf16[16,128,128]{2,1,0:T(8,128)(2,1)}), bf16[16,128,128]{2,1,0:T(8,128)(2,1)S(1)}, u32[]{:S(2)}, u32[]{:S(2)}) async-start(bf16[16,128,128]{2,1,0:T(8,128)(2,1)} %shard_map.218), calls=%async_computation.1 | async-start | bytes 1048576 | tf_op jit(solution)/shard_map/all_to_all | solution.py:432
  52.2 2.4 %shard_map.221.disp_in = bf16[1024,256]{1,0:T(8,128)(2,1)} custom-call(s32[2,128]{1,0:T(2,128)} %bitcast.49, f32[2,128]{1,0:T(2,128)} %bitcast.51), custom_call_target="tpu_custom_call" | custom-call | flops 2000000000 | bytes 1000000 | tf_op jit(solution)/shard_map/pallas_call | solution.py:49
  54.5 0.0 collective-permute-done.halo_in
  54.5 4.0 %shard_map.219 = (f32[128,2048]{1,0:T(8,128)}, bf16[128,1024]{1,0:T(8,128)(2,1)}) custom-call(bf16[128,2048]{1,0:T(8,128)(2,1)} %bitcast.35, bf16[128,1024]{1,0:T(8,128)(2,1)} %bitcast.37, bf16[128,1024]{1,0:T(8,128)(2,1)} %bitcast.39, bf16[8,4096]{1,0:T(8,128)(2,1)S(1)} %collective-permute-done.halo_in, bf16[4,2048]{1,0:T(4,128)(2,1)} %cw_in.3, ...), custom_call_target="tpu_custom_call" | custom-call | flops 4000000000 | bytes 1000000 | tf_op jit(solution)/shard_map/pallas_call | solution.py:49
  58.5 4.5 %all-to-all-done.1 = bf16[16,128,128]{2,1,0:T(8,128)(2,1)S(1)} async-done(((bf16[16,128,128]{2,1,0:T(8,128)(2,1)}), bf16[16,128,128]{2,1,0:T(8,128)(2,1)S(1)}, u32[]{:S(2)}, u32[]{:S(2)}) %all-to-all-start.1) | async-done | bytes 524320 | tf_op jit(solution)/shard_map/all_to_all | solution.py:432
  63.0 4.5 %shard_map.220 = (f32[128,2048]{1,0:T(8,128)S(1)}, bf16[128,256]{1,0:T(8,128)(2,1)S(1)}) custom-call(bf16[8,256,128]{2,1,0:T(8,128)(2,1)S(1)} %bitcast.29, f32[128,32]{1,0:T(8,128)} %get-tuple-element.17.ec_in, f32[128,2048]{1,0:T(8,128)} %get-tuple-element.20.a_in, bf16[128,1024]{1,0:T(8,128)(2,1)} %get-tuple-element.21.cm_in, bf16[128,2048]{1,0:T(8,128)(2,1)} %bitcast.33, ...), custom_call_target="tpu_custom_call" | custom-call | flops 2000000000 | bytes 1000000 | tf_op jit(solution)/shard_map/pallas_call | solution.py:49
  67.5 0.0 collective-permute-done.7.w7
  67.5 3.8 %shard_map.222 = (bf16[128,2048]{1,0:T(8,128)(2,1)}, bf16[128,2048]{1,0:T(8,128)(2,1)}, bf16[1024,1024]{1,0:T(8,128)(2,1)}) custom-call(f32[128,2048]{1,0:T(8,128)S(1)} %get-tuple-element.22.proj_in, bf16[128,256]{1,0:T(8,128)(2,1)S(1)} %get-tuple-element.23.rest, f32[1,2048]{1,0:T(1,128)} %bitcast.48, bf16[128,2048]{1,0:T(8,128)(2,1)} %bitcast.47, ...), custom_call_target="tpu_custom_call" | custom-call | flops 2000000000 | bytes 1000000 | tf_op jit(solution)/shard_map/pallas_call | solution.py:49
  71.3 36.0 %all_to_all.20 = bf16[128,8,1024]{2,1,0:T(8,128)(2,1)S(1)} all-to-all(bf16[128,8,1024]{2,1,0:T(8,128)(2,1)} %bitcast.32), channel_id=1, replica_groups=mesh['sp'=16,'dp'=8] {'sp','dp'}, dimensions={0} | all-to-all | bytes 4194304 | tf_op jit(solution)/shard_map/all_to_all | solution.py:432
  107.3 5.4 %shard_map.223 = bf16[1024,1024]{1,0:T(8,128)(2,1)S(1)} custom-call(bf16[1024,1024]{1,0:T(8,128)(2,1)S(1)} %bitcast.31, bf16[2048,512]{1,0:T(8,128)(2,1)} %bitcast.44, bf16[2048,512]{1,0:T(8,128)(2,1)} %bitcast.45, bf16[512,2048]{1,0:T(8,128)(2,1)} %bitcast.46), custom_call_target="tpu_custom_call" | custom-call | flops 3000000000 | bytes 1000000 | tf_op jit(solution)/shard_map/pallas_call | solution.py:49
  112.7 1.3 copy-done
  114.1 4.4 %all-to-all-start.3 = ((bf16[128,8,1024]{2,1,0:T(8,128)(2,1)}), bf16[128,8,1024]{2,1,0:T(8,128)(2,1)S(1)}, u32[]{:S(2)}, u32[]{:S(2)}) async-start(bf16[128,8,1024]{2,1,0:T(8,128)(2,1)} %bitcast.30), calls=%async_computation.3 | async-start | bytes 4194304 | tf_op jit(solution)/shard_map/all_to_all | solution.py:432
  118.5 2.3 %shard_map.224.w_in = bf16[256,1024]{1,0:T(8,128)(2,1)} custom-call(s32[2,128]{1,0:T(2,128)} %bitcast.50, f32[2,128]{1,0:T(2,128)} %bitcast.52), custom_call_target="tpu_custom_call" | custom-call | flops 2000000000 | bytes 1000000 | tf_op jit(solution)/shard_map/pallas_call | solution.py:49
  120.7 5.3 %shard_map.225.base_in = f32[128,2048]{1,0:T(8,128)} custom-call(bf16[128,2048]{1,0:T(8,128)(2,1)} %get-tuple-element.25.ein, bf16[128,2048]{1,0:T(8,128)(2,1)} %get-tuple-element.26.mixed, bf16[2048,512]{1,0:T(8,128)(2,1)} %sg.1, bf16[2048,512]{1,0:T(8,128)(2,1)} %su.1, bf16[512,2048]{1,0:T(8,128)(2,1)} %sd.1), custom_call_target="tpu_custom_call" | custom-call | flops 4000000000 | bytes 1000000 | tf_op jit(solution)/shard_map/pallas_call | solution.py:49
  126.0 23.1 %all-to-all-done.3 = bf16[128,8,1024]{2,1,0:T(8,128)(2,1)S(1)} async-done(((bf16[128,8,1024]{2,1,0:T(8,128)(2,1)}), bf16[128,8,1024]{2,1,0:T(8,128)(2,1)S(1)}, u32[]{:S(2)}, u32[]{:S(2)}) %all-to-all-start.3) | async-done | bytes 2097184 | tf_op jit(solution)/shard_map/all_to_all | solution.py:432
  149.1 2.7 %shard_map.226 = bf16[128,2048]{1,0:T(8,128)(2,1)} custom-call(bf16[1024,1024]{1,0:T(8,128)(2,1)S(1)} %bitcast.28, bf16[256,1024]{1,0:T(8,128)(2,1)} %shard_map.224.w_in, f32[128,2048]{1,0:T(8,128)} %shard_map.225.base_in), custom_call_target="tpu_custom_call" | custom-call | flops 1000000 | bytes 1000000 | tf_op jit(solution)/shard_map/pallas_call | solution.py:49
  (3 shorter events, 0.0 us)
Async XLA Ops:
  0.0 4.0 %collective-permute-start.1 = (bf16[256,2048]{1,0:T(8,128)(2,1)}, bf16[256,2048]{1,0:T(8,128)(2,1)S(1)}, u32[]{:S(2)}, u32[]{:S(2)}) collective-permute-start(bf16[256,2048]{1,0:T(8,128)(2,1)} %w0.1), channel_id=1, source_target_pairs={{0,1},{1,0},{2,3},{3,2},{4,5},{5,4},{6,7},{7,6},{8,9},{9,8},{10,11... | collective-permute-start | bytes 3145736 | tf_op jit(solution)/shard_map/ppermute | solution.py:450
  1.4 14.7 %collective-permute-start.2 = (bf16[256,2048]{1,0:T(8,128)(2,1)}, bf16[256,2048]{1,0:T(8,128)(2,1)S(1)}, u32[]{:S(2)}, u32[]{:S(2)}) collective-permute-start(bf16[256,2048]{1,0:T(8,128)(2,1)} %w0.1), channel_id=1, source_target_pairs={{0,2},{1,7},{2,4},{3,1},{4,6},{5,3},{6,0},{7,5},{8,10},{9,15},{10,... | collective-permute-start | bytes 3145736 | tf_op jit(solution)/shard_map/ppermute | solution.py:447
  4.0 26.7 %collective-permute-start.3 = (bf16[256,2048]{1,0:T(8,128)(2,1)S(1)}, bf16[256,2048]{1,0:T(8,128)(2,1)}, u32[]{:S(2)}, u32[]{:S(2)}) collective-permute-start(bf16[256,2048]{1,0:T(8,128)(2,1)S(1)} %collective-permute-done.1.w1), channel_id=1, source_target_pairs={{0,2},{1,7},{2,4},{3,1},{4,6},{5,3},{6,0},{7,5},{8,10},{9,15},{10,... | collective-permute-start | bytes 3145736 | tf_op jit(solution)/shard_map/ppermute | solution.py:447
  16.0 22.4 %collective-permute-start.6 = (bf16[256,2048]{1,0:T(8,128)(2,1)S(1)}, bf16[256,2048]{1,0:T(8,128)(2,1)}, u32[]{:S(2)}, u32[]{:S(2)}) collective-permute-start(bf16[256,2048]{1,0:T(8,128)(2,1)S(1)} %collective-permute-done.2.w2), channel_id=1, source_target_pairs={{0,2},{1,7},{2,4},{3,1},{4,6},{5,3},{6,0},{7,5},{8,10},{9,15},{10,... | collective-permute-start | bytes 3145736 | tf_op jit(solution)/shard_map/ppermute | solution.py:447
  22.8 21.0 %all-to-all-start = ((bf16[16,160,128]{2,1,0:T(8,128)(2,1)}), bf16[16,160,128]{2,1,0:T(8,128)(2,1)S(1)}, u32[]{:S(2)}, u32[]{:S(2)}) async-start(bf16[16,160,128]{2,1,0:T(8,128)(2,1)} %get-tuple-element.16), calls=%async_computation | async-start | bytes 1310720 | tf_op jit(solution)/shard_map/all_to_all | solution.py:432
  30.6 32.4 %collective-permute-start.4 = (bf16[256,2048]{1,0:T(8,128)(2,1)S(1)}, bf16[256,2048]{1,0:T(8,128)(2,1)}, u32[]{:S(2)}, u32[]{:S(2)}) collective-permute-start(bf16[256,2048]{1,0:T(8,128)(2,1)S(1)} %collective-permute-done.2.w2), channel_id=1, source_target_pairs={{0,1},{1,0},{2,3},{3,2},{4,5},{5,4},{6,7},{7,6},{8,9},{9,8},{10,11... | collective-permute-start | bytes 3145736 | tf_op jit(solution)/shard_map/ppermute | solution.py:450
  30.7 32.3 %collective-permute-start.5 = (bf16[256,2048]{1,0:T(8,128)(2,1)}, bf16[256,2048]{1,0:T(8,128)(2,1)}, u32[]{:S(2)}, u32[]{:S(2)}) collective-permute-start(bf16[256,2048]{1,0:T(8,128)(2,1)} %collective-permute-done.3.w3), channel_id=1, source_target_pairs={{0,1},{1,0},{2,3},{3,2},{4,5},{5,4},{6,7},{7,6},{8,9},{9,8},{10,11... | collective-permute-start | bytes 3145736 | tf_op jit(solution)/shard_map/ppermute | solution.py:450
  38.4 29.1 %collective-permute-start.7 = (bf16[256,2048]{1,0:T(8,128)(2,1)}, bf16[256,2048]{1,0:T(8,128)(2,1)}, u32[]{:S(2)}, u32[]{:S(2)}) collective-permute-start(bf16[256,2048]{1,0:T(8,128)(2,1)} %collective-permute-done.6.w6), channel_id=1, source_target_pairs={{0,1},{1,0},{2,3},{3,2},{4,5},{5,4},{6,7},{7,6},{8,9},{9,8},{10,11... | collective-permute-start | bytes 3145736 | tf_op jit(solution)/shard_map/ppermute | solution.py:450
  40.2 14.3 %collective-permute-start = (bf16[8,4096]{1,0:T(8,128)(2,1)}, bf16[8,4096]{1,0:T(8,128)(2,1)S(1)}, u32[]{:S(2)}, u32[]{:S(2)}) collective-permute-start(bf16[8,4096]{1,0:T(8,128)(2,1)} %get-tuple-element.18), channel_id=1, source_target_pairs={{0,8},{8,16},{16,24},{24,32},{32,40},{40,48},{48,56},{56,64},{64,7... | collective-permute-start | bytes 196616 | tf_op jit(solution)/shard_map/ppermute | solution.py:477
  45.0 18.0 %all-to-all-start.1 = ((bf16[16,128,128]{2,1,0:T(8,128)(2,1)}), bf16[16,128,128]{2,1,0:T(8,128)(2,1)S(1)}, u32[]{:S(2)}, u32[]{:S(2)}) async-start(bf16[16,128,128]{2,1,0:T(8,128)(2,1)} %shard_map.218), calls=%async_computation.1 | async-start | bytes 1048576 | tf_op jit(solution)/shard_map/all_to_all | solution.py:432
  112.7 1.3 copy-start
  114.1 35.0 %all-to-all-start.3 = ((bf16[128,8,1024]{2,1,0:T(8,128)(2,1)}), bf16[128,8,1024]{2,1,0:T(8,128)(2,1)S(1)}, u32[]{:S(2)}, u32[]{:S(2)}) async-start(bf16[128,8,1024]{2,1,0:T(8,128)(2,1)} %bitcast.30), calls=%async_computation.3 | async-start | bytes 4194304 | tf_op jit(solution)/shard_map/all_to_all | solution.py:432
